TPU v7x, 512 devices: a whole 4x8x8 slice. The times are simulated.
512 devices in a mesh: sp: 64 (over z, y), fs: 4 (over x), tp: 2 (over core).
Axes of the slice: x: 4, y: 8, z: 8, core: 2. Of those that a mesh axis runs over, the one named last changes fastest.
Arguments:
- activations: bfloat16 [4, 16384, 2048], P('fs', 'sp'), may hold values from -600 to 600
- norm_gain: float32 [2048], replicated, may hold values from 0.1 to 1.9
- w_conv_gate: bfloat16 [2048, 1024], P('sp', ('fs', 'tp')), may hold values from -0.125 to 0.125
- w_conv_mult: bfloat16 [2048, 1024], P('sp', ('fs', 'tp')), may hold values from -0.125 to 0.125
- w_conv_in: bfloat16 [2048, 1024], P('sp', ('fs', 'tp')), may hold values from -0.125 to 0.125
- conv_taps: float32 [3, 1024], replicated, may hold values from -3.5 to 3.5
- w_query: bfloat16 [2048, 1024], P('sp', ('fs', 'tp')), may hold values from -0.125 to 0.125
- w_key: bfloat16 [2048, 1024], P('sp', ('fs', 'tp')), may hold values from -0.125 to 0.125
- w_value: bfloat16 [2048, 1024], P('sp', ('fs', 'tp')), may hold values from -0.125 to 0.125
- w_input_gate: bfloat16 [2048, 8], replicated, may hold values from -0.125 to 0.125
- w_forget_gate: bfloat16 [2048, 8], replicated, may hold values from -0.125 to 0.125
- gate_bias: float32 [2, 8], replicated, may hold values from -1 to 120
- decay_shift: float32 [4, 16384, 8], P(None, 'sp'), may hold values from -2 to 0, as said below
- head_gain: float32 [1024], replicated, may hold values from 0.1 to 1.9
- w_out_conv: bfloat16 [1024, 2048], P(('fs', 'tp'), 'sp'), may hold values from -0.125 to 0.125
- w_out_mem: bfloat16 [1024, 2048], P(('fs', 'tp'), 'sp'), may hold values from -0.125 to 0.125
Outputs:
- output: bfloat16 [4, 16384, 2048], P('fs', ('sp', 'tp'))
Inputs may be any that keep to these rules, and one draw needn't show every extreme that they name: `decay_shift`: never positive.
All inputs are finite; a program needn't handle non-finite values.
Results may differ from a plain program's by a relative error of at most 0.015.
Values may be sent and summed in bfloat16 or wider, within the bound.
No kernel may reach another device: no remote copies, remote signals or barrier semaphores. Data moves between devices by JAX's collectives and lax.ppermute only.
A program may use at most 64 MiB of HBM per device.

v0:
```python
import jax
import jax.numpy as jnp
from jax import lax
from jax.sharding import Mesh
from jax.sharding import PartitionSpec as P

MEMORY_HEADS = 8
HEAD_DIM = 128
BLOCK = 64
SP = ("sp_0", "sp_1")
SP_TP = ("sp_0", "sp_1", "tp")


EPSILON = 1e-06
FAR_BELOW = -1e30
HIGHEST_PRECISION = lax.Precision.HIGHEST


def neutral_like(array, identity):
    return jax.tree.map(
        lambda part, zero: jnp.zeros_like(part) + jnp.asarray(zero, part.dtype), array, identity
    )


def collected_together(array, axis):
    leaves = jax.tree.leaves(array)
    sequence = sorted(range(len(leaves)), key=lambda k: -leaves[k].size)
    width = (1, *leaves[sequence[0]].shape)[-1]
    lines = [
        jnp.pad(leaves[k].reshape(-1), (0, -leaves[k].size % width)).reshape(-1, width)
        for k in sequence
    ]
    both, at, found = (lax.all_gather(jnp.concatenate(lines), axis), 0, {})
    for k, line in zip(sequence, lines):
        section = both[:, at : at + len(line)].reshape(len(both), -1)
        found[k] = section[:, : leaves[k].size].reshape(-1, *leaves[k].shape)
        at += len(line)
    numbers = iter(range(len(leaves)))
    return jax.tree.map(lambda _: found[next(numbers)], array)


def prefix_by_axis(array, axes, combine, identity):
    before = start = neutral_like(array, identity)
    subtotal = array
    for axis in reversed(axes):
        peers, here = (lax.axis_size(axis), lax.axis_index(axis))
        pieces = collected_together(subtotal, axis)
        inside, subtotal = (start, start)
        for k in range(peers):
            passed = k < here
            subtotal = combine(subtotal, jax.tree.map(lambda part: part[k], pieces))
            inside = jax.tree.map(lambda new, old: jnp.where(passed, new, old), subtotal, inside)
        before = combine(inside, before)
    return before


def from_everyone(array, axis):
    copies = jnp.broadcast_to(array, (lax.axis_size(axis), *array.shape))
    return lax.all_to_all(copies, axis, split_axis=0, concat_axis=0, tiled=True)


def laid_out(parts, dim):
    lengths = list(parts.shape[1:])
    lengths[dim] *= parts.shape[0]
    return jnp.moveaxis(parts, 0, dim).reshape(lengths)


def collect(array, axis, dim):
    parts = from_everyone(array, axis)
    return laid_out(parts, dim)


def in_one_piece(arrays, axis, dim, along):
    both = jnp.concatenate(arrays, axis=along)
    result, at, finished = (lax.all_gather(both, axis, axis=dim, tiled=True), 0, [])
    for a in arrays:
        finished.append(lax.slice_in_dim(result, at, at + a.shape[along], axis=along))
        at += a.shape[along]
    return tuple(finished)


def from_behind(array, axis, by):
    peers = lax.axis_size(axis)
    pairs = [(i, i + by) for i in range(peers) if 0 <= i + by < peers]
    return lax.ppermute(array, axis, pairs)


def in_one_piece_2(arrays, axis, split_dim, concat_dim, along):
    widths = [a.shape[along] for a in arrays]
    both = jnp.concatenate(arrays, axis=along)
    result = lax.all_to_all(both, axis, split_axis=split_dim, concat_axis=concat_dim, tiled=True)
    return tuple(jnp.split(result, [sum(widths[:k]) for k in range(1, len(widths))], axis=along))


def turned_gather(arrays, axis, dims):
    turned = [jnp.moveaxis(a, dim, 0) for a, dim in zip(arrays, dims)]
    widths = [t[0].size for t in turned]
    both = jnp.concatenate([t.reshape(-1, w) for t, w in zip(turned, widths)], axis=1)
    result = lax.all_gather(both, axis, axis=0, tiled=True)
    parts = jnp.split(result, [sum(widths[:k]) for k in range(1, len(widths))], axis=1)
    return tuple(
        (
            jnp.moveaxis(b.reshape(-1, *t.shape[1:]), 0, dim)
            for b, t, dim in zip(parts, turned, dims)
        )
    )


def cut_along(array, dim, peers):
    before, after = (array.shape[:dim], array.shape[dim + 1 :])
    return jnp.moveaxis(array.reshape(*before, peers, -1, *after), dim, 0)


def sum_at_owner(array, axis, dim):
    peers = lax.axis_size(axis)
    parts = lax.all_to_all(cut_along(array, dim, peers), axis, 0, 0, tiled=True)
    return jnp.sum(parts.astype(jnp.float32), axis=0)


def combine_states(earlier, later):
    total_one, peak_one, state_one = earlier
    total_two, peak_two, state_two = later
    peak_new = jnp.maximum(total_two + peak_one, peak_two)
    scale_old = jnp.exp(total_two + peak_one - peak_new)
    scale_new = jnp.exp(peak_two - peak_new)
    return (
        total_one + total_two,
        peak_new,
        scale_old[..., None, None] * state_one + scale_new[..., None, None] * state_two,
    )


def head_rows(values, seq_count, heads_here):
    tokens = values.shape[1]
    split_heads = values.reshape(seq_count, tokens, heads_here, HEAD_DIM).transpose(0, 2, 1, 3)
    return split_heads.reshape(seq_count * heads_here, tokens, HEAD_DIM).astype(jnp.float32)


def gate_rows(values, seq_count, heads_here):
    tokens = values.shape[1]
    return values.transpose(0, 2, 1).reshape(seq_count * heads_here, tokens)


def memory_cell(query_rows, key_rows, value_rows, entry_gate, log_forget):
    members = query_rows.shape[0]
    tokens = query_rows.shape[1]
    head_width = query_rows.shape[2]
    nblocks = tokens // BLOCK
    block_shape = (members, nblocks, BLOCK, head_width)
    query_blocks = query_rows.reshape(block_shape)
    key_blocks = key_rows.reshape(block_shape) * head_width ** (-0.5)
    value_blocks = value_rows.reshape(block_shape)
    entry_blocks = entry_gate.reshape(members, nblocks, BLOCK)
    forget_sums = jnp.cumsum(log_forget.reshape(members, nblocks, BLOCK), axis=-1)
    block_total = forget_sums[..., -1]
    local_logs = block_total[..., None] - forget_sums + entry_blocks
    local_peak = jnp.max(local_logs, axis=-1)
    local_weights = jnp.exp(local_logs - local_peak[..., None])
    local_state = jnp.einsum(
        "bclv,bclk->bcvk",
        local_weights[..., None] * value_blocks,
        key_blocks,
        precision=HIGHEST_PRECISION,
    )

    def advance(running, block_item):
        return (combine_states(running, block_item), running)

    zero_sums = jnp.zeros((members,), jnp.float32)
    low_peaks = jnp.full((members,), FAR_BELOW, jnp.float32)
    zero_states = jnp.zeros((members, head_width, head_width), jnp.float32)
    block_items = (
        jnp.moveaxis(block_total, 1, 0),
        jnp.moveaxis(local_peak, 1, 0),
        jnp.moveaxis(local_state, 1, 0),
    )
    device_total, inner_states = lax.scan(advance, (zero_sums, low_peaks, zero_states), block_items)
    inner_states = tuple((jnp.moveaxis(tensor, 0, 1) for tensor in inner_states))
    total_sum, total_peak, total_state = device_total
    before = prefix_by_axis(
        (total_sum, total_peak, total_state),
        SP,
        combine_states,
        (zero_sums, low_peaks, zero_states),
    )
    opening = combine_states((zero_sums, zero_sums, zero_states), before)
    opening = tuple((tensor[:, None] for tensor in opening))
    _, prior_peak, prior_state = combine_states(opening, inner_states)
    positions = jnp.arange(BLOCK)
    causal_mask = positions[:, None] >= positions[None, :]
    pair_logs = jnp.where(
        causal_mask,
        forget_sums[..., :, None] - forget_sums[..., None, :] + entry_blocks[..., None, :],
        -jnp.inf,
    )
    carried_logs = forget_sums + prior_peak[..., None]
    row_peak = jnp.maximum(carried_logs, jnp.max(pair_logs, axis=-1))
    inner_weights = jnp.exp(pair_logs - row_peak[..., None])
    carried_weights = jnp.exp(carried_logs - row_peak)
    scores = inner_weights * jnp.einsum(
        "bcld,bcsd->bcls", query_blocks, key_blocks, precision=HIGHEST_PRECISION
    )
    numerator = carried_weights[..., None] * jnp.einsum(
        "bcvk,bclk->bclv", prior_state, query_blocks, precision=HIGHEST_PRECISION
    ) + jnp.einsum("bcls,bcsv->bclv", scores, value_blocks, precision=HIGHEST_PRECISION)
    return numerator.reshape(members, tokens, head_width)


def shards(
    activations,
    norm_gain,
    w_conv_gate,
    w_conv_mult,
    w_conv_in,
    conv_taps,
    w_query,
    w_key,
    w_value,
    w_input_gate,
    w_forget_gate,
    gate_bias,
    decay_shift,
    head_gain,
    w_out_conv,
    w_out_mem,
):
    group_index = lax.axis_index(("fs", "tp"))
    heads_here = MEMORY_HEADS // (lax.axis_size("fs") * lax.axis_size("tp"))
    channels = w_conv_gate.shape[1]
    sequences = collect(activations, "fs", 0)
    seq_count = sequences.shape[0]
    tokens = sequences.shape[1]
    model_width = sequences.shape[2]
    row_count = seq_count * tokens
    flat_rows = sequences.reshape(row_count, model_width).astype(jnp.float32)
    normed = (
        flat_rows
        * lax.rsqrt(jnp.mean(flat_rows * flat_rows, axis=-1, keepdims=True) + EPSILON)
        * norm_gain
    ).astype(jnp.bfloat16)
    pieces = in_one_piece((w_conv_gate, w_conv_mult, w_conv_in, w_query, w_key, w_value), SP, 0, 1)
    projected = tuple(
        (jnp.dot(normed, shard_piece, preferred_element_type=jnp.float32) for shard_piece in pieces)
    )
    conv_gate, conv_mult, conv_in, query, keys_proj, value = [
        tensor.astype(jnp.bfloat16).reshape(seq_count, tokens, -1) for tensor in projected
    ]
    product = (conv_mult.astype(jnp.float32) * conv_in.astype(jnp.float32)).astype(jnp.bfloat16)
    ntaps = conv_taps.shape[0]
    rim_rows = from_behind(product[:, tokens - (ntaps - 1) :, :], SP, 1)
    padded = jnp.concatenate([rim_rows, product], axis=1).astype(jnp.float32)
    tap_weights = lax.dynamic_slice_in_dim(conv_taps, group_index * channels, channels, 1)
    mixed_sum = jnp.zeros((seq_count, tokens, channels), jnp.float32)
    for tap_index in range(ntaps):
        mixed_sum = (
            mixed_sum + tap_weights[tap_index] * padded[:, tap_index : tap_index + tokens, :]
        )
    conv_out = (conv_gate.astype(jnp.float32) * mixed_sum).astype(jnp.bfloat16)
    entry_cols = lax.dynamic_slice_in_dim(w_input_gate, group_index * heads_here, heads_here, 1)
    forget_cols = lax.dynamic_slice_in_dim(w_forget_gate, group_index * heads_here, heads_here, 1)
    gate_values = jnp.dot(
        normed,
        jnp.concatenate([entry_cols, forget_cols], axis=1),
        preferred_element_type=jnp.float32,
    ).reshape(seq_count, tokens, 2 * heads_here)
    bias_rows = lax.dynamic_slice_in_dim(gate_bias, group_index * heads_here, heads_here, 1)
    decay_rows = lax.dynamic_slice_in_dim(decay_shift, group_index * heads_here, heads_here, 2)
    entry = gate_values[..., :heads_here] + bias_rows[0]
    log_forget = jax.nn.log_sigmoid(gate_values[..., heads_here:] + bias_rows[1]) + decay_rows
    cell = memory_cell(
        head_rows(query, seq_count, heads_here),
        head_rows(keys_proj, seq_count, heads_here),
        head_rows(value, seq_count, heads_here),
        gate_rows(entry, seq_count, heads_here),
        gate_rows(log_forget, seq_count, heads_here),
    )
    cell = cell * lax.rsqrt(jnp.mean(cell * cell, axis=-1, keepdims=True) + EPSILON)
    gain_rows = lax.dynamic_slice_in_dim(
        head_gain, group_index * heads_here * HEAD_DIM, heads_here * HEAD_DIM, 0
    ).reshape(1, heads_here, 1, HEAD_DIM)
    scaled = cell.reshape(seq_count, heads_here, tokens, HEAD_DIM) * gain_rows
    mem_out = (
        scaled.transpose(0, 2, 1, 3)
        .reshape(seq_count, tokens, heads_here * HEAD_DIM)
        .astype(jnp.bfloat16)
    )
    conv_seq, mem_seq = in_one_piece_2((conv_out, mem_out), "fs", 0, 2, 1)
    rows_conv, rows_mem = in_one_piece((w_out_conv, w_out_mem), "fs", 0, 1)
    full_conv, full_mem = turned_gather((rows_conv, rows_mem), SP, (1, 1))
    conv_flat = conv_seq[0]
    mem_flat = mem_seq[0]
    output = sum_at_owner(
        (
            jnp.dot(conv_flat, full_conv, preferred_element_type=jnp.float32)
            + jnp.dot(mem_flat, full_mem, preferred_element_type=jnp.float32)
        ).astype(jnp.bfloat16),
        "tp",
        0,
    )
    return output.astype(jnp.bfloat16).reshape(1, output.shape[0], -1)


def solution(mesh):
    finer = Mesh(
        mesh.devices.reshape(8, 8, mesh.shape["fs"], mesh.shape["tp"]), ("sp_0", "sp_1", "fs", "tp")
    )
    return jax.shard_map(
        shards,
        mesh=finer,
        in_specs=(
            P("fs", SP, None),
            P(),
            P(SP, ("fs", "tp")),
            P(SP, ("fs", "tp")),
            P(SP, ("fs", "tp")),
            P(),
            P(SP, ("fs", "tp")),
            P(SP, ("fs", "tp")),
            P(SP, ("fs", "tp")),
            P(),
            P(),
            P(),
            P(None, SP, None),
            P(),
            P(("fs", "tp"), SP),
            P(("fs", "tp"), SP),
        ),
        out_specs=P("fs", SP_TP, None),
        check_vma=False,
    )
```

profile of v0, /device:TPU:1, one launch (start us, length us, event | category | flops | bytes accessed | tf_op | source)
XLA Modules:
  0.0 308.3 jit_solution(6878134085907053953)
XLA Ops:
  6.5 0.7 constant_dynamic-update-slice_fusion.5
  7.2 0.7 constant_dynamic-update-slice_fusion.4
  8.0 0.7 constant_dynamic-update-slice_fusion.3
  8.7 0.7 constant_dynamic-update-slice_fusion.2
  9.4 0.7 constant_dynamic-update-slice_fusion.1
  10.1 0.7 constant_dynamic-update-slice_fusion
  10.8 0.6 copy-done.18
  11.4 3.8 %broadcast_in_dim.25 = bf16[4,1,256,2048]{3,2,1,0:T(8,128)(2,1)} broadcast(bf16[256,2048]{1,0:T(8,128)(2,1)} %bitcast.546), dimensions={2,3} | broadcast | bytes 5242880 | tf_op jit(solution)/shard_map/broadcast_in_dim | solution.py:58
  15.2 5.0 %all-to-all-start = ((bf16[4,1,256,2048]{3,2,1,0:T(8,128)(2,1)}), bf16[4,1,256,2048]{3,2,1,0:T(8,128)(2,1)}, u32[]{:S(2)}, u32[]{:S(2)}) async-start(bf16[4,1,256,2048]{3,2,1,0:T(8,128)(2,1)} %broadcast_in_dim.25), calls=%async_computation | async-start | bytes 8388608 | tf_op jit(solution)/shard_map/all_to_all | solution.py:59
  20.4 0.5 fusion.98
  20.9 0.8 constant_dynamic-slice_fusion.3
  21.7 41.7 %all-to-all-done = bf16[4,1,256,2048]{3,2,1,0:T(8,128)(2,1)} async-done(((bf16[4,1,256,2048]{3,2,1,0:T(8,128)(2,1)}), bf16[4,1,256,2048]{3,2,1,0:T(8,128)(2,1)}, u32[]{:S(2)}, u32[]{:S(2)}) %all-to-all-start) | async-done | bytes 4194336 | tf_op jit(solution)/shard_map/all_to_all | solution.py:59
  63.5 3.1 multiply_reduce_fusion
  66.6 3.5 %fusion.12 = f32[4,256,2]{1,2,0:T(2,128)S(1)} fusion(bf16[4,1,256,2048]{3,2,1,0:T(8,128)(2,1)} %all-to-all-done, f32[2048]{0:T(1024)S(1)} %copy-done.19, f32[4,256]{1,0:T(4,128)S(1)} %get-tuple-element.237, bf16[2048,1]{0,1:T(2,128)(2,1)S(1)} %get-tuple-element.254, bf16[2048,1]{0,1:T(2,128)(2,1)S(1)} %get-tuple-element.255), kind=kOutput, calls=%fused_computation.23 | convolution fusion | flops 16793600 | bytes 4222976 | tf_op jit(solution)/shard_map/dot_general | solution.py:261
  70.0 2.0 fusion.65
  72.2 0.9 reduce_window_sum.11
  73.7 5.2 %fusion.11 = bf16[1024,2048]{1,0:T(8,128)(2,1)} fusion(bf16[4,1,256,2048]{3,2,1,0:T(8,128)(2,1)} %all-to-all-done, f32[2048]{0:T(1024)S(1)} %copy-done.19, f32[1024]{0:T(1024)S(1)} %bitcast.584), kind=kLoop, calls=%fused_computation.21 | loop fusion | flops 8388608 | bytes 8400896 | tf_op jit(solution)/shard_map/convert_element_type | solution.py:240
  79.0 19.4 %all-gather.9.cloned.1.call-done = bf16[2048,768]{1,0:T(8,128)(2,1)} async-done(((bf16[32,768]{1,0:T(8,128)(2,1)}), bf16[2048,768]{1,0:T(8,128)(2,1)}) %all-gather.9.cloned.1.call-update) | async-done | bytes 3145744 | tf_op jit(solution)/shard_map/all_gather | solution.py:75
  98.4 3.7 %fusion.23 = f32[1024,128]{1,0:T(8,128)S(1)} fusion(bf16[1024,2048]{1,0:T(8,128)(2,1)} %fusion.11, bf16[2048,768]{1,0:T(8,128)(2,1)} %all-gather.9.cloned.1.call-done), kind=kOutput, calls=%fused_computation.39 | convolution fusion | flops 537264128 | bytes 5242880 | tf_op jit(solution)/shard_map/dot_general | solution.py:243
  102.1 2.3 convolution_convert_fusion.2
  104.4 2.0 convolution_bitcast_fusion
  106.4 3.8 %while.21 = (s32[]{:T(128)}, f32[4]{0:T(128)S(1)}, f32[4]{0:T(128)S(1)}, f32[4,128,128]{2,1,0:T(8,128)S(1)}, f32[4,4]{1,0:T(4,128)S(1)}, /*index=5*/f32[4,4]{1,0...) while((s32[]{:T(128)}, f32[4]{0:T(128)S(1)}, ...), condition=%wide.region_4.5_spmd.clone, body=%wide.region_3.4_spmd.clone.sunk | while | flops 327711 | bytes 1311669 | solution.py:177
  106.5 0.7 bitcast_dynamic-update-slice_fusion.2
  107.4 0.7 bitcast_dynamic-update-slice_fusion.2
  108.4 0.7 bitcast_dynamic-update-slice_fusion.2
  109.3 0.7 bitcast_dynamic-update-slice_fusion.2
  110.3 0.7 maximum_bitcast_fusion
  111.1 39.8 %all-gather.13.cloned.1.call-done = f32[8,514,128]{2,1,0:T(8,128)} async-done(((f32[1,514,128]{2,1,0:T(8,128)}), f32[8,514,128]{2,1,0:T(8,128)}) %all-gather.13.cloned.1.call-update) | async-done | bytes 2105360 | tf_op jit(solution)/shard_map/all_gather | solution.py:33
  150.8 0.8 fusion.97
  153.4 2.7 fusion.43
  156.1 0.7 maximum_bitcast_fusion.1
  156.9 8.7 %all_gather.26 = bf16[512,64]{0,1:T(8,128)(2,1)S(1)} all-gather(bf16[128,64]{0,1:T(8,128)(2,1)S(1)} %pad_maximum_fusion.2), channel_id=1, replica_groups=mesh['sp_0'=8,'sp_1'=8,'fs'=4,'tp'=2] {'fs'}, dimensions={0}, use_global_device_ids=true | all-gather | bytes 81920 | tf_op jit(solution)/shard_map/all_gather | solution.py:75
  165.6 0.6 pad_maximum_fusion.1
  166.2 1.5 dynamic_slice.34
  167.8 0.6 slice_bitcast_fusion.8
  168.4 0.4 fusion.40
  168.8 3.5 %fusion.27 = f32[1024,128]{1,0:T(8,128)S(1)} fusion(bf16[1024,2048]{1,0:T(8,128)(2,1)} %fusion.11, bf16[2048,768]{1,0:T(8,128)(2,1)} %all-gather.9.cloned.1.call-done), kind=kOutput, calls=%fused_computation.46 | convolution fusion | flops 537133056 | bytes 5242880 | tf_op jit(solution)/shard_map/dot_general | solution.py:243
  172.3 2.3 fusion.26
  174.8 0.8 slice.361
  175.5 3.6 %collective-permute-start = (bf16[4,2,128]{1,2,0:T(8,128)(2,1)}, bf16[4,2,128]{1,2,0:T(8,128)(2,1)}, u32[]{:S(2)}, u32[]{:S(2)}) collective-permute-start(bf16[4,2,128]{1,2,0:T(8,128)(2,1)} %slice.361), channel_id=1, source_target_pairs={{0,8},{8,16},{16,24},{24,32},{32,40},{40,48},{48,56},{56,64},{64,7... | collective-permute-start | bytes 6152 | tf_op jit(solution)/shard_map/ppermute | solution.py:85
  179.2 4.3 %convolution_convert_fusion = bf16[1024,128]{1,0:T(8,128)(2,1)} fusion(bf16[1024,2048]{1,0:T(8,128)(2,1)} %fusion.11, bf16[2048,768]{1,0:T(8,128)(2,1)} %all-gather.9.cloned.1.call-done), kind=kOutput, calls=%fused_computation.36 | convolution fusion | flops 537001984 | bytes 4980736 | tf_op jit(solution)/shard_map/dot_general | solution.py:243
  183.5 3.2 %convolution_convert_fusion.5 = bf16[1024,128]{1,0:T(8,128)(2,1)} fusion(bf16[1024,2048]{1,0:T(8,128)(2,1)S(1)} %copy-done.5, bf16[2048,768]{1,0:T(8,128)(2,1)} %all-gather.9.cloned.1.call-done), kind=kOutput, calls=%fused_computation.47 | convolution fusion | flops 537001984 | bytes 4980736 | tf_op jit(solution)/shard_map/dot_general | solution.py:243
  186.6 1.1 copy.33
  187.7 1.1 maximum_convert_fusion
  188.8 1.7 fusion.35
  190.6 1.2 fusion.95
  191.8 10.4 %all-gather.15.cloned.1.call-done = f32[8,514,128]{2,1,0:T(8,128)} async-done(((f32[1,514,128]{2,1,0:T(8,128)}), f32[8,514,128]{2,1,0:T(8,128)}) %all-gather.15.cloned.1.call-update) | async-done | bytes 2105360 | tf_op jit(solution)/shard_map/all_gather | solution.py:33
  202.2 0.9 fusion.96
  203.1 0.7 exponential_multiply_fusion.2
  203.8 0.7 fusion.67
  204.6 0.8 subtract_exponential_fusion.14
  205.4 0.7 fusion.78
  206.1 0.7 subtract_exponential_fusion.12
  206.9 1.5 convolution_multiply_fusion.1
  208.4 0.4 fusion.99
  209.1 1.8 multiply_add_fusion
  210.9 1.3 multiply_reduce_fusion.1
  212.7 0.8 pad_maximum_fusion
  213.5 4.4 %all-to-all-start.1 = ((bf16[4,512,128]{1,2,0:T(8,128)(2,1)}), bf16[4,512,128]{1,2,0:T(8,128)(2,1)S(1)}, u32[]{:S(2)}, u32[]{:S(2)}) async-start(bf16[4,512,128]{1,2,0:T(8,128)(2,1)} %pad_maximum_fusion), calls=%async_computation.1 | async-start | bytes 1048576 | tf_op jit(solution)/shard_map/all_to_all | solution.py:91
  217.9 70.2 %all-gather.11.cloned.1.call-done = bf16[2048,1024]{1,0:T(8,128)(2,1)} async-done(((bf16[32,1024]{1,0:T(8,128)(2,1)}), bf16[2048,1024]{1,0:T(8,128)(2,1)}) %all-gather.11.cloned.1.call-update) | async-done | bytes 4194320 | tf_op jit(solution)/shard_map/all_gather | solution.py:99
  288.1 2.5 fusion.19
  290.9 0.8 fusion.17
  291.7 9.0 %all_to_all.28 = bf16[2,128,2048]{2,1,0:T(8,128)(2,1)S(1)} all-to-all(bf16[2,128,2048]{2,1,0:T(8,128)(2,1)S(1)} %bitcast.540), channel_id=1, replica_groups=mesh['sp_0'=8,'sp_1'=8,'fs'=4,'tp'=2] {'tp'}, dimensions={0} | all-to-all | bytes 2097152 | tf_op jit(solution)/shard_map/all_to_all | solution.py:116
  300.7 1.1 reduce_sum.32
  (163 shorter events, 4.8 us)
Async XLA Ops:
  6.5 161.2 %copy-start = (f32[3,1024]{1,0:T(4,128)S(1)}, f32[3,1024]{1,0:T(4,128)}, u32[]{:S(2)}) copy-start(f32[3,1024]{1,0:T(4,128)} %param.23) | copy-start | bytes 36868
  6.5 91.8 %all-gather.9.cloned.1.call-start = ((), (), s32[]{:S(2)}) async-start(), calls=%async_computation.3 | async-start | bytes 3194880 | tf_op jit(solution)/shard_map/all_gather | solution.py:75
  10.8 0.6 copy-start.18
  15.2 5.1 %copy-start.38 = (f32[2,8]{1,0:T(2,128)S(1)}, f32[2,8]{1,0:T(2,128)}, u32[]{:S(2)}) copy-start(f32[2,8]{1,0:T(2,128)} %param.29) | copy-start | bytes 196
  15.2 48.3 %all-to-all-start = ((bf16[4,1,256,2048]{3,2,1,0:T(8,128)(2,1)}), bf16[4,1,256,2048]{3,2,1,0:T(8,128)(2,1)}, u32[]{:S(2)}, u32[]{:S(2)}) async-start(bf16[4,1,256,2048]{3,2,1,0:T(8,128)(2,1)} %broadcast_in_dim.25), calls=%async_computation | async-start | bytes 8388608 | tf_op jit(solution)/shard_map/all_to_all | solution.py:59
  20.2 46.3 %copy-start.19 = (f32[2048]{0:T(1024)S(1)}, f32[2048]{0:T(1024)}, u32[]{:S(2)}) copy-start(f32[2048]{0:T(1024)} %param.19) | copy-start | bytes 24580
  20.2 130.6 %all-gather.13.cloned.1.call-start = ((), (), s32[]{:S(2)}) async-start(), calls=%async_computation.5 | async-start | bytes 2396160 | tf_op jit(solution)/shard_map/all_gather | solution.py:33
  98.4 3.7 %copy-start.3 = (bf16[1024,2048]{1,0:T(8,128)(2,1)S(1)}, bf16[1024,2048]{1,0:T(8,128)(2,1)}, u32[]{:S(2)}) copy-start(bf16[1024,2048]{1,0:T(8,128)(2,1)} %fusion.11) | copy-start | bytes 12582916
  104.4 2.0 copy-start.8
  106.4 50.5 %copy-start.20 = (bf16[128,32]{0,1:T(8,128)(2,1)S(1)}, bf16[128,32]{0,1:T(8,128)(2,1)}, u32[]{:S(2)}) copy-start(bf16[128,32]{0,1:T(8,128)(2,1)} %param.33) | copy-start | bytes 24580
  106.4 50.5 %copy-start.21 = (bf16[128,32]{0,1:T(8,128)(2,1)S(1)}, bf16[128,32]{0,1:T(8,128)(2,1)}, u32[]{:S(2)}) copy-start(bf16[128,32]{0,1:T(8,128)(2,1)} %param.32) | copy-start | bytes 24580
  110.2 0.8 copy-start.37
  111.0 91.1 %all-gather.15.cloned.1.call-start = ((), (), s32[]{:S(2)}) async-start(), calls=%async_computation.6 | async-start | bytes 2396160 | tf_op jit(solution)/shard_map/all_gather | solution.py:33
  151.7 1.1 copy-start.33
  151.7 0.6 copy-start.30
  151.8 0.6 copy-start.29
  151.8 0.7 copy-start.28
  151.8 0.8 copy-start.27
  151.8 0.8 copy-start.26
  151.8 0.9 copy-start.32
  151.8 0.9 copy-start.31
  151.8 1.1 copy-start.25
  151.9 1.1 copy-start.24
  151.9 15.9 %copy-start.22 = (f32[4]{0:T(128)}, f32[4]{0:T(128)S(1)}, u32[]{:S(2)}) copy-start(f32[4]{0:T(128)S(1)} %get-tuple-element.233) | copy-start | bytes 52
  151.9 15.9 %copy-start.23 = (f32[4]{0:T(128)}, f32[4]{0:T(128)S(1)}, u32[]{:S(2)}) copy-start(f32[4]{0:T(128)S(1)} %get-tuple-element.234) | copy-start | bytes 52
  156.8 131.3 %all-gather.11.cloned.1.call-start = ((), (), s32[]{:S(2)}) async-start(), calls=%async_computation.4 | async-start | bytes 4259840 | tf_op jit(solution)/shard_map/all_gather | solution.py:99
  166.2 6.1 %copy-start.4 = (bf16[1024,2048]{1,0:T(8,128)(2,1)S(1)}, bf16[1024,2048]{1,0:T(8,128)(2,1)}, u32[]{:S(2)}) copy-start(bf16[1024,2048]{1,0:T(8,128)(2,1)} %fusion.11) | copy-start | bytes 12582916
  174.8 8.7 %copy-start.5 = (bf16[1024,2048]{1,0:T(8,128)(2,1)S(1)}, bf16[1024,2048]{1,0:T(8,128)(2,1)}, u32[]{:S(2)}) copy-start(bf16[1024,2048]{1,0:T(8,128)(2,1)} %fusion.11) | copy-start | bytes 12582916
  175.5 12.2 %collective-permute-start = (bf16[4,2,128]{1,2,0:T(8,128)(2,1)}, bf16[4,2,128]{1,2,0:T(8,128)(2,1)}, u32[]{:S(2)}, u32[]{:S(2)}) collective-permute-start(bf16[4,2,128]{1,2,0:T(8,128)(2,1)} %slice.361), channel_id=1, source_target_pairs={{0,8},{8,16},{16,24},{24,32},{32,40},{40,48},{48,56},{56,64},{64,7... | collective-permute-start | bytes 6152 | tf_op jit(solution)/shard_map/ppermute | solution.py:85
  183.5 5.4 %copy-start.36 = (f32[128]{0:T(128)S(1)}, f32[128]{0:T(128)}, u32[]{:S(2)}) copy-start(f32[128]{0:T(128)} %get-tuple-element.240) | copy-start | bytes 1540
  183.5 7.1 %copy-start.1 = (f32[8,514,128]{2,1,0:T(8,128)S(1)}, f32[8,514,128]{2,1,0:T(8,128)}, u32[]{:S(2)}) copy-start(f32[8,514,128]{2,1,0:T(8,128)} %all-gather.13.cloned.1.call-done) | copy-start | bytes 6316036
  188.8 19.6 %copy-start.9 = (bf16[1024,128]{1,0:T(8,128)(2,1)S(1)}, bf16[1024,128]{1,0:T(8,128)(2,1)}, u32[]{:S(2)}) copy-start(bf16[1024,128]{1,0:T(8,128)(2,1)} %copy-done.8) | copy-start | bytes 786436
  202.2 6.6 %copy-start.6 = (f32[8,514,128]{2,1,0:T(8,128)S(1)}, f32[8,514,128]{2,1,0:T(8,128)}, u32[]{:S(2)}) copy-start(f32[8,514,128]{2,1,0:T(8,128)} %all-gather.15.cloned.1.call-done) | copy-start | bytes 6316036
  203.8 0.7 copy-start.34
  204.6 4.5 %copy-start.10 = (f32[1,512,128]{2,1,0:T(8,128)S(1)}, f32[1,512,128]{2,1,0:T(8,128)}, u32[]{:S(2)}) copy-start(f32[1,512,128]{2,1,0:T(8,128)} %get-tuple-element.192) | copy-start | bytes 786436
  204.6 4.5 %copy-start.11 = (f32[1,512,128]{2,1,0:T(8,128)S(1)}, f32[1,512,128]{2,1,0:T(8,128)}, u32[]{:S(2)}) copy-start(f32[1,512,128]{2,1,0:T(8,128)} %get-tuple-element.193) | copy-start | bytes 786436
  204.6 4.5 %copy-start.12 = (f32[1,512,128]{2,1,0:T(8,128)S(1)}, f32[1,512,128]{2,1,0:T(8,128)}, u32[]{:S(2)}) copy-start(f32[1,512,128]{2,1,0:T(8,128)} %get-tuple-element.194) | copy-start | bytes 786436
  204.6 4.5 %copy-start.13 = (f32[1,512,128]{2,1,0:T(8,128)S(1)}, f32[1,512,128]{2,1,0:T(8,128)}, u32[]{:S(2)}) copy-start(f32[1,512,128]{2,1,0:T(8,128)} %get-tuple-element.195) | copy-start | bytes 786436
  204.6 4.5 %copy-start.14 = (f32[1,512,128]{2,1,0:T(8,128)S(1)}, f32[1,512,128]{2,1,0:T(8,128)}, u32[]{:S(2)}) copy-start(f32[1,512,128]{2,1,0:T(8,128)} %get-tuple-element.196) | copy-start | bytes 786436
  204.6 4.5 %copy-start.15 = (f32[1,512,128]{2,1,0:T(8,128)S(1)}, f32[1,512,128]{2,1,0:T(8,128)}, u32[]{:S(2)}) copy-start(f32[1,512,128]{2,1,0:T(8,128)} %get-tuple-element.197) | copy-start | bytes 786436
  204.6 4.5 %copy-start.35 = (f32[4]{0:T(128)S(1)}, f32[4]{0:T(128)}, u32[]{:S(2)}) copy-start(f32[4]{0:T(128)} %get-tuple-element.157) | copy-start | bytes 52
  208.8 2.1 copy-start.7
  208.8 2.1 copy-start.17
  209.0 3.6 %copy-start.39 = (f32[128]{0:T(128)S(1)}, f32[128]{0:T(128)}, u32[]{:S(2)}) copy-start(f32[128]{0:T(128)} %dynamic_slice.34) | copy-start | bytes 1540
  209.1 3.6 %copy-start.16 = (bf16[4,256,128]{1,2,0:T(8,128)(2,1)S(1)}, bf16[4,256,128]{1,2,0:T(8,128)(2,1)}, u32[]{:S(2)}) copy-start(bf16[4,256,128]{1,2,0:T(8,128)(2,1)} %fusion.35) | copy-start | bytes 786436
  213.5 74.6 %all-to-all-start.1 = ((bf16[4,512,128]{1,2,0:T(8,128)(2,1)}), bf16[4,512,128]{1,2,0:T(8,128)(2,1)S(1)}, u32[]{:S(2)}, u32[]{:S(2)}) async-start(bf16[4,512,128]{1,2,0:T(8,128)(2,1)} %pad_maximum_fusion), calls=%async_computation.1 | async-start | bytes 1048576 | tf_op jit(solution)/shard_map/all_to_all | solution.py:91
  288.1 2.8 copy-start.2
Sparse Core Ops, SparseCore 0:
  11.5 86.7 all-gather.8
  111.1 39.6 all-gather.12
  156.9 45.1 all-gather.14
  205.1 82.9 all-gather.10
where the time goes:
time: 310 us; the launch traced here: 308 us
  waiting for transfers between devices  182 us (59%)
  matrix products  31.2 us (10%)
  other arithmetic  30.5 us (10%)
  local copies, waits for them, and re-layouts  20.3 us (7%)
  blocking collectives  17.7 us (6%)
  between operations  13.9 us (4%)
  starting transfers between devices  13.1 us (4%)
    all_gather x1, waiting for transfers between devices, turned_gather(): result = lax.all_gather(both, axis, axis=0, tiled=True)  70.2 us
    all_gather x2, waiting for transfers between devices, collected_together(): both, at, found = (lax.all_gather(jnp.concatenate(lines), axis), 0, {})  50.2 us
    all_to_all x1, waiting for transfers between devices, from_everyone(): return lax.all_to_all(copies, axis, split_axis=0, concat_axis=0, tiled=True)  41.7 us
    all_gather x1, waiting for transfers between devices, in_one_piece(): lax.all_gather(both, axis, axis=dim, tiled=True)  19.4 us
    dot_general x6, matrix products, shards(): jnp.dot(normed, shard_piece, preferred_element_type=jnp.float32)  19.3 us
    all_to_all x1, blocking collectives, sum_at_owner(): parts = lax.all_to_all(cut_along(array, dim, peers), axis, 0, 0, tiled=True)  9.01 us
    all_gather x1, blocking collectives, in_one_piece(): lax.all_gather(both, axis, axis=dim, tiled=True)  8.65 us
  transfers between devices with their start and end apart: 7, of which 5 were waited for; matrix products, arithmetic and copies ran while one was open for 18% of the time, Pallas kernels for 0%

commit v1 on v0

v1 whole, which is shorter than its diff:
```python
import jax
import jax.numpy as jnp
from jax import lax
from jax.experimental import pallas as pl
from jax.experimental.pallas import tpu as pltpu
from jax.sharding import Mesh
from jax.sharding import PartitionSpec as P


HEAD_DIM = 128
SP = ("sp_0", "sp_1")
SP_TP = ("sp_0", "sp_1", "tp")
EPSILON = 1e-06
HIGHEST = lax.Precision.HIGHEST
F32 = jnp.float32
BF16 = jnp.bfloat16


def everyone(array, axis):
    copies = jnp.broadcast_to(array, (lax.axis_size(axis), *array.shape))
    return lax.all_to_all(copies, axis, split_axis=0, concat_axis=0, tiled=True)


def exchanged(array, axis):
    return lax.all_to_all(array, axis, split_axis=0, concat_axis=0, tiled=True)


def other_core(array):
    return lax.ppermute(array, "tp", [(0, 1), (1, 0)])


def from_behind(array, axis):
    peers = lax.axis_size(axis)
    return lax.ppermute(array, axis, [(i, i + 1) for i in range(peers - 1)])


def thirds(x):
    first = lax.reduce_precision(x, 8, 7)
    second = lax.reduce_precision(x - first, 8, 7)
    third = lax.reduce_precision(x - first - second, 8, 7)
    return jnp.stack([first, second, third])


def dot(a, b, dims):
    return lax.dot_general(a, b, dims, preferred_element_type=F32)


def ring(array, axis, by):
    peers = lax.axis_size(axis)
    return lax.ppermute(array, axis, [(i, (i + by) % peers) for i in range(peers)])


def around(array, axis):
    behind = ring(array, axis, 1)
    ahead = ring(array, axis, -1)
    cut = array.shape[0] // 2
    far = jnp.concatenate(
        [ring(behind[:cut], axis, 1), ring(ahead[cut:], axis, -1)], axis=0
    )
    return behind, ahead, far


def returned(blocks, axis):
    own, behind, ahead, far = blocks
    return own, ring(ahead, axis, 1), ring(behind, axis, -1), ring(far, axis, 2)


def project_kernel(core, *refs):
    pieces, weights, gate_rows, out, gates = refs[:8], refs[8], refs[9], refs[10], refs[11]
    half = pieces[0].shape[1]
    first = pl.multiple_of(core[0] * half, half)
    second = pl.multiple_of((1 - core[0]) * half, half)
    for k in range(4):
        a, b = pieces[2 * k][...], pieces[2 * k + 1][...]
        mixed = jnp.dot(a, weights[pl.ds(first, half), :], preferred_element_type=F32)
        mixed += jnp.dot(b, weights[pl.ds(second, half), :], preferred_element_type=F32)
        out[k] = mixed.astype(BF16)
        dims = (((1,), (1,)), ((), ()))
        rows = dot(gate_rows[core[0]], a, dims)
        gates[k] = rows + dot(gate_rows[1 - core[0]], b, dims)


def project_only_kernel(core, *refs):
    pieces, weights, out = refs[:8], refs[8], refs[9]
    half = pieces[0].shape[1]
    first = pl.multiple_of(core[0] * half, half)
    second = pl.multiple_of((1 - core[0]) * half, half)
    for k in range(4):
        mixed = jnp.dot(
            pieces[2 * k][...], weights[pl.ds(first, half), :], preferred_element_type=F32
        )
        mixed += jnp.dot(
            pieces[2 * k + 1][...], weights[pl.ds(second, half), :], preferred_element_type=F32
        )
        out[k] = mixed.astype(BF16)


def in_vmem(count):
    return [pl.BlockSpec(memory_space=pltpu.VMEM)] * count


def project(core, pieces, weights, gate_rows=None):
    tokens = pieces[0].shape[0]
    shape = jax.ShapeDtypeStruct((4, tokens, weights.shape[1]), BF16)
    smem = [pl.BlockSpec(memory_space=pltpu.SMEM)]
    flops = 8 * tokens * weights.size
    cost = pl.CostEstimate(flops=flops, bytes_accessed=6 << 20, transcendentals=0)
    if gate_rows is None:
        return pl.pallas_call(
            project_only_kernel,
            out_shape=shape,
            in_specs=smem + in_vmem(9),
            out_specs=in_vmem(1)[0],
            cost_estimate=cost,
        )(core, *pieces, weights)
    return pl.pallas_call(
        project_kernel,
        out_shape=(shape, jax.ShapeDtypeStruct((4, gate_rows.shape[1], tokens), F32)),
        in_specs=smem + in_vmem(10),
        out_specs=in_vmem(2),
        cost_estimate=cost,
    )(core, *pieces, weights, gate_rows)


def shards(
    activations,
    norm_gain,
    w_conv_gate,
    w_conv_mult,
    w_conv_in,
    conv_taps,
    w_query,
    w_key,
    w_value,
    w_input_gate,
    w_forget_gate,
    gate_bias,
    decay_shift,
    head_gain,
    w_out_conv,
    w_out_mem,
):
    head = lax.axis_index("fs") * lax.axis_size("tp") + lax.axis_index("tp")
    core = lax.axis_index("tp")
    tokens, width = activations.shape[1:]
    half = width // 2
    seqs = lax.axis_size("fs")

    place_x = lax.axis_index("fs")
    order = [(place_x + by) % seqs for by in (0, seqs - 1, 1, 2)]

    w_conv = jnp.concatenate([w_conv_gate, w_conv_mult, w_conv_in], axis=1)
    w_conv = lax.all_gather(w_conv, SP, axis=0, tiled=True)
    w_mem = everyone(jnp.concatenate([w_query, w_key, w_value], axis=1), SP)
    w_mem = w_mem.reshape(width, -1)

    turned = jnp.concatenate([w_out_conv.T, w_out_mem.T], axis=1)
    turned, w_mem = lax.optimization_barrier((turned, w_mem))
    w_own = everyone(turned, SP).reshape(width, -1)
    w_out = (w_own, *around(w_own, "fs"))

    x = activations[0].astype(F32)
    normed = (
        x * lax.rsqrt(jnp.mean(x * x, axis=-1, keepdims=True) + EPSILON) * norm_gain
    ).astype(BF16)
    mine = lax.dynamic_slice_in_dim(normed, core * half, half, 1)
    pieces = [mine, lax.dynamic_slice_in_dim(normed, (1 - core) * half, half, 1)]
    for piece in around(mine, "fs"):
        pieces += [piece, other_core(piece)]
    core_row = core.reshape(1).astype(jnp.int32)

    gate_rows = jnp.concatenate(
        [
            lax.dynamic_slice_in_dim(w_input_gate, head, 1, 1),
            lax.dynamic_slice_in_dim(w_forget_gate, head, 1, 1),
        ],
        axis=1,
    ).T
    gate_rows = jnp.pad(gate_rows, ((0, 14), (0, 0))).reshape(16, 2, half).transpose(1, 0, 2)
    qkv, gates = project(core_row, pieces, w_mem, gate_rows)
    query, key, value = (qkv[..., k * HEAD_DIM : (k + 1) * HEAD_DIM] for k in range(3))
    bias = lax.dynamic_slice_in_dim(gate_bias, head, 1, 1)
    decay = lax.dynamic_slice_in_dim(decay_shift, head, 1, 2)[..., 0]
    decay = jnp.concatenate([lax.dynamic_slice_in_dim(decay, k, 1, 0) for k in order], axis=0)
    entry = gates[:, 0] + bias[0]
    log_forget = jax.nn.log_sigmoid(gates[:, 1] + bias[1]) + decay
    sums = jnp.cumsum(log_forget, axis=-1)
    total = sums[:, -1]
    local_logs = total[:, None] - sums + entry
    peak = jnp.max(local_logs, axis=-1)
    scale = HEAD_DIM ** (-0.5)
    local_weights = jnp.exp(local_logs - peak[:, None]) * scale

    weighted = (local_weights[..., None] * value.astype(F32)).astype(BF16)
    state = dot(weighted, key, (((1,), (1,)), ((0,), (0,))))

    places = lax.axis_size(SP)
    cut = HEAD_DIM // places
    slices = state.astype(BF16).reshape(seqs, places, cut, HEAD_DIM).transpose(1, 0, 2, 3)
    slices = slices.reshape(places, seqs * cut, HEAD_DIM)
    numbers = thirds(jnp.stack([total, peak])).astype(BF16).reshape(1, 1, -1)
    count = numbers.shape[2]
    numbers = jnp.pad(numbers, ((0, 0), (0, seqs * cut - 1), (0, HEAD_DIM - count)))
    numbers = jnp.broadcast_to(numbers, slices.shape)
    packed = jnp.concatenate([slices, numbers], axis=1)
    everywhere = exchanged(packed, SP)
    found = everywhere[:, seqs * cut, :count].astype(F32).reshape(places, 3, 2, seqs)
    found = found[:, 0] + found[:, 1] + found[:, 2]
    totals, peaks = found[:, 0].T, found[:, 1].T
    spots = jnp.arange(places)
    earlier = spots[:, None] > spots[None, :]
    masked = jnp.where(earlier, totals[:, None, :], 0.0)
    between = lax.dot_general(
        masked, earlier.astype(F32), (((2,), (0,)), ((), ())), precision=HIGHEST
    )
    since_start = jnp.sum(masked, axis=-1)
    logs = jnp.where(earlier, between + peaks[:, None, :], -jnp.inf)
    carried_peak = jnp.maximum(since_start, jnp.max(logs, axis=-1))
    mixing = jnp.exp(logs - carried_peak[..., None]).astype(BF16)
    states = everywhere[:, : seqs * cut].reshape(places, seqs, cut * HEAD_DIM)
    carried = dot(mixing, states, (((2,), (0,)), ((0,), (1,)))).astype(BF16)
    carried = carried.transpose(1, 0, 2).reshape(places, seqs * cut, HEAD_DIM)
    carried = exchanged(carried, SP)
    carried = carried.reshape(places, seqs, cut, HEAD_DIM).transpose(1, 0, 2, 3)
    prior_state = carried.reshape(seqs, HEAD_DIM, HEAD_DIM)
    place = lax.axis_index(SP)
    prior_peak = lax.dynamic_slice_in_dim(carried_peak, place, 1, 1)

    conv = project(core_row, pieces, w_conv)
    channels = conv.shape[2] // 3
    gate, mult, inlet = (conv[..., k * channels : (k + 1) * channels] for k in range(3))
    product = (mult.astype(F32) * inlet.astype(F32)).astype(BF16)
    taps = conv_taps.shape[0]
    rim = from_behind(product[:, tokens - (taps - 1) :], SP)
    padded = jnp.concatenate([rim, product], axis=1).astype(F32)
    tap_rows = lax.dynamic_slice_in_dim(conv_taps, head * channels, channels, 1)
    mixed = tap_rows[0] * padded[:, :tokens]
    for j in range(1, taps):
        mixed = mixed + tap_rows[j] * padded[:, j : j + tokens]
    conv_out = (gate.astype(F32) * mixed).astype(BF16)
    last = (((1,), (1,)), ((), ()))
    conv_parts = returned([conv_out[k] for k in range(seqs)], "fs")
    output = sum(dot(a, w[:, :channels], last) for a, w in zip(conv_parts, w_out))

    spans = jnp.arange(tokens)
    causal = spans[:, None] >= spans[None, :]
    pair_logs = jnp.where(
        causal, sums[:, :, None] - sums[:, None, :] + entry[:, None, :], -jnp.inf
    )
    carried_logs = sums + prior_peak
    row_peak = jnp.maximum(carried_logs, jnp.max(pair_logs, axis=-1))
    inner_weights = jnp.exp(pair_logs - row_peak[..., None]) * scale
    carried_weights = jnp.exp(carried_logs - row_peak)
    scores = inner_weights * dot(query, key, (((2,), (2,)), ((0,), (0,))))
    cell = carried_weights[..., None] * dot(query, prior_state, (((2,), (2,)), ((0,), (0,))))
    cell = cell + dot(scores.astype(BF16), value, (((2,), (1,)), ((0,), (0,))))
    cell = cell * lax.rsqrt(jnp.mean(cell * cell, axis=-1, keepdims=True) + EPSILON)
    gain = lax.dynamic_slice_in_dim(head_gain, head * HEAD_DIM, HEAD_DIM, 0)
    mem_out = (cell * gain).astype(BF16)
    mem_parts = returned([mem_out[k] for k in range(seqs)], "fs")
    output = output + sum(dot(a, w[:, channels:], last) for a, w in zip(mem_parts, w_out))

    cores = lax.axis_size("tp")
    parts = exchanged(output.astype(BF16).reshape(cores, tokens // cores, width), "tp")
    return jnp.sum(parts.astype(F32), axis=0).astype(BF16)[None]


def solution(mesh):
    finer = Mesh(
        mesh.devices.reshape(8, 8, mesh.shape["fs"], mesh.shape["tp"]), ("sp_0", "sp_1", "fs", "tp")
    )
    weights = P(SP, ("fs", "tp"))
    return jax.shard_map(
        shards,
        mesh=finer,
        in_specs=(
            P("fs", SP, None),
            P(),
            weights,
            weights,
            weights,
            P(),
            weights,
            weights,
            weights,
            P(),
            P(),
            P(),
            P(None, SP, None),
            P(),
            P(("fs", "tp"), SP),
            P(("fs", "tp"), SP),
        ),
        out_specs=P("fs", SP_TP, None),
        check_vma=False,
    )
```

time: 310 us -> 234 us (0.75); the launches traced: 308 us -> 229 us
  waiting for transfers between devices: 182 us -> 59.2 us
  starting transfers between devices: 13.1 us -> 94.3 us
  matrix products: 31.2 us -> 8.11 us
  other arithmetic: 30.5 us -> 12 us
  Pallas kernels: 0 us -> 12.9 us
  local copies, waits for them, and re-layouts: 20.3 us -> 14.5 us
  blocking collectives: 17.7 us -> 13.9 us
    all_gather x4 -> x1, waiting for transfers between devices: 140 us -> 0.02 us  [shards(): w_conv = lax.all_gather(w_conv, SP, axis=0, tiled=True)]
    ppermute x1 -> x18, starting transfers between devices: 3.62 us -> 55.7 us  [the longest x14 44.5 us: ring(): lax.ppermute(array, axis, [(i, (i + by) % peers) for i in range(peers)])]
    ppermute x1 -> x18, waiting for transfers between devices: 0.01 us -> 34.8 us  [the longest x14 28.8 us: ring(): lax.ppermute(array, axis, [(i, (i + by) % peers) for i in range(peers)])]
    all_to_all x2 -> x4, starting transfers between devices: 9.37 us -> 38.6 us  [the longest x2 22.1 us: everyone(): return lax.all_to_all(copies, axis, split_axis=0, concat_axis=0, tiled=True)]
    dot_general x13, matrix products: 31.2 us -> 8.11 us  [the longest x12 7.8 us: dot(): return lax.dot_general(a, b, dims, preferred_element_type=F32)]
    all_to_all x2 -> x4, waiting for transfers between devices: 41.7 us -> 24.4 us  [the longest x2 23.7 us: exchanged(): return lax.all_to_all(array, axis, split_axis=0, concat_axis=0, tiled=True)]
    pallas_call x0 -> x2, Pallas kernels: none -> 12.9 us  [the longest x1 6.94 us: project(): pl.pallas_call(project_kernel, out_shape=(shape, jax.ShapeDtypeStruct((4,...]
    all_gather x1 -> x0, blocking collectives: 8.65 us -> none  [in_one_piece(): lax.all_gather(both, axis, axis=dim, tiled=True)]
  transfers between devices with their start and end apart: 7 -> 23, of which waited for: 5 -> 8; matrix products, arithmetic and copies ran while one was open for 18% -> 13% of each run, Pallas kernels for 0% -> 6%
where the time goes in v1:
time: 234 us; the launch traced here: 229 us
  starting transfers between devices  94.3 us (40%)
  waiting for transfers between devices  59.2 us (25%)
  local copies, waits for them, and re-layouts  14.5 us (6%)
  between operations  14.2 us (6%)
  blocking collectives  13.9 us (6%)
  Pallas kernels  12.9 us (6%)
  other arithmetic  12 us (5%)
  matrix products  8.11 us (3%)
    ppermute x14, starting transfers between devices, ring(): lax.ppermute(array, axis, [(i, (i + by) % peers) for i in range(peers)])  44.5 us
    ppermute x14, waiting for transfers between devices, ring(): lax.ppermute(array, axis, [(i, (i + by) % peers) for i in range(peers)])  28.8 us
    all_to_all x2, waiting for transfers between devices, exchanged(): return lax.all_to_all(array, axis, split_axis=0, concat_axis=0, tiled=True)  23.7 us
    all_to_all x2, starting transfers between devices, everyone(): return lax.all_to_all(copies, axis, split_axis=0, concat_axis=0, tiled=True)  22.1 us
    all_to_all x2, starting transfers between devices, exchanged(): return lax.all_to_all(array, axis, split_axis=0, concat_axis=0, tiled=True)  16.5 us
    all_to_all x1, blocking collectives, exchanged(): return lax.all_to_all(array, axis, split_axis=0, concat_axis=0, tiled=True)  13.9 us
    ppermute x3, starting transfers between devices, other_core(): return lax.ppermute(array, 'tp', [(0, 1), (1, 0)])  8.6 us
    dot_general x12, matrix products, dot(): return lax.dot_general(a, b, dims, preferred_element_type=F32)  7.8 us
  transfers between devices with their start and end apart: 23, of which 8 were waited for; matrix products, arithmetic and copies ran while one was open for 13% of the time, Pallas kernels for 6%

profile of v1, /device:TPU:1, one launch (start us, length us, event | category | flops | bytes accessed | tf_op | source)
XLA Modules:
  0.0 229.2 jit_solution(4312257653395586187)
XLA Ops:
  6.5 0.7 pad_maximum_fusion.2
  7.3 1.3 broadcast_in_dim.66
  8.6 17.3 %all-to-all-start = ((bf16[64,32,384]{2,1,0:T(8,128)(2,1)}), bf16[64,32,384]{2,1,0:T(8,128)(2,1)S(1)}, u32[]{:S(2)}, u32[]{:S(2)}) async-start(bf16[64,32,384]{2,1,0:T(8,128)(2,1)} %broadcast_in_dim.66), calls=%async_computation | async-start | bytes 3145728 | tf_op jit(solution)/shard_map/all_to_all | solution.py:21
  26.6 0.9 constant_dynamic-slice_fusion.9
  27.5 3.1 %collective-permute-start = (bf16[256,1024]{1,0:T(8,128)(2,1)S(1)}, bf16[256,1024]{1,0:T(8,128)(2,1)S(1)}, u32[]{:S(2)}, u32[]{:S(2)}) collective-permute-start(bf16[256,1024]{1,0:T(8,128)(2,1)S(1)} %get-tuple-element.16.refs_0_), channel_id=1, source_target_pairs={{0,2},{2,4},{4,6},{6,0},{1,3},{3,5},{5,7},{7,1},{8,10},{10,12},{12... | collective-permute-start | bytes 1572872 | tf_op jit(solution)/shard_map/ppermute | solution.py:50
  30.6 3.4 %collective-permute-start.2 = (bf16[256,1024]{1,0:T(8,128)(2,1)S(1)}, bf16[256,1024]{1,0:T(8,128)(2,1)S(1)}, u32[]{:S(2)}, u32[]{:S(2)}) collective-permute-start(bf16[256,1024]{1,0:T(8,128)(2,1)S(1)} %get-tuple-element.16.refs_0_), channel_id=1, source_target_pairs={{0,6},{2,0},{4,2},{6,4},{1,7},{3,1},{5,3},{7,5},{8,14},{10,8},{12,... | collective-permute-start | bytes 1572872 | tf_op jit(solution)/shard_map/ppermute | solution.py:50
  34.0 9.1 %collective-permute-done.refs_2_ = bf16[256,1024]{1,0:T(8,128)(2,1)S(1)} collective-permute-done((bf16[256,1024]{1,0:T(8,128)(2,1)S(1)}, bf16[256,1024]{1,0:T(8,128)(2,1)S(1)}, u32[]{:S(2)}, u32[]{:S(2)}) %collective-permute-start) | collective-permute-done | bytes 524320 | tf_op jit(solution)/shard_map/ppermute | solution.py:50
  43.1 0.7 slice.191
  43.8 1.9 collective-permute-start.4
  45.8 0.6 pad_maximum_fusion.1
  46.5 4.6 %collective-permute-start.5 = (bf16[128,1024]{1,0:T(8,128)(2,1)S(1)}, bf16[128,1024]{1,0:T(8,128)(2,1)S(1)}, u32[]{:S(2)}, u32[]{:S(2)}) collective-permute-start(bf16[128,1024]{1,0:T(8,128)(2,1)S(1)} %slice.192), channel_id=1, source_target_pairs={{0,6},{2,0},{4,2},{6,4},{1,7},{3,1},{5,3},{7,5},{8,14},{10,8},{12,... | collective-permute-start | bytes 786440 | tf_op jit(solution)/shard_map/ppermute | solution.py:50
  51.1 0.8 constant_dynamic-slice_fusion.6
  51.9 4.3 %collective-permute-start.3 = (bf16[256,1024]{1,0:T(8,128)(2,1)S(1)}, bf16[256,1024]{1,0:T(8,128)(2,1)}, u32[]{:S(2)}, u32[]{:S(2)}) collective-permute-start(bf16[256,1024]{1,0:T(8,128)(2,1)S(1)} %collective-permute-done.2.refs_4_), channel_id=1, source_target_pairs={{0,1},{1,0},{2,3},{3,2},{4,5},{5,4},{6,7},{7,6},{8,9},{9,8},{10,11... | collective-permute-start | bytes 1572872 | tf_op jit(solution)/shard_map/ppermute | solution.py:29
  56.2 1.9 collective-permute-start.1
  58.1 0.8 constant_dynamic-update-slice_fusion.1
  58.9 0.8 constant_dynamic-update-slice_fusion.refs_6_
  59.6 2.4 %collective-permute-start.6 = (bf16[256,1024]{1,0:T(8,128)(2,1)}, bf16[256,1024]{1,0:T(8,128)(2,1)}, u32[]{:S(2)}, u32[]{:S(2)}) collective-permute-start(bf16[256,1024]{1,0:T(8,128)(2,1)} %constant_dynamic-update-slice_fusion.refs_6_), channel_id=1, source_target_pairs={{0,1},{1,0},{2,3},{3,2},{4,5},{5,4},{6,7},{7,6},{8,9},{9,8},{10,11... | collective-permute-start | bytes 1572872 | tf_op jit(solution)/shard_map/ppermute | solution.py:29
  62.1 0.6 copy.107
  62.8 0.8 constant_dynamic-slice_fusion.4
  63.6 0.5 fusion.64
  64.2 0.7 all-to-all-done
  65.0 1.1 copy-done.3
  66.0 6.9 %shard_map.155 = (bf16[4,256,384]{2,1,0:T(8,128)(2,1)}, f32[4,16,256]{2,1,0:T(8,128)}) custom-call(s32[1]{0:T(128)} %bitcast.core, bf16[256,1024]{1,0:T(8,128)(2,1)} %copy-done.2, bf16[256,1024]{1,0:T(8,128)(2,1)} %get-tuple-element.15.refs_1_, bf16[256,1024]{1,0:T(8,128)(2,1)} %copy-done.4, bf16[256,1024]{1,0:T(8,128)(2,1)} %collective-permute-done.1.refs_3_, ...), custom_call_target="tpu_custom_call" | custom-call | flops 1610612736 | bytes 6291456 | tf_op jit(solution)/shard_map/pallas_call | solution.py:116
  73.0 1.4 add_negate_fusion
  74.4 1.2 reduce-window.6
  76.3 1.6 add_reduce_fusion
  78.1 1.5 convolution_convert_fusion
  79.7 0.9 copy.75
  80.6 11.4 %all-to-all-start.2 = ((bf16[64,16,128]{2,1,0:T(8,128)(2,1)}), bf16[64,16,128]{2,1,0:T(8,128)(2,1)S(1)}, u32[]{:S(2)}, u32[]{:S(2)}) async-start(bf16[64,16,128]{2,1,0:T(8,128)(2,1)} %copy.75), calls=%async_computation.2 | async-start | bytes 524288 | tf_op jit(solution)/shard_map/all_to_all | solution.py:25
  92.0 13.5 %all-to-all-done.2 = bf16[64,16,128]{2,1,0:T(8,128)(2,1)S(1)} async-done(((bf16[64,16,128]{2,1,0:T(8,128)(2,1)}), bf16[64,16,128]{2,1,0:T(8,128)(2,1)S(1)}, u32[]{:S(2)}, u32[]{:S(2)}) %all-to-all-start.2) | async-done | bytes 262176 | tf_op jit(solution)/shard_map/all_to_all | solution.py:25
  106.6 0.7 reshape.388
  107.3 5.1 %all-to-all-start.3 = ((bf16[64,8,128]{2,1,0:T(8,128)(2,1)}), bf16[64,8,128]{2,1,0:T(8,128)(2,1)S(1)}, u32[]{:S(2)}, u32[]{:S(2)}) async-start(bf16[64,8,128]{2,1,0:T(8,128)(2,1)} %reshape.388), calls=%async_computation.3 | async-start | bytes 262144 | tf_op jit(solution)/shard_map/all_to_all | solution.py:25
  112.4 1.4 dynamic_slice.51
  113.8 10.2 %all-to-all-done.3 = bf16[64,8,128]{2,1,0:T(8,128)(2,1)S(1)} async-done(((bf16[64,8,128]{2,1,0:T(8,128)(2,1)}), bf16[64,8,128]{2,1,0:T(8,128)(2,1)S(1)}, u32[]{:S(2)}, u32[]{:S(2)}) %all-to-all-start.3) | async-done | bytes 131104 | tf_op jit(solution)/shard_map/all_to_all | solution.py:25
  123.9 1.1 broadcast_in_dim.67
  125.0 4.8 %all-to-all-start.1 = ((bf16[64,32,256]{2,1,0:T(8,128)(2,1)}), bf16[64,32,256]{2,1,0:T(8,128)(2,1)S(1)}, u32[]{:S(2)}, u32[]{:S(2)}) async-start(bf16[64,32,256]{2,1,0:T(8,128)(2,1)} %broadcast_in_dim.67), calls=%async_computation.1 | async-start | bytes 2097152 | tf_op jit(solution)/shard_map/all_to_all | solution.py:21
  129.9 5.9 %shard_map.154 = bf16[4,256,384]{2,1,0:T(8,128)(2,1)} custom-call(s32[1]{0:T(128)} %bitcast.core, bf16[256,1024]{1,0:T(8,128)(2,1)} %copy-done.2, bf16[256,1024]{1,0:T(8,128)(2,1)} %get-tuple-element.15.refs_1_, bf16[256,1024]{1,0:T(8,128)(2,1)} %copy-done.4, bf16[256,1024]{1,0:T(8,128)(2,1)} %collective-permute-done.1.refs_3_, bf16[256,1024]{1,0:T(8,128)(2,1)} %copy-done.5, ...), custom_call_target="tpu_custom_call" | custom-call | flops 1610612736 | bytes 6291456 | tf_op jit(solution)/shard_map/pallas_call | solution.py:109
  135.8 1.2 multiply_convert_fusion.2
  137.0 2.6 %collective-permute-start.7 = (bf16[4,2,128]{2,1,0:T(2,128)(2,1)S(1)}, bf16[4,2,128]{2,1,0:T(2,128)(2,1)S(1)}, u32[]{:S(2)}, u32[]{:S(2)}) collective-permute-start(bf16[4,2,128]{2,1,0:T(2,128)(2,1)S(1)} %slice.196), channel_id=1, source_target_pairs={{0,8},{8,16},{16,24},{24,32},{32,40},{40,48},{48,56},{56,64},{64,7... | collective-permute-start | bytes 6152 | tf_op jit(solution)/shard_map/ppermute | solution.py:34
  140.0 6.0 %collective-permute-done.7 = bf16[4,2,128]{2,1,0:T(2,128)(2,1)S(1)} collective-permute-done((bf16[4,2,128]{2,1,0:T(2,128)(2,1)S(1)}, bf16[4,2,128]{2,1,0:T(2,128)(2,1)S(1)}, u32[]{:S(2)}, u32[]{:S(2)}) %collective-permute-start.7) | collective-permute-done | bytes 2080 | tf_op jit(solution)/shard_map/ppermute | solution.py:34
  146.1 1.2 fusion.30
  147.2 0.6 slice_bitcast_fusion.6
  147.9 5.0 %collective-permute-start.10 = (bf16[256,128]{1,0:T(8,128)(2,1)S(1)}, bf16[256,128]{1,0:T(8,128)(2,1)S(1)}, u32[]{:S(2)}, u32[]{:S(2)}) collective-permute-start(bf16[256,128]{1,0:T(8,128)(2,1)S(1)} %get-tuple-element.17), channel_id=1, source_target_pairs={{0,6},{2,0},{4,2},{6,4},{1,7},{3,1},{5,3},{7,5},{8,14},{10,8},{12,... | collective-permute-start | bytes 196616 | tf_op jit(solution)/shard_map/ppermute | solution.py:50
  152.8 1.9 collective-permute-start.12
  155.0 0.7 subtract_exponential_fusion
  155.6 0.7 fusion.8
  156.5 0.9 multiply_reduce_fusion
  157.4 2.7 %collective-permute-start.11 = (bf16[2048,256]{1,0:T(8,128)(2,1)S(1)}, bf16[2048,256]{1,0:T(8,128)(2,1)S(1)}, u32[]{:S(2)}, u32[]{:S(2)}) collective-permute-start(bf16[2048,256]{1,0:T(8,128)(2,1)S(1)} %bitcast.110), channel_id=1, source_target_pairs={{0,6},{2,0},{4,2},{6,4},{1,7},{3,1},{5,3},{7,5},{8,14},{10,8},{12,... | collective-permute-start | bytes 3145736 | tf_op jit(solution)/shard_map/ppermute | solution.py:50
  160.1 2.6 %collective-permute-start.9 = (bf16[2048,256]{1,0:T(8,128)(2,1)S(1)}, bf16[2048,256]{1,0:T(8,128)(2,1)S(1)}, u32[]{:S(2)}, u32[]{:S(2)}) collective-permute-start(bf16[2048,256]{1,0:T(8,128)(2,1)S(1)} %bitcast.111), channel_id=1, source_target_pairs={{0,2},{2,4},{4,6},{6,0},{1,3},{3,5},{5,7},{7,1},{8,10},{10,12},{12... | collective-permute-start | bytes 3145736 | tf_op jit(solution)/shard_map/ppermute | solution.py:50
  162.7 0.8 multiply_convert_fusion
  163.5 3.2 %collective-permute-start.15 = (bf16[256,128]{0,1:T(8,128)(2,1)S(1)}, bf16[256,128]{0,1:T(8,128)(2,1)S(1)}, u32[]{:S(2)}, u32[]{:S(2)}) collective-permute-start(bf16[256,128]{0,1:T(8,128)(2,1)S(1)} %get-tuple-element.22), channel_id=1, source_target_pairs={{0,2},{2,4},{4,6},{6,0},{1,3},{3,5},{5,7},{7,1},{8,10},{10,12},{12... | collective-permute-start | bytes 196616 | tf_op jit(solution)/shard_map/ppermute | solution.py:50
  167.7 11.9 %collective-permute-done.11 = bf16[2048,256]{1,0:T(8,128)(2,1)S(1)} collective-permute-done((bf16[2048,256]{1,0:T(8,128)(2,1)S(1)}, bf16[2048,256]{1,0:T(8,128)(2,1)S(1)}, u32[]{:S(2)}, u32[]{:S(2)}) %collective-permute-start.11) | collective-permute-done | bytes 1048608 | tf_op jit(solution)/shard_map/ppermute | solution.py:50
  179.6 4.2 %collective-permute-start.8 = (bf16[256,128]{1,0:T(8,128)(2,1)S(1)}, bf16[256,128]{1,0:T(8,128)(2,1)S(1)}, u32[]{:S(2)}, u32[]{:S(2)}) collective-permute-start(bf16[256,128]{1,0:T(8,128)(2,1)S(1)} %copy-done.7), channel_id=1, source_target_pairs={{0,2},{2,4},{4,6},{6,0},{1,3},{3,5},{5,7},{7,1},{8,10},{10,12},{12... | collective-permute-start | bytes 196616 | tf_op jit(solution)/shard_map/ppermute | solution.py:50
  183.9 2.3 collective-permute-start.14
  186.2 3.0 %collective-permute-start.13 = (bf16[1024,256]{1,0:T(8,128)(2,1)S(1)}, bf16[1024,256]{1,0:T(8,128)(2,1)S(1)}, u32[]{:S(2)}, u32[]{:S(2)}) collective-permute-start(bf16[1024,256]{1,0:T(8,128)(2,1)S(1)} %slice.207), channel_id=1, source_target_pairs={{0,2},{2,4},{4,6},{6,0},{1,3},{3,5},{5,7},{7,1},{8,10},{10,12},{12... | collective-permute-start | bytes 1572872 | tf_op jit(solution)/shard_map/ppermute | solution.py:50
  189.7 3.5 %collective-permute-start.16 = (bf16[256,128]{0,1:T(8,128)(2,1)S(1)}, bf16[256,128]{0,1:T(8,128)(2,1)S(1)}, u32[]{:S(2)}, u32[]{:S(2)}) collective-permute-start(bf16[256,128]{0,1:T(8,128)(2,1)S(1)} %get-tuple-element.20), channel_id=1, source_target_pairs={{0,6},{2,0},{4,2},{6,4},{1,7},{3,1},{5,3},{7,5},{8,14},{10,8},{12,... | collective-permute-start | bytes 196616 | tf_op jit(solution)/shard_map/ppermute | solution.py:50
  193.6 3.7 %collective-permute-done.13 = bf16[1024,256]{1,0:T(8,128)(2,1)S(1)} collective-permute-done((bf16[1024,256]{1,0:T(8,128)(2,1)S(1)}, bf16[1024,256]{1,0:T(8,128)(2,1)S(1)}, u32[]{:S(2)}, u32[]{:S(2)}) %collective-permute-start.13) | collective-permute-done | bytes 524320 | tf_op jit(solution)/shard_map/ppermute | solution.py:50
  197.3 3.1 %collective-permute-start.17 = (bf16[256,128]{0,1:T(8,128)(2,1)S(1)}, bf16[256,128]{0,1:T(8,128)(2,1)S(1)}, u32[]{:S(2)}, u32[]{:S(2)}) collective-permute-start(bf16[256,128]{0,1:T(8,128)(2,1)S(1)} %get-tuple-element.21), channel_id=1, source_target_pairs={{0,4},{2,6},{4,0},{6,2},{1,5},{3,7},{5,1},{7,3},{8,12},{10,14},{12... | collective-permute-start | bytes 196616 | tf_op jit(solution)/shard_map/ppermute | solution.py:50
  200.6 4.0 %collective-permute-done.17 = bf16[256,128]{0,1:T(8,128)(2,1)S(1)} collective-permute-done((bf16[256,128]{0,1:T(8,128)(2,1)S(1)}, bf16[256,128]{0,1:T(8,128)(2,1)S(1)}, u32[]{:S(2)}, u32[]{:S(2)}) %collective-permute-start.17) | collective-permute-done | bytes 65568 | tf_op jit(solution)/shard_map/ppermute | solution.py:50
  205.1 0.5 fusion
  205.6 1.3 fusion.22
  206.9 0.5 fusion.3
  207.3 13.9 %all_to_all.25 = bf16[2,128,2048]{2,1,0:T(8,128)(2,1)S(1)} all-to-all(bf16[2,128,2048]{2,1,0:T(8,128)(2,1)S(1)} %bitcast.109), channel_id=1, replica_groups=mesh['sp_0'=8,'sp_1'=8,'fs'=4,'tp'=2] {'tp'}, dimensions={0} | all-to-all | bytes 2097152 | tf_op jit(solution)/shard_map/all_to_all | solution.py:25
  221.3 1.1 reduce_sum.42
  (106 shorter events, 6.1 us)
Async XLA Ops:
  6.5 105.8 %copy-start = (f32[3,1024]{1,0:T(4,128)S(1)}, f32[3,1024]{1,0:T(4,128)}, u32[]{:S(2)}) copy-start(f32[3,1024]{1,0:T(4,128)} %param.21) | copy-start | bytes 36868
  7.3 18.6 %copy-start.1 = (bf16[1,256,2048]{2,1,0:T(8,128)(2,1)S(1)}, bf16[1,256,2048]{2,1,0:T(8,128)(2,1)}, u32[]{:S(2)}) copy-start(bf16[1,256,2048]{2,1,0:T(8,128)(2,1)} %param.16) | copy-start | bytes 3145732
  8.6 17.6 %copy-start.8 = (f32[2048]{0:T(1024)S(1)}, f32[2048]{0:T(1024)}, u32[]{:S(2)}) copy-start(f32[2048]{0:T(1024)} %param.17) | copy-start | bytes 24580
  8.6 56.3 %all-to-all-start = ((bf16[64,32,384]{2,1,0:T(8,128)(2,1)}), bf16[64,32,384]{2,1,0:T(8,128)(2,1)S(1)}, u32[]{:S(2)}, u32[]{:S(2)}) async-start(bf16[64,32,384]{2,1,0:T(8,128)(2,1)} %broadcast_in_dim.66), calls=%async_computation | async-start | bytes 3145728 | tf_op jit(solution)/shard_map/all_to_all | solution.py:21
  25.8 104.1 %all-gather.2.cloned.1.call-start = ((), (), s32[]{:S(2)}) async-start(), calls=%async_computation.5 | async-start | bytes 1597440 | tf_op jit(solution)/shard_map/all_gather | solution.py:153
  26.2 19.6 %copy-start.9 = (bf16[32,128]{1,0:T(8,128)(2,1)S(1)}, bf16[32,128]{1,0:T(8,128)(2,1)}, u32[]{:S(2)}) copy-start(bf16[32,128]{1,0:T(8,128)(2,1)} %param.20) | copy-start | bytes 24580
  26.2 19.6 %copy-start.10 = (bf16[32,128]{1,0:T(8,128)(2,1)S(1)}, bf16[32,128]{1,0:T(8,128)(2,1)}, u32[]{:S(2)}) copy-start(bf16[32,128]{1,0:T(8,128)(2,1)} %param.19) | copy-start | bytes 24580
  26.2 19.6 %copy-start.11 = (bf16[32,128]{1,0:T(8,128)(2,1)S(1)}, bf16[32,128]{1,0:T(8,128)(2,1)}, u32[]{:S(2)}) copy-start(bf16[32,128]{1,0:T(8,128)(2,1)} %param.18) | copy-start | bytes 24580
  26.6 36.2 %copy-start.14 = (f32[2,8]{1,0:T(2,128)S(1)}, f32[2,8]{1,0:T(2,128)}, u32[]{:S(2)}) copy-start(f32[2,8]{1,0:T(2,128)} %param.27) | copy-start | bytes 196
  26.6 37.6 %copy-start.12 = (bf16[128,32]{0,1:T(8,128)(2,1)S(1)}, bf16[128,32]{0,1:T(8,128)(2,1)}, u32[]{:S(2)}) copy-start(bf16[128,32]{0,1:T(8,128)(2,1)} %param.31) | copy-start | bytes 24580
  26.6 37.6 %copy-start.13 = (bf16[128,32]{0,1:T(8,128)(2,1)S(1)}, bf16[128,32]{0,1:T(8,128)(2,1)}, u32[]{:S(2)}) copy-start(bf16[128,32]{0,1:T(8,128)(2,1)} %param.30) | copy-start | bytes 24580
  27.5 37.4 %copy-start.2 = (bf16[256,1024]{1,0:T(8,128)(2,1)}, bf16[256,1024]{1,0:T(8,128)(2,1)S(1)}, u32[]{:S(2)}) copy-start(bf16[256,1024]{1,0:T(8,128)(2,1)S(1)} %get-tuple-element.16.refs_0_) | copy-start | bytes 1572868
  27.5 15.6 %collective-permute-start = (bf16[256,1024]{1,0:T(8,128)(2,1)S(1)}, bf16[256,1024]{1,0:T(8,128)(2,1)S(1)}, u32[]{:S(2)}, u32[]{:S(2)}) collective-permute-start(bf16[256,1024]{1,0:T(8,128)(2,1)S(1)} %get-tuple-element.16.refs_0_), channel_id=1, source_target_pairs={{0,2},{2,4},{4,6},{6,0},{1,3},{3,5},{5,7},{7,1},{8,10},{10,12},{12... | collective-permute-start | bytes 1572872 | tf_op jit(solution)/shard_map/ppermute | solution.py:50
  30.6 15.8 %collective-permute-start.2 = (bf16[256,1024]{1,0:T(8,128)(2,1)S(1)}, bf16[256,1024]{1,0:T(8,128)(2,1)S(1)}, u32[]{:S(2)}, u32[]{:S(2)}) collective-permute-start(bf16[256,1024]{1,0:T(8,128)(2,1)S(1)} %get-tuple-element.16.refs_0_), channel_id=1, source_target_pairs={{0,6},{2,0},{4,2},{6,4},{1,7},{3,1},{5,3},{7,5},{8,14},{10,8},{12,... | collective-permute-start | bytes 1572872 | tf_op jit(solution)/shard_map/ppermute | solution.py:50
  43.1 21.8 %copy-start.4 = (bf16[256,1024]{1,0:T(8,128)(2,1)}, bf16[256,1024]{1,0:T(8,128)(2,1)S(1)}, u32[]{:S(2)}) copy-start(bf16[256,1024]{1,0:T(8,128)(2,1)S(1)} %collective-permute-done.refs_2_) | copy-start | bytes 1572868
  43.8 14.2 %collective-permute-start.4 = (bf16[128,1024]{1,0:T(8,128)(2,1)}, bf16[128,1024]{1,0:T(8,128)(2,1)S(1)}, u32[]{:S(2)}, u32[]{:S(2)}) collective-permute-start(bf16[128,1024]{1,0:T(8,128)(2,1)} %slice.191), channel_id=1, source_target_pairs={{0,2},{2,4},{4,6},{6,0},{1,3},{3,5},{5,7},{7,1},{8,10},{10,12},{12... | collective-permute-start | bytes 786440 | tf_op jit(solution)/shard_map/ppermute | solution.py:50
  46.4 18.5 %copy-start.5 = (bf16[256,1024]{1,0:T(8,128)(2,1)}, bf16[256,1024]{1,0:T(8,128)(2,1)S(1)}, u32[]{:S(2)}) copy-start(bf16[256,1024]{1,0:T(8,128)(2,1)S(1)} %collective-permute-done.2.refs_4_) | copy-start | bytes 1572868
  46.5 12.4 %collective-permute-start.5 = (bf16[128,1024]{1,0:T(8,128)(2,1)S(1)}, bf16[128,1024]{1,0:T(8,128)(2,1)S(1)}, u32[]{:S(2)}, u32[]{:S(2)}) collective-permute-start(bf16[128,1024]{1,0:T(8,128)(2,1)S(1)} %slice.192), channel_id=1, source_target_pairs={{0,6},{2,0},{4,2},{6,4},{1,7},{3,1},{5,3},{7,5},{8,14},{10,8},{12,... | collective-permute-start | bytes 786440 | tf_op jit(solution)/shard_map/ppermute | solution.py:50
  51.9 13.0 %collective-permute-start.3 = (bf16[256,1024]{1,0:T(8,128)(2,1)S(1)}, bf16[256,1024]{1,0:T(8,128)(2,1)}, u32[]{:S(2)}, u32[]{:S(2)}) collective-permute-start(bf16[256,1024]{1,0:T(8,128)(2,1)S(1)} %collective-permute-done.2.refs_4_), channel_id=1, source_target_pairs={{0,1},{1,0},{2,3},{3,2},{4,5},{5,4},{6,7},{7,6},{8,9},{9,8},{10,11... | collective-permute-start | bytes 1572872 | tf_op jit(solution)/shard_map/ppermute | solution.py:29
  56.2 8.8 %collective-permute-start.1 = (bf16[256,1024]{1,0:T(8,128)(2,1)S(1)}, bf16[256,1024]{1,0:T(8,128)(2,1)}, u32[]{:S(2)}, u32[]{:S(2)}) collective-permute-start(bf16[256,1024]{1,0:T(8,128)(2,1)S(1)} %collective-permute-done.refs_2_), channel_id=1, source_target_pairs={{0,1},{1,0},{2,3},{3,2},{4,5},{5,4},{6,7},{7,6},{8,9},{9,8},{10,11... | collective-permute-start | bytes 1572872 | tf_op jit(solution)/shard_map/ppermute | solution.py:29
  59.6 5.3 %collective-permute-start.6 = (bf16[256,1024]{1,0:T(8,128)(2,1)}, bf16[256,1024]{1,0:T(8,128)(2,1)}, u32[]{:S(2)}, u32[]{:S(2)}) collective-permute-start(bf16[256,1024]{1,0:T(8,128)(2,1)} %constant_dynamic-update-slice_fusion.refs_6_), channel_id=1, source_target_pairs={{0,1},{1,0},{2,3},{3,2},{4,5},{5,4},{6,7},{7,6},{8,9},{9,8},{10,11... | collective-permute-start | bytes 1572872 | tf_op jit(solution)/shard_map/ppermute | solution.py:29
  64.9 1.1 copy-start.3
  80.6 25.0 %all-to-all-start.2 = ((bf16[64,16,128]{2,1,0:T(8,128)(2,1)}), bf16[64,16,128]{2,1,0:T(8,128)(2,1)S(1)}, u32[]{:S(2)}, u32[]{:S(2)}) async-start(bf16[64,16,128]{2,1,0:T(8,128)(2,1)} %copy.75), calls=%async_computation.2 | async-start | bytes 524288 | tf_op jit(solution)/shard_map/all_to_all | solution.py:25
  107.3 16.6 %all-to-all-start.3 = ((bf16[64,8,128]{2,1,0:T(8,128)(2,1)}), bf16[64,8,128]{2,1,0:T(8,128)(2,1)S(1)}, u32[]{:S(2)}, u32[]{:S(2)}) async-start(bf16[64,8,128]{2,1,0:T(8,128)(2,1)} %reshape.388), calls=%async_computation.3 | async-start | bytes 262144 | tf_op jit(solution)/shard_map/all_to_all | solution.py:25
  125.0 32.4 %all-to-all-start.1 = ((bf16[64,32,256]{2,1,0:T(8,128)(2,1)}), bf16[64,32,256]{2,1,0:T(8,128)(2,1)S(1)}, u32[]{:S(2)}, u32[]{:S(2)}) async-start(bf16[64,32,256]{2,1,0:T(8,128)(2,1)} %broadcast_in_dim.67), calls=%async_computation.1 | async-start | bytes 2097152 | tf_op jit(solution)/shard_map/all_to_all | solution.py:21
  135.8 19.8 %copy-start.6 = (bf16[4,256,384]{2,1,0:T(8,128)(2,1)S(1)}, bf16[4,256,384]{2,1,0:T(8,128)(2,1)}, u32[]{:S(2)}) copy-start(bf16[4,256,384]{2,1,0:T(8,128)(2,1)} %get-tuple-element.12) | copy-start | bytes 2359300
  137.0 9.0 %collective-permute-start.7 = (bf16[4,2,128]{2,1,0:T(2,128)(2,1)S(1)}, bf16[4,2,128]{2,1,0:T(2,128)(2,1)S(1)}, u32[]{:S(2)}, u32[]{:S(2)}) collective-permute-start(bf16[4,2,128]{2,1,0:T(2,128)(2,1)S(1)} %slice.196), channel_id=1, source_target_pairs={{0,8},{8,16},{16,24},{24,32},{32,40},{40,48},{48,56},{56,64},{64,7... | collective-permute-start | bytes 6152 | tf_op jit(solution)/shard_map/ppermute | solution.py:34
  147.9 59.0 %collective-permute-start.10 = (bf16[256,128]{1,0:T(8,128)(2,1)S(1)}, bf16[256,128]{1,0:T(8,128)(2,1)S(1)}, u32[]{:S(2)}, u32[]{:S(2)}) collective-permute-start(bf16[256,128]{1,0:T(8,128)(2,1)S(1)} %get-tuple-element.17), channel_id=1, source_target_pairs={{0,6},{2,0},{4,2},{6,4},{1,7},{3,1},{5,3},{7,5},{8,14},{10,8},{12,... | collective-permute-start | bytes 196616 | tf_op jit(solution)/shard_map/ppermute | solution.py:50
  152.8 52.7 %collective-permute-start.12 = (bf16[256,128]{1,0:T(8,128)(2,1)S(1)}, bf16[256,128]{1,0:T(8,128)(2,1)}, u32[]{:S(2)}, u32[]{:S(2)}) collective-permute-start(bf16[256,128]{1,0:T(8,128)(2,1)S(1)} %get-tuple-element.18), channel_id=1, source_target_pairs={{0,4},{2,6},{4,0},{6,2},{1,5},{3,7},{5,1},{7,3},{8,12},{10,14},{12... | collective-permute-start | bytes 196616 | tf_op jit(solution)/shard_map/ppermute | solution.py:50
  157.4 22.2 %collective-permute-start.11 = (bf16[2048,256]{1,0:T(8,128)(2,1)S(1)}, bf16[2048,256]{1,0:T(8,128)(2,1)S(1)}, u32[]{:S(2)}, u32[]{:S(2)}) collective-permute-start(bf16[2048,256]{1,0:T(8,128)(2,1)S(1)} %bitcast.110), channel_id=1, source_target_pairs={{0,6},{2,0},{4,2},{6,4},{1,7},{3,1},{5,3},{7,5},{8,14},{10,8},{12,... | collective-permute-start | bytes 3145736 | tf_op jit(solution)/shard_map/ppermute | solution.py:50
  160.1 23.7 %collective-permute-start.9 = (bf16[2048,256]{1,0:T(8,128)(2,1)S(1)}, bf16[2048,256]{1,0:T(8,128)(2,1)S(1)}, u32[]{:S(2)}, u32[]{:S(2)}) collective-permute-start(bf16[2048,256]{1,0:T(8,128)(2,1)S(1)} %bitcast.111), channel_id=1, source_target_pairs={{0,2},{2,4},{4,6},{6,0},{1,3},{3,5},{5,7},{7,1},{8,10},{10,12},{12... | collective-permute-start | bytes 3145736 | tf_op jit(solution)/shard_map/ppermute | solution.py:50
  163.5 16.1 %copy-start.7 = (bf16[256,128]{1,0:T(8,128)(2,1)S(1)}, bf16[256,128]{1,0:T(8,128)(2,1)}, u32[]{:S(2)}) copy-start(bf16[256,128]{1,0:T(8,128)(2,1)} %get-tuple-element.19) | copy-start | bytes 196612
  163.5 22.6 %collective-permute-start.15 = (bf16[256,128]{0,1:T(8,128)(2,1)S(1)}, bf16[256,128]{0,1:T(8,128)(2,1)S(1)}, u32[]{:S(2)}, u32[]{:S(2)}) collective-permute-start(bf16[256,128]{0,1:T(8,128)(2,1)S(1)} %get-tuple-element.22), channel_id=1, source_target_pairs={{0,2},{2,4},{4,6},{6,0},{1,3},{3,5},{5,7},{7,1},{8,10},{10,12},{12... | collective-permute-start | bytes 196616 | tf_op jit(solution)/shard_map/ppermute | solution.py:50
  179.6 10.1 %collective-permute-start.8 = (bf16[256,128]{1,0:T(8,128)(2,1)S(1)}, bf16[256,128]{1,0:T(8,128)(2,1)S(1)}, u32[]{:S(2)}, u32[]{:S(2)}) collective-permute-start(bf16[256,128]{1,0:T(8,128)(2,1)S(1)} %copy-done.7), channel_id=1, source_target_pairs={{0,2},{2,4},{4,6},{6,0},{1,3},{3,5},{5,7},{7,1},{8,10},{10,12},{12... | collective-permute-start | bytes 196616 | tf_op jit(solution)/shard_map/ppermute | solution.py:50
  183.9 16.7 %collective-permute-start.14 = (bf16[1024,256]{1,0:T(8,128)(2,1)S(1)}, bf16[1024,256]{1,0:T(8,128)(2,1)S(1)}, u32[]{:S(2)}, u32[]{:S(2)}) collective-permute-start(bf16[1024,256]{1,0:T(8,128)(2,1)S(1)} %slice.208), channel_id=1, source_target_pairs={{0,6},{2,0},{4,2},{6,4},{1,7},{3,1},{5,3},{7,5},{8,14},{10,8},{12,... | collective-permute-start | bytes 1572872 | tf_op jit(solution)/shard_map/ppermute | solution.py:50
  186.2 11.1 %collective-permute-start.13 = (bf16[1024,256]{1,0:T(8,128)(2,1)S(1)}, bf16[1024,256]{1,0:T(8,128)(2,1)S(1)}, u32[]{:S(2)}, u32[]{:S(2)}) collective-permute-start(bf16[1024,256]{1,0:T(8,128)(2,1)S(1)} %slice.207), channel_id=1, source_target_pairs={{0,2},{2,4},{4,6},{6,0},{1,3},{3,5},{5,7},{7,1},{8,10},{10,12},{12... | collective-permute-start | bytes 1572872 | tf_op jit(solution)/shard_map/ppermute | solution.py:50
  189.7 15.4 %collective-permute-start.16 = (bf16[256,128]{0,1:T(8,128)(2,1)S(1)}, bf16[256,128]{0,1:T(8,128)(2,1)S(1)}, u32[]{:S(2)}, u32[]{:S(2)}) collective-permute-start(bf16[256,128]{0,1:T(8,128)(2,1)S(1)} %get-tuple-element.20), channel_id=1, source_target_pairs={{0,6},{2,0},{4,2},{6,4},{1,7},{3,1},{5,3},{7,5},{8,14},{10,8},{12,... | collective-permute-start | bytes 196616 | tf_op jit(solution)/shard_map/ppermute | solution.py:50
  197.3 7.3 %collective-permute-start.17 = (bf16[256,128]{0,1:T(8,128)(2,1)S(1)}, bf16[256,128]{0,1:T(8,128)(2,1)S(1)}, u32[]{:S(2)}, u32[]{:S(2)}) collective-permute-start(bf16[256,128]{0,1:T(8,128)(2,1)S(1)} %get-tuple-element.21), channel_id=1, source_target_pairs={{0,4},{2,6},{4,0},{6,2},{1,5},{3,7},{5,1},{7,3},{8,12},{10,14},{12... | collective-permute-start | bytes 196616 | tf_op jit(solution)/shard_map/ppermute | solution.py:50
Sparse Core Ops, SparseCore 0:
  46.5 81.0 all-gather.1

commit v2 on v1

--- a/solution.py
+++ b/solution.py
@@ -65,26 +65,22 @@
     return own, ring(ahead, axis, 1), ring(behind, axis, -1), ring(far, axis, 2)
 
 
-def project_kernel(core, *refs):
-    pieces, weights, gate_rows, out, gates = refs[:8], refs[8], refs[9], refs[10], refs[11]
+def ring_gather(array, axis):
+    behind, ahead = [array], [array]
+    for k in range(4):
+        behind.append(ring(behind[-1], axis, 1))
+        if k < 3:
+            ahead.append(ring(ahead[-1], axis, -1))
+    return behind + ahead[1:]
+
+
+OFFSETS = (0, 7, 6, 5, 4, 1, 2, 3)
+
+
+def matmuls(core, pieces, weights, out):
     half = pieces[0].shape[1]
-    first = pl.multiple_of(core[0] * half, half)
-    second = pl.multiple_of((1 - core[0]) * half, half)
-    for k in range(4):
-        a, b = pieces[2 * k][...], pieces[2 * k + 1][...]
-        mixed = jnp.dot(a, weights[pl.ds(first, half), :], preferred_element_type=F32)
-        mixed += jnp.dot(b, weights[pl.ds(second, half), :], preferred_element_type=F32)
-        out[k] = mixed.astype(BF16)
-        dims = (((1,), (1,)), ((), ()))
-        rows = dot(gate_rows[core[0]], a, dims)
-        gates[k] = rows + dot(gate_rows[1 - core[0]], b, dims)
-
-
-def project_only_kernel(core, *refs):
-    pieces, weights, out = refs[:8], refs[8], refs[9]
-    half = pieces[0].shape[1]
-    first = pl.multiple_of(core[0] * half, half)
-    second = pl.multiple_of((1 - core[0]) * half, half)
+    first = pl.multiple_of(core * half, half)
+    second = pl.multiple_of((1 - core) * half, half)
     for k in range(4):
         mixed = jnp.dot(
             pieces[2 * k][...], weights[pl.ds(first, half), :], preferred_element_type=F32
@@ -95,31 +91,58 @@
         out[k] = mixed.astype(BF16)
 
 
+def project_mem_kernel(spot, *refs):
+    parts, pieces, gate_rows = refs[:8], refs[8:16], refs[16]
+    out, gates, weights = refs[17:]
+    core = spot[0]
+    for part, offset in zip(parts, OFFSETS):
+        place = (spot[2] + offset) % 8
+        for k in range(8):
+            start = pl.multiple_of((k * 8 + place) * 32, 32)
+            weights[pl.ds(start, 32), :] = part[pl.ds(k * 32, 32), :]
+    matmuls(core, pieces, weights, out)
+    dims = (((1,), (1,)), ((), ()))
+    for k in range(4):
+        rows = dot(gate_rows[core], pieces[2 * k][...], dims)
+        gates[k] = rows + dot(gate_rows[1 - core], pieces[2 * k + 1][...], dims)
+
+
+def project_conv_kernel(spot, *refs):
+    matmuls(spot[0], refs[:8], refs[8], refs[9])
+
+
+def arrange_kernel(spot, *refs):
+    parts, left, right = refs[:8], refs[8], refs[9]
+    wide, size = left.shape[1], parts[0].shape[0]
+    for part, offset in zip(parts, OFFSETS):
+        start = pl.multiple_of(((spot[1] + offset) % 8) * size, size)
+        left[pl.ds(start, size), :] = part[:, :wide]
+        right[pl.ds(start, size), :] = part[:, wide:]
+
+
+def output_kernel(*refs):
+    parts, weights, out = refs[:4], refs[4:8], refs[8]
+    dims = (((1,), (1,)), ((), ()))
+    mixed = dot(parts[0][...], weights[0][...], dims)
+    for part, weight in zip(parts[1:], weights[1:]):
+        mixed += dot(part[...], weight[...], dims)
+    out[...] = mixed.astype(BF16)
+
+
 def in_vmem(count):
     return [pl.BlockSpec(memory_space=pltpu.VMEM)] * count
 
 
-def project(core, pieces, weights, gate_rows=None):
-    tokens = pieces[0].shape[0]
-    shape = jax.ShapeDtypeStruct((4, tokens, weights.shape[1]), BF16)
-    smem = [pl.BlockSpec(memory_space=pltpu.SMEM)]
-    flops = 8 * tokens * weights.size
-    cost = pl.CostEstimate(flops=flops, bytes_accessed=6 << 20, transcendentals=0)
-    if gate_rows is None:
-        return pl.pallas_call(
-            project_only_kernel,
-            out_shape=shape,
-            in_specs=smem + in_vmem(9),
-            out_specs=in_vmem(1)[0],
-            cost_estimate=cost,
-        )(core, *pieces, weights)
+def call(kernel, shapes, spot, arrays, flops, scratch=()):
+    smem = [pl.BlockSpec(memory_space=pltpu.SMEM)] if spot is not None else []
     return pl.pallas_call(
-        project_kernel,
-        out_shape=(shape, jax.ShapeDtypeStruct((4, gate_rows.shape[1], tokens), F32)),
-        in_specs=smem + in_vmem(10),
-        out_specs=in_vmem(2),
-        cost_estimate=cost,
-    )(core, *pieces, weights, gate_rows)
+        kernel,
+        out_shape=tuple(jax.ShapeDtypeStruct(shape, dtype) for shape, dtype in shapes),
+        in_specs=smem + in_vmem(len(arrays)),
+        out_specs=tuple(in_vmem(len(shapes))),
+        scratch_shapes=list(scratch),
+        cost_estimate=pl.CostEstimate(flops=flops, bytes_accessed=6 << 20, transcendentals=0),
+    )(*([spot] if spot is not None else []), *arrays)
 
 
 def shards(
@@ -149,14 +172,26 @@
     place_x = lax.axis_index("fs")
     order = [(place_x + by) % seqs for by in (0, seqs - 1, 1, 2)]
 
-    w_conv = jnp.concatenate([w_conv_gate, w_conv_mult, w_conv_in], axis=1)
-    w_conv = lax.all_gather(w_conv, SP, axis=0, tiled=True)
-    w_mem = everyone(jnp.concatenate([w_query, w_key, w_value], axis=1), SP)
-    w_mem = w_mem.reshape(width, -1)
-
-    turned = jnp.concatenate([w_out_conv.T, w_out_mem.T], axis=1)
-    turned, w_mem = lax.optimization_barrier((turned, w_mem))
-    w_own = everyone(turned, SP).reshape(width, -1)
+    spots = [lax.axis_index(name) for name in ("tp", "sp_0", "sp_1")]
+    spot = jnp.stack(spots).astype(jnp.int32)
+
+    w_mem = jnp.concatenate([w_query, w_key, w_value], axis=1)
+    w_rest = jnp.concatenate(
+        [w_conv_gate, w_conv_mult, w_conv_in, w_out_conv.T, w_out_mem.T], axis=1
+    )
+    channels = w_conv_gate.shape[1]
+    w_mem = everyone(w_mem, "sp_0").reshape(-1, w_mem.shape[1])
+    w_rest, w_mem = lax.optimization_barrier((w_rest, w_mem))
+    w_rest = everyone(w_rest, "sp_1").reshape(-1, w_rest.shape[1])
+    w_mem = ring_gather(w_mem, "sp_1")
+    w_rest = ring_gather(w_rest, "sp_0")
+    w_conv, w_own = call(
+        arrange_kernel,
+        [((width, 3 * channels), BF16), ((width, 2 * channels), BF16)],
+        spot,
+        w_rest,
+        10**9,
+    )
     w_out = (w_own, *around(w_own, "fs"))
 
     x = activations[0].astype(F32)
@@ -167,7 +202,6 @@
     pieces = [mine, lax.dynamic_slice_in_dim(normed, (1 - core) * half, half, 1)]
     for piece in around(mine, "fs"):
         pieces += [piece, other_core(piece)]
-    core_row = core.reshape(1).astype(jnp.int32)
 
     gate_rows = jnp.concatenate(
         [
@@ -177,7 +211,14 @@
         axis=1,
     ).T
     gate_rows = jnp.pad(gate_rows, ((0, 14), (0, 0))).reshape(16, 2, half).transpose(1, 0, 2)
-    qkv, gates = project(core_row, pieces, w_mem, gate_rows)
+    qkv, gates = call(
+        project_mem_kernel,
+        [((seqs, tokens, 3 * HEAD_DIM), BF16), ((seqs, 16, tokens), F32)],
+        spot,
+        [*w_mem, *pieces, gate_rows],
+        10**9 * 3,
+        [pltpu.VMEM((width, 3 * HEAD_DIM), BF16)],
+    )
     query, key, value = (qkv[..., k * HEAD_DIM : (k + 1) * HEAD_DIM] for k in range(3))
     bias = lax.dynamic_slice_in_dim(gate_bias, head, 1, 1)
     decay = lax.dynamic_slice_in_dim(decay_shift, head, 1, 2)[..., 0]
@@ -207,8 +248,8 @@
     found = everywhere[:, seqs * cut, :count].astype(F32).reshape(places, 3, 2, seqs)
     found = found[:, 0] + found[:, 1] + found[:, 2]
     totals, peaks = found[:, 0].T, found[:, 1].T
-    spots = jnp.arange(places)
-    earlier = spots[:, None] > spots[None, :]
+    line = jnp.arange(places)
+    earlier = line[:, None] > line[None, :]
     masked = jnp.where(earlier, totals[:, None, :], 0.0)
     between = lax.dot_general(
         masked, earlier.astype(F32), (((2,), (0,)), ((), ())), precision=HIGHEST
@@ -226,8 +267,13 @@
     place = lax.axis_index(SP)
     prior_peak = lax.dynamic_slice_in_dim(carried_peak, place, 1, 1)
 
-    conv = project(core_row, pieces, w_conv)
-    channels = conv.shape[2] // 3
+    (conv,) = call(
+        project_conv_kernel,
+        [((seqs, tokens, 3 * channels), BF16)],
+        spot,
+        [*pieces, w_conv],
+        10**9 * 3,
+    )
     gate, mult, inlet = (conv[..., k * channels : (k + 1) * channels] for k in range(3))
     product = (mult.astype(F32) * inlet.astype(F32)).astype(BF16)
     taps = conv_taps.shape[0]
@@ -238,10 +284,6 @@
     for j in range(1, taps):
         mixed = mixed + tap_rows[j] * padded[:, j : j + tokens]
     conv_out = (gate.astype(F32) * mixed).astype(BF16)
-    last = (((1,), (1,)), ((), ()))
-    conv_parts = returned([conv_out[k] for k in range(seqs)], "fs")
-    output = sum(dot(a, w[:, :channels], last) for a, w in zip(conv_parts, w_out))
-
     spans = jnp.arange(tokens)
     causal = spans[:, None] >= spans[None, :]
     pair_logs = jnp.where(
@@ -257,11 +299,12 @@
     cell = cell * lax.rsqrt(jnp.mean(cell * cell, axis=-1, keepdims=True) + EPSILON)
     gain = lax.dynamic_slice_in_dim(head_gain, head * HEAD_DIM, HEAD_DIM, 0)
     mem_out = (cell * gain).astype(BF16)
-    mem_parts = returned([mem_out[k] for k in range(seqs)], "fs")
-    output = output + sum(dot(a, w[:, channels:], last) for a, w in zip(mem_parts, w_out))
+    both = jnp.concatenate([conv_out, mem_out], axis=-1)
+    parts = returned([both[k] for k in range(seqs)], "fs")
+    (output,) = call(output_kernel, [((tokens, width), BF16)], None, [*parts, *w_out], 10**9 * 2)
 
     cores = lax.axis_size("tp")
-    parts = exchanged(output.astype(BF16).reshape(cores, tokens // cores, width), "tp")
+    parts = exchanged(output.reshape(cores, tokens // cores, width), "tp")
     return jnp.sum(parts.astype(F32), axis=0).astype(BF16)[None]
 
 

time: 234 us -> 230 us (0.983); the launches traced: 229 us -> 228 us
  starting transfers between devices: 94.3 us -> 131 us
  waiting for transfers between devices: 59.2 us -> 34.2 us
  between operations: 14.2 us -> 1.12 us
  Pallas kernels: 12.9 us -> 20.9 us
  blocking collectives: 13.9 us -> 10.9 us
  matrix products: 8.11 us -> 5.13 us
  local copies, waits for them, and re-layouts: 14.5 us -> 11.9 us
    ppermute x14 -> x25, starting transfers between devices: 44.5 us -> 78.2 us  [ring(): lax.ppermute(array, axis, [(i, (i + by) % peers) for i in range(peers)])]
    all_to_all x2, waiting for transfers between devices: 23.7 us -> 0.01 us  [exchanged(): return lax.all_to_all(array, axis, split_axis=0, concat_axis=0, tiled=True)]
    pallas_call x2 -> x4, Pallas kernels: 12.9 us -> 20.9 us  [call(): pl.pallas_call(kernel, out_shape=tuple((jax.ShapeDtypeStruct(shape, dtype...]
    all_to_all x2, starting transfers between devices: 16.5 us -> 22.5 us  [exchanged(): return lax.all_to_all(array, axis, split_axis=0, concat_axis=0, tiled=True)]
    ppermute x1, waiting for transfers between devices: 5.96 us -> 0.01 us  [from_behind(): return lax.ppermute(array, axis, [(i, i + 1) for i in range(peers - 1)])]
    all_to_all x2, starting transfers between devices: 22.1 us -> 16.3 us  [everyone(): return lax.all_to_all(copies, axis, split_axis=0, concat_axis=0, tiled=True)]
    all_to_all x2, waiting for transfers between devices: 0.75 us -> 5.31 us  [everyone(): return lax.all_to_all(copies, axis, split_axis=0, concat_axis=0, tiled=True)]
    all_to_all x1, blocking collectives: 13.9 us -> 10.9 us  [exchanged(): return lax.all_to_all(array, axis, split_axis=0, concat_axis=0, tiled=True)]
  transfers between devices with their start and end apart: 23 -> 33, of which waited for: 8 -> 11; matrix products, arithmetic and copies ran while one was open for 13% -> 10% of each run, Pallas kernels for 6% -> 7%
where the time goes in v2:
time: 230 us; the launch traced here: 228 us
  starting transfers between devices  131 us (57%)
  waiting for transfers between devices  34.2 us (15%)
  Pallas kernels  20.9 us (9%)
  other arithmetic  13.8 us (6%)
  local copies, waits for them, and re-layouts  11.9 us (5%)
  blocking collectives  10.9 us (5%)
  matrix products  5.13 us (2%)
    ppermute x25, starting transfers between devices, ring(): lax.ppermute(array, axis, [(i, (i + by) % peers) for i in range(peers)])  78.2 us
    ppermute x25, waiting for transfers between devices, ring(): lax.ppermute(array, axis, [(i, (i + by) % peers) for i in range(peers)])  28.8 us
    all_to_all x2, starting transfers between devices, exchanged(): return lax.all_to_all(array, axis, split_axis=0, concat_axis=0, tiled=True)  22.5 us
    pallas_call x4, Pallas kernels, call(): pl.pallas_call(kernel, out_shape=tuple((jax.ShapeDtypeStruct(shape, dtype...  20.9 us
    all_to_all x2, starting transfers between devices, everyone(): return lax.all_to_all(copies, axis, split_axis=0, concat_axis=0, tiled=True)  16.3 us
    all_to_all x1, blocking collectives, exchanged(): return lax.all_to_all(array, axis, split_axis=0, concat_axis=0, tiled=True)  10.9 us
    ppermute x3, starting transfers between devices, other_core(): return lax.ppermute(array, 'tp', [(0, 1), (1, 0)])  10.6 us
    all_to_all x2, waiting for transfers between devices, everyone(): return lax.all_to_all(copies, axis, split_axis=0, concat_axis=0, tiled=True)  5.31 us
  transfers between devices with their start and end apart: 33, of which 11 were waited for; matrix products, arithmetic and copies ran while one was open for 10% of the time, Pallas kernels for 7%

profile of v2, /device:TPU:1, one launch (start us, length us, event | category | flops | bytes accessed | tf_op | source)
XLA Modules:
  0.0 228.5 jit_solution(16705651919558905311)
XLA Ops:
  0.0 1.6 fusion
  1.6 1.0 fusion.2
  2.7 0.9 constant_dynamic-slice_fusion.9
  3.6 5.2 %collective-permute-start.2 = (bf16[256,1024]{1,0:T(8,128)(2,1)S(1)}, bf16[256,1024]{1,0:T(8,128)(2,1)S(1)}, u32[]{:S(2)}, u32[]{:S(2)}) collective-permute-start(bf16[256,1024]{1,0:T(8,128)(2,1)S(1)} %get-tuple-element.20.refs_0_.refs_8_), channel_id=1, source_target_pairs={{0,6},{2,0},{4,2},{6,4},{1,7},{3,1},{5,3},{7,5},{8,14},{10,8},{12,... | collective-permute-start | bytes 1572872 | tf_op jit(solution)/shard_map/ppermute | solution.py:50
  8.8 1.9 collective-permute-start
  11.5 10.0 %all-to-all-start = ((bf16[8,32,384]{2,1,0:T(8,128)(2,1)}), bf16[8,32,384]{2,1,0:T(8,128)(2,1)S(1)}, u32[]{:S(2)}, u32[]{:S(2)}) async-start(bf16[8,32,384]{2,1,0:T(8,128)(2,1)} %broadcast_in_dim.66), calls=%async_computation | async-start | bytes 393216 | tf_op jit(solution)/shard_map/all_to_all | solution.py:21
  21.9 2.1 collective-permute-start.4
  23.9 0.8 constant_dynamic-slice_fusion.6
  24.8 5.3 %all-to-all-done = bf16[8,32,384]{2,1,0:T(8,128)(2,1)S(1)} async-done(((bf16[8,32,384]{2,1,0:T(8,128)(2,1)}), bf16[8,32,384]{2,1,0:T(8,128)(2,1)S(1)}, u32[]{:S(2)}, u32[]{:S(2)}) %all-to-all-start) | async-done | bytes 196640 | tf_op jit(solution)/shard_map/all_to_all | solution.py:21
  30.1 3.2 %collective-permute-start.15 = (bf16[256,384]{1,0:T(8,128)(2,1)S(1)}, bf16[256,384]{1,0:T(8,128)(2,1)}, u32[]{:S(2)}, u32[]{:S(2)}) collective-permute-start(bf16[256,384]{1,0:T(8,128)(2,1)S(1)} %bitcast.105), channel_id=1, source_target_pairs={{0,8},{8,16},{16,24},{24,32},{32,40},{40,48},{48,56},{56,0},{1,9},... | collective-permute-start | bytes 589832 | tf_op jit(solution)/shard_map/ppermute | solution.py:50
  33.4 4.4 %collective-permute-start.5 = (bf16[128,1024]{1,0:T(8,128)(2,1)S(1)}, bf16[128,1024]{1,0:T(8,128)(2,1)S(1)}, u32[]{:S(2)}, u32[]{:S(2)}) collective-permute-start(bf16[128,1024]{1,0:T(8,128)(2,1)S(1)} %slice.144), channel_id=1, source_target_pairs={{0,6},{2,0},{4,2},{6,4},{1,7},{3,1},{5,3},{7,5},{8,14},{10,8},{12,... | collective-permute-start | bytes 786440 | tf_op jit(solution)/shard_map/ppermute | solution.py:50
  38.5 3.8 %collective-permute-start.19 = (bf16[256,384]{1,0:T(8,128)(2,1)S(1)}, bf16[256,384]{1,0:T(8,128)(2,1)}, u32[]{:S(2)}, u32[]{:S(2)}) collective-permute-start(bf16[256,384]{1,0:T(8,128)(2,1)S(1)} %bitcast.106), channel_id=1, source_target_pairs={{0,56},{8,0},{16,8},{24,16},{32,24},{40,32},{48,40},{56,48},{1,57}... | collective-permute-start | bytes 589832 | tf_op jit(solution)/shard_map/ppermute | solution.py:50
  42.3 0.8 broadcast_in_dim.67
  43.1 6.3 %all-to-all-start.1 = ((bf16[8,32,640]{2,1,0:T(8,128)(2,1)}), bf16[8,32,640]{2,1,0:T(8,128)(2,1)S(1)}, u32[]{:S(2)}, u32[]{:S(2)}) async-start(bf16[8,32,640]{2,1,0:T(8,128)(2,1)} %broadcast_in_dim.67), calls=%async_computation.1 | async-start | bytes 655360 | tf_op jit(solution)/shard_map/all_to_all | solution.py:21
  49.4 6.0 %collective-permute-start.3 = (bf16[256,1024]{1,0:T(8,128)(2,1)S(1)}, bf16[256,1024]{1,0:T(8,128)(2,1)}, u32[]{:S(2)}, u32[]{:S(2)}) collective-permute-start(bf16[256,1024]{1,0:T(8,128)(2,1)S(1)} %collective-permute-done.2.refs_4_.refs_12_), channel_id=1, source_target_pairs={{0,1},{1,0},{2,3},{3,2},{4,5},{5,4},{6,7},{7,6},{8,9},{9,8},{10,11... | collective-permute-start | bytes 1572872 | tf_op jit(solution)/shard_map/ppermute | solution.py:29
  55.4 1.9 collective-permute-start.1
  57.3 3.6 %collective-permute-start.16 = (bf16[256,384]{1,0:T(8,128)(2,1)}, bf16[256,384]{1,0:T(8,128)(2,1)S(1)}, u32[]{:S(2)}, u32[]{:S(2)}) collective-permute-start(bf16[256,384]{1,0:T(8,128)(2,1)} %collective-permute-done.15.refs_1_), channel_id=1, source_target_pairs={{0,8},{8,16},{16,24},{24,32},{32,40},{40,48},{48,56},{56,0},{1,9},... | collective-permute-start | bytes 589832 | tf_op jit(solution)/shard_map/ppermute | solution.py:50
  61.1 2.7 %collective-permute-start.6 = (bf16[256,1024]{1,0:T(8,128)(2,1)S(1)}, bf16[256,1024]{1,0:T(8,128)(2,1)S(1)}, u32[]{:S(2)}, u32[]{:S(2)}) collective-permute-start(bf16[256,1024]{1,0:T(8,128)(2,1)S(1)} %constant_dynamic-update-slice_fusion.refs_6_.refs_14_), channel_id=1, source_target_pairs={{0,1},{1,0},{2,3},{3,2},{4,5},{5,4},{6,7},{7,6},{8,9},{9,8},{10,11... | collective-permute-start | bytes 1572872 | tf_op jit(solution)/shard_map/ppermute | solution.py:29
  63.8 0.8 constant_dynamic-slice_fusion.4
  64.5 2.9 %collective-permute-start.20 = (bf16[256,384]{1,0:T(8,128)(2,1)}, bf16[256,384]{1,0:T(8,128)(2,1)S(1)}, u32[]{:S(2)}, u32[]{:S(2)}) collective-permute-start(bf16[256,384]{1,0:T(8,128)(2,1)} %collective-permute-done.19.refs_5_), channel_id=1, source_target_pairs={{0,56},{8,0},{16,8},{24,16},{32,24},{40,32},{48,40},{56,48},{1,57}... | collective-permute-start | bytes 589832 | tf_op jit(solution)/shard_map/ppermute | solution.py:50
  68.0 1.9 collective-permute-start.17
  70.6 2.5 %collective-permute-done.20.refs_6_ = bf16[256,384]{1,0:T(8,128)(2,1)S(1)} collective-permute-done((bf16[256,384]{1,0:T(8,128)(2,1)}, bf16[256,384]{1,0:T(8,128)(2,1)S(1)}, u32[]{:S(2)}, u32[]{:S(2)}) %collective-permute-start.20) | collective-permute-done | bytes 196640 | tf_op jit(solution)/shard_map/ppermute | solution.py:50
  73.1 4.1 %collective-permute-start.21 = (bf16[256,384]{1,0:T(8,128)(2,1)S(1)}, bf16[256,384]{1,0:T(8,128)(2,1)}, u32[]{:S(2)}, u32[]{:S(2)}) collective-permute-start(bf16[256,384]{1,0:T(8,128)(2,1)S(1)} %collective-permute-done.20.refs_6_), channel_id=1, source_target_pairs={{0,56},{8,0},{16,8},{24,16},{32,24},{40,32},{48,40},{56,48},{1,57}... | collective-permute-start | bytes 589832 | tf_op jit(solution)/shard_map/ppermute | solution.py:50
  77.2 1.9 collective-permute-start.18
  79.7 0.9 collective-permute-done.21.refs_7_
  80.7 7.2 %collective-permute-start.11 = (bf16[256,640]{1,0:T(8,128)(2,1)S(1)}, bf16[256,640]{1,0:T(8,128)(2,1)}, u32[]{:S(2)}, u32[]{:S(2)}) collective-permute-start(bf16[256,640]{1,0:T(8,128)(2,1)S(1)} %bitcast.101), channel_id=1, source_target_pairs={{0,448},{64,0},{128,64},{192,128},{256,192},{320,256},{384,320},{4... | collective-permute-start | bytes 983048 | tf_op jit(solution)/shard_map/ppermute | solution.py:50
  87.9 1.9 collective-permute-start.7
  89.9 0.7 copy-done.19
  90.7 6.9 %shard_map.156 = (bf16[4,256,384]{2,1,0:T(8,128)(2,1)}, f32[4,16,256]{2,1,0:T(8,128)}) custom-call(s32[3]{0:T(128)} %pad_add_fusion.spot, bf16[256,384]{1,0:T(8,128)(2,1)} %bitcast.107, bf16[256,384]{1,0:T(8,128)(2,1)} %collective-permute-done.15.refs_1_, bf16[256,384]{1,0:T(8,128)(2,1)} %copy-done.25, bf16[256,384]{1,0:T(8,128)(2,1)} %copy-done.27, ...), custom_call_target="tpu_custom_call" | custom-call | flops 3000000000 | bytes 6291456 | tf_op jit(solution)/shard_map/pallas_call | solution.py:138
  97.6 1.4 add_negate_fusion
  99.0 1.2 reduce-window.6
  100.9 1.6 add_reduce_fusion
  102.7 1.5 convolution_convert_fusion
  104.3 0.9 copy.83
  105.2 11.3 %all-to-all-start.2 = ((bf16[64,16,128]{2,1,0:T(8,128)(2,1)}), bf16[64,16,128]{2,1,0:T(8,128)(2,1)S(1)}, u32[]{:S(2)}, u32[]{:S(2)}) async-start(bf16[64,16,128]{2,1,0:T(8,128)(2,1)} %copy.83), calls=%async_computation.2 | async-start | bytes 524288 | tf_op jit(solution)/shard_map/all_to_all | solution.py:25
  116.5 0.8 dynamic_slice.51
  117.3 4.4 %collective-permute-start.12 = (bf16[256,640]{1,0:T(8,128)(2,1)}, bf16[256,640]{1,0:T(8,128)(2,1)S(1)}, u32[]{:S(2)}, u32[]{:S(2)}) collective-permute-start(bf16[256,640]{1,0:T(8,128)(2,1)} %collective-permute-done.11.refs_5_), channel_id=1, source_target_pairs={{0,448},{64,0},{128,64},{192,128},{256,192},{320,256},{384,320},{4... | collective-permute-start | bytes 983048 | tf_op jit(solution)/shard_map/ppermute | solution.py:50
  121.7 1.9 collective-permute-start.8
  124.1 8.5 %collective-permute-done.12.refs_6_ = bf16[256,640]{1,0:T(8,128)(2,1)S(1)} collective-permute-done((bf16[256,640]{1,0:T(8,128)(2,1)}, bf16[256,640]{1,0:T(8,128)(2,1)S(1)}, u32[]{:S(2)}, u32[]{:S(2)}) %collective-permute-start.12) | collective-permute-done | bytes 327712 | tf_op jit(solution)/shard_map/ppermute | solution.py:50
  132.6 3.6 %collective-permute-start.13 = (bf16[256,640]{1,0:T(8,128)(2,1)S(1)}, bf16[256,640]{1,0:T(8,128)(2,1)S(1)}, u32[]{:S(2)}, u32[]{:S(2)}) collective-permute-start(bf16[256,640]{1,0:T(8,128)(2,1)S(1)} %collective-permute-done.12.refs_6_), channel_id=1, source_target_pairs={{0,448},{64,0},{128,64},{192,128},{256,192},{320,256},{384,320},{4... | collective-permute-start | bytes 983048 | tf_op jit(solution)/shard_map/ppermute | solution.py:50
  136.2 1.9 collective-permute-start.9
  138.8 7.8 %collective-permute-done.9.refs_3_ = bf16[256,640]{1,0:T(8,128)(2,1)S(1)} collective-permute-done((bf16[256,640]{1,0:T(8,128)(2,1)S(1)}, bf16[256,640]{1,0:T(8,128)(2,1)S(1)}, u32[]{:S(2)}, u32[]{:S(2)}) %collective-permute-start.9) | collective-permute-done | bytes 327712 | tf_op jit(solution)/shard_map/ppermute | solution.py:50
  146.6 1.9 collective-permute-start.10
  149.8 11.2 %all-to-all-start.3 = ((bf16[64,8,128]{2,1,0:T(8,128)(2,1)}), bf16[64,8,128]{2,1,0:T(8,128)(2,1)S(1)}, u32[]{:S(2)}, u32[]{:S(2)}) async-start(bf16[64,8,128]{2,1,0:T(8,128)(2,1)} %reshape.384), calls=%async_computation.3 | async-start | bytes 262144 | tf_op jit(solution)/shard_map/all_to_all | solution.py:25
  162.5 3.4 %shard_map.154 = (bf16[2048,384]{1,0:T(8,128)(2,1)}, bf16[2048,256]{1,0:T(8,128)(2,1)}) custom-call(s32[3]{0:T(128)} %pad_add_fusion.spot, bf16[256,640]{1,0:T(8,128)(2,1)} %bitcast.103, bf16[256,640]{1,0:T(8,128)(2,1)} %collective-permute-done.7.refs_1_, bf16[256,640]{1,0:T(8,128)(2,1)} %copy-done.21, bf16[256,640]{1,0:T(8,128)(2,1)} %copy-done.23, ...), custom_call_target="tpu_custom_call" | custom-call | flops 1000000000 | bytes 6291456 | tf_op jit(solution)/shard_map/pallas_call | solution.py:138
  165.9 1.9 collective-permute-start.26
  167.8 3.5 %collective-permute-start.25 = (bf16[2048,256]{1,0:T(8,128)(2,1)}, bf16[2048,256]{1,0:T(8,128)(2,1)S(1)}, u32[]{:S(2)}, u32[]{:S(2)}) collective-permute-start(bf16[2048,256]{1,0:T(8,128)(2,1)} %get-tuple-element.16.refs_4_), channel_id=1, source_target_pairs={{0,2},{2,4},{4,6},{6,0},{1,3},{3,5},{5,7},{7,1},{8,10},{10,12},{12... | collective-permute-start | bytes 3145736 | tf_op jit(solution)/shard_map/ppermute | solution.py:50
  171.4 1.7 fusion.4
  173.3 1.4 multiply_reduce_fusion
  174.6 6.0 %shard_map.155 = bf16[4,256,384]{2,1,0:T(8,128)(2,1)} custom-call(s32[3]{0:T(128)} %pad_add_fusion.spot, bf16[256,1024]{1,0:T(8,128)(2,1)} %copy-done.2, bf16[256,1024]{1,0:T(8,128)(2,1)} %get-tuple-element.19.refs_1_.refs_9_, bf16[256,1024]{1,0:T(8,128)(2,1)} %copy-done.8, bf16[256,1024]{1,0:T(8,128)(2,1)} %collective-permute-done.1.refs_3_.refs_11_, ...), custom_call_target="tpu_custom_call" | custom-call | flops 3000000000 | bytes 6291456 | tf_op jit(solution)/shard_map/pallas_call | solution.py:138
  180.6 1.1 multiply_convert_fusion.2
  181.7 2.9 %collective-permute-start.14 = (bf16[4,2,128]{2,1,0:T(2,128)(2,1)S(1)}, bf16[4,2,128]{2,1,0:T(2,128)(2,1)S(1)}, u32[]{:S(2)}, u32[]{:S(2)}) collective-permute-start(bf16[4,2,128]{2,1,0:T(2,128)(2,1)S(1)} %slice.148), channel_id=1, source_target_pairs={{0,8},{8,16},{16,24},{24,32},{32,40},{40,48},{48,56},{56,64},{64,7... | collective-permute-start | bytes 6152 | tf_op jit(solution)/shard_map/ppermute | solution.py:34
  184.6 5.5 %collective-permute-done.26.refs_6_ = bf16[2048,256]{1,0:T(8,128)(2,1)S(1)} collective-permute-done((bf16[2048,256]{1,0:T(8,128)(2,1)}, bf16[2048,256]{1,0:T(8,128)(2,1)S(1)}, u32[]{:S(2)}, u32[]{:S(2)}) %collective-permute-start.26) | collective-permute-done | bytes 1048608 | tf_op jit(solution)/shard_map/ppermute | solution.py:50
  190.2 3.4 %collective-permute-start.28 = (bf16[1024,256]{1,0:T(8,128)(2,1)S(1)}, bf16[1024,256]{1,0:T(8,128)(2,1)S(1)}, u32[]{:S(2)}, u32[]{:S(2)}) collective-permute-start(bf16[1024,256]{1,0:T(8,128)(2,1)S(1)} %slice.168), channel_id=1, source_target_pairs={{0,6},{2,0},{4,2},{6,4},{1,7},{3,1},{5,3},{7,5},{8,14},{10,8},{12,... | collective-permute-start | bytes 1572872 | tf_op jit(solution)/shard_map/ppermute | solution.py:50
  193.6 1.9 collective-permute-start.27
  195.9 1.2 fusion.14
  197.8 3.1 %collective-permute-start.24 = (bf16[256,256]{1,0:T(8,128)(2,1)S(1)}, bf16[256,256]{1,0:T(8,128)(2,1)S(1)}, u32[]{:S(2)}, u32[]{:S(2)}) collective-permute-start(bf16[256,256]{1,0:T(8,128)(2,1)S(1)} %get-tuple-element.21), channel_id=1, source_target_pairs={{0,4},{2,6},{4,0},{6,2},{1,5},{3,7},{5,1},{7,3},{8,12},{10,14},{12... | collective-permute-start | bytes 393224 | tf_op jit(solution)/shard_map/ppermute | solution.py:50
  200.9 4.0 %collective-permute-start.22 = (bf16[256,256]{1,0:T(8,128)(2,1)S(1)}, bf16[256,256]{1,0:T(8,128)(2,1)S(1)}, u32[]{:S(2)}, u32[]{:S(2)}) collective-permute-start(bf16[256,256]{1,0:T(8,128)(2,1)S(1)} %get-tuple-element.23), channel_id=1, source_target_pairs={{0,2},{2,4},{4,6},{6,0},{1,3},{3,5},{5,7},{7,1},{8,10},{10,12},{12... | collective-permute-start | bytes 393224 | tf_op jit(solution)/shard_map/ppermute | solution.py:50
  204.8 2.5 %collective-permute-start.23 = (bf16[256,256]{1,0:T(8,128)(2,1)S(1)}, bf16[256,256]{1,0:T(8,128)(2,1)S(1)}, u32[]{:S(2)}, u32[]{:S(2)}) collective-permute-start(bf16[256,256]{1,0:T(8,128)(2,1)S(1)} %get-tuple-element.24), channel_id=1, source_target_pairs={{0,6},{2,0},{4,2},{6,4},{1,7},{3,1},{5,3},{7,5},{8,14},{10,8},{12,... | collective-permute-start | bytes 393224 | tf_op jit(solution)/shard_map/ppermute | solution.py:50
  208.0 1.0 pad_maximum_fusion.refs_7_
  209.0 2.0 collective-permute-done.22.refs_1_
  211.8 4.6 %shard_map.157 = bf16[256,2048]{1,0:T(8,128)(2,1)} custom-call(bf16[256,256]{1,0:T(8,128)(2,1)} %get-tuple-element.22.refs_0_, bf16[256,256]{1,0:T(8,128)(2,1)} %copy-done.29, bf16[256,256]{1,0:T(8,128)(2,1)} %copy-done.30, bf16[256,256]{1,0:T(8,128)(2,1)} %copy-done.28, bf16[2048,256]{1,0:T(8,128)(2,1)} %get-tuple-element.16.refs_4_, ...), custom_call_target="tpu_custom_call" | custom-call | flops 2000000000 | bytes 6291456 | tf_op jit(solution)/shard_map/pallas_call | solution.py:138
  216.4 10.9 %all_to_all.25 = bf16[2,128,2048]{2,1,0:T(8,128)(2,1)S(1)} all-to-all(bf16[2,128,2048]{2,1,0:T(8,128)(2,1)} %bitcast.97), channel_id=1, replica_groups=mesh['sp_0'=8,'sp_1'=8,'fs'=4,'tp'=2] {'tp'}, dimensions={0} | all-to-all | bytes 2097152 | tf_op jit(solution)/shard_map/all_to_all | solution.py:25
  227.4 1.1 reduce_sum.42
  (153 shorter events, 11.1 us)
Async XLA Ops:
  0.0 116.5 %copy-start = (f32[3,1024]{1,0:T(4,128)S(1)}, f32[3,1024]{1,0:T(4,128)}, u32[]{:S(2)}) copy-start(f32[3,1024]{1,0:T(4,128)} %param.21) | copy-start | bytes 36868
  0.0 1.6 copy-start.1
  2.6 8.1 %copy-start.15 = (bf16[32,128]{1,0:T(8,128)(2,1)S(1)}, bf16[32,128]{1,0:T(8,128)(2,1)}, u32[]{:S(2)}) copy-start(bf16[32,128]{1,0:T(8,128)(2,1)} %param.24) | copy-start | bytes 24580
  2.6 8.1 %copy-start.16 = (bf16[32,128]{1,0:T(8,128)(2,1)S(1)}, bf16[32,128]{1,0:T(8,128)(2,1)}, u32[]{:S(2)}) copy-start(bf16[32,128]{1,0:T(8,128)(2,1)} %param.23) | copy-start | bytes 24580
  2.7 8.1 %copy-start.17 = (bf16[32,128]{1,0:T(8,128)(2,1)S(1)}, bf16[32,128]{1,0:T(8,128)(2,1)}, u32[]{:S(2)}) copy-start(bf16[32,128]{1,0:T(8,128)(2,1)} %param.22) | copy-start | bytes 24580
  2.7 18.9 %copy-start.10 = (bf16[32,128]{1,0:T(8,128)(2,1)S(1)}, bf16[32,128]{1,0:T(8,128)(2,1)}, u32[]{:S(2)}) copy-start(bf16[32,128]{1,0:T(8,128)(2,1)} %param.18) | copy-start | bytes 24580
  2.7 18.9 %copy-start.11 = (bf16[32,128]{1,0:T(8,128)(2,1)S(1)}, bf16[32,128]{1,0:T(8,128)(2,1)}, u32[]{:S(2)}) copy-start(bf16[32,128]{1,0:T(8,128)(2,1)} %param.19) | copy-start | bytes 24580
  2.7 18.9 %copy-start.12 = (bf16[32,128]{1,0:T(8,128)(2,1)S(1)}, bf16[32,128]{1,0:T(8,128)(2,1)}, u32[]{:S(2)}) copy-start(bf16[32,128]{1,0:T(8,128)(2,1)} %param.20) | copy-start | bytes 24580
  2.7 18.9 %copy-start.13 = (bf16[128,32]{0,1:T(8,128)(2,1)S(1)}, bf16[128,32]{0,1:T(8,128)(2,1)}, u32[]{:S(2)}) copy-start(bf16[128,32]{0,1:T(8,128)(2,1)} %param.30) | copy-start | bytes 24580
  2.7 18.9 %copy-start.14 = (bf16[128,32]{0,1:T(8,128)(2,1)S(1)}, bf16[128,32]{0,1:T(8,128)(2,1)}, u32[]{:S(2)}) copy-start(bf16[128,32]{0,1:T(8,128)(2,1)} %param.31) | copy-start | bytes 24580
  3.6 39.5 %copy-start.2 = (bf16[256,1024]{1,0:T(8,128)(2,1)}, bf16[256,1024]{1,0:T(8,128)(2,1)S(1)}, u32[]{:S(2)}) copy-start(bf16[256,1024]{1,0:T(8,128)(2,1)S(1)} %get-tuple-element.20.refs_0_.refs_8_) | copy-start | bytes 1572868
  3.6 29.7 %collective-permute-start.2 = (bf16[256,1024]{1,0:T(8,128)(2,1)S(1)}, bf16[256,1024]{1,0:T(8,128)(2,1)S(1)}, u32[]{:S(2)}, u32[]{:S(2)}) collective-permute-start(bf16[256,1024]{1,0:T(8,128)(2,1)S(1)} %get-tuple-element.20.refs_0_.refs_8_), channel_id=1, source_target_pairs={{0,6},{2,0},{4,2},{6,4},{1,7},{3,1},{5,3},{7,5},{8,14},{10,8},{12,... | collective-permute-start | bytes 1572872 | tf_op jit(solution)/shard_map/ppermute | solution.py:50
  8.8 13.0 %collective-permute-start = (bf16[256,1024]{1,0:T(8,128)(2,1)S(1)}, bf16[256,1024]{1,0:T(8,128)(2,1)S(1)}, u32[]{:S(2)}, u32[]{:S(2)}) collective-permute-start(bf16[256,1024]{1,0:T(8,128)(2,1)S(1)} %get-tuple-element.20.refs_0_.refs_8_), channel_id=1, source_target_pairs={{0,2},{2,4},{4,6},{6,0},{1,3},{3,5},{5,7},{7,1},{8,10},{10,12},{12... | collective-permute-start | bytes 1572872 | tf_op jit(solution)/shard_map/ppermute | solution.py:50
  11.5 18.6 %all-to-all-start = ((bf16[8,32,384]{2,1,0:T(8,128)(2,1)}), bf16[8,32,384]{2,1,0:T(8,128)(2,1)S(1)}, u32[]{:S(2)}, u32[]{:S(2)}) async-start(bf16[8,32,384]{2,1,0:T(8,128)(2,1)} %broadcast_in_dim.66), calls=%async_computation | async-start | bytes 393216 | tf_op jit(solution)/shard_map/all_to_all | solution.py:21
  21.8 39.2 %copy-start.8 = (bf16[256,1024]{1,0:T(8,128)(2,1)}, bf16[256,1024]{1,0:T(8,128)(2,1)S(1)}, u32[]{:S(2)}) copy-start(bf16[256,1024]{1,0:T(8,128)(2,1)S(1)} %collective-permute-done.refs_2_.refs_10_) | copy-start | bytes 1572868
  21.9 48.1 %copy-start.18 = (f32[2,8]{1,0:T(2,128)S(1)}, f32[2,8]{1,0:T(2,128)}, u32[]{:S(2)}) copy-start(f32[2,8]{1,0:T(2,128)} %param.27) | copy-start | bytes 196
  21.9 35.4 %collective-permute-start.4 = (bf16[128,1024]{1,0:T(8,128)(2,1)S(1)}, bf16[128,1024]{1,0:T(8,128)(2,1)S(1)}, u32[]{:S(2)}, u32[]{:S(2)}) collective-permute-start(bf16[128,1024]{1,0:T(8,128)(2,1)S(1)} %slice.143), channel_id=1, source_target_pairs={{0,2},{2,4},{4,6},{6,0},{1,3},{3,5},{5,7},{7,1},{8,10},{10,12},{12... | collective-permute-start | bytes 786440 | tf_op jit(solution)/shard_map/ppermute | solution.py:50
  30.1 59.8 %copy-start.6 = (bf16[8,32,384]{2,1,0:T(8,128)(2,1)}, bf16[8,32,384]{2,1,0:T(8,128)(2,1)S(1)}, u32[]{:S(2)}) copy-start(bf16[8,32,384]{2,1,0:T(8,128)(2,1)S(1)} %all-to-all-done) | copy-start | bytes 589828
  30.1 25.2 %collective-permute-start.15 = (bf16[256,384]{1,0:T(8,128)(2,1)S(1)}, bf16[256,384]{1,0:T(8,128)(2,1)}, u32[]{:S(2)}, u32[]{:S(2)}) collective-permute-start(bf16[256,384]{1,0:T(8,128)(2,1)S(1)} %bitcast.105), channel_id=1, source_target_pairs={{0,8},{8,16},{16,24},{24,32},{32,40},{40,48},{48,56},{56,0},{1,9},... | collective-permute-start | bytes 589832 | tf_op jit(solution)/shard_map/ppermute | solution.py:50
  33.4 56.5 %copy-start.7 = (bf16[256,1024]{1,0:T(8,128)(2,1)}, bf16[256,1024]{1,0:T(8,128)(2,1)S(1)}, u32[]{:S(2)}) copy-start(bf16[256,1024]{1,0:T(8,128)(2,1)S(1)} %collective-permute-done.2.refs_4_.refs_12_) | copy-start | bytes 1572868
  33.4 27.6 %collective-permute-start.5 = (bf16[128,1024]{1,0:T(8,128)(2,1)S(1)}, bf16[128,1024]{1,0:T(8,128)(2,1)S(1)}, u32[]{:S(2)}, u32[]{:S(2)}) collective-permute-start(bf16[128,1024]{1,0:T(8,128)(2,1)S(1)} %slice.144), channel_id=1, source_target_pairs={{0,6},{2,0},{4,2},{6,4},{1,7},{3,1},{5,3},{7,5},{8,14},{10,8},{12,... | collective-permute-start | bytes 786440 | tf_op jit(solution)/shard_map/ppermute | solution.py:50
  38.5 26.0 %collective-permute-start.19 = (bf16[256,384]{1,0:T(8,128)(2,1)S(1)}, bf16[256,384]{1,0:T(8,128)(2,1)}, u32[]{:S(2)}, u32[]{:S(2)}) collective-permute-start(bf16[256,384]{1,0:T(8,128)(2,1)S(1)} %bitcast.106), channel_id=1, source_target_pairs={{0,56},{8,0},{16,8},{24,16},{32,24},{40,32},{48,40},{56,48},{1,57}... | collective-permute-start | bytes 589832 | tf_op jit(solution)/shard_map/ppermute | solution.py:50
  43.1 36.6 %all-to-all-start.1 = ((bf16[8,32,640]{2,1,0:T(8,128)(2,1)}), bf16[8,32,640]{2,1,0:T(8,128)(2,1)S(1)}, u32[]{:S(2)}, u32[]{:S(2)}) async-start(bf16[8,32,640]{2,1,0:T(8,128)(2,1)} %broadcast_in_dim.67), calls=%async_computation.1 | async-start | bytes 655360 | tf_op jit(solution)/shard_map/all_to_all | solution.py:21
  49.4 38.5 %collective-permute-start.3 = (bf16[256,1024]{1,0:T(8,128)(2,1)S(1)}, bf16[256,1024]{1,0:T(8,128)(2,1)}, u32[]{:S(2)}, u32[]{:S(2)}) collective-permute-start(bf16[256,1024]{1,0:T(8,128)(2,1)S(1)} %collective-permute-done.2.refs_4_.refs_12_), channel_id=1, source_target_pairs={{0,1},{1,0},{2,3},{3,2},{4,5},{5,4},{6,7},{7,6},{8,9},{9,8},{10,11... | collective-permute-start | bytes 1572872 | tf_op jit(solution)/shard_map/ppermute | solution.py:29
  55.4 34.5 %collective-permute-start.1 = (bf16[256,1024]{1,0:T(8,128)(2,1)S(1)}, bf16[256,1024]{1,0:T(8,128)(2,1)}, u32[]{:S(2)}, u32[]{:S(2)}) collective-permute-start(bf16[256,1024]{1,0:T(8,128)(2,1)S(1)} %collective-permute-done.refs_2_.refs_10_), channel_id=1, source_target_pairs={{0,1},{1,0},{2,3},{3,2},{4,5},{5,4},{6,7},{7,6},{8,9},{9,8},{10,11... | collective-permute-start | bytes 1572872 | tf_op jit(solution)/shard_map/ppermute | solution.py:29
  57.3 10.7 %collective-permute-start.16 = (bf16[256,384]{1,0:T(8,128)(2,1)}, bf16[256,384]{1,0:T(8,128)(2,1)S(1)}, u32[]{:S(2)}, u32[]{:S(2)}) collective-permute-start(bf16[256,384]{1,0:T(8,128)(2,1)} %collective-permute-done.15.refs_1_), channel_id=1, source_target_pairs={{0,8},{8,16},{16,24},{24,32},{32,40},{40,48},{48,56},{56,0},{1,9},... | collective-permute-start | bytes 589832 | tf_op jit(solution)/shard_map/ppermute | solution.py:50
  61.1 28.9 %copy-start.9 = (bf16[256,1024]{1,0:T(8,128)(2,1)}, bf16[256,1024]{1,0:T(8,128)(2,1)S(1)}, u32[]{:S(2)}) copy-start(bf16[256,1024]{1,0:T(8,128)(2,1)S(1)} %constant_dynamic-update-slice_fusion.refs_6_.refs_14_) | copy-start | bytes 1572868
  61.1 28.8 %collective-permute-start.6 = (bf16[256,1024]{1,0:T(8,128)(2,1)S(1)}, bf16[256,1024]{1,0:T(8,128)(2,1)S(1)}, u32[]{:S(2)}, u32[]{:S(2)}) collective-permute-start(bf16[256,1024]{1,0:T(8,128)(2,1)S(1)} %constant_dynamic-update-slice_fusion.refs_6_.refs_14_), channel_id=1, source_target_pairs={{0,1},{1,0},{2,3},{3,2},{4,5},{5,4},{6,7},{7,6},{8,9},{9,8},{10,11... | collective-permute-start | bytes 1572872 | tf_op jit(solution)/shard_map/ppermute | solution.py:29
  64.5 8.5 %collective-permute-start.20 = (bf16[256,384]{1,0:T(8,128)(2,1)}, bf16[256,384]{1,0:T(8,128)(2,1)S(1)}, u32[]{:S(2)}, u32[]{:S(2)}) collective-permute-start(bf16[256,384]{1,0:T(8,128)(2,1)} %collective-permute-done.19.refs_5_), channel_id=1, source_target_pairs={{0,56},{8,0},{16,8},{24,16},{32,24},{40,32},{48,40},{56,48},{1,57}... | collective-permute-start | bytes 589832 | tf_op jit(solution)/shard_map/ppermute | solution.py:50
  68.0 21.9 %copy-start.25 = (bf16[256,384]{1,0:T(8,128)(2,1)}, bf16[256,384]{1,0:T(8,128)(2,1)S(1)}, u32[]{:S(2)}) copy-start(bf16[256,384]{1,0:T(8,128)(2,1)S(1)} %collective-permute-done.16.refs_2_) | copy-start | bytes 589828
  68.0 9.1 %collective-permute-start.17 = (bf16[256,384]{1,0:T(8,128)(2,1)S(1)}, bf16[256,384]{1,0:T(8,128)(2,1)S(1)}, u32[]{:S(2)}, u32[]{:S(2)}) collective-permute-start(bf16[256,384]{1,0:T(8,128)(2,1)S(1)} %collective-permute-done.16.refs_2_), channel_id=1, source_target_pairs={{0,8},{8,16},{16,24},{24,32},{32,40},{40,48},{48,56},{56,0},{1,9},... | collective-permute-start | bytes 589832 | tf_op jit(solution)/shard_map/ppermute | solution.py:50
  73.1 16.9 %copy-start.26 = (bf16[256,384]{1,0:T(8,128)(2,1)}, bf16[256,384]{1,0:T(8,128)(2,1)S(1)}, u32[]{:S(2)}) copy-start(bf16[256,384]{1,0:T(8,128)(2,1)S(1)} %collective-permute-done.20.refs_6_) | copy-start | bytes 589828
  73.1 7.6 %collective-permute-start.21 = (bf16[256,384]{1,0:T(8,128)(2,1)S(1)}, bf16[256,384]{1,0:T(8,128)(2,1)}, u32[]{:S(2)}, u32[]{:S(2)}) collective-permute-start(bf16[256,384]{1,0:T(8,128)(2,1)S(1)} %collective-permute-done.20.refs_6_), channel_id=1, source_target_pairs={{0,56},{8,0},{16,8},{24,16},{32,24},{40,32},{48,40},{56,48},{1,57}... | collective-permute-start | bytes 589832 | tf_op jit(solution)/shard_map/ppermute | solution.py:50
  77.2 12.8 %copy-start.27 = (bf16[256,384]{1,0:T(8,128)(2,1)}, bf16[256,384]{1,0:T(8,128)(2,1)S(1)}, u32[]{:S(2)}) copy-start(bf16[256,384]{1,0:T(8,128)(2,1)S(1)} %collective-permute-done.17.refs_3_) | copy-start | bytes 589828
  77.2 12.7 %collective-permute-start.18 = (bf16[256,384]{1,0:T(8,128)(2,1)S(1)}, bf16[256,384]{1,0:T(8,128)(2,1)}, u32[]{:S(2)}, u32[]{:S(2)}) collective-permute-start(bf16[256,384]{1,0:T(8,128)(2,1)S(1)} %collective-permute-done.17.refs_3_), channel_id=1, source_target_pairs={{0,8},{8,16},{16,24},{24,32},{32,40},{40,48},{48,56},{56,0},{1,9},... | collective-permute-start | bytes 589832 | tf_op jit(solution)/shard_map/ppermute | solution.py:50
  79.7 17.9 %copy-start.3 = (bf16[8,32,640]{2,1,0:T(8,128)(2,1)}, bf16[8,32,640]{2,1,0:T(8,128)(2,1)S(1)}, u32[]{:S(2)}) copy-start(bf16[8,32,640]{2,1,0:T(8,128)(2,1)S(1)} %all-to-all-done.1) | copy-start | bytes 983044
  80.7 36.6 %collective-permute-start.11 = (bf16[256,640]{1,0:T(8,128)(2,1)S(1)}, bf16[256,640]{1,0:T(8,128)(2,1)}, u32[]{:S(2)}, u32[]{:S(2)}) collective-permute-start(bf16[256,640]{1,0:T(8,128)(2,1)S(1)} %bitcast.101), channel_id=1, source_target_pairs={{0,448},{64,0},{128,64},{192,128},{256,192},{320,256},{384,320},{4... | collective-permute-start | bytes 983048 | tf_op jit(solution)/shard_map/ppermute | solution.py:50
  87.9 33.8 %collective-permute-start.7 = (bf16[256,640]{1,0:T(8,128)(2,1)S(1)}, bf16[256,640]{1,0:T(8,128)(2,1)}, u32[]{:S(2)}, u32[]{:S(2)}) collective-permute-start(bf16[256,640]{1,0:T(8,128)(2,1)S(1)} %bitcast.102), channel_id=1, source_target_pairs={{0,64},{64,128},{128,192},{192,256},{256,320},{320,384},{384,448},... | collective-permute-start | bytes 983048 | tf_op jit(solution)/shard_map/ppermute | solution.py:50
  89.9 0.8 copy-start.19
  105.2 33.0 %all-to-all-start.2 = ((bf16[64,16,128]{2,1,0:T(8,128)(2,1)}), bf16[64,16,128]{2,1,0:T(8,128)(2,1)S(1)}, u32[]{:S(2)}, u32[]{:S(2)}) async-start(bf16[64,16,128]{2,1,0:T(8,128)(2,1)} %copy.83), calls=%async_computation.2 | async-start | bytes 524288 | tf_op jit(solution)/shard_map/all_to_all | solution.py:25
  117.3 15.3 %collective-permute-start.12 = (bf16[256,640]{1,0:T(8,128)(2,1)}, bf16[256,640]{1,0:T(8,128)(2,1)S(1)}, u32[]{:S(2)}, u32[]{:S(2)}) collective-permute-start(bf16[256,640]{1,0:T(8,128)(2,1)} %collective-permute-done.11.refs_5_), channel_id=1, source_target_pairs={{0,448},{64,0},{128,64},{192,128},{256,192},{320,256},{384,320},{4... | collective-permute-start | bytes 983048 | tf_op jit(solution)/shard_map/ppermute | solution.py:50
  121.7 14.5 %collective-permute-start.8 = (bf16[256,640]{1,0:T(8,128)(2,1)}, bf16[256,640]{1,0:T(8,128)(2,1)S(1)}, u32[]{:S(2)}, u32[]{:S(2)}) collective-permute-start(bf16[256,640]{1,0:T(8,128)(2,1)} %collective-permute-done.7.refs_1_), channel_id=1, source_target_pairs={{0,64},{64,128},{128,192},{192,256},{256,320},{320,384},{384,448},... | collective-permute-start | bytes 983048 | tf_op jit(solution)/shard_map/ppermute | solution.py:50
  132.6 28.5 %copy-start.20 = (bf16[256,640]{1,0:T(8,128)(2,1)}, bf16[256,640]{1,0:T(8,128)(2,1)S(1)}, u32[]{:S(2)}) copy-start(bf16[256,640]{1,0:T(8,128)(2,1)S(1)} %collective-permute-done.12.refs_6_) | copy-start | bytes 983044
  132.6 28.5 %collective-permute-start.13 = (bf16[256,640]{1,0:T(8,128)(2,1)S(1)}, bf16[256,640]{1,0:T(8,128)(2,1)S(1)}, u32[]{:S(2)}, u32[]{:S(2)}) collective-permute-start(bf16[256,640]{1,0:T(8,128)(2,1)S(1)} %collective-permute-done.12.refs_6_), channel_id=1, source_target_pairs={{0,448},{64,0},{128,64},{192,128},{256,192},{320,256},{384,320},{4... | collective-permute-start | bytes 983048 | tf_op jit(solution)/shard_map/ppermute | solution.py:50
  136.2 24.9 %copy-start.21 = (bf16[256,640]{1,0:T(8,128)(2,1)}, bf16[256,640]{1,0:T(8,128)(2,1)S(1)}, u32[]{:S(2)}) copy-start(bf16[256,640]{1,0:T(8,128)(2,1)S(1)} %collective-permute-done.8.refs_2_) | copy-start | bytes 983044
  136.2 10.4 %collective-permute-start.9 = (bf16[256,640]{1,0:T(8,128)(2,1)S(1)}, bf16[256,640]{1,0:T(8,128)(2,1)S(1)}, u32[]{:S(2)}, u32[]{:S(2)}) collective-permute-start(bf16[256,640]{1,0:T(8,128)(2,1)S(1)} %collective-permute-done.8.refs_2_), channel_id=1, source_target_pairs={{0,64},{64,128},{128,192},{192,256},{256,320},{320,384},{384,448},... | collective-permute-start | bytes 983048 | tf_op jit(solution)/shard_map/ppermute | solution.py:50
  146.6 14.5 %copy-start.23 = (bf16[256,640]{1,0:T(8,128)(2,1)}, bf16[256,640]{1,0:T(8,128)(2,1)S(1)}, u32[]{:S(2)}) copy-start(bf16[256,640]{1,0:T(8,128)(2,1)S(1)} %collective-permute-done.9.refs_3_) | copy-start | bytes 983044
  146.6 14.4 %collective-permute-start.10 = (bf16[256,640]{1,0:T(8,128)(2,1)S(1)}, bf16[256,640]{1,0:T(8,128)(2,1)S(1)}, u32[]{:S(2)}, u32[]{:S(2)}) collective-permute-start(bf16[256,640]{1,0:T(8,128)(2,1)S(1)} %collective-permute-done.9.refs_3_), channel_id=1, source_target_pairs={{0,64},{64,128},{128,192},{192,256},{256,320},{320,384},{384,448},... | collective-permute-start | bytes 983048 | tf_op jit(solution)/shard_map/ppermute | solution.py:50
  149.8 23.3 %all-to-all-start.3 = ((bf16[64,8,128]{2,1,0:T(8,128)(2,1)}), bf16[64,8,128]{2,1,0:T(8,128)(2,1)S(1)}, u32[]{:S(2)}, u32[]{:S(2)}) async-start(bf16[64,8,128]{2,1,0:T(8,128)(2,1)} %reshape.384), calls=%async_computation.3 | async-start | bytes 262144 | tf_op jit(solution)/shard_map/all_to_all | solution.py:25
  161.1 0.8 copy-start.22
  161.8 0.7 copy-start.24
  165.9 24.2 %collective-permute-start.26 = (bf16[2048,256]{1,0:T(8,128)(2,1)}, bf16[2048,256]{1,0:T(8,128)(2,1)S(1)}, u32[]{:S(2)}, u32[]{:S(2)}) collective-permute-start(bf16[2048,256]{1,0:T(8,128)(2,1)} %get-tuple-element.16.refs_4_), channel_id=1, source_target_pairs={{0,6},{2,0},{4,2},{6,4},{1,7},{3,1},{5,3},{7,5},{8,14},{10,8},{12,... | collective-permute-start | bytes 3145736 | tf_op jit(solution)/shard_map/ppermute | solution.py:50
  167.8 25.7 %collective-permute-start.25 = (bf16[2048,256]{1,0:T(8,128)(2,1)}, bf16[2048,256]{1,0:T(8,128)(2,1)S(1)}, u32[]{:S(2)}, u32[]{:S(2)}) collective-permute-start(bf16[2048,256]{1,0:T(8,128)(2,1)} %get-tuple-element.16.refs_4_), channel_id=1, source_target_pairs={{0,2},{2,4},{4,6},{6,0},{1,3},{3,5},{5,7},{7,1},{8,10},{10,12},{12... | collective-permute-start | bytes 3145736 | tf_op jit(solution)/shard_map/ppermute | solution.py:50
  181.7 14.1 %collective-permute-start.14 = (bf16[4,2,128]{2,1,0:T(2,128)(2,1)S(1)}, bf16[4,2,128]{2,1,0:T(2,128)(2,1)S(1)}, u32[]{:S(2)}, u32[]{:S(2)}) collective-permute-start(bf16[4,2,128]{2,1,0:T(2,128)(2,1)S(1)} %slice.148), channel_id=1, source_target_pairs={{0,8},{8,16},{16,24},{24,32},{32,40},{40,48},{48,56},{56,64},{64,7... | collective-permute-start | bytes 6152 | tf_op jit(solution)/shard_map/ppermute | solution.py:34
  190.1 5.7 %copy-start.4 = (bf16[2048,256]{1,0:T(8,128)(2,1)}, bf16[2048,256]{1,0:T(8,128)(2,1)S(1)}, u32[]{:S(2)}) copy-start(bf16[2048,256]{1,0:T(8,128)(2,1)S(1)} %collective-permute-done.26.refs_6_) | copy-start | bytes 3145732
  190.2 17.2 %collective-permute-start.28 = (bf16[1024,256]{1,0:T(8,128)(2,1)S(1)}, bf16[1024,256]{1,0:T(8,128)(2,1)S(1)}, u32[]{:S(2)}, u32[]{:S(2)}) collective-permute-start(bf16[1024,256]{1,0:T(8,128)(2,1)S(1)} %slice.168), channel_id=1, source_target_pairs={{0,6},{2,0},{4,2},{6,4},{1,7},{3,1},{5,3},{7,5},{8,14},{10,8},{12,... | collective-permute-start | bytes 1572872 | tf_op jit(solution)/shard_map/ppermute | solution.py:50
  193.6 3.4 %copy-start.5 = (bf16[2048,256]{1,0:T(8,128)(2,1)}, bf16[2048,256]{1,0:T(8,128)(2,1)S(1)}, u32[]{:S(2)}) copy-start(bf16[2048,256]{1,0:T(8,128)(2,1)S(1)} %collective-permute-done.25.refs_5_) | copy-start | bytes 3145732
  193.6 14.3 %collective-permute-start.27 = (bf16[1024,256]{1,0:T(8,128)(2,1)S(1)}, bf16[1024,256]{1,0:T(8,128)(2,1)S(1)}, u32[]{:S(2)}, u32[]{:S(2)}) collective-permute-start(bf16[1024,256]{1,0:T(8,128)(2,1)S(1)} %slice.167), channel_id=1, source_target_pairs={{0,2},{2,4},{4,6},{6,0},{1,3},{3,5},{5,7},{7,1},{8,10},{10,12},{12... | collective-permute-start | bytes 1572872 | tf_op jit(solution)/shard_map/ppermute | solution.py:50
  197.8 11.2 %collective-permute-start.24 = (bf16[256,256]{1,0:T(8,128)(2,1)S(1)}, bf16[256,256]{1,0:T(8,128)(2,1)S(1)}, u32[]{:S(2)}, u32[]{:S(2)}) collective-permute-start(bf16[256,256]{1,0:T(8,128)(2,1)S(1)} %get-tuple-element.21), channel_id=1, source_target_pairs={{0,4},{2,6},{4,0},{6,2},{1,5},{3,7},{5,1},{7,3},{8,12},{10,14},{12... | collective-permute-start | bytes 393224 | tf_op jit(solution)/shard_map/ppermute | solution.py:50
  200.9 10.1 %collective-permute-start.22 = (bf16[256,256]{1,0:T(8,128)(2,1)S(1)}, bf16[256,256]{1,0:T(8,128)(2,1)S(1)}, u32[]{:S(2)}, u32[]{:S(2)}) collective-permute-start(bf16[256,256]{1,0:T(8,128)(2,1)S(1)} %get-tuple-element.23), channel_id=1, source_target_pairs={{0,2},{2,4},{4,6},{6,0},{1,3},{3,5},{5,7},{7,1},{8,10},{10,12},{12... | collective-permute-start | bytes 393224 | tf_op jit(solution)/shard_map/ppermute | solution.py:50
  204.8 6.3 %collective-permute-start.23 = (bf16[256,256]{1,0:T(8,128)(2,1)S(1)}, bf16[256,256]{1,0:T(8,128)(2,1)S(1)}, u32[]{:S(2)}, u32[]{:S(2)}) collective-permute-start(bf16[256,256]{1,0:T(8,128)(2,1)S(1)} %get-tuple-element.24), channel_id=1, source_target_pairs={{0,6},{2,0},{4,2},{6,4},{1,7},{3,1},{5,3},{7,5},{8,14},{10,8},{12,... | collective-permute-start | bytes 393224 | tf_op jit(solution)/shard_map/ppermute | solution.py:50
  209.0 2.2 copy-start.28
  211.0 0.6 copy-start.29
  211.1 0.6 copy-start.30

commit v3 on v2

--- a/solution.py
+++ b/solution.py
@@ -51,56 +51,38 @@
 
 
 def around(array, axis):
-    behind = ring(array, axis, 1)
-    ahead = ring(array, axis, -1)
-    cut = array.shape[0] // 2
-    far = jnp.concatenate(
-        [ring(behind[:cut], axis, 1), ring(ahead[cut:], axis, -1)], axis=0
-    )
-    return behind, ahead, far
-
-
-def returned(blocks, axis):
-    own, behind, ahead, far = blocks
-    return own, ring(ahead, axis, 1), ring(behind, axis, -1), ring(far, axis, 2)
-
-
-def ring_gather(array, axis):
-    behind, ahead = [array], [array]
-    for k in range(4):
-        behind.append(ring(behind[-1], axis, 1))
-        if k < 3:
-            ahead.append(ring(ahead[-1], axis, -1))
-    return behind + ahead[1:]
-
-
-OFFSETS = (0, 7, 6, 5, 4, 1, 2, 3)
-
-
-def matmuls(core, pieces, weights, out):
+    return ring(array, axis, -1), ring(array, axis, 2), ring(array, axis, 1)
+
+
+def rolled(array, by):
+    size = array.shape[0]
+    twice = jnp.concatenate([array, array], axis=0)
+    return lax.dynamic_slice_in_dim(twice, (size - by) % size, size, 0)
+
+
+def matmuls(core, pieces, weights, left, out):
     half = pieces[0].shape[1]
     first = pl.multiple_of(core * half, half)
     second = pl.multiple_of((1 - core) * half, half)
+    right = left + out.shape[2]
     for k in range(4):
         mixed = jnp.dot(
-            pieces[2 * k][...], weights[pl.ds(first, half), :], preferred_element_type=F32
+            pieces[2 * k][...],
+            weights[pl.ds(first, half), left:right],
+            preferred_element_type=F32,
         )
         mixed += jnp.dot(
-            pieces[2 * k + 1][...], weights[pl.ds(second, half), :], preferred_element_type=F32
+            pieces[2 * k + 1][...],
+            weights[pl.ds(second, half), left:right],
+            preferred_element_type=F32,
         )
         out[k] = mixed.astype(BF16)
 
 
 def project_mem_kernel(spot, *refs):
-    parts, pieces, gate_rows = refs[:8], refs[8:16], refs[16]
-    out, gates, weights = refs[17:]
+    pieces, weights, gate_rows, out, gates = refs[:8], refs[8], refs[9], refs[10], refs[11]
     core = spot[0]
-    for part, offset in zip(parts, OFFSETS):
-        place = (spot[2] + offset) % 8
-        for k in range(8):
-            start = pl.multiple_of((k * 8 + place) * 32, 32)
-            weights[pl.ds(start, 32), :] = part[pl.ds(k * 32, 32), :]
-    matmuls(core, pieces, weights, out)
+    matmuls(core, pieces, weights, 0, out)
     dims = (((1,), (1,)), ((), ()))
     for k in range(4):
         rows = dot(gate_rows[core], pieces[2 * k][...], dims)
@@ -108,24 +90,15 @@
 
 
 def project_conv_kernel(spot, *refs):
-    matmuls(spot[0], refs[:8], refs[8], refs[9])
-
-
-def arrange_kernel(spot, *refs):
-    parts, left, right = refs[:8], refs[8], refs[9]
-    wide, size = left.shape[1], parts[0].shape[0]
-    for part, offset in zip(parts, OFFSETS):
-        start = pl.multiple_of(((spot[1] + offset) % 8) * size, size)
-        left[pl.ds(start, size), :] = part[:, :wide]
-        right[pl.ds(start, size), :] = part[:, wide:]
-
-
-def output_kernel(*refs):
-    parts, weights, out = refs[:4], refs[4:8], refs[8]
+    matmuls(spot[0], refs[:8], refs[8], refs[9].shape[2], refs[9])
+
+
+def output_kernel(parts, weights, out):
     dims = (((1,), (1,)), ((), ()))
-    mixed = dot(parts[0][...], weights[0][...], dims)
-    for part, weight in zip(parts[1:], weights[1:]):
-        mixed += dot(part[...], weight[...], dims)
+    wide = parts.shape[2]
+    mixed = dot(parts[0], weights[:, :wide], dims)
+    for k in range(1, parts.shape[0]):
+        mixed += dot(parts[k], weights[:, k * wide : (k + 1) * wide], dims)
     out[...] = mixed.astype(BF16)
 
 
@@ -170,29 +143,15 @@
     seqs = lax.axis_size("fs")
 
     place_x = lax.axis_index("fs")
-    order = [(place_x + by) % seqs for by in (0, seqs - 1, 1, 2)]
-
-    spots = [lax.axis_index(name) for name in ("tp", "sp_0", "sp_1")]
-    spot = jnp.stack(spots).astype(jnp.int32)
-
-    w_mem = jnp.concatenate([w_query, w_key, w_value], axis=1)
-    w_rest = jnp.concatenate(
-        [w_conv_gate, w_conv_mult, w_conv_in, w_out_conv.T, w_out_mem.T], axis=1
+    order = [(place_x + by) % seqs for by in range(seqs)]
+
+    spot = core.reshape(1).astype(jnp.int32)
+
+    w_all = jnp.concatenate(
+        [w_query, w_key, w_value, w_conv_gate, w_conv_mult, w_conv_in], axis=1
     )
     channels = w_conv_gate.shape[1]
-    w_mem = everyone(w_mem, "sp_0").reshape(-1, w_mem.shape[1])
-    w_rest, w_mem = lax.optimization_barrier((w_rest, w_mem))
-    w_rest = everyone(w_rest, "sp_1").reshape(-1, w_rest.shape[1])
-    w_mem = ring_gather(w_mem, "sp_1")
-    w_rest = ring_gather(w_rest, "sp_0")
-    w_conv, w_own = call(
-        arrange_kernel,
-        [((width, 3 * channels), BF16), ((width, 2 * channels), BF16)],
-        spot,
-        w_rest,
-        10**9,
-    )
-    w_out = (w_own, *around(w_own, "fs"))
+    w_all = everyone(w_all, SP).reshape(width, -1)
 
     x = activations[0].astype(F32)
     normed = (
@@ -200,8 +159,15 @@
     ).astype(BF16)
     mine = lax.dynamic_slice_in_dim(normed, core * half, half, 1)
     pieces = [mine, lax.dynamic_slice_in_dim(normed, (1 - core) * half, half, 1)]
-    for piece in around(mine, "fs"):
-        pieces += [piece, other_core(piece)]
+    others = around(mine, "fs")
+    swapped = other_core(jnp.concatenate(others, axis=0))
+    for k, piece in enumerate(others):
+        pieces += [piece, swapped[k * tokens : (k + 1) * tokens]]
+
+    turned = jnp.concatenate([w_out_conv.T, w_out_mem.T], axis=1)
+    turned = jnp.stack([turned, *around(turned, "fs")])
+    turned = rolled(turned, place_x).transpose(1, 0, 2).reshape(turned.shape[1], -1)
+    w_out = lax.all_gather(turned, SP, axis=0, tiled=True)
 
     gate_rows = jnp.concatenate(
         [
@@ -215,9 +181,8 @@
         project_mem_kernel,
         [((seqs, tokens, 3 * HEAD_DIM), BF16), ((seqs, 16, tokens), F32)],
         spot,
-        [*w_mem, *pieces, gate_rows],
+        [*pieces, w_all, gate_rows],
         10**9 * 3,
-        [pltpu.VMEM((width, 3 * HEAD_DIM), BF16)],
     )
     query, key, value = (qkv[..., k * HEAD_DIM : (k + 1) * HEAD_DIM] for k in range(3))
     bias = lax.dynamic_slice_in_dim(gate_bias, head, 1, 1)
@@ -271,7 +236,7 @@
         project_conv_kernel,
         [((seqs, tokens, 3 * channels), BF16)],
         spot,
-        [*pieces, w_conv],
+        [*pieces, w_all],
         10**9 * 3,
     )
     gate, mult, inlet = (conv[..., k * channels : (k + 1) * channels] for k in range(3))
@@ -299,9 +264,11 @@
     cell = cell * lax.rsqrt(jnp.mean(cell * cell, axis=-1, keepdims=True) + EPSILON)
     gain = lax.dynamic_slice_in_dim(head_gain, head * HEAD_DIM, HEAD_DIM, 0)
     mem_out = (cell * gain).astype(BF16)
-    both = jnp.concatenate([conv_out, mem_out], axis=-1)
-    parts = returned([both[k] for k in range(seqs)], "fs")
-    (output,) = call(output_kernel, [((tokens, width), BF16)], None, [*parts, *w_out], 10**9 * 2)
+    both = rolled(jnp.concatenate([conv_out, mem_out], axis=-1), place_x)
+    both = exchanged(both, "fs")
+    (output,) = call(
+        output_kernel, [((tokens, width), BF16)], None, [both, w_out], 10**9 * 2
+    )
 
     cores = lax.axis_size("tp")
     parts = exchanged(output.reshape(cores, tokens // cores, width), "tp")

time: 230 us -> 231 us (level)
  starting transfers between devices: 131 us -> 75.3 us
  waiting for transfers between devices: 34.2 us -> 69.4 us
  between operations: 1.12 us -> 14 us
  blocking collectives: 10.9 us -> 22.1 us
  local copies, waits for them, and re-layouts: 11.9 us -> 16.5 us
  other arithmetic: 13.8 us -> 11.1 us
  Pallas kernels: 20.9 us -> 18.2 us
    ppermute x25 -> x6, starting transfers between devices: 78.2 us -> 19 us  [ring(): lax.ppermute(array, axis, [(i, (i + by) % peers) for i in range(peers)])]
    all_to_all x2 -> x1, waiting for transfers between devices: 5.31 us -> 31.3 us  [everyone(): return lax.all_to_all(copies, axis, split_axis=0, concat_axis=0, tiled=True)]
    all_to_all x2, waiting for transfers between devices: 0.01 us -> 23.8 us  [exchanged(): return lax.all_to_all(array, axis, split_axis=0, concat_axis=0, tiled=True)]
    ppermute x25 -> x6, waiting for transfers between devices: 28.8 us -> 14.3 us  [ring(): lax.ppermute(array, axis, [(i, (i + by) % peers) for i in range(peers)])]
    all_to_all x1 -> x2, blocking collectives: 10.9 us -> 22.1 us  [exchanged(): return lax.all_to_all(array, axis, split_axis=0, concat_axis=0, tiled=True)]
    all_to_all x2, starting transfers between devices: 22.5 us -> 29.7 us  [exchanged(): return lax.all_to_all(array, axis, split_axis=0, concat_axis=0, tiled=True)]
    ppermute x3 -> x1, starting transfers between devices: 10.6 us -> 4.26 us  [other_core(): return lax.ppermute(array, 'tp', [(0, 1), (1, 0)])]
    pallas_call x4 -> x3, Pallas kernels: 20.9 us -> 18.2 us  [call(): pl.pallas_call(kernel, out_shape=tuple((jax.ShapeDtypeStruct(shape, dtype...]
  transfers between devices with their start and end apart: 33 -> 12, of which waited for: 11 -> 6; matrix products, arithmetic and copies ran while one was open for 10% -> 10% of each run, Pallas kernels for 7% -> 6%
where the time goes in v3:
time: 231 us; the launch traced here: 230 us
  starting transfers between devices  75.3 us (33%)
  waiting for transfers between devices  69.4 us (30%)
  blocking collectives  22.1 us (10%)
  Pallas kernels  18.2 us (8%)
  local copies, waits for them, and re-layouts  16.5 us (7%)
  between operations  14 us (6%)
  other arithmetic  11.1 us (5%)
  matrix products  3.06 us (1%)
    all_to_all x1, waiting for transfers between devices, everyone(): return lax.all_to_all(copies, axis, split_axis=0, concat_axis=0, tiled=True)  31.3 us
    all_to_all x2, starting transfers between devices, exchanged(): return lax.all_to_all(array, axis, split_axis=0, concat_axis=0, tiled=True)  29.7 us
    all_to_all x2, waiting for transfers between devices, exchanged(): return lax.all_to_all(array, axis, split_axis=0, concat_axis=0, tiled=True)  23.8 us
    all_to_all x2, blocking collectives, exchanged(): return lax.all_to_all(array, axis, split_axis=0, concat_axis=0, tiled=True)  22.1 us
    ppermute x6, starting transfers between devices, ring(): lax.ppermute(array, axis, [(i, (i + by) % peers) for i in range(peers)])  19 us
    pallas_call x3, Pallas kernels, call(): pl.pallas_call(kernel, out_shape=tuple((jax.ShapeDtypeStruct(shape, dtype...  18.2 us
    all_to_all x1, starting transfers between devices, everyone(): return lax.all_to_all(copies, axis, split_axis=0, concat_axis=0, tiled=True)  17.5 us
    ppermute x6, waiting for transfers between devices, ring(): lax.ppermute(array, axis, [(i, (i + by) % peers) for i in range(peers)])  14.3 us
  transfers between devices with their start and end apart: 12, of which 6 were waited for; matrix products, arithmetic and copies ran while one was open for 10% of the time, Pallas kernels for 6%

profile of v3, /device:TPU:1, one launch (start us, length us, event | category | flops | bytes accessed | tf_op | source)
XLA Modules:
  0.0 229.7 jit_solution(15217399809640692898)
XLA Ops:
  6.5 0.7 constant_dynamic-update-slice_fusion.5
  7.2 0.7 constant_dynamic-update-slice_fusion.4
  8.0 0.7 constant_dynamic-update-slice_fusion.3
  8.7 0.7 constant_dynamic-update-slice_fusion.2
  9.4 0.7 constant_dynamic-update-slice_fusion.1
  10.1 0.7 constant_dynamic-update-slice_fusion
  10.8 2.1 broadcast_in_dim.40
  12.9 17.5 %all-to-all-start = ((bf16[64,32,768]{2,1,0:T(8,128)(2,1)}), bf16[64,32,768]{2,1,0:T(8,128)(2,1)}, u32[]{:S(2)}, u32[]{:S(2)}) async-start(bf16[64,32,768]{2,1,0:T(8,128)(2,1)} %broadcast_in_dim.40), calls=%async_computation | async-start | bytes 6291456 | tf_op jit(solution)/shard_map/all_to_all | solution.py:21
  30.4 0.3 fusion
  30.8 0.3 fusion.2
  31.1 0.9 constant_dynamic-slice_fusion.9
  32.0 4.4 %collective-permute-start = (bf16[256,1024]{1,0:T(8,128)(2,1)S(1)}, bf16[256,1024]{1,0:T(8,128)(2,1)S(1)}, u32[]{:S(2)}, u32[]{:S(2)}) collective-permute-start(bf16[256,1024]{1,0:T(8,128)(2,1)S(1)} %get-tuple-element.15.refs_0_), channel_id=1, source_target_pairs={{0,6},{2,0},{4,2},{6,4},{1,7},{3,1},{5,3},{7,5},{8,14},{10,8},{12,... | collective-permute-start | bytes 1572872 | tf_op jit(solution)/shard_map/ppermute | solution.py:50
  36.3 1.9 collective-permute-start.2
  38.3 3.6 %collective-permute-start.1 = (bf16[256,1024]{1,0:T(8,128)(2,1)S(1)}, bf16[256,1024]{1,0:T(8,128)(2,1)}, u32[]{:S(2)}, u32[]{:S(2)}) collective-permute-start(bf16[256,1024]{1,0:T(8,128)(2,1)S(1)} %get-tuple-element.15.refs_0_), channel_id=1, source_target_pairs={{0,4},{2,6},{4,0},{6,2},{1,5},{3,7},{5,1},{7,3},{8,12},{10,14},{12... | collective-permute-start | bytes 1572872 | tf_op jit(solution)/shard_map/ppermute | solution.py:50
  41.9 2.9 %collective-permute-start.5 = (bf16[32,256]{1,0:T(8,128)(2,1)S(1)}, bf16[32,256]{1,0:T(8,128)(2,1)S(1)}, u32[]{:S(2)}, u32[]{:S(2)}) collective-permute-start(bf16[32,256]{1,0:T(8,128)(2,1)S(1)} %pad_maximum_fusion.2), channel_id=1, source_target_pairs={{0,6},{2,0},{4,2},{6,4},{1,7},{3,1},{5,3},{7,5},{8,14},{10,8},{12,... | collective-permute-start | bytes 49160 | tf_op jit(solution)/shard_map/ppermute | solution.py:50
  44.8 4.3 %collective-permute-start.6 = (bf16[32,256]{1,0:T(8,128)(2,1)S(1)}, bf16[32,256]{1,0:T(8,128)(2,1)S(1)}, u32[]{:S(2)}, u32[]{:S(2)}) collective-permute-start(bf16[32,256]{1,0:T(8,128)(2,1)S(1)} %pad_maximum_fusion.2), channel_id=1, source_target_pairs={{0,4},{2,6},{4,0},{6,2},{1,5},{3,7},{5,1},{7,3},{8,12},{10,14},{12... | collective-permute-start | bytes 49160 | tf_op jit(solution)/shard_map/ppermute | solution.py:50
  49.1 9.0 %collective-permute-done.5 = bf16[32,256]{1,0:T(8,128)(2,1)S(1)} collective-permute-done((bf16[32,256]{1,0:T(8,128)(2,1)S(1)}, bf16[32,256]{1,0:T(8,128)(2,1)S(1)}, u32[]{:S(2)}, u32[]{:S(2)}) %collective-permute-start.5) | collective-permute-done | bytes 16416 | tf_op jit(solution)/shard_map/ppermute | solution.py:50
  58.1 1.9 collective-permute-start.7
  60.0 2.4 %collective-permute-done.6 = bf16[32,256]{1,0:T(8,128)(2,1)S(1)} collective-permute-done((bf16[32,256]{1,0:T(8,128)(2,1)S(1)}, bf16[32,256]{1,0:T(8,128)(2,1)S(1)}, u32[]{:S(2)}, u32[]{:S(2)}) %collective-permute-start.6) | collective-permute-done | bytes 16416 | tf_op jit(solution)/shard_map/ppermute | solution.py:50
  62.5 2.9 %collective-permute-done.7 = bf16[32,256]{1,0:T(8,128)(2,1)S(1)} collective-permute-done((bf16[32,256]{1,0:T(8,128)(2,1)S(1)}, bf16[32,256]{1,0:T(8,128)(2,1)S(1)}, u32[]{:S(2)}, u32[]{:S(2)}) %collective-permute-start.7) | collective-permute-done | bytes 16416 | tf_op jit(solution)/shard_map/ppermute | solution.py:50
  65.4 0.6 copy.108
  66.1 0.7 copy-done.3
  66.8 0.2 copy-done.4
  67.1 1.2 pad_maximum_fusion
  68.2 4.3 %collective-permute-start.3 = (bf16[768,1024]{1,0:T(8,128)(2,1)S(1)}, bf16[768,1024]{1,0:T(8,128)(2,1)S(1)}, u32[]{:S(2)}, u32[]{:S(2)}) collective-permute-start(bf16[768,1024]{1,0:T(8,128)(2,1)S(1)} %pad_maximum_fusion), channel_id=1, source_target_pairs={{0,1},{1,0},{2,3},{3,2},{4,5},{5,4},{6,7},{7,6},{8,9},{9,8},{10,11... | collective-permute-start | bytes 4718600 | tf_op jit(solution)/shard_map/ppermute | solution.py:29
  72.5 0.8 constant_dynamic-slice_fusion.6
  73.4 0.6 copy.125
  74.0 0.8 dynamic_slice.57
  74.9 0.8 constant_dynamic-slice_fusion.4
  75.6 0.6 fusion.52
  76.3 1.2 fusion.51
  77.5 31.3 %all-to-all-done = bf16[64,32,768]{2,1,0:T(8,128)(2,1)} async-done(((bf16[64,32,768]{2,1,0:T(8,128)(2,1)}), bf16[64,32,768]{2,1,0:T(8,128)(2,1)}, u32[]{:S(2)}, u32[]{:S(2)}) %all-to-all-start) | async-done | bytes 3145760 | tf_op jit(solution)/shard_map/all_to_all | solution.py:21
  108.7 6.4 %shard_map.154 = bf16[4,256,384]{2,1,0:T(8,128)(2,1)} custom-call(s32[1]{0:T(128)} %bitcast.spot, bf16[256,1024]{1,0:T(8,128)(2,1)} %copy-done.2, bf16[256,1024]{1,0:T(8,128)(2,1)} %get-tuple-element.14.refs_1_, bf16[256,1024]{1,0:T(8,128)(2,1)} %copy-done.3, bf16[256,1024]{1,0:T(8,128)(2,1)} %get-tuple-element.13.refs_3_, ...), custom_call_target="tpu_custom_call" | custom-call | flops 3000000000 | bytes 6291456 | tf_op jit(solution)/shard_map/pallas_call | solution.py:111
  115.1 1.1 multiply_convert_fusion.2
  116.3 4.8 %collective-permute-start.4 = (bf16[4,2,128]{2,1,0:T(2,128)(2,1)S(1)}, bf16[4,2,128]{2,1,0:T(2,128)(2,1)S(1)}, u32[]{:S(2)}, u32[]{:S(2)}) collective-permute-start(bf16[4,2,128]{2,1,0:T(2,128)(2,1)S(1)} %slice.129), channel_id=1, source_target_pairs={{0,8},{8,16},{16,24},{24,32},{32,40},{40,48},{48,56},{56,64},{64,7... | collective-permute-start | bytes 6152 | tf_op jit(solution)/shard_map/ppermute | solution.py:34
  121.1 7.2 %shard_map.155 = (bf16[4,256,384]{2,1,0:T(8,128)(2,1)}, f32[4,16,256]{2,1,0:T(8,128)}) custom-call(s32[1]{0:T(128)} %bitcast.spot, bf16[256,1024]{1,0:T(8,128)(2,1)} %copy-done.2, bf16[256,1024]{1,0:T(8,128)(2,1)} %get-tuple-element.14.refs_1_, bf16[256,1024]{1,0:T(8,128)(2,1)} %copy-done.3, bf16[256,1024]{1,0:T(8,128)(2,1)} %get-tuple-element.13.refs_3_, ...), custom_call_target="tpu_custom_call" | custom-call | flops 3000000000 | bytes 6291456 | tf_op jit(solution)/shard_map/pallas_call | solution.py:111
  128.3 1.5 add_negate_fusion
  129.8 1.2 reduce-window.6
  131.1 0.1 copy.83
  131.4 0.2 slice_reduce_fusion
  131.6 1.6 add_reduce_fusion
  133.5 1.5 convolution_convert_fusion
  135.1 0.9 copy.87
  136.0 23.9 %all-to-all-start.1 = ((bf16[64,16,128]{2,1,0:T(8,128)(2,1)}), bf16[64,16,128]{2,1,0:T(8,128)(2,1)S(1)}, u32[]{:S(2)}, u32[]{:S(2)}) async-start(bf16[64,16,128]{2,1,0:T(8,128)(2,1)} %copy.87), calls=%async_computation.1 | async-start | bytes 524288 | tf_op jit(solution)/shard_map/all_to_all | solution.py:25
  159.8 0.4 fusion.11
  160.3 1.2 fusion.17
  161.5 13.0 %all-to-all-done.1 = bf16[64,16,128]{2,1,0:T(8,128)(2,1)S(1)} async-done(((bf16[64,16,128]{2,1,0:T(8,128)(2,1)}), bf16[64,16,128]{2,1,0:T(8,128)(2,1)S(1)}, u32[]{:S(2)}, u32[]{:S(2)}) %all-to-all-start.1) | async-done | bytes 262176 | tf_op jit(solution)/shard_map/all_to_all | solution.py:25
  174.8 0.1 select_reduce_fusion
  174.9 0.3 fusion.53
  175.2 0.2 fusion.45
  175.4 0.2 fusion.6
  175.6 0.1 copy.92
  175.7 0.7 reshape.387
  176.4 5.9 %all-to-all-start.2 = ((bf16[64,8,128]{2,1,0:T(8,128)(2,1)}), bf16[64,8,128]{2,1,0:T(8,128)(2,1)S(1)}, u32[]{:S(2)}, u32[]{:S(2)}) async-start(bf16[64,8,128]{2,1,0:T(8,128)(2,1)} %reshape.387), calls=%async_computation.2 | async-start | bytes 262144 | tf_op jit(solution)/shard_map/all_to_all | solution.py:25
  182.4 0.6 fusion.4
  183.0 10.9 %all-to-all-done.2 = bf16[64,8,128]{2,1,0:T(8,128)(2,1)S(1)} async-done(((bf16[64,8,128]{2,1,0:T(8,128)(2,1)}), bf16[64,8,128]{2,1,0:T(8,128)(2,1)S(1)}, u32[]{:S(2)}, u32[]{:S(2)}) %all-to-all-start.2) | async-done | bytes 131104 | tf_op jit(solution)/shard_map/all_to_all | solution.py:25
  193.9 0.1 copy.94
  194.0 0.4 multiply_reduce_fusion
  194.4 0.2 multiply_convert_fusion
  194.7 0.3 fusion.13
  195.0 11.0 %all_to_all.25.parts = bf16[4,256,256]{2,1,0:T(8,128)(2,1)} all-to-all(bf16[4,256,256]{2,1,0:T(8,128)(2,1)S(1)} %fusion.13), channel_id=1, replica_groups=mesh['sp_0'=8,'sp_1'=8,'fs'=4,'tp'=2] {'fs'}, dimensions={0} | all-to-all | bytes 1048576 | tf_op jit(solution)/shard_map/all_to_all | solution.py:25
  206.1 4.6 %shard_map.156 = bf16[256,2048]{1,0:T(8,128)(2,1)} custom-call(bf16[4,256,256]{2,1,0:T(8,128)(2,1)} %all_to_all.25.parts, bf16[2048,1024]{1,0:T(8,128)(2,1)} %all-gather.2.cloned.1.call-done.weights), custom_call_target="tpu_custom_call" | custom-call | flops 2000000000 | bytes 6291456 | tf_op jit(solution)/shard_map/pallas_call | solution.py:111
  210.7 11.1 %all_to_all.26 = bf16[2,128,2048]{2,1,0:T(8,128)(2,1)S(1)} all-to-all(bf16[2,128,2048]{2,1,0:T(8,128)(2,1)} %bitcast.100), channel_id=1, replica_groups=mesh['sp_0'=8,'sp_1'=8,'fs'=4,'tp'=2] {'tp'}, dimensions={0} | all-to-all | bytes 2097152 | tf_op jit(solution)/shard_map/all_to_all | solution.py:25
  221.7 1.1 reduce_sum.42
  (74 shorter events, 1.4 us)
Async XLA Ops:
  6.5 68.3 %copy-start = (f32[3,1024]{1,0:T(4,128)S(1)}, f32[3,1024]{1,0:T(4,128)}, u32[]{:S(2)}) copy-start(f32[3,1024]{1,0:T(4,128)} %param.21) | copy-start | bytes 36868
  12.9 17.6 %copy-start.1 = (bf16[1,256,2048]{2,1,0:T(8,128)(2,1)S(1)}, bf16[1,256,2048]{2,1,0:T(8,128)(2,1)}, u32[]{:S(2)}) copy-start(bf16[1,256,2048]{2,1,0:T(8,128)(2,1)} %param.16) | copy-start | bytes 3145732
  12.9 17.9 %copy-start.8 = (f32[2048]{0:T(1024)S(1)}, f32[2048]{0:T(1024)}, u32[]{:S(2)}) copy-start(f32[2048]{0:T(1024)} %param.17) | copy-start | bytes 24580
  12.9 95.9 %all-to-all-start = ((bf16[64,32,768]{2,1,0:T(8,128)(2,1)}), bf16[64,32,768]{2,1,0:T(8,128)(2,1)}, u32[]{:S(2)}, u32[]{:S(2)}) async-start(bf16[64,32,768]{2,1,0:T(8,128)(2,1)} %broadcast_in_dim.40), calls=%async_computation | async-start | bytes 6291456 | tf_op jit(solution)/shard_map/all_to_all | solution.py:21
  30.4 175.7 %all-gather.2.cloned.1.call-start = ((), (), s32[]{:S(2)}) async-start(), calls=%async_computation.5 | async-start | bytes 4259840 | tf_op jit(solution)/shard_map/all_gather | solution.py:170
  30.7 11.2 %copy-start.6 = (bf16[128,32]{0,1:T(8,128)(2,1)S(1)}, bf16[128,32]{0,1:T(8,128)(2,1)}, u32[]{:S(2)}) copy-start(bf16[128,32]{0,1:T(8,128)(2,1)} %param.31) | copy-start | bytes 24580
  30.7 11.2 %copy-start.7 = (bf16[128,32]{0,1:T(8,128)(2,1)S(1)}, bf16[128,32]{0,1:T(8,128)(2,1)}, u32[]{:S(2)}) copy-start(bf16[128,32]{0,1:T(8,128)(2,1)} %param.30) | copy-start | bytes 24580
  32.0 34.1 %copy-start.2 = (bf16[256,1024]{1,0:T(8,128)(2,1)}, bf16[256,1024]{1,0:T(8,128)(2,1)S(1)}, u32[]{:S(2)}) copy-start(bf16[256,1024]{1,0:T(8,128)(2,1)S(1)} %get-tuple-element.15.refs_0_) | copy-start | bytes 1572868
  32.0 34.1 %collective-permute-start = (bf16[256,1024]{1,0:T(8,128)(2,1)S(1)}, bf16[256,1024]{1,0:T(8,128)(2,1)S(1)}, u32[]{:S(2)}, u32[]{:S(2)}) collective-permute-start(bf16[256,1024]{1,0:T(8,128)(2,1)S(1)} %get-tuple-element.15.refs_0_), channel_id=1, source_target_pairs={{0,6},{2,0},{4,2},{6,4},{1,7},{3,1},{5,3},{7,5},{8,14},{10,8},{12,... | collective-permute-start | bytes 1572872 | tf_op jit(solution)/shard_map/ppermute | solution.py:50
  36.3 29.7 %collective-permute-start.2 = (bf16[256,1024]{1,0:T(8,128)(2,1)S(1)}, bf16[256,1024]{1,0:T(8,128)(2,1)S(1)}, u32[]{:S(2)}, u32[]{:S(2)}) collective-permute-start(bf16[256,1024]{1,0:T(8,128)(2,1)S(1)} %get-tuple-element.15.refs_0_), channel_id=1, source_target_pairs={{0,2},{2,4},{4,6},{6,0},{1,3},{3,5},{5,7},{7,1},{8,10},{10,12},{12... | collective-permute-start | bytes 1572872 | tf_op jit(solution)/shard_map/ppermute | solution.py:50
  38.3 27.8 %collective-permute-start.1 = (bf16[256,1024]{1,0:T(8,128)(2,1)S(1)}, bf16[256,1024]{1,0:T(8,128)(2,1)}, u32[]{:S(2)}, u32[]{:S(2)}) collective-permute-start(bf16[256,1024]{1,0:T(8,128)(2,1)S(1)} %get-tuple-element.15.refs_0_), channel_id=1, source_target_pairs={{0,4},{2,6},{4,0},{6,2},{1,5},{3,7},{5,1},{7,3},{8,12},{10,14},{12... | collective-permute-start | bytes 1572872 | tf_op jit(solution)/shard_map/ppermute | solution.py:50
  41.9 16.2 %collective-permute-start.5 = (bf16[32,256]{1,0:T(8,128)(2,1)S(1)}, bf16[32,256]{1,0:T(8,128)(2,1)S(1)}, u32[]{:S(2)}, u32[]{:S(2)}) collective-permute-start(bf16[32,256]{1,0:T(8,128)(2,1)S(1)} %pad_maximum_fusion.2), channel_id=1, source_target_pairs={{0,6},{2,0},{4,2},{6,4},{1,7},{3,1},{5,3},{7,5},{8,14},{10,8},{12,... | collective-permute-start | bytes 49160 | tf_op jit(solution)/shard_map/ppermute | solution.py:50
  44.8 17.7 %collective-permute-start.6 = (bf16[32,256]{1,0:T(8,128)(2,1)S(1)}, bf16[32,256]{1,0:T(8,128)(2,1)S(1)}, u32[]{:S(2)}, u32[]{:S(2)}) collective-permute-start(bf16[32,256]{1,0:T(8,128)(2,1)S(1)} %pad_maximum_fusion.2), channel_id=1, source_target_pairs={{0,4},{2,6},{4,0},{6,2},{1,5},{3,7},{5,1},{7,3},{8,12},{10,14},{12... | collective-permute-start | bytes 49160 | tf_op jit(solution)/shard_map/ppermute | solution.py:50
  49.1 25.7 %copy-start.9 = (f32[2,8]{1,0:T(2,128)S(1)}, f32[2,8]{1,0:T(2,128)}, u32[]{:S(2)}) copy-start(f32[2,8]{1,0:T(2,128)} %param.27) | copy-start | bytes 196
  58.1 7.2 %collective-permute-start.7 = (bf16[32,256]{1,0:T(8,128)(2,1)S(1)}, bf16[32,256]{1,0:T(8,128)(2,1)S(1)}, u32[]{:S(2)}, u32[]{:S(2)}) collective-permute-start(bf16[32,256]{1,0:T(8,128)(2,1)S(1)} %pad_maximum_fusion.2), channel_id=1, source_target_pairs={{0,2},{2,4},{4,6},{6,0},{1,3},{3,5},{5,7},{7,1},{8,10},{10,12},{12... | collective-permute-start | bytes 49160 | tf_op jit(solution)/shard_map/ppermute | solution.py:50
  66.1 0.8 copy-start.3
  66.1 1.0 copy-start.4
  68.2 8.1 %collective-permute-start.3 = (bf16[768,1024]{1,0:T(8,128)(2,1)S(1)}, bf16[768,1024]{1,0:T(8,128)(2,1)S(1)}, u32[]{:S(2)}, u32[]{:S(2)}) collective-permute-start(bf16[768,1024]{1,0:T(8,128)(2,1)S(1)} %pad_maximum_fusion), channel_id=1, source_target_pairs={{0,1},{1,0},{2,3},{3,2},{4,5},{5,4},{6,7},{7,6},{8,9},{9,8},{10,11... | collective-permute-start | bytes 4718600 | tf_op jit(solution)/shard_map/ppermute | solution.py:29
  116.3 44.0 %collective-permute-start.4 = (bf16[4,2,128]{2,1,0:T(2,128)(2,1)S(1)}, bf16[4,2,128]{2,1,0:T(2,128)(2,1)S(1)}, u32[]{:S(2)}, u32[]{:S(2)}) collective-permute-start(bf16[4,2,128]{2,1,0:T(2,128)(2,1)S(1)} %slice.129), channel_id=1, source_target_pairs={{0,8},{8,16},{16,24},{24,32},{32,40},{40,48},{48,56},{56,64},{64,7... | collective-permute-start | bytes 6152 | tf_op jit(solution)/shard_map/ppermute | solution.py:34
  136.0 38.5 %all-to-all-start.1 = ((bf16[64,16,128]{2,1,0:T(8,128)(2,1)}), bf16[64,16,128]{2,1,0:T(8,128)(2,1)S(1)}, u32[]{:S(2)}, u32[]{:S(2)}) async-start(bf16[64,16,128]{2,1,0:T(8,128)(2,1)} %copy.87), calls=%async_computation.1 | async-start | bytes 524288 | tf_op jit(solution)/shard_map/all_to_all | solution.py:25
  160.3 22.1 %copy-start.5 = (bf16[4,256,384]{2,1,0:T(8,128)(2,1)S(1)}, bf16[4,256,384]{2,1,0:T(8,128)(2,1)}, u32[]{:S(2)}) copy-start(bf16[4,256,384]{2,1,0:T(8,128)(2,1)} %get-tuple-element.8) | copy-start | bytes 2359300
  176.4 17.4 %all-to-all-start.2 = ((bf16[64,8,128]{2,1,0:T(8,128)(2,1)}), bf16[64,8,128]{2,1,0:T(8,128)(2,1)S(1)}, u32[]{:S(2)}, u32[]{:S(2)}) async-start(bf16[64,8,128]{2,1,0:T(8,128)(2,1)} %reshape.387), calls=%async_computation.2 | async-start | bytes 262144 | tf_op jit(solution)/shard_map/all_to_all | solution.py:25
Sparse Core Ops, SparseCore 0:
  66.2 108.4 all-gather.1

commit v4 on v3

--- a/solution.py
+++ b/solution.py
@@ -52,6 +52,15 @@
 
 def around(array, axis):
     return ring(array, axis, -1), ring(array, axis, 2), ring(array, axis, 1)
+
+
+def relayed(array, axis):
+    cut = array.shape[0] // 2
+    ahead = ring(array, axis, -1)
+    behind = ring(array, axis, 1)
+    first = ring(behind[:cut], axis, 1)
+    second = ring(ahead[cut:], axis, -1)
+    return ahead, jnp.concatenate([first, second], axis=0), behind
 
 
 def rolled(array, by):
@@ -93,12 +102,12 @@
     matmuls(spot[0], refs[:8], refs[8], refs[9].shape[2], refs[9])
 
 
-def output_kernel(parts, weights, out):
+def output_kernel(spot, parts, *refs):
+    weights, out = refs[:4], refs[4]
     dims = (((1,), (1,)), ((), ()))
-    wide = parts.shape[2]
-    mixed = dot(parts[0], weights[:, :wide], dims)
-    for k in range(1, parts.shape[0]):
-        mixed += dot(parts[k], weights[:, k * wide : (k + 1) * wide], dims)
+    mixed = dot(parts[spot[1]], weights[0][...], dims)
+    for k in range(1, 4):
+        mixed += dot(parts[(spot[1] + k) % 4], weights[k][...], dims)
     out[...] = mixed.astype(BF16)
 
 
@@ -145,13 +154,25 @@
     place_x = lax.axis_index("fs")
     order = [(place_x + by) % seqs for by in range(seqs)]
 
-    spot = core.reshape(1).astype(jnp.int32)
+    spot = jnp.stack([core, place_x]).astype(jnp.int32)
 
     w_all = jnp.concatenate(
-        [w_query, w_key, w_value, w_conv_gate, w_conv_mult, w_conv_in], axis=1
+        [
+            w_query,
+            w_key,
+            w_value,
+            w_conv_gate,
+            w_conv_mult,
+            w_conv_in,
+            w_out_conv.T,
+            w_out_mem.T,
+        ],
+        axis=1,
     )
     channels = w_conv_gate.shape[1]
     w_all = everyone(w_all, SP).reshape(width, -1)
+    w_own = w_all[:, 6 * channels :]
+    w_out = (w_own, *relayed(w_own, "fs"))
 
     x = activations[0].astype(F32)
     normed = (
@@ -163,11 +184,6 @@
     swapped = other_core(jnp.concatenate(others, axis=0))
     for k, piece in enumerate(others):
         pieces += [piece, swapped[k * tokens : (k + 1) * tokens]]
-
-    turned = jnp.concatenate([w_out_conv.T, w_out_mem.T], axis=1)
-    turned = jnp.stack([turned, *around(turned, "fs")])
-    turned = rolled(turned, place_x).transpose(1, 0, 2).reshape(turned.shape[1], -1)
-    w_out = lax.all_gather(turned, SP, axis=0, tiled=True)
 
     gate_rows = jnp.concatenate(
         [
@@ -267,7 +283,7 @@
     both = rolled(jnp.concatenate([conv_out, mem_out], axis=-1), place_x)
     both = exchanged(both, "fs")
     (output,) = call(
-        output_kernel, [((tokens, width), BF16)], None, [both, w_out], 10**9 * 2
+        output_kernel, [((tokens, width), BF16)], spot, [both, *w_out], 10**9 * 2
     )
 
     cores = lax.axis_size("tp")

time: 231 us -> 271 us (1.17)
  waiting for transfers between devices: 69.4 us -> 110 us
  starting transfers between devices: 75.3 us -> 89 us
  between operations: 14 us -> 0.5 us
  blocking collectives: 22.1 us -> 11.4 us
  local copies, waits for them, and re-layouts: 16.5 us -> 21.5 us
    all_to_all x1, waiting for transfers between devices: 31.3 us -> 61 us  [everyone(): return lax.all_to_all(copies, axis, split_axis=0, concat_axis=0, tiled=True)]
    all_to_all x2 -> x1, blocking collectives: 22.1 us -> 11.4 us  [exchanged(): return lax.all_to_all(array, axis, split_axis=0, concat_axis=0, tiled=True)]
    ppermute x6 -> x7, waiting for transfers between devices: 14.3 us -> 24.1 us  [ring(): lax.ppermute(array, axis, [(i, (i + by) % peers) for i in range(peers)])]
    ppermute x1, starting transfers between devices: 4.81 us -> 11 us  [from_behind(): return lax.ppermute(array, axis, [(i, i + 1) for i in range(peers - 1)])]
    ppermute x6 -> x7, starting transfers between devices: 19 us -> 22.9 us  [ring(): lax.ppermute(array, axis, [(i, (i + by) % peers) for i in range(peers)])]
    all_to_all x2 -> x3, starting transfers between devices: 29.7 us -> 32.7 us  [exchanged(): return lax.all_to_all(array, axis, split_axis=0, concat_axis=0, tiled=True)]
    unnamed x34 -> x32, local copies, waits for them, and re-layouts: 4.63 us -> 7.46 us
    all_to_all x2 -> x3, waiting for transfers between devices: 23.8 us -> 25.2 us  [exchanged(): return lax.all_to_all(array, axis, split_axis=0, concat_axis=0, tiled=True)]
  transfers between devices with their start and end apart: 12 -> 13, of which waited for: 6 -> 8; matrix products, arithmetic and copies ran while one was open for 10% -> 8% of each run, Pallas kernels for 6% -> 2%
where the time goes in v4:
time: 271 us; the launch traced here: 269 us
  waiting for transfers between devices  110 us (41%)
  starting transfers between devices  89 us (33%)
  local copies, waits for them, and re-layouts  21.5 us (8%)
  Pallas kernels  18.8 us (7%)
  other arithmetic  12.4 us (5%)
  blocking collectives  11.4 us (4%)
  matrix products  5.12 us (2%)
    all_to_all x1, waiting for transfers between devices, everyone(): return lax.all_to_all(copies, axis, split_axis=0, concat_axis=0, tiled=True)  61 us
    all_to_all x3, starting transfers between devices, exchanged(): return lax.all_to_all(array, axis, split_axis=0, concat_axis=0, tiled=True)  32.7 us
    all_to_all x3, waiting for transfers between devices, exchanged(): return lax.all_to_all(array, axis, split_axis=0, concat_axis=0, tiled=True)  25.2 us
    ppermute x7, waiting for transfers between devices, ring(): lax.ppermute(array, axis, [(i, (i + by) % peers) for i in range(peers)])  24.1 us
    ppermute x7, starting transfers between devices, ring(): lax.ppermute(array, axis, [(i, (i + by) % peers) for i in range(peers)])  22.9 us
    pallas_call x3, Pallas kernels, call(): pl.pallas_call(kernel, out_shape=tuple((jax.ShapeDtypeStruct(shape, dtype...  18.8 us
    all_to_all x1, starting transfers between devices, everyone(): return lax.all_to_all(copies, axis, split_axis=0, concat_axis=0, tiled=True)  17.5 us
    all_to_all x1, blocking collectives, exchanged(): return lax.all_to_all(array, axis, split_axis=0, concat_axis=0, tiled=True)  11.4 us
  transfers between devices with their start and end apart: 13, of which 8 were waited for; matrix products, arithmetic and copies ran while one was open for 8% of the time, Pallas kernels for 2%

profile of v4, /device:TPU:1, one launch (start us, length us, event | category | flops | bytes accessed | tf_op | source)
XLA Modules:
  0.0 269.1 jit_solution(8109347872111895553)
XLA Ops:
  0.0 0.7 constant_dynamic-update-slice_fusion.7
  0.7 0.7 constant_dynamic-update-slice_fusion.6
  1.4 0.7 constant_dynamic-update-slice_fusion.5
  2.1 0.7 constant_dynamic-update-slice_fusion.4
  2.8 0.7 constant_dynamic-update-slice_fusion.3
  3.5 0.7 constant_dynamic-update-slice_fusion.2
  4.2 0.7 constant_dynamic-update-slice_fusion.1
  4.9 0.7 constant_dynamic-update-slice_fusion
  5.6 2.5 broadcast_in_dim.40
  8.2 17.5 %all-to-all-start = ((bf16[64,32,1024]{2,1,0:T(8,128)(2,1)}), bf16[64,32,1024]{2,1,0:T(8,128)(2,1)}, u32[]{:S(2)}, u32[]{:S(2)}) async-start(bf16[64,32,1024]{2,1,0:T(8,128)(2,1)} %broadcast_in_dim.40), calls=%async_computation | async-start | bytes 8388608 | tf_op jit(solution)/shard_map/all_to_all | solution.py:21
  25.7 0.3 fusion
  26.0 0.3 fusion.2
  26.3 0.9 constant_dynamic-slice_fusion.9
  27.2 4.5 %collective-permute-start = (bf16[256,1024]{1,0:T(8,128)(2,1)S(1)}, bf16[256,1024]{1,0:T(8,128)(2,1)S(1)}, u32[]{:S(2)}, u32[]{:S(2)}) collective-permute-start(bf16[256,1024]{1,0:T(8,128)(2,1)S(1)} %get-tuple-element.15.refs_0_), channel_id=1, source_target_pairs={{0,6},{2,0},{4,2},{6,4},{1,7},{3,1},{5,3},{7,5},{8,14},{10,8},{12,... | collective-permute-start | bytes 1572872 | tf_op jit(solution)/shard_map/ppermute | solution.py:50
  31.7 1.9 collective-permute-start.2
  33.7 3.6 %collective-permute-start.1 = (bf16[256,1024]{1,0:T(8,128)(2,1)S(1)}, bf16[256,1024]{1,0:T(8,128)(2,1)S(1)}, u32[]{:S(2)}, u32[]{:S(2)}) collective-permute-start(bf16[256,1024]{1,0:T(8,128)(2,1)S(1)} %get-tuple-element.15.refs_0_), channel_id=1, source_target_pairs={{0,4},{2,6},{4,0},{6,2},{1,5},{3,7},{5,1},{7,3},{8,12},{10,14},{12... | collective-permute-start | bytes 1572872 | tf_op jit(solution)/shard_map/ppermute | solution.py:50
  37.3 5.5 %collective-permute-done.refs_2_ = bf16[256,1024]{1,0:T(8,128)(2,1)S(1)} collective-permute-done((bf16[256,1024]{1,0:T(8,128)(2,1)S(1)}, bf16[256,1024]{1,0:T(8,128)(2,1)S(1)}, u32[]{:S(2)}, u32[]{:S(2)}) %collective-permute-start) | collective-permute-done | bytes 524320 | tf_op jit(solution)/shard_map/ppermute | solution.py:50
  42.8 5.3 %collective-permute-done.2.refs_6_ = bf16[256,1024]{1,0:T(8,128)(2,1)S(1)} collective-permute-done((bf16[256,1024]{1,0:T(8,128)(2,1)S(1)}, bf16[256,1024]{1,0:T(8,128)(2,1)S(1)}, u32[]{:S(2)}, u32[]{:S(2)}) %collective-permute-start.2) | collective-permute-done | bytes 524320 | tf_op jit(solution)/shard_map/ppermute | solution.py:50
  48.1 9.4 %collective-permute-done.1.refs_4_ = bf16[256,1024]{1,0:T(8,128)(2,1)S(1)} collective-permute-done((bf16[256,1024]{1,0:T(8,128)(2,1)S(1)}, bf16[256,1024]{1,0:T(8,128)(2,1)S(1)}, u32[]{:S(2)}, u32[]{:S(2)}) %collective-permute-start.1) | collective-permute-done | bytes 524320 | tf_op jit(solution)/shard_map/ppermute | solution.py:50
  57.7 0.7 copy-done.7
  58.3 5.0 %collective-permute-start.3 = (bf16[768,1024]{1,0:T(8,128)(2,1)S(1)}, bf16[768,1024]{1,0:T(8,128)(2,1)S(1)}, u32[]{:S(2)}, u32[]{:S(2)}) collective-permute-start(bf16[768,1024]{1,0:T(8,128)(2,1)S(1)} %pad_maximum_fusion), channel_id=1, source_target_pairs={{0,1},{1,0},{2,3},{3,2},{4,5},{5,4},{6,7},{7,6},{8,9},{9,8},{10,11... | collective-permute-start | bytes 4718600 | tf_op jit(solution)/shard_map/ppermute | solution.py:29
  63.3 0.8 constant_dynamic-slice_fusion.6
  64.2 0.6 copy.119
  64.8 0.8 dynamic_slice.54
  65.6 0.6 pad_add_fusion.spot
  66.3 0.8 constant_dynamic-slice_fusion.4
  67.1 0.6 fusion.52
  67.7 1.2 fusion.51
  68.9 61.0 %all-to-all-done = bf16[64,32,1024]{2,1,0:T(8,128)(2,1)} async-done(((bf16[64,32,1024]{2,1,0:T(8,128)(2,1)}), bf16[64,32,1024]{2,1,0:T(8,128)(2,1)}, u32[]{:S(2)}, u32[]{:S(2)}) %all-to-all-start) | async-done | bytes 4194336 | tf_op jit(solution)/shard_map/all_to_all | solution.py:21
  129.9 7.5 %shard_map.155 = (bf16[4,256,384]{2,1,0:T(8,128)(2,1)}, f32[4,16,256]{2,1,0:T(8,128)}) custom-call(s32[2]{0:T(128)} %pad_add_fusion.spot, bf16[256,1024]{1,0:T(8,128)(2,1)} %copy-done.4, bf16[256,1024]{1,0:T(8,128)(2,1)} %get-tuple-element.14.refs_1_, bf16[256,1024]{1,0:T(8,128)(2,1)} %copy-done.5, bf16[256,1024]{1,0:T(8,128)(2,1)} %get-tuple-element.13.refs_3_, ...), custom_call_target="tpu_custom_call" | custom-call | flops 3000000000 | bytes 6291456 | tf_op jit(solution)/shard_map/pallas_call | solution.py:120
  137.4 1.4 add_negate_fusion
  138.8 1.2 reduce-window.6
  140.5 1.3 slice.154.refs_0_
  141.8 4.4 %collective-permute-start.5 = (bf16[2048,256]{1,0:T(8,128)(2,1)S(1)}, bf16[2048,256]{1,0:T(8,128)(2,1)S(1)}, u32[]{:S(2)}, u32[]{:S(2)}) collective-permute-start(bf16[2048,256]{1,0:T(8,128)(2,1)S(1)} %slice.154.refs_0_), channel_id=1, source_target_pairs={{0,6},{2,0},{4,2},{6,4},{1,7},{3,1},{5,3},{7,5},{8,14},{10,8},{12,... | collective-permute-start | bytes 3145736 | tf_op jit(solution)/shard_map/ppermute | solution.py:50
  146.2 1.9 collective-permute-start.6
  148.1 6.7 %shard_map.154 = bf16[4,256,384]{2,1,0:T(8,128)(2,1)} custom-call(s32[2]{0:T(128)} %pad_add_fusion.spot, bf16[256,1024]{1,0:T(8,128)(2,1)} %copy-done.4, bf16[256,1024]{1,0:T(8,128)(2,1)} %get-tuple-element.14.refs_1_, bf16[256,1024]{1,0:T(8,128)(2,1)} %copy-done.5, bf16[256,1024]{1,0:T(8,128)(2,1)} %get-tuple-element.13.refs_3_, ...), custom_call_target="tpu_custom_call" | custom-call | flops 3000000000 | bytes 6291456 | tf_op jit(solution)/shard_map/pallas_call | solution.py:120
  154.8 1.1 multiply_convert_fusion.2
  155.9 11.0 %collective-permute-start.4 = (bf16[4,2,128]{2,1,0:T(2,128)(2,1)S(1)}, bf16[4,2,128]{2,1,0:T(2,128)(2,1)S(1)}, u32[]{:S(2)}, u32[]{:S(2)}) collective-permute-start(bf16[4,2,128]{2,1,0:T(2,128)(2,1)S(1)} %slice.141), channel_id=1, source_target_pairs={{0,8},{8,16},{16,24},{24,32},{32,40},{40,48},{48,56},{56,64},{64,7... | collective-permute-start | bytes 6152 | tf_op jit(solution)/shard_map/ppermute | solution.py:34
  167.1 1.5 add_reduce_fusion
  168.8 1.5 convolution_convert_fusion
  170.5 0.9 copy.83
  171.3 24.2 %all-to-all-start.1 = ((bf16[64,16,128]{2,1,0:T(8,128)(2,1)}), bf16[64,16,128]{2,1,0:T(8,128)(2,1)S(1)}, u32[]{:S(2)}, u32[]{:S(2)}) async-start(bf16[64,16,128]{2,1,0:T(8,128)(2,1)} %copy.83), calls=%async_computation.1 | async-start | bytes 524288 | tf_op jit(solution)/shard_map/all_to_all | solution.py:25
  195.5 0.4 fusion.11
  196.0 1.2 fusion.17
  197.1 10.7 %all-to-all-done.1 = bf16[64,16,128]{2,1,0:T(8,128)(2,1)S(1)} async-done(((bf16[64,16,128]{2,1,0:T(8,128)(2,1)}), bf16[64,16,128]{2,1,0:T(8,128)(2,1)S(1)}, u32[]{:S(2)}, u32[]{:S(2)}) %all-to-all-start.1) | async-done | bytes 262176 | tf_op jit(solution)/shard_map/all_to_all | solution.py:25
  208.1 0.3 fusion.53
  209.1 0.7 reshape.380
  209.8 4.6 %all-to-all-start.2 = ((bf16[64,8,128]{2,1,0:T(8,128)(2,1)}), bf16[64,8,128]{2,1,0:T(8,128)(2,1)S(1)}, u32[]{:S(2)}, u32[]{:S(2)}) async-start(bf16[64,8,128]{2,1,0:T(8,128)(2,1)} %reshape.380), calls=%async_computation.2 | async-start | bytes 262144 | tf_op jit(solution)/shard_map/all_to_all | solution.py:25
  214.5 1.7 fusion.4
  216.2 9.8 %all-to-all-done.2 = bf16[64,8,128]{2,1,0:T(8,128)(2,1)S(1)} async-done(((bf16[64,8,128]{2,1,0:T(8,128)(2,1)}), bf16[64,8,128]{2,1,0:T(8,128)(2,1)S(1)}, u32[]{:S(2)}, u32[]{:S(2)}) %all-to-all-start.2) | async-done | bytes 131104 | tf_op jit(solution)/shard_map/all_to_all | solution.py:25
  226.1 1.4 multiply_reduce_fusion
  227.5 1.0 copy-done.8
  228.5 4.6 %collective-permute-start.8 = (bf16[1024,256]{1,0:T(8,128)(2,1)S(1)}, bf16[1024,256]{1,0:T(8,128)(2,1)S(1)}, u32[]{:S(2)}, u32[]{:S(2)}) collective-permute-start(bf16[1024,256]{1,0:T(8,128)(2,1)S(1)} %slice.156), channel_id=1, source_target_pairs={{0,6},{2,0},{4,2},{6,4},{1,7},{3,1},{5,3},{7,5},{8,14},{10,8},{12,... | collective-permute-start | bytes 1572872 | tf_op jit(solution)/shard_map/ppermute | solution.py:50
  233.1 1.1 slice.155
  234.2 1.9 collective-permute-start.7
  236.3 1.1 fusion.13
  237.5 3.9 %all-to-all-start.3 = ((bf16[4,256,256]{2,1,0:T(8,128)(2,1)}), bf16[4,256,256]{2,1,0:T(8,128)(2,1)S(1)}, u32[]{:S(2)}, u32[]{:S(2)}) async-start(bf16[4,256,256]{2,1,0:T(8,128)(2,1)} %fusion.13), calls=%async_computation.3 | async-start | bytes 1048576 | tf_op jit(solution)/shard_map/all_to_all | solution.py:25
  241.4 3.9 %collective-permute-done.7 = bf16[1024,256]{1,0:T(8,128)(2,1)S(1)} collective-permute-done((bf16[1024,256]{1,0:T(8,128)(2,1)S(1)}, bf16[1024,256]{1,0:T(8,128)(2,1)S(1)}, u32[]{:S(2)}, u32[]{:S(2)}) %collective-permute-start.7) | collective-permute-done | bytes 524320 | tf_op jit(solution)/shard_map/ppermute | solution.py:50
  245.3 1.1 pad_maximum_fusion.1.refs_2_
  246.4 4.7 %all-to-all-done.3.parts = bf16[4,256,256]{2,1,0:T(8,128)(2,1)S(1)} async-done(((bf16[4,256,256]{2,1,0:T(8,128)(2,1)}), bf16[4,256,256]{2,1,0:T(8,128)(2,1)S(1)}, u32[]{:S(2)}, u32[]{:S(2)}) %all-to-all-start.3) | async-done | bytes 524320 | tf_op jit(solution)/shard_map/all_to_all | solution.py:25
  251.2 0.8 copy-done.3
  252.0 4.6 %shard_map.156 = bf16[256,2048]{1,0:T(8,128)(2,1)} custom-call(s32[2]{0:T(128)} %pad_add_fusion.spot, bf16[4,256,256]{2,1,0:T(8,128)(2,1)} %copy-done.3, bf16[2048,256]{1,0:T(8,128)(2,1)} %copy-done.2, bf16[2048,256]{1,0:T(8,128)(2,1)} %copy-done.8, bf16[2048,256]{1,0:T(8,128)(2,1)} %pad_maximum_fusion.1.refs_2_, ...), custom_call_target="tpu_custom_call" | custom-call | flops 2000000000 | bytes 6291456 | tf_op jit(solution)/shard_map/pallas_call | solution.py:120
  256.6 11.4 %all_to_all.25 = bf16[2,128,2048]{2,1,0:T(8,128)(2,1)S(1)} all-to-all(bf16[2,128,2048]{2,1,0:T(8,128)(2,1)} %bitcast.87), channel_id=1, replica_groups=mesh['sp_0'=8,'sp_1'=8,'fs'=4,'tp'=2] {'tp'}, dimensions={0} | all-to-all | bytes 2097152 | tf_op jit(solution)/shard_map/all_to_all | solution.py:25
  268.0 1.1 reduce_sum.42
  (72 shorter events, 2.7 us)
Async XLA Ops:
  0.0 66.3 %copy-start = (f32[3,1024]{1,0:T(4,128)S(1)}, f32[3,1024]{1,0:T(4,128)}, u32[]{:S(2)}) copy-start(f32[3,1024]{1,0:T(4,128)} %param.21) | copy-start | bytes 36868
  8.2 17.5 %copy-start.1 = (bf16[1,256,2048]{2,1,0:T(8,128)(2,1)S(1)}, bf16[1,256,2048]{2,1,0:T(8,128)(2,1)}, u32[]{:S(2)}) copy-start(bf16[1,256,2048]{2,1,0:T(8,128)(2,1)} %param.16) | copy-start | bytes 3145732
  8.2 17.8 %copy-start.9 = (f32[2048]{0:T(1024)S(1)}, f32[2048]{0:T(1024)}, u32[]{:S(2)}) copy-start(f32[2048]{0:T(1024)} %param.17) | copy-start | bytes 24580
  8.2 121.7 %all-to-all-start = ((bf16[64,32,1024]{2,1,0:T(8,128)(2,1)}), bf16[64,32,1024]{2,1,0:T(8,128)(2,1)}, u32[]{:S(2)}, u32[]{:S(2)}) async-start(bf16[64,32,1024]{2,1,0:T(8,128)(2,1)} %broadcast_in_dim.40), calls=%async_computation | async-start | bytes 8388608 | tf_op jit(solution)/shard_map/all_to_all | solution.py:21
  27.2 20.9 %copy-start.4 = (bf16[256,1024]{1,0:T(8,128)(2,1)}, bf16[256,1024]{1,0:T(8,128)(2,1)S(1)}, u32[]{:S(2)}) copy-start(bf16[256,1024]{1,0:T(8,128)(2,1)S(1)} %get-tuple-element.15.refs_0_) | copy-start | bytes 1572868
  27.2 39.0 %copy-start.10 = (f32[2,8]{1,0:T(2,128)S(1)}, f32[2,8]{1,0:T(2,128)}, u32[]{:S(2)}) copy-start(f32[2,8]{1,0:T(2,128)} %param.27) | copy-start | bytes 196
  27.2 15.6 %collective-permute-start = (bf16[256,1024]{1,0:T(8,128)(2,1)S(1)}, bf16[256,1024]{1,0:T(8,128)(2,1)S(1)}, u32[]{:S(2)}, u32[]{:S(2)}) collective-permute-start(bf16[256,1024]{1,0:T(8,128)(2,1)S(1)} %get-tuple-element.15.refs_0_), channel_id=1, source_target_pairs={{0,6},{2,0},{4,2},{6,4},{1,7},{3,1},{5,3},{7,5},{8,14},{10,8},{12,... | collective-permute-start | bytes 1572872 | tf_op jit(solution)/shard_map/ppermute | solution.py:50
  31.7 16.4 %collective-permute-start.2 = (bf16[256,1024]{1,0:T(8,128)(2,1)S(1)}, bf16[256,1024]{1,0:T(8,128)(2,1)S(1)}, u32[]{:S(2)}, u32[]{:S(2)}) collective-permute-start(bf16[256,1024]{1,0:T(8,128)(2,1)S(1)} %get-tuple-element.15.refs_0_), channel_id=1, source_target_pairs={{0,2},{2,4},{4,6},{6,0},{1,3},{3,5},{5,7},{7,1},{8,10},{10,12},{12... | collective-permute-start | bytes 1572872 | tf_op jit(solution)/shard_map/ppermute | solution.py:50
  33.7 23.9 %collective-permute-start.1 = (bf16[256,1024]{1,0:T(8,128)(2,1)S(1)}, bf16[256,1024]{1,0:T(8,128)(2,1)S(1)}, u32[]{:S(2)}, u32[]{:S(2)}) collective-permute-start(bf16[256,1024]{1,0:T(8,128)(2,1)S(1)} %get-tuple-element.15.refs_0_), channel_id=1, source_target_pairs={{0,4},{2,6},{4,0},{6,2},{1,5},{3,7},{5,1},{7,3},{8,12},{10,14},{12... | collective-permute-start | bytes 1572872 | tf_op jit(solution)/shard_map/ppermute | solution.py:50
  42.8 14.7 %copy-start.5 = (bf16[256,1024]{1,0:T(8,128)(2,1)}, bf16[256,1024]{1,0:T(8,128)(2,1)S(1)}, u32[]{:S(2)}) copy-start(bf16[256,1024]{1,0:T(8,128)(2,1)S(1)} %collective-permute-done.refs_2_) | copy-start | bytes 1572868
  48.1 9.5 %copy-start.6 = (bf16[256,1024]{1,0:T(8,128)(2,1)}, bf16[256,1024]{1,0:T(8,128)(2,1)S(1)}, u32[]{:S(2)}) copy-start(bf16[256,1024]{1,0:T(8,128)(2,1)S(1)} %collective-permute-done.2.refs_6_) | copy-start | bytes 1572868
  57.5 0.8 copy-start.7
  58.3 9.4 %collective-permute-start.3 = (bf16[768,1024]{1,0:T(8,128)(2,1)S(1)}, bf16[768,1024]{1,0:T(8,128)(2,1)S(1)}, u32[]{:S(2)}, u32[]{:S(2)}) collective-permute-start(bf16[768,1024]{1,0:T(8,128)(2,1)S(1)} %pad_maximum_fusion), channel_id=1, source_target_pairs={{0,1},{1,0},{2,3},{3,2},{4,5},{5,4},{6,7},{7,6},{8,9},{9,8},{10,11... | collective-permute-start | bytes 4718600 | tf_op jit(solution)/shard_map/ppermute | solution.py:29
  141.8 13.1 %copy-start.2 = (bf16[2048,256]{1,0:T(8,128)(2,1)}, bf16[2048,256]{1,0:T(8,128)(2,1)S(1)}, u32[]{:S(2)}) copy-start(bf16[2048,256]{1,0:T(8,128)(2,1)S(1)} %slice.154.refs_0_) | copy-start | bytes 3145732
  141.8 85.7 %collective-permute-start.5 = (bf16[2048,256]{1,0:T(8,128)(2,1)S(1)}, bf16[2048,256]{1,0:T(8,128)(2,1)S(1)}, u32[]{:S(2)}, u32[]{:S(2)}) collective-permute-start(bf16[2048,256]{1,0:T(8,128)(2,1)S(1)} %slice.154.refs_0_), channel_id=1, source_target_pairs={{0,6},{2,0},{4,2},{6,4},{1,7},{3,1},{5,3},{7,5},{8,14},{10,8},{12,... | collective-permute-start | bytes 3145736 | tf_op jit(solution)/shard_map/ppermute | solution.py:50
  146.2 86.9 %collective-permute-start.6 = (bf16[2048,256]{1,0:T(8,128)(2,1)S(1)}, bf16[2048,256]{1,0:T(8,128)(2,1)}, u32[]{:S(2)}, u32[]{:S(2)}) collective-permute-start(bf16[2048,256]{1,0:T(8,128)(2,1)S(1)} %slice.154.refs_0_), channel_id=1, source_target_pairs={{0,2},{2,4},{4,6},{6,0},{1,3},{3,5},{5,7},{7,1},{8,10},{10,12},{12... | collective-permute-start | bytes 3145736 | tf_op jit(solution)/shard_map/ppermute | solution.py:50
  155.9 39.9 %collective-permute-start.4 = (bf16[4,2,128]{2,1,0:T(2,128)(2,1)S(1)}, bf16[4,2,128]{2,1,0:T(2,128)(2,1)S(1)}, u32[]{:S(2)}, u32[]{:S(2)}) collective-permute-start(bf16[4,2,128]{2,1,0:T(2,128)(2,1)S(1)} %slice.141), channel_id=1, source_target_pairs={{0,8},{8,16},{16,24},{24,32},{32,40},{40,48},{48,56},{56,64},{64,7... | collective-permute-start | bytes 6152 | tf_op jit(solution)/shard_map/ppermute | solution.py:34
  171.3 36.5 %all-to-all-start.1 = ((bf16[64,16,128]{2,1,0:T(8,128)(2,1)}), bf16[64,16,128]{2,1,0:T(8,128)(2,1)S(1)}, u32[]{:S(2)}, u32[]{:S(2)}) async-start(bf16[64,16,128]{2,1,0:T(8,128)(2,1)} %copy.83), calls=%async_computation.1 | async-start | bytes 524288 | tf_op jit(solution)/shard_map/all_to_all | solution.py:25
  209.8 16.2 %all-to-all-start.2 = ((bf16[64,8,128]{2,1,0:T(8,128)(2,1)}), bf16[64,8,128]{2,1,0:T(8,128)(2,1)S(1)}, u32[]{:S(2)}, u32[]{:S(2)}) async-start(bf16[64,8,128]{2,1,0:T(8,128)(2,1)} %reshape.380), calls=%async_computation.2 | async-start | bytes 262144 | tf_op jit(solution)/shard_map/all_to_all | solution.py:25
  227.5 1.0 copy-start.8
  228.5 12.9 %collective-permute-start.8 = (bf16[1024,256]{1,0:T(8,128)(2,1)S(1)}, bf16[1024,256]{1,0:T(8,128)(2,1)S(1)}, u32[]{:S(2)}, u32[]{:S(2)}) collective-permute-start(bf16[1024,256]{1,0:T(8,128)(2,1)S(1)} %slice.156), channel_id=1, source_target_pairs={{0,6},{2,0},{4,2},{6,4},{1,7},{3,1},{5,3},{7,5},{8,14},{10,8},{12,... | collective-permute-start | bytes 1572872 | tf_op jit(solution)/shard_map/ppermute | solution.py:50
  234.2 11.1 %collective-permute-start.7 = (bf16[1024,256]{1,0:T(8,128)(2,1)S(1)}, bf16[1024,256]{1,0:T(8,128)(2,1)S(1)}, u32[]{:S(2)}, u32[]{:S(2)}) collective-permute-start(bf16[1024,256]{1,0:T(8,128)(2,1)S(1)} %slice.155), channel_id=1, source_target_pairs={{0,2},{2,4},{4,6},{6,0},{1,3},{3,5},{5,7},{7,1},{8,10},{10,12},{12... | collective-permute-start | bytes 1572872 | tf_op jit(solution)/shard_map/ppermute | solution.py:50
  237.5 13.7 %all-to-all-start.3 = ((bf16[4,256,256]{2,1,0:T(8,128)(2,1)}), bf16[4,256,256]{2,1,0:T(8,128)(2,1)S(1)}, u32[]{:S(2)}, u32[]{:S(2)}) async-start(bf16[4,256,256]{2,1,0:T(8,128)(2,1)} %fusion.13), calls=%async_computation.3 | async-start | bytes 1048576 | tf_op jit(solution)/shard_map/all_to_all | solution.py:25
  251.2 0.8 copy-start.3

commit v5 on v4

--- a/solution.py
+++ b/solution.py
@@ -67,6 +67,18 @@
     size = array.shape[0]
     twice = jnp.concatenate([array, array], axis=0)
     return lax.dynamic_slice_in_dim(twice, (size - by) % size, size, 0)
+
+
+def ring_gather(array, axis):
+    behind, ahead = [array], [array]
+    for k in range(4):
+        behind.append(ring(behind[-1], axis, 1))
+        if k < 3:
+            ahead.append(ring(ahead[-1], axis, -1))
+    return behind + ahead[1:]
+
+
+OFFSETS = (0, 7, 6, 5, 4, 1, 2, 3)
 
 
 def matmuls(core, pieces, weights, left, out):
@@ -89,8 +101,14 @@
 
 
 def project_mem_kernel(spot, *refs):
-    pieces, weights, gate_rows, out, gates = refs[:8], refs[8], refs[9], refs[10], refs[11]
+    parts, pieces, gate_rows = refs[:8], refs[8:16], refs[16]
+    out, gates, weights = refs[17:]
     core = spot[0]
+    for part, offset in zip(parts, OFFSETS):
+        place = (spot[2] + offset) % 8
+        for k in range(8):
+            start = pl.multiple_of((k * 8 + place) * 32, 32)
+            weights[pl.ds(start, 32), :] = part[pl.ds(k * 32, 32), :]
     matmuls(core, pieces, weights, 0, out)
     dims = (((1,), (1,)), ((), ()))
     for k in range(4):
@@ -99,7 +117,7 @@
 
 
 def project_conv_kernel(spot, *refs):
-    matmuls(spot[0], refs[:8], refs[8], refs[9].shape[2], refs[9])
+    matmuls(spot[0], refs[:8], refs[8], 0, refs[9])
 
 
 def output_kernel(spot, parts, *refs):
@@ -154,24 +172,20 @@
     place_x = lax.axis_index("fs")
     order = [(place_x + by) % seqs for by in range(seqs)]
 
-    spot = jnp.stack([core, place_x]).astype(jnp.int32)
-
-    w_all = jnp.concatenate(
-        [
-            w_query,
-            w_key,
-            w_value,
-            w_conv_gate,
-            w_conv_mult,
-            w_conv_in,
-            w_out_conv.T,
-            w_out_mem.T,
-        ],
-        axis=1,
-    )
+    place_y = lax.axis_index("sp_1")
+    spot = jnp.stack([core, place_x, place_y]).astype(jnp.int32)
+
     channels = w_conv_gate.shape[1]
-    w_all = everyone(w_all, SP).reshape(width, -1)
-    w_own = w_all[:, 6 * channels :]
+    w_rest = jnp.concatenate(
+        [w_conv_gate, w_conv_mult, w_conv_in, w_out_conv.T, w_out_mem.T], axis=1
+    )
+    w_mem = jnp.concatenate([w_query, w_key, w_value], axis=1)
+    w_rest, w_mem = lax.optimization_barrier((w_rest, w_mem))
+    w_mem = everyone(w_mem, "sp_0").reshape(-1, w_mem.shape[1])
+    w_mem = ring_gather(w_mem, "sp_1")
+
+    w_rest = lax.all_gather(w_rest, SP, axis=0, tiled=True)
+    w_own = w_rest[:, 3 * channels :]
     w_out = (w_own, *relayed(w_own, "fs"))
 
     x = activations[0].astype(F32)
@@ -197,8 +211,9 @@
         project_mem_kernel,
         [((seqs, tokens, 3 * HEAD_DIM), BF16), ((seqs, 16, tokens), F32)],
         spot,
-        [*pieces, w_all, gate_rows],
+        [*w_mem, *pieces, gate_rows],
         10**9 * 3,
+        [pltpu.VMEM((width, 3 * HEAD_DIM), BF16)],
     )
     query, key, value = (qkv[..., k * HEAD_DIM : (k + 1) * HEAD_DIM] for k in range(3))
     bias = lax.dynamic_slice_in_dim(gate_bias, head, 1, 1)
@@ -252,7 +267,7 @@
         project_conv_kernel,
         [((seqs, tokens, 3 * channels), BF16)],
         spot,
-        [*pieces, w_all],
+        [*pieces, w_rest],
         10**9 * 3,
     )
     gate, mult, inlet = (conv[..., k * channels : (k + 1) * channels] for k in range(3))

time: 271 us -> 231 us (0.85)
  waiting for transfers between devices: 110 us -> 74.5 us
  between operations: 0.5 us -> 14.2 us
  starting transfers between devices: 89 us -> 77.7 us
  local copies, waits for them, and re-layouts: 21.5 us -> 13.3 us
    all_to_all x1, waiting for transfers between devices: 61 us -> 9.25 us  [everyone(): return lax.all_to_all(copies, axis, split_axis=0, concat_axis=0, tiled=True)]
    ppermute x7 -> x14, starting transfers between devices: 22.9 us -> 45.6 us  [ring(): lax.ppermute(array, axis, [(i, (i + by) % peers) for i in range(peers)])]
    all_to_all x3, starting transfers between devices: 32.7 us -> 17.1 us  [exchanged(): return lax.all_to_all(array, axis, split_axis=0, concat_axis=0, tiled=True)]
    ppermute x7 -> x14, waiting for transfers between devices: 24.1 us -> 35.1 us  [ring(): lax.ppermute(array, axis, [(i, (i + by) % peers) for i in range(peers)])]
    ppermute x1, starting transfers between devices: 11 us -> 2.41 us  [from_behind(): return lax.ppermute(array, axis, [(i, i + 1) for i in range(peers - 1)])]
    all_to_all x1, starting transfers between devices: 17.5 us -> 10 us  [everyone(): return lax.all_to_all(copies, axis, split_axis=0, concat_axis=0, tiled=True)]
    unnamed x32 -> x59, local copies, waits for them, and re-layouts: 7.46 us -> 1.7 us
    all_to_all x3, waiting for transfers between devices: 25.2 us -> 29.4 us  [exchanged(): return lax.all_to_all(array, axis, split_axis=0, concat_axis=0, tiled=True)]
  transfers between devices with their start and end apart: 13 -> 21, of which waited for: 8 -> 13; matrix products, arithmetic and copies ran while one was open for 8% -> 10% of each run, Pallas kernels for 2% -> 6%
where the time goes in v5:
time: 231 us; the launch traced here: 230 us
  starting transfers between devices  77.7 us (34%)
  waiting for transfers between devices  74.5 us (32%)
  Pallas kernels  17.8 us (8%)
  other arithmetic  14.8 us (6%)
  between operations  14.2 us (6%)
  local copies, waits for them, and re-layouts  13.3 us (6%)
  blocking collectives  13.2 us (6%)
  matrix products  4.01 us (2%)
    ppermute x14, starting transfers between devices, ring(): lax.ppermute(array, axis, [(i, (i + by) % peers) for i in range(peers)])  45.6 us
    ppermute x14, waiting for transfers between devices, ring(): lax.ppermute(array, axis, [(i, (i + by) % peers) for i in range(peers)])  35.1 us
    all_to_all x3, waiting for transfers between devices, exchanged(): return lax.all_to_all(array, axis, split_axis=0, concat_axis=0, tiled=True)  29.4 us
    pallas_call x3, Pallas kernels, call(): pl.pallas_call(kernel, out_shape=tuple((jax.ShapeDtypeStruct(shape, dtype...  17.8 us
    all_to_all x3, starting transfers between devices, exchanged(): return lax.all_to_all(array, axis, split_axis=0, concat_axis=0, tiled=True)  17.1 us
    all_to_all x1, blocking collectives, exchanged(): return lax.all_to_all(array, axis, split_axis=0, concat_axis=0, tiled=True)  13.2 us
    all_to_all x1, starting transfers between devices, everyone(): return lax.all_to_all(copies, axis, split_axis=0, concat_axis=0, tiled=True)  10 us
    all_to_all x1, waiting for transfers between devices, everyone(): return lax.all_to_all(copies, axis, split_axis=0, concat_axis=0, tiled=True)  9.25 us
  transfers between devices with their start and end apart: 21, of which 13 were waited for; matrix products, arithmetic and copies ran while one was open for 10% of the time, Pallas kernels for 6%

profile of v5, /device:TPU:1, one launch (start us, length us, event | category | flops | bytes accessed | tf_op | source)
XLA Modules:
  0.0 229.5 jit_solution(17556610519309248217)
XLA Ops:
  6.5 1.5 fusion
  8.1 1.6 fusion.2
  9.7 0.9 constant_dynamic-slice_fusion.9
  10.6 5.3 %collective-permute-start = (bf16[256,1024]{1,0:T(8,128)(2,1)S(1)}, bf16[256,1024]{1,0:T(8,128)(2,1)S(1)}, u32[]{:S(2)}, u32[]{:S(2)}) collective-permute-start(bf16[256,1024]{1,0:T(8,128)(2,1)S(1)} %get-tuple-element.19.refs_0_.refs_8_), channel_id=1, source_target_pairs={{0,6},{2,0},{4,2},{6,4},{1,7},{3,1},{5,3},{7,5},{8,14},{10,8},{12,... | collective-permute-start | bytes 1572872 | tf_op jit(solution)/shard_map/ppermute | solution.py:50
  15.9 2.4 %collective-permute-start.1 = (bf16[256,1024]{1,0:T(8,128)(2,1)S(1)}, bf16[256,1024]{1,0:T(8,128)(2,1)S(1)}, u32[]{:S(2)}, u32[]{:S(2)}) collective-permute-start(bf16[256,1024]{1,0:T(8,128)(2,1)S(1)} %get-tuple-element.19.refs_0_.refs_8_), channel_id=1, source_target_pairs={{0,4},{2,6},{4,0},{6,2},{1,5},{3,7},{5,1},{7,3},{8,12},{10,14},{12... | collective-permute-start | bytes 1572872 | tf_op jit(solution)/shard_map/ppermute | solution.py:50
  18.4 2.5 %collective-permute-start.2 = (bf16[256,1024]{1,0:T(8,128)(2,1)S(1)}, bf16[256,1024]{1,0:T(8,128)(2,1)S(1)}, u32[]{:S(2)}, u32[]{:S(2)}) collective-permute-start(bf16[256,1024]{1,0:T(8,128)(2,1)S(1)} %get-tuple-element.19.refs_0_.refs_8_), channel_id=1, source_target_pairs={{0,2},{2,4},{4,6},{6,0},{1,3},{3,5},{5,7},{7,1},{8,10},{10,12},{12... | collective-permute-start | bytes 1572872 | tf_op jit(solution)/shard_map/ppermute | solution.py:50
  21.0 6.8 %collective-permute-done.refs_2_.refs_10_ = bf16[256,1024]{1,0:T(8,128)(2,1)S(1)} collective-permute-done((bf16[256,1024]{1,0:T(8,128)(2,1)S(1)}, bf16[256,1024]{1,0:T(8,128)(2,1)S(1)}, u32[]{:S(2)}, u32[]{:S(2)}) %collective-permute-start) | collective-permute-done | bytes 524320 | tf_op jit(solution)/shard_map/ppermute | solution.py:50
  27.9 1.5 collective-permute-done.1.refs_4_.refs_12_
  29.3 15.1 %collective-permute-done.2.refs_6_.refs_14_ = bf16[256,1024]{1,0:T(8,128)(2,1)S(1)} collective-permute-done((bf16[256,1024]{1,0:T(8,128)(2,1)S(1)}, bf16[256,1024]{1,0:T(8,128)(2,1)S(1)}, u32[]{:S(2)}, u32[]{:S(2)}) %collective-permute-start.2) | collective-permute-done | bytes 524320 | tf_op jit(solution)/shard_map/ppermute | solution.py:50
  44.5 2.4 %collective-permute-start.3 = (bf16[768,1024]{1,0:T(8,128)(2,1)S(1)}, bf16[768,1024]{1,0:T(8,128)(2,1)S(1)}, u32[]{:S(2)}, u32[]{:S(2)}) collective-permute-start(bf16[768,1024]{1,0:T(8,128)(2,1)S(1)} %pad_maximum_fusion), channel_id=1, source_target_pairs={{0,1},{1,0},{2,3},{3,2},{4,5},{5,4},{6,7},{7,6},{8,9},{9,8},{10,11... | collective-permute-start | bytes 4718600 | tf_op jit(solution)/shard_map/ppermute | solution.py:29
  47.0 0.7 broadcast_in_dim.40
  47.7 10.0 %all-to-all-start = ((bf16[8,32,384]{2,1,0:T(8,128)(2,1)}), bf16[8,32,384]{2,1,0:T(8,128)(2,1)S(1)}, u32[]{:S(2)}, u32[]{:S(2)}) async-start(bf16[8,32,384]{2,1,0:T(8,128)(2,1)} %broadcast_in_dim.40), calls=%async_computation | async-start | bytes 393216 | tf_op jit(solution)/shard_map/all_to_all | solution.py:21
  57.8 0.7 all-gather.2.cloned.1.call-update
  58.5 0.8 constant_dynamic-slice_fusion.6
  59.3 9.2 %all-to-all-done = bf16[8,32,384]{2,1,0:T(8,128)(2,1)S(1)} async-done(((bf16[8,32,384]{2,1,0:T(8,128)(2,1)}), bf16[8,32,384]{2,1,0:T(8,128)(2,1)S(1)}, u32[]{:S(2)}, u32[]{:S(2)}) %all-to-all-start) | async-done | bytes 196640 | tf_op jit(solution)/shard_map/all_to_all | solution.py:21
  68.6 3.2 %collective-permute-start.5 = (bf16[256,384]{1,0:T(8,128)(2,1)S(1)}, bf16[256,384]{1,0:T(8,128)(2,1)}, u32[]{:S(2)}, u32[]{:S(2)}) collective-permute-start(bf16[256,384]{1,0:T(8,128)(2,1)S(1)} %bitcast.93), channel_id=1, source_target_pairs={{0,8},{8,16},{16,24},{24,32},{32,40},{40,48},{48,56},{56,0},{1,9},... | collective-permute-start | bytes 589832 | tf_op jit(solution)/shard_map/ppermute | solution.py:50
  71.9 0.6 copy.119
  72.6 3.8 %collective-permute-start.9 = (bf16[256,384]{1,0:T(8,128)(2,1)S(1)}, bf16[256,384]{1,0:T(8,128)(2,1)S(1)}, u32[]{:S(2)}, u32[]{:S(2)}) collective-permute-start(bf16[256,384]{1,0:T(8,128)(2,1)S(1)} %bitcast.94), channel_id=1, source_target_pairs={{0,56},{8,0},{16,8},{24,16},{32,24},{40,32},{48,40},{56,48},{1,57}... | collective-permute-start | bytes 589832 | tf_op jit(solution)/shard_map/ppermute | solution.py:50
  76.4 2.0 collective-permute-done.5.refs_1_
  78.4 1.9 collective-permute-start.6
  80.3 0.6 fusion.52
  80.9 0.8 constant_dynamic-slice_fusion.4
  81.7 4.6 %collective-permute-start.10 = (bf16[256,384]{1,0:T(8,128)(2,1)S(1)}, bf16[256,384]{1,0:T(8,128)(2,1)S(1)}, u32[]{:S(2)}, u32[]{:S(2)}) collective-permute-start(bf16[256,384]{1,0:T(8,128)(2,1)S(1)} %collective-permute-done.9.refs_5_), channel_id=1, source_target_pairs={{0,56},{8,0},{16,8},{24,16},{32,24},{40,32},{48,40},{56,48},{1,57}... | collective-permute-start | bytes 589832 | tf_op jit(solution)/shard_map/ppermute | solution.py:50
  86.2 1.0 collective-permute-done.6.refs_2_
  87.3 1.9 collective-permute-start.7
  89.2 0.6 pad_add_fusion.spot
  89.8 4.9 %collective-permute-start.11 = (bf16[256,384]{1,0:T(8,128)(2,1)S(1)}, bf16[256,384]{1,0:T(8,128)(2,1)S(1)}, u32[]{:S(2)}, u32[]{:S(2)}) collective-permute-start(bf16[256,384]{1,0:T(8,128)(2,1)S(1)} %collective-permute-done.10.refs_6_), channel_id=1, source_target_pairs={{0,56},{8,0},{16,8},{24,16},{32,24},{40,32},{48,40},{56,48},{1,57}... | collective-permute-start | bytes 589832 | tf_op jit(solution)/shard_map/ppermute | solution.py:50
  95.1 1.9 collective-permute-start.8
  97.0 1.3 fusion.51
  98.3 4.4 %collective-permute-done.8.refs_4_ = bf16[256,384]{1,0:T(8,128)(2,1)S(1)} collective-permute-done((bf16[256,384]{1,0:T(8,128)(2,1)S(1)}, bf16[256,384]{1,0:T(8,128)(2,1)S(1)}, u32[]{:S(2)}, u32[]{:S(2)}) %collective-permute-start.8) | collective-permute-done | bytes 196640 | tf_op jit(solution)/shard_map/ppermute | solution.py:50
  102.7 0.7 copy-done.25
  103.4 6.9 %shard_map.155 = (bf16[4,256,384]{2,1,0:T(8,128)(2,1)}, f32[4,16,256]{2,1,0:T(8,128)}) custom-call(s32[3]{0:T(128)} %pad_add_fusion.spot, bf16[256,384]{1,0:T(8,128)(2,1)} %bitcast.95, bf16[256,384]{1,0:T(8,128)(2,1)} %collective-permute-done.5.refs_1_, bf16[256,384]{1,0:T(8,128)(2,1)} %copy-done.21, bf16[256,384]{1,0:T(8,128)(2,1)} %copy-done.23, ...), custom_call_target="tpu_custom_call" | custom-call | flops 3000000000 | bytes 6291456 | tf_op jit(solution)/shard_map/pallas_call | solution.py:138
  110.3 1.4 add_negate_fusion
  111.7 1.2 reduce-window.6
  113.6 1.6 add_reduce_fusion
  115.3 1.5 convolution_convert_fusion
  117.0 0.9 copy.83
  117.9 7.1 %all-to-all-start.1 = ((bf16[64,16,128]{2,1,0:T(8,128)(2,1)}), bf16[64,16,128]{2,1,0:T(8,128)(2,1)S(1)}, u32[]{:S(2)}, u32[]{:S(2)}) async-start(bf16[64,16,128]{2,1,0:T(8,128)(2,1)} %copy.83), calls=%async_computation.1 | async-start | bytes 524288 | tf_op jit(solution)/shard_map/all_to_all | solution.py:25
  125.1 0.8 dynamic_slice.54
  126.3 11.7 %all-to-all-done.1 = bf16[64,16,128]{2,1,0:T(8,128)(2,1)S(1)} async-done(((bf16[64,16,128]{2,1,0:T(8,128)(2,1)}), bf16[64,16,128]{2,1,0:T(8,128)(2,1)S(1)}, u32[]{:S(2)}, u32[]{:S(2)}) %all-to-all-start.1) | async-done | bytes 262176 | tf_op jit(solution)/shard_map/all_to_all | solution.py:25
  139.1 0.7 reshape.380
  139.8 6.5 %all-to-all-start.2 = ((bf16[64,8,128]{2,1,0:T(8,128)(2,1)}), bf16[64,8,128]{2,1,0:T(8,128)(2,1)S(1)}, u32[]{:S(2)}, u32[]{:S(2)}) async-start(bf16[64,8,128]{2,1,0:T(8,128)(2,1)} %reshape.380), calls=%async_computation.2 | async-start | bytes 262144 | tf_op jit(solution)/shard_map/all_to_all | solution.py:25
  146.6 0.6 fusion.4
  147.2 10.7 %all-to-all-done.2 = bf16[64,8,128]{2,1,0:T(8,128)(2,1)S(1)} async-done(((bf16[64,8,128]{2,1,0:T(8,128)(2,1)}), bf16[64,8,128]{2,1,0:T(8,128)(2,1)S(1)}, u32[]{:S(2)}, u32[]{:S(2)}) %all-to-all-start.2) | async-done | bytes 131104 | tf_op jit(solution)/shard_map/all_to_all | solution.py:25
  158.0 1.3 slice.154.refs_0_
  159.3 1.9 collective-permute-start.13
  161.3 4.8 %collective-permute-start.12 = (bf16[2048,256]{1,0:T(8,128)(2,1)S(1)}, bf16[2048,256]{1,0:T(8,128)(2,1)}, u32[]{:S(2)}, u32[]{:S(2)}) collective-permute-start(bf16[2048,256]{1,0:T(8,128)(2,1)S(1)} %slice.154.refs_0_), channel_id=1, source_target_pairs={{0,6},{2,0},{4,2},{6,4},{1,7},{3,1},{5,3},{7,5},{8,14},{10,8},{12,... | collective-permute-start | bytes 3145736 | tf_op jit(solution)/shard_map/ppermute | solution.py:50
  166.0 1.4 multiply_reduce_fusion
  167.4 6.3 %shard_map.154 = bf16[4,256,384]{2,1,0:T(8,128)(2,1)} custom-call(s32[3]{0:T(128)} %pad_add_fusion.spot, bf16[256,1024]{1,0:T(8,128)(2,1)} %copy-done.3, bf16[256,1024]{1,0:T(8,128)(2,1)} %get-tuple-element.18.refs_1_.refs_9_, bf16[256,1024]{1,0:T(8,128)(2,1)} %copy-done.4, bf16[256,1024]{1,0:T(8,128)(2,1)} %get-tuple-element.17.refs_3_.refs_11_, ...), custom_call_target="tpu_custom_call" | custom-call | flops 3000000000 | bytes 6291456 | tf_op jit(solution)/shard_map/pallas_call | solution.py:138
  173.7 1.1 multiply_convert_fusion.2
  174.8 2.4 %collective-permute-start.4 = (bf16[4,2,128]{2,1,0:T(2,128)(2,1)S(1)}, bf16[4,2,128]{2,1,0:T(2,128)(2,1)S(1)}, u32[]{:S(2)}, u32[]{:S(2)}) collective-permute-start(bf16[4,2,128]{2,1,0:T(2,128)(2,1)S(1)} %slice.141), channel_id=1, source_target_pairs={{0,8},{8,16},{16,24},{24,32},{32,40},{40,48},{48,56},{56,64},{64,7... | collective-permute-start | bytes 6152 | tf_op jit(solution)/shard_map/ppermute | solution.py:34
  177.5 3.6 %collective-permute-done.13.refs_3_ = bf16[2048,256]{1,0:T(8,128)(2,1)S(1)} collective-permute-done((bf16[2048,256]{1,0:T(8,128)(2,1)S(1)}, bf16[2048,256]{1,0:T(8,128)(2,1)S(1)}, u32[]{:S(2)}, u32[]{:S(2)}) %collective-permute-start.13) | collective-permute-done | bytes 1048608 | tf_op jit(solution)/shard_map/ppermute | solution.py:50
  181.2 1.9 collective-permute-start.14
  183.1 1.1 slice.156
  184.2 4.6 %collective-permute-start.15 = (bf16[1024,256]{1,0:T(8,128)(2,1)S(1)}, bf16[1024,256]{1,0:T(8,128)(2,1)S(1)}, u32[]{:S(2)}, u32[]{:S(2)}) collective-permute-start(bf16[1024,256]{1,0:T(8,128)(2,1)S(1)} %slice.156), channel_id=1, source_target_pairs={{0,6},{2,0},{4,2},{6,4},{1,7},{3,1},{5,3},{7,5},{8,14},{10,8},{12,... | collective-permute-start | bytes 1572872 | tf_op jit(solution)/shard_map/ppermute | solution.py:50
  188.8 1.2 fusion.17
  190.0 1.1 fusion.13
  191.1 3.5 %all-to-all-start.3 = ((bf16[4,256,256]{2,1,0:T(8,128)(2,1)}), bf16[4,256,256]{2,1,0:T(8,128)(2,1)S(1)}, u32[]{:S(2)}, u32[]{:S(2)}) async-start(bf16[4,256,256]{2,1,0:T(8,128)(2,1)} %fusion.13), calls=%async_computation.3 | async-start | bytes 1048576 | tf_op jit(solution)/shard_map/all_to_all | solution.py:25
  194.9 1.0 pad_maximum_fusion.1.refs_2_
  195.9 7.0 %all-to-all-done.3.parts = bf16[4,256,256]{2,1,0:T(8,128)(2,1)S(1)} async-done(((bf16[4,256,256]{2,1,0:T(8,128)(2,1)}), bf16[4,256,256]{2,1,0:T(8,128)(2,1)S(1)}, u32[]{:S(2)}, u32[]{:S(2)}) %all-to-all-start.3) | async-done | bytes 524320 | tf_op jit(solution)/shard_map/all_to_all | solution.py:25
  202.9 0.8 copy-done.2
  203.7 4.6 %shard_map.156 = bf16[256,2048]{1,0:T(8,128)(2,1)} custom-call(s32[3]{0:T(128)} %pad_add_fusion.spot, bf16[4,256,256]{2,1,0:T(8,128)(2,1)} %copy-done.2, bf16[2048,256]{1,0:T(8,128)(2,1)} %copy-done.1, bf16[2048,256]{1,0:T(8,128)(2,1)} %collective-permute-done.12.refs_1_, bf16[2048,256]{1,0:T(8,128)(2,1)} %pad_maximum_fusion.1.refs_2_, ...), custom_call_target="tpu_custom_call" | custom-call | flops 2000000000 | bytes 6291456 | tf_op jit(solution)/shard_map/pallas_call | solution.py:138
  208.3 13.2 %all_to_all.25 = bf16[2,128,2048]{2,1,0:T(8,128)(2,1)S(1)} all-to-all(bf16[2,128,2048]{2,1,0:T(8,128)(2,1)} %bitcast.88), channel_id=1, replica_groups=mesh['sp_0'=8,'sp_1'=8,'fs'=4,'tp'=2] {'tp'}, dimensions={0} | all-to-all | bytes 2097152 | tf_op jit(solution)/shard_map/all_to_all | solution.py:25
  221.5 1.1 reduce_sum.42
  (117 shorter events, 4.2 us)
Async XLA Ops:
  6.5 118.5 %copy-start = (f32[3,1024]{1,0:T(4,128)S(1)}, f32[3,1024]{1,0:T(4,128)}, u32[]{:S(2)}) copy-start(f32[3,1024]{1,0:T(4,128)} %param.21) | copy-start | bytes 36868
  8.1 12.8 %copy-start.11 = (bf16[32,128]{1,0:T(8,128)(2,1)S(1)}, bf16[32,128]{1,0:T(8,128)(2,1)}, u32[]{:S(2)}) copy-start(bf16[32,128]{1,0:T(8,128)(2,1)} %param.18) | copy-start | bytes 24580
  8.1 12.8 %copy-start.12 = (bf16[32,128]{1,0:T(8,128)(2,1)S(1)}, bf16[32,128]{1,0:T(8,128)(2,1)}, u32[]{:S(2)}) copy-start(bf16[32,128]{1,0:T(8,128)(2,1)} %param.19) | copy-start | bytes 24580
  8.1 12.8 %copy-start.13 = (bf16[32,128]{1,0:T(8,128)(2,1)S(1)}, bf16[32,128]{1,0:T(8,128)(2,1)}, u32[]{:S(2)}) copy-start(bf16[32,128]{1,0:T(8,128)(2,1)} %param.20) | copy-start | bytes 24580
  8.1 12.8 %copy-start.16 = (bf16[32,128]{1,0:T(8,128)(2,1)S(1)}, bf16[32,128]{1,0:T(8,128)(2,1)}, u32[]{:S(2)}) copy-start(bf16[32,128]{1,0:T(8,128)(2,1)} %param.24) | copy-start | bytes 24580
  8.1 12.8 %copy-start.17 = (bf16[32,128]{1,0:T(8,128)(2,1)S(1)}, bf16[32,128]{1,0:T(8,128)(2,1)}, u32[]{:S(2)}) copy-start(bf16[32,128]{1,0:T(8,128)(2,1)} %param.23) | copy-start | bytes 24580
  8.1 12.8 %copy-start.18 = (bf16[32,128]{1,0:T(8,128)(2,1)S(1)}, bf16[32,128]{1,0:T(8,128)(2,1)}, u32[]{:S(2)}) copy-start(bf16[32,128]{1,0:T(8,128)(2,1)} %param.22) | copy-start | bytes 24580
  10.6 18.7 %copy-start.3 = (bf16[256,1024]{1,0:T(8,128)(2,1)}, bf16[256,1024]{1,0:T(8,128)(2,1)S(1)}, u32[]{:S(2)}) copy-start(bf16[256,1024]{1,0:T(8,128)(2,1)S(1)} %get-tuple-element.19.refs_0_.refs_8_) | copy-start | bytes 1572868
  10.6 36.4 %copy-start.14 = (bf16[128,32]{0,1:T(8,128)(2,1)S(1)}, bf16[128,32]{0,1:T(8,128)(2,1)}, u32[]{:S(2)}) copy-start(bf16[128,32]{0,1:T(8,128)(2,1)} %param.30) | copy-start | bytes 24580
  10.6 36.4 %copy-start.15 = (bf16[128,32]{0,1:T(8,128)(2,1)S(1)}, bf16[128,32]{0,1:T(8,128)(2,1)}, u32[]{:S(2)}) copy-start(bf16[128,32]{0,1:T(8,128)(2,1)} %param.31) | copy-start | bytes 24580
  10.6 17.3 %collective-permute-start = (bf16[256,1024]{1,0:T(8,128)(2,1)S(1)}, bf16[256,1024]{1,0:T(8,128)(2,1)S(1)}, u32[]{:S(2)}, u32[]{:S(2)}) collective-permute-start(bf16[256,1024]{1,0:T(8,128)(2,1)S(1)} %get-tuple-element.19.refs_0_.refs_8_), channel_id=1, source_target_pairs={{0,6},{2,0},{4,2},{6,4},{1,7},{3,1},{5,3},{7,5},{8,14},{10,8},{12,... | collective-permute-start | bytes 1572872 | tf_op jit(solution)/shard_map/ppermute | solution.py:50
  15.9 13.4 %collective-permute-start.1 = (bf16[256,1024]{1,0:T(8,128)(2,1)S(1)}, bf16[256,1024]{1,0:T(8,128)(2,1)S(1)}, u32[]{:S(2)}, u32[]{:S(2)}) collective-permute-start(bf16[256,1024]{1,0:T(8,128)(2,1)S(1)} %get-tuple-element.19.refs_0_.refs_8_), channel_id=1, source_target_pairs={{0,4},{2,6},{4,0},{6,2},{1,5},{3,7},{5,1},{7,3},{8,12},{10,14},{12... | collective-permute-start | bytes 1572872 | tf_op jit(solution)/shard_map/ppermute | solution.py:50
  18.4 26.0 %collective-permute-start.2 = (bf16[256,1024]{1,0:T(8,128)(2,1)S(1)}, bf16[256,1024]{1,0:T(8,128)(2,1)S(1)}, u32[]{:S(2)}, u32[]{:S(2)}) collective-permute-start(bf16[256,1024]{1,0:T(8,128)(2,1)S(1)} %get-tuple-element.19.refs_0_.refs_8_), channel_id=1, source_target_pairs={{0,2},{2,4},{4,6},{6,0},{1,3},{3,5},{5,7},{7,1},{8,10},{10,12},{12... | collective-permute-start | bytes 1572872 | tf_op jit(solution)/shard_map/ppermute | solution.py:50
  21.0 51.5 %copy-start.19 = (f32[2,8]{1,0:T(2,128)S(1)}, f32[2,8]{1,0:T(2,128)}, u32[]{:S(2)}) copy-start(f32[2,8]{1,0:T(2,128)} %param.27) | copy-start | bytes 196
  27.9 19.1 %copy-start.4 = (bf16[256,1024]{1,0:T(8,128)(2,1)}, bf16[256,1024]{1,0:T(8,128)(2,1)S(1)}, u32[]{:S(2)}) copy-start(bf16[256,1024]{1,0:T(8,128)(2,1)S(1)} %collective-permute-done.refs_2_.refs_10_) | copy-start | bytes 1572868
  29.3 17.6 %copy-start.5 = (bf16[256,1024]{1,0:T(8,128)(2,1)}, bf16[256,1024]{1,0:T(8,128)(2,1)S(1)}, u32[]{:S(2)}) copy-start(bf16[256,1024]{1,0:T(8,128)(2,1)S(1)} %collective-permute-done.1.refs_4_.refs_12_) | copy-start | bytes 1572868
  44.4 2.6 %copy-start.6 = (bf16[256,1024]{1,0:T(8,128)(2,1)}, bf16[256,1024]{1,0:T(8,128)(2,1)S(1)}, u32[]{:S(2)}) copy-start(bf16[256,1024]{1,0:T(8,128)(2,1)S(1)} %collective-permute-done.2.refs_6_.refs_14_) | copy-start | bytes 1572868
  44.5 52.5 %collective-permute-start.3 = (bf16[768,1024]{1,0:T(8,128)(2,1)S(1)}, bf16[768,1024]{1,0:T(8,128)(2,1)S(1)}, u32[]{:S(2)}, u32[]{:S(2)}) collective-permute-start(bf16[768,1024]{1,0:T(8,128)(2,1)S(1)} %pad_maximum_fusion), channel_id=1, source_target_pairs={{0,1},{1,0},{2,3},{3,2},{4,5},{5,4},{6,7},{7,6},{8,9},{9,8},{10,11... | collective-permute-start | bytes 4718600 | tf_op jit(solution)/shard_map/ppermute | solution.py:29
  47.0 10.8 %copy-start.10 = (bf16[32,640]{1,0:T(8,128)(2,1)}, bf16[32,640]{1,0:T(8,128)(2,1)S(1)}, u32[]{:S(2)}) copy-start(bf16[32,640]{1,0:T(8,128)(2,1)S(1)} %constant_dynamic-update-slice_fusion) | copy-start | bytes 122884
  47.7 20.8 %all-to-all-start = ((bf16[8,32,384]{2,1,0:T(8,128)(2,1)}), bf16[8,32,384]{2,1,0:T(8,128)(2,1)S(1)}, u32[]{:S(2)}, u32[]{:S(2)}) async-start(bf16[8,32,384]{2,1,0:T(8,128)(2,1)} %broadcast_in_dim.40), calls=%async_computation | async-start | bytes 393216 | tf_op jit(solution)/shard_map/all_to_all | solution.py:21
  57.8 100.3 %all-gather.2.cloned.1.call-start = ((), (), s32[]{:S(2)}) async-start(), calls=%async_computation.5 | async-start | bytes 2662400 | tf_op jit(solution)/shard_map/all_gather | solution.py:187
  68.6 34.8 %copy-start.8 = (bf16[8,32,384]{2,1,0:T(8,128)(2,1)}, bf16[8,32,384]{2,1,0:T(8,128)(2,1)S(1)}, u32[]{:S(2)}) copy-start(bf16[8,32,384]{2,1,0:T(8,128)(2,1)S(1)} %all-to-all-done) | copy-start | bytes 589828
  68.6 9.8 %collective-permute-start.5 = (bf16[256,384]{1,0:T(8,128)(2,1)S(1)}, bf16[256,384]{1,0:T(8,128)(2,1)}, u32[]{:S(2)}, u32[]{:S(2)}) collective-permute-start(bf16[256,384]{1,0:T(8,128)(2,1)S(1)} %bitcast.93), channel_id=1, source_target_pairs={{0,8},{8,16},{16,24},{24,32},{32,40},{40,48},{48,56},{56,0},{1,9},... | collective-permute-start | bytes 589832 | tf_op jit(solution)/shard_map/ppermute | solution.py:50
  72.6 9.1 %collective-permute-start.9 = (bf16[256,384]{1,0:T(8,128)(2,1)S(1)}, bf16[256,384]{1,0:T(8,128)(2,1)S(1)}, u32[]{:S(2)}, u32[]{:S(2)}) collective-permute-start(bf16[256,384]{1,0:T(8,128)(2,1)S(1)} %bitcast.94), channel_id=1, source_target_pairs={{0,56},{8,0},{16,8},{24,16},{32,24},{40,32},{48,40},{56,48},{1,57}... | collective-permute-start | bytes 589832 | tf_op jit(solution)/shard_map/ppermute | solution.py:50
  78.4 8.9 %collective-permute-start.6 = (bf16[256,384]{1,0:T(8,128)(2,1)}, bf16[256,384]{1,0:T(8,128)(2,1)S(1)}, u32[]{:S(2)}, u32[]{:S(2)}) collective-permute-start(bf16[256,384]{1,0:T(8,128)(2,1)} %collective-permute-done.5.refs_1_), channel_id=1, source_target_pairs={{0,8},{8,16},{16,24},{24,32},{32,40},{40,48},{48,56},{56,0},{1,9},... | collective-permute-start | bytes 589832 | tf_op jit(solution)/shard_map/ppermute | solution.py:50
  81.6 13.5 %copy-start.20 = (bf16[256,384]{1,0:T(8,128)(2,1)}, bf16[256,384]{1,0:T(8,128)(2,1)S(1)}, u32[]{:S(2)}) copy-start(bf16[256,384]{1,0:T(8,128)(2,1)S(1)} %collective-permute-done.9.refs_5_) | copy-start | bytes 589828
  81.7 8.1 %collective-permute-start.10 = (bf16[256,384]{1,0:T(8,128)(2,1)S(1)}, bf16[256,384]{1,0:T(8,128)(2,1)S(1)}, u32[]{:S(2)}, u32[]{:S(2)}) collective-permute-start(bf16[256,384]{1,0:T(8,128)(2,1)S(1)} %collective-permute-done.9.refs_5_), channel_id=1, source_target_pairs={{0,56},{8,0},{16,8},{24,16},{32,24},{40,32},{48,40},{56,48},{1,57}... | collective-permute-start | bytes 589832 | tf_op jit(solution)/shard_map/ppermute | solution.py:50
  87.3 9.8 %copy-start.21 = (bf16[256,384]{1,0:T(8,128)(2,1)}, bf16[256,384]{1,0:T(8,128)(2,1)S(1)}, u32[]{:S(2)}) copy-start(bf16[256,384]{1,0:T(8,128)(2,1)S(1)} %collective-permute-done.6.refs_2_) | copy-start | bytes 589828
  87.3 7.8 %collective-permute-start.7 = (bf16[256,384]{1,0:T(8,128)(2,1)S(1)}, bf16[256,384]{1,0:T(8,128)(2,1)S(1)}, u32[]{:S(2)}, u32[]{:S(2)}) collective-permute-start(bf16[256,384]{1,0:T(8,128)(2,1)S(1)} %collective-permute-done.6.refs_2_), channel_id=1, source_target_pairs={{0,8},{8,16},{16,24},{24,32},{32,40},{40,48},{48,56},{56,0},{1,9},... | collective-permute-start | bytes 589832 | tf_op jit(solution)/shard_map/ppermute | solution.py:50
  89.8 8.5 %copy-start.22 = (bf16[256,384]{1,0:T(8,128)(2,1)}, bf16[256,384]{1,0:T(8,128)(2,1)S(1)}, u32[]{:S(2)}) copy-start(bf16[256,384]{1,0:T(8,128)(2,1)S(1)} %collective-permute-done.10.refs_6_) | copy-start | bytes 589828
  89.8 8.5 %collective-permute-start.11 = (bf16[256,384]{1,0:T(8,128)(2,1)S(1)}, bf16[256,384]{1,0:T(8,128)(2,1)S(1)}, u32[]{:S(2)}, u32[]{:S(2)}) collective-permute-start(bf16[256,384]{1,0:T(8,128)(2,1)S(1)} %collective-permute-done.10.refs_6_), channel_id=1, source_target_pairs={{0,56},{8,0},{16,8},{24,16},{32,24},{40,32},{48,40},{56,48},{1,57}... | collective-permute-start | bytes 589832 | tf_op jit(solution)/shard_map/ppermute | solution.py:50
  95.1 3.2 %copy-start.23 = (bf16[256,384]{1,0:T(8,128)(2,1)}, bf16[256,384]{1,0:T(8,128)(2,1)S(1)}, u32[]{:S(2)}) copy-start(bf16[256,384]{1,0:T(8,128)(2,1)S(1)} %collective-permute-done.7.refs_3_) | copy-start | bytes 589828
  95.1 7.6 %collective-permute-start.8 = (bf16[256,384]{1,0:T(8,128)(2,1)S(1)}, bf16[256,384]{1,0:T(8,128)(2,1)S(1)}, u32[]{:S(2)}, u32[]{:S(2)}) collective-permute-start(bf16[256,384]{1,0:T(8,128)(2,1)S(1)} %collective-permute-done.7.refs_3_), channel_id=1, source_target_pairs={{0,8},{8,16},{16,24},{24,32},{32,40},{40,48},{48,56},{56,0},{1,9},... | collective-permute-start | bytes 589832 | tf_op jit(solution)/shard_map/ppermute | solution.py:50
  98.3 4.4 %copy-start.24 = (bf16[256,384]{1,0:T(8,128)(2,1)}, bf16[256,384]{1,0:T(8,128)(2,1)S(1)}, u32[]{:S(2)}) copy-start(bf16[256,384]{1,0:T(8,128)(2,1)S(1)} %collective-permute-done.11.refs_7_) | copy-start | bytes 589828
  102.7 0.7 copy-start.25
  116.8 29.8 %copy-start.9 = (bf16[4,256,384]{2,1,0:T(8,128)(2,1)S(1)}, bf16[4,256,384]{2,1,0:T(8,128)(2,1)}, u32[]{:S(2)}) copy-start(bf16[4,256,384]{2,1,0:T(8,128)(2,1)} %get-tuple-element.12) | copy-start | bytes 2359300
  117.9 20.1 %all-to-all-start.1 = ((bf16[64,16,128]{2,1,0:T(8,128)(2,1)}), bf16[64,16,128]{2,1,0:T(8,128)(2,1)S(1)}, u32[]{:S(2)}, u32[]{:S(2)}) async-start(bf16[64,16,128]{2,1,0:T(8,128)(2,1)} %copy.83), calls=%async_computation.1 | async-start | bytes 524288 | tf_op jit(solution)/shard_map/all_to_all | solution.py:25
  139.8 18.1 %all-to-all-start.2 = ((bf16[64,8,128]{2,1,0:T(8,128)(2,1)}), bf16[64,8,128]{2,1,0:T(8,128)(2,1)S(1)}, u32[]{:S(2)}, u32[]{:S(2)}) async-start(bf16[64,8,128]{2,1,0:T(8,128)(2,1)} %reshape.380), calls=%async_computation.2 | async-start | bytes 262144 | tf_op jit(solution)/shard_map/all_to_all | solution.py:25
  159.3 14.4 %copy-start.1 = (bf16[2048,256]{1,0:T(8,128)(2,1)}, bf16[2048,256]{1,0:T(8,128)(2,1)S(1)}, u32[]{:S(2)}) copy-start(bf16[2048,256]{1,0:T(8,128)(2,1)S(1)} %slice.154.refs_0_) | copy-start | bytes 3145732
  159.3 21.8 %collective-permute-start.13 = (bf16[2048,256]{1,0:T(8,128)(2,1)S(1)}, bf16[2048,256]{1,0:T(8,128)(2,1)S(1)}, u32[]{:S(2)}, u32[]{:S(2)}) collective-permute-start(bf16[2048,256]{1,0:T(8,128)(2,1)S(1)} %slice.154.refs_0_), channel_id=1, source_target_pairs={{0,2},{2,4},{4,6},{6,0},{1,3},{3,5},{5,7},{7,1},{8,10},{10,12},{12... | collective-permute-start | bytes 3145736 | tf_op jit(solution)/shard_map/ppermute | solution.py:50
  161.3 21.8 %collective-permute-start.12 = (bf16[2048,256]{1,0:T(8,128)(2,1)S(1)}, bf16[2048,256]{1,0:T(8,128)(2,1)}, u32[]{:S(2)}, u32[]{:S(2)}) collective-permute-start(bf16[2048,256]{1,0:T(8,128)(2,1)S(1)} %slice.154.refs_0_), channel_id=1, source_target_pairs={{0,6},{2,0},{4,2},{6,4},{1,7},{3,1},{5,3},{7,5},{8,14},{10,8},{12,... | collective-permute-start | bytes 3145736 | tf_op jit(solution)/shard_map/ppermute | solution.py:50
  174.8 13.9 %collective-permute-start.4 = (bf16[4,2,128]{2,1,0:T(2,128)(2,1)S(1)}, bf16[4,2,128]{2,1,0:T(2,128)(2,1)S(1)}, u32[]{:S(2)}, u32[]{:S(2)}) collective-permute-start(bf16[4,2,128]{2,1,0:T(2,128)(2,1)S(1)} %slice.141), channel_id=1, source_target_pairs={{0,8},{8,16},{16,24},{24,32},{32,40},{40,48},{48,56},{56,64},{64,7... | collective-permute-start | bytes 6152 | tf_op jit(solution)/shard_map/ppermute | solution.py:34
  181.1 8.9 %copy-start.7 = (bf16[2048,256]{1,0:T(8,128)(2,1)}, bf16[2048,256]{1,0:T(8,128)(2,1)S(1)}, u32[]{:S(2)}) copy-start(bf16[2048,256]{1,0:T(8,128)(2,1)S(1)} %collective-permute-done.13.refs_3_) | copy-start | bytes 3145732
  181.2 13.5 %collective-permute-start.14 = (bf16[1024,256]{1,0:T(8,128)(2,1)S(1)}, bf16[1024,256]{1,0:T(8,128)(2,1)S(1)}, u32[]{:S(2)}, u32[]{:S(2)}) collective-permute-start(bf16[1024,256]{1,0:T(8,128)(2,1)S(1)} %slice.155), channel_id=1, source_target_pairs={{0,2},{2,4},{4,6},{6,0},{1,3},{3,5},{5,7},{7,1},{8,10},{10,12},{12... | collective-permute-start | bytes 1572872 | tf_op jit(solution)/shard_map/ppermute | solution.py:50
  184.2 10.7 %collective-permute-start.15 = (bf16[1024,256]{1,0:T(8,128)(2,1)S(1)}, bf16[1024,256]{1,0:T(8,128)(2,1)S(1)}, u32[]{:S(2)}, u32[]{:S(2)}) collective-permute-start(bf16[1024,256]{1,0:T(8,128)(2,1)S(1)} %slice.156), channel_id=1, source_target_pairs={{0,6},{2,0},{4,2},{6,4},{1,7},{3,1},{5,3},{7,5},{8,14},{10,8},{12,... | collective-permute-start | bytes 1572872 | tf_op jit(solution)/shard_map/ppermute | solution.py:50
  191.1 11.8 %all-to-all-start.3 = ((bf16[4,256,256]{2,1,0:T(8,128)(2,1)}), bf16[4,256,256]{2,1,0:T(8,128)(2,1)S(1)}, u32[]{:S(2)}, u32[]{:S(2)}) async-start(bf16[4,256,256]{2,1,0:T(8,128)(2,1)} %fusion.13), calls=%async_computation.3 | async-start | bytes 1048576 | tf_op jit(solution)/shard_map/all_to_all | solution.py:25
  202.9 0.8 copy-start.2
Sparse Core Ops, SparseCore 0:
  61.6 81.1 all-gather.1

commit v6 on v5

--- a/solution.py
+++ b/solution.py
@@ -8,9 +8,11 @@
 
 
 HEAD_DIM = 128
-SP = ("sp_0", "sp_1")
-SP_TP = ("sp_0", "sp_1", "tp")
+Y = ("y_hi", "y_lo")
+SP = ("z", *Y)
+SP_TP = (*SP, "tp")
 EPSILON = 1e-06
+FAR_BELOW = -1e30
 HIGHEST = lax.Precision.HIGHEST
 F32 = jnp.float32
 BF16 = jnp.bfloat16
@@ -39,6 +41,25 @@
     second = lax.reduce_precision(x - first, 8, 7)
     third = lax.reduce_precision(x - first - second, 8, 7)
     return jnp.stack([first, second, third])
+
+
+def numbers_row(total, peak):
+    numbers = thirds(jnp.stack([total, peak])).astype(BF16).reshape(1, -1)
+    return jnp.pad(numbers, ((0, 0), (0, HEAD_DIM - numbers.shape[1])))
+
+
+def numbers_of(rows, seqs):
+    found = rows[:, : 6 * seqs].astype(F32).reshape(-1, 3, 2, seqs)
+    found = found[:, 0] + found[:, 1] + found[:, 2]
+    return found[:, 0].T, found[:, 1].T
+
+
+def segment_logs(totals, peaks, earlier, after):
+    masked = jnp.where(earlier, totals[:, None, :], 0.0)
+    dims = (((2,), (0,)), ((), ()))
+    between = lax.dot_general(masked, after, dims, precision=HIGHEST)
+    logs = jnp.where(earlier, between + peaks[:, None, :], -jnp.inf)
+    return jnp.sum(masked, axis=-1), logs
 
 
 def dot(a, b, dims):
@@ -67,18 +88,6 @@
     size = array.shape[0]
     twice = jnp.concatenate([array, array], axis=0)
     return lax.dynamic_slice_in_dim(twice, (size - by) % size, size, 0)
-
-
-def ring_gather(array, axis):
-    behind, ahead = [array], [array]
-    for k in range(4):
-        behind.append(ring(behind[-1], axis, 1))
-        if k < 3:
-            ahead.append(ring(ahead[-1], axis, -1))
-    return behind + ahead[1:]
-
-
-OFFSETS = (0, 7, 6, 5, 4, 1, 2, 3)
 
 
 def matmuls(core, pieces, weights, left, out):
@@ -101,14 +110,14 @@
 
 
 def project_mem_kernel(spot, *refs):
-    parts, pieces, gate_rows = refs[:8], refs[8:16], refs[16]
-    out, gates, weights = refs[17:]
+    parts, pieces, gate_rows = refs[:4], refs[4:12], refs[12]
+    out, gates, weights = refs[13:]
     core = spot[0]
-    for part, offset in zip(parts, OFFSETS):
-        place = (spot[2] + offset) % 8
-        for k in range(8):
-            start = pl.multiple_of((k * 8 + place) * 32, 32)
-            weights[pl.ds(start, 32), :] = part[pl.ds(k * 32, 32), :]
+    for k in range(4):
+        place = (spot[2] + k) % 4
+        for z in range(8):
+            start = pl.multiple_of((z * 4 + place) * 64, 64)
+            weights[pl.ds(start, 64), :] = parts[k][pl.ds(z * 64, 64), :]
     matmuls(core, pieces, weights, 0, out)
     dims = (((1,), (1,)), ((), ()))
     for k in range(4):
@@ -172,7 +181,7 @@
     place_x = lax.axis_index("fs")
     order = [(place_x + by) % seqs for by in range(seqs)]
 
-    place_y = lax.axis_index("sp_1")
+    place_y = lax.axis_index("y_hi")
     spot = jnp.stack([core, place_x, place_y]).astype(jnp.int32)
 
     channels = w_conv_gate.shape[1]
@@ -181,8 +190,8 @@
     )
     w_mem = jnp.concatenate([w_query, w_key, w_value], axis=1)
     w_rest, w_mem = lax.optimization_barrier((w_rest, w_mem))
-    w_mem = everyone(w_mem, "sp_0").reshape(-1, w_mem.shape[1])
-    w_mem = ring_gather(w_mem, "sp_1")
+    w_mem = everyone(w_mem, ("z", "y_lo")).reshape(-1, w_mem.shape[1])
+    w_mem = (w_mem, *relayed(w_mem, "y_hi"))
 
     w_rest = lax.all_gather(w_rest, SP, axis=0, tiled=True)
     w_own = w_rest[:, 3 * channels :]
@@ -231,37 +240,48 @@
     weighted = (local_weights[..., None] * value.astype(F32)).astype(BF16)
     state = dot(weighted, key, (((1,), (1,)), ((0,), (0,))))
 
-    places = lax.axis_size(SP)
+    places = lax.axis_size(Y)
     cut = HEAD_DIM // places
     slices = state.astype(BF16).reshape(seqs, places, cut, HEAD_DIM).transpose(1, 0, 2, 3)
     slices = slices.reshape(places, seqs * cut, HEAD_DIM)
-    numbers = thirds(jnp.stack([total, peak])).astype(BF16).reshape(1, 1, -1)
-    count = numbers.shape[2]
-    numbers = jnp.pad(numbers, ((0, 0), (0, seqs * cut - 1), (0, HEAD_DIM - count)))
-    numbers = jnp.broadcast_to(numbers, slices.shape)
+    numbers = jnp.broadcast_to(numbers_row(total, peak), (places, 16, HEAD_DIM))
     packed = jnp.concatenate([slices, numbers], axis=1)
-    everywhere = exchanged(packed, SP)
-    found = everywhere[:, seqs * cut, :count].astype(F32).reshape(places, 3, 2, seqs)
-    found = found[:, 0] + found[:, 1] + found[:, 2]
-    totals, peaks = found[:, 0].T, found[:, 1].T
+    packed = exchanged(packed, Y)
     line = jnp.arange(places)
-    earlier = line[:, None] > line[None, :]
-    masked = jnp.where(earlier, totals[:, None, :], 0.0)
-    between = lax.dot_general(
-        masked, earlier.astype(F32), (((2,), (0,)), ((), ())), precision=HIGHEST
-    )
-    since_start = jnp.sum(masked, axis=-1)
-    logs = jnp.where(earlier, between + peaks[:, None, :], -jnp.inf)
-    carried_peak = jnp.maximum(since_start, jnp.max(logs, axis=-1))
-    mixing = jnp.exp(logs - carried_peak[..., None]).astype(BF16)
-    states = everywhere[:, : seqs * cut].reshape(places, seqs, cut * HEAD_DIM)
-    carried = dot(mixing, states, (((2,), (0,)), ((0,), (1,)))).astype(BF16)
-    carried = carried.transpose(1, 0, 2).reshape(places, seqs * cut, HEAD_DIM)
-    carried = exchanged(carried, SP)
+    after = (line[:, None] > line[None, :]).astype(F32)
+    totals, peaks = numbers_of(packed[:, seqs * cut], seqs)
+    states = packed[:, : seqs * cut].reshape(places, seqs, cut * HEAD_DIM)
+    earlier = jnp.arange(places + 1)[:, None] > line[None, :]
+    sums_in, logs = segment_logs(totals, peaks, earlier, after)
+    peak_in = jnp.maximum(jnp.max(logs, axis=-1), FAR_BELOW)
+    row_mixing = jnp.exp(logs[:, places] - peak_in[:, places, None])
+    row_state = jnp.einsum("sj,jsk->sk", row_mixing.astype(BF16), states, preferred_element_type=F32)
+    row_numbers = jnp.broadcast_to(
+        numbers_row(sums_in[:, places], peak_in[:, places]), (16, HEAD_DIM)
+    )
+    row_packed = jnp.concatenate(
+        [row_state.astype(BF16).reshape(seqs * cut, HEAD_DIM), row_numbers], axis=0
+    )
+    row_packed = everyone(row_packed, "z")
+    row_totals, row_peaks = numbers_of(row_packed[:, seqs * cut], seqs)
+    row_states = row_packed[:, : seqs * cut].reshape(places, seqs, cut * HEAD_DIM)
+    earlier_rows = (line < lax.axis_index("z"))[None]
+    before, row_logs = segment_logs(row_totals, row_peaks, earlier_rows, after)
+    start_peak = jnp.maximum(before, jnp.max(row_logs, axis=-1))
+    start_mixing = jnp.exp(row_logs - start_peak[..., None])[:, 0]
+    start_state = jnp.einsum(
+        "sj,jsk->sk", start_mixing.astype(BF16), row_states, preferred_element_type=F32
+    )
+    moved = sums_in[:, :places] + start_peak
+    carried_peak = jnp.maximum(moved, peak_in[:, :places])
+    mixing = jnp.exp(logs[:, :places] - carried_peak[..., None]).astype(BF16)
+    carried = jnp.einsum("spj,jsk->spk", mixing, states, preferred_element_type=F32)
+    carried = carried + jnp.exp(moved - carried_peak)[..., None] * start_state[:, None]
+    carried = carried.astype(BF16).transpose(1, 0, 2).reshape(places, seqs * cut, HEAD_DIM)
+    carried = exchanged(carried, Y)
     carried = carried.reshape(places, seqs, cut, HEAD_DIM).transpose(1, 0, 2, 3)
     prior_state = carried.reshape(seqs, HEAD_DIM, HEAD_DIM)
-    place = lax.axis_index(SP)
-    prior_peak = lax.dynamic_slice_in_dim(carried_peak, place, 1, 1)
+    prior_peak = lax.dynamic_slice_in_dim(carried_peak, lax.axis_index(Y), 1, 1)
 
     (conv,) = call(
         project_conv_kernel,
@@ -307,9 +327,8 @@
 
 
 def solution(mesh):
-    finer = Mesh(
-        mesh.devices.reshape(8, 8, mesh.shape["fs"], mesh.shape["tp"]), ("sp_0", "sp_1", "fs", "tp")
-    )
+    sizes = (8, 4, 2, mesh.shape["fs"], mesh.shape["tp"])
+    finer = Mesh(mesh.devices.reshape(sizes), (*SP, "fs", "tp"))
     weights = P(SP, ("fs", "tp"))
     return jax.shard_map(
         shards,

time: 231 us -> 232 us (level)
  waiting for transfers between devices: 74.5 us -> 65.7 us
  local copies, waits for them, and re-layouts: 13.3 us -> 18.1 us
  other arithmetic: 14.8 us -> 19 us
    all_to_all x1 -> x2, starting transfers between devices: 10 us -> 21.8 us  [everyone(): return lax.all_to_all(copies, axis, split_axis=0, concat_axis=0, tiled=True)]
    all_to_all x3, waiting for transfers between devices: 29.4 us -> 22.9 us  [exchanged(): return lax.all_to_all(array, axis, split_axis=0, concat_axis=0, tiled=True)]
    all_to_all x3, starting transfers between devices: 17.1 us -> 11.3 us  [exchanged(): return lax.all_to_all(array, axis, split_axis=0, concat_axis=0, tiled=True)]
    ppermute x14 -> x11, starting transfers between devices: 45.6 us -> 40.8 us  [ring(): lax.ppermute(array, axis, [(i, (i + by) % peers) for i in range(peers)])]
    all_to_all x1 -> x2, waiting for transfers between devices: 9.25 us -> 7.16 us  [everyone(): return lax.all_to_all(copies, axis, split_axis=0, concat_axis=0, tiled=True)]
    ppermute x14 -> x11, waiting for transfers between devices: 35.1 us -> 35.6 us  [ring(): lax.ppermute(array, axis, [(i, (i + by) % peers) for i in range(peers)])]
  transfers between devices with their start and end apart: 21 -> 19, of which waited for: 13 -> 10; matrix products, arithmetic and copies ran while one was open for 10% -> 15% of each run, Pallas kernels for 6% -> 6%
where the time goes in v6:
time: 232 us; the launch traced here: 231 us
  starting transfers between devices  78.6 us (34%)
  waiting for transfers between devices  65.7 us (28%)
  other arithmetic  19 us (8%)
  local copies, waits for them, and re-layouts  18.1 us (8%)
  Pallas kernels  17.7 us (8%)
  between operations  14.2 us (6%)
  blocking collectives  12.6 us (5%)
  matrix products  4.66 us (2%)
    ppermute x11, starting transfers between devices, ring(): lax.ppermute(array, axis, [(i, (i + by) % peers) for i in range(peers)])  40.8 us
    ppermute x11, waiting for transfers between devices, ring(): lax.ppermute(array, axis, [(i, (i + by) % peers) for i in range(peers)])  35.6 us
    all_to_all x3, waiting for transfers between devices, exchanged(): return lax.all_to_all(array, axis, split_axis=0, concat_axis=0, tiled=True)  22.9 us
    all_to_all x2, starting transfers between devices, everyone(): return lax.all_to_all(copies, axis, split_axis=0, concat_axis=0, tiled=True)  21.8 us
    pallas_call x3, Pallas kernels, call(): pl.pallas_call(kernel, out_shape=tuple((jax.ShapeDtypeStruct(shape, dtype...  17.7 us
    all_to_all x1, blocking collectives, exchanged(): return lax.all_to_all(array, axis, split_axis=0, concat_axis=0, tiled=True)  12.6 us
    all_to_all x3, starting transfers between devices, exchanged(): return lax.all_to_all(array, axis, split_axis=0, concat_axis=0, tiled=True)  11.3 us
    all_to_all x2, waiting for transfers between devices, everyone(): return lax.all_to_all(copies, axis, split_axis=0, concat_axis=0, tiled=True)  7.16 us
  transfers between devices with their start and end apart: 19, of which 10 were waited for; matrix products, arithmetic and copies ran while one was open for 15% of the time, Pallas kernels for 6%

profile of v6, /device:TPU:1, one launch (start us, length us, event | category | flops | bytes accessed | tf_op | source)
XLA Modules:
  0.0 230.5 jit_solution(4784366831506944200)
XLA Ops:
  6.5 1.5 fusion.2
  8.2 1.6 fusion.4
  9.7 0.9 constant_dynamic-slice_fusion.9
  10.6 5.2 %collective-permute-start = (bf16[256,1024]{1,0:T(8,128)(2,1)S(1)}, bf16[256,1024]{1,0:T(8,128)(2,1)S(1)}, u32[]{:S(2)}, u32[]{:S(2)}) collective-permute-start(bf16[256,1024]{1,0:T(8,128)(2,1)S(1)} %get-tuple-element.21.refs_0_.refs_4_), channel_id=1, source_target_pairs={{0,6},{2,0},{4,2},{6,4},{1,7},{3,1},{5,3},{7,5},{8,14},{10,8},{12,... | collective-permute-start | bytes 1572872 | tf_op jit(solution)/shard_map/ppermute | solution.py:71
  15.8 2.4 %collective-permute-start.1 = (bf16[256,1024]{1,0:T(8,128)(2,1)S(1)}, bf16[256,1024]{1,0:T(8,128)(2,1)S(1)}, u32[]{:S(2)}, u32[]{:S(2)}) collective-permute-start(bf16[256,1024]{1,0:T(8,128)(2,1)S(1)} %get-tuple-element.21.refs_0_.refs_4_), channel_id=1, source_target_pairs={{0,4},{2,6},{4,0},{6,2},{1,5},{3,7},{5,1},{7,3},{8,12},{10,14},{12... | collective-permute-start | bytes 1572872 | tf_op jit(solution)/shard_map/ppermute | solution.py:71
  18.3 2.5 %collective-permute-start.2 = (bf16[256,1024]{1,0:T(8,128)(2,1)S(1)}, bf16[256,1024]{1,0:T(8,128)(2,1)}, u32[]{:S(2)}, u32[]{:S(2)}) collective-permute-start(bf16[256,1024]{1,0:T(8,128)(2,1)S(1)} %get-tuple-element.21.refs_0_.refs_4_), channel_id=1, source_target_pairs={{0,2},{2,4},{4,6},{6,0},{1,3},{3,5},{5,7},{7,1},{8,10},{10,12},{12... | collective-permute-start | bytes 1572872 | tf_op jit(solution)/shard_map/ppermute | solution.py:71
  20.9 0.8 broadcast_in_dim.93
  21.7 11.2 %all-to-all-start = ((bf16[16,32,384]{2,1,0:T(8,128)(2,1)}), bf16[16,32,384]{2,1,0:T(8,128)(2,1)S(1)}, u32[]{:S(2)}, u32[]{:S(2)}) async-start(bf16[16,32,384]{2,1,0:T(8,128)(2,1)} %broadcast_in_dim.93), calls=%async_computation | async-start | bytes 786432 | tf_op jit(solution)/shard_map/all_to_all | solution.py:23
  33.0 11.4 %collective-permute-done.2.refs_6_.refs_10_ = bf16[256,1024]{1,0:T(8,128)(2,1)} collective-permute-done((bf16[256,1024]{1,0:T(8,128)(2,1)S(1)}, bf16[256,1024]{1,0:T(8,128)(2,1)}, u32[]{:S(2)}, u32[]{:S(2)}) %collective-permute-start.2) | collective-permute-done | bytes 524320 | tf_op jit(solution)/shard_map/ppermute | solution.py:71
  44.4 1.2 pad_maximum_fusion
  45.6 2.4 %collective-permute-start.3 = (bf16[768,1024]{1,0:T(8,128)(2,1)S(1)}, bf16[768,1024]{1,0:T(8,128)(2,1)S(1)}, u32[]{:S(2)}, u32[]{:S(2)}) collective-permute-start(bf16[768,1024]{1,0:T(8,128)(2,1)S(1)} %pad_maximum_fusion), channel_id=1, source_target_pairs={{0,1},{1,0},{2,3},{3,2},{4,5},{5,4},{6,7},{7,6},{8,9},{9,8},{10,11... | collective-permute-start | bytes 4718600 | tf_op jit(solution)/shard_map/ppermute | solution.py:31
  48.0 1.4 constant_dynamic-slice_fusion.6
  49.4 4.2 %collective-permute-start.6 = (bf16[512,384]{1,0:T(8,128)(2,1)S(1)}, bf16[512,384]{1,0:T(8,128)(2,1)}, u32[]{:S(2)}, u32[]{:S(2)}) collective-permute-start(bf16[512,384]{1,0:T(8,128)(2,1)S(1)} %bitcast.135), channel_id=1, source_target_pairs={{0,16},{16,32},{32,48},{48,0},{1,17},{17,33},{33,49},{49,1},{2,18}... | collective-permute-start | bytes 1179656 | tf_op jit(solution)/shard_map/ppermute | solution.py:71
  53.7 3.6 %collective-permute-start.5 = (bf16[512,384]{1,0:T(8,128)(2,1)S(1)}, bf16[512,384]{1,0:T(8,128)(2,1)}, u32[]{:S(2)}, u32[]{:S(2)}) collective-permute-start(bf16[512,384]{1,0:T(8,128)(2,1)S(1)} %bitcast.136), channel_id=1, source_target_pairs={{0,48},{16,0},{32,16},{48,32},{1,49},{17,1},{33,17},{49,33},{2,50}... | collective-permute-start | bytes 1179656 | tf_op jit(solution)/shard_map/ppermute | solution.py:71
  57.2 1.3 maximum_bitcast_fusion
  58.6 0.7 pad.13
  59.3 0.6 copy.125
  59.9 0.7 constant_dynamic-slice_fusion.5
  61.3 1.3 constant_dynamic-slice_fusion.4
  62.6 7.4 %collective-permute-done.6.refs_3_ = bf16[512,384]{1,0:T(8,128)(2,1)} collective-permute-done((bf16[512,384]{1,0:T(8,128)(2,1)S(1)}, bf16[512,384]{1,0:T(8,128)(2,1)}, u32[]{:S(2)}, u32[]{:S(2)}) %collective-permute-start.6) | collective-permute-done | bytes 393248 | tf_op jit(solution)/shard_map/ppermute | solution.py:71
  70.0 0.9 slice.214
  70.9 6.4 %collective-permute-start.7 = (bf16[256,384]{1,0:T(8,128)(2,1)S(1)}, bf16[256,384]{1,0:T(8,128)(2,1)S(1)}, u32[]{:S(2)}, u32[]{:S(2)}) collective-permute-start(bf16[256,384]{1,0:T(8,128)(2,1)S(1)} %slice.214), channel_id=1, source_target_pairs={{0,16},{16,32},{32,48},{48,0},{1,17},{17,33},{33,49},{49,1},{2,18}... | collective-permute-start | bytes 589832 | tf_op jit(solution)/shard_map/ppermute | solution.py:71
  77.6 0.9 slice.215
  78.5 3.3 %collective-permute-start.8 = (bf16[256,384]{1,0:T(8,128)(2,1)S(1)}, bf16[256,384]{1,0:T(8,128)(2,1)S(1)}, u32[]{:S(2)}, u32[]{:S(2)}) collective-permute-start(bf16[256,384]{1,0:T(8,128)(2,1)S(1)} %slice.215), channel_id=1, source_target_pairs={{0,48},{16,0},{32,16},{48,32},{1,49},{17,1},{33,17},{49,33},{2,50}... | collective-permute-start | bytes 589832 | tf_op jit(solution)/shard_map/ppermute | solution.py:71
  81.9 0.7 pad_add_fusion.spot
  83.1 11.2 %collective-permute-done.8 = bf16[256,384]{1,0:T(8,128)(2,1)S(1)} collective-permute-done((bf16[256,384]{1,0:T(8,128)(2,1)S(1)}, bf16[256,384]{1,0:T(8,128)(2,1)S(1)}, u32[]{:S(2)}, u32[]{:S(2)}) %collective-permute-start.8) | collective-permute-done | bytes 196640 | tf_op jit(solution)/shard_map/ppermute | solution.py:71
  94.3 0.8 pad_maximum_fusion.2.refs_2_
  95.0 1.2 fusion.74
  96.3 6.8 %shard_map.155 = (bf16[4,256,384]{2,1,0:T(8,128)(2,1)}, f32[4,16,256]{2,1,0:T(8,128)}) custom-call(s32[3]{0:T(128)} %pad_add_fusion.spot, bf16[512,384]{1,0:T(8,128)(2,1)} %bitcast.137, bf16[512,384]{1,0:T(8,128)(2,1)} %collective-permute-done.5.refs_1_, bf16[512,384]{1,0:T(8,128)(2,1)} %pad_maximum_fusion.2.refs_2_, ...), custom_call_target="tpu_custom_call" | custom-call | flops 3000000000 | bytes 6291456 | tf_op jit(solution)/shard_map/pallas_call | solution.py:147
  103.1 1.4 add_negate_fusion
  104.5 1.2 reduce-window.6
  106.4 1.6 add_reduce_fusion
  108.0 1.6 convolution_convert_fusion
  109.8 0.7 pad_maximum_fusion.3
  110.5 4.5 %all-to-all-start.1 = ((bf16[8,80,128]{2,1,0:T(8,128)(2,1)}), bf16[8,80,128]{2,1,0:T(8,128)(2,1)S(1)}, u32[]{:S(2)}, u32[]{:S(2)}) async-start(bf16[8,80,128]{2,1,0:T(8,128)(2,1)} %pad_maximum_fusion.3), calls=%async_computation.1 | async-start | bytes 327680 | tf_op jit(solution)/shard_map/all_to_all | solution.py:27
  115.0 10.3 %all-to-all-done.1 = bf16[8,80,128]{2,1,0:T(8,128)(2,1)S(1)} async-done(((bf16[8,80,128]{2,1,0:T(8,128)(2,1)}), bf16[8,80,128]{2,1,0:T(8,128)(2,1)S(1)}, u32[]{:S(2)}, u32[]{:S(2)}) %all-to-all-start.1) | async-done | bytes 163872 | tf_op jit(solution)/shard_map/all_to_all | solution.py:27
  126.8 0.7 broadcast_in_dim.102
  127.5 10.6 %all-to-all-start.2 = ((bf16[8,80,128]{2,1,0:T(8,128)(2,1)}), bf16[8,80,128]{2,1,0:T(8,128)(2,1)S(1)}, u32[]{:S(2)}, u32[]{:S(2)}) async-start(bf16[8,80,128]{2,1,0:T(8,128)(2,1)} %broadcast_in_dim.102), calls=%async_computation.2 | async-start | bytes 327680 | tf_op jit(solution)/shard_map/all_to_all | solution.py:23
  138.2 0.8 dynamic_slice.54
  139.4 7.2 %all-to-all-done.2 = bf16[8,80,128]{2,1,0:T(8,128)(2,1)S(1)} async-done(((bf16[8,80,128]{2,1,0:T(8,128)(2,1)}), bf16[8,80,128]{2,1,0:T(8,128)(2,1)S(1)}, u32[]{:S(2)}, u32[]{:S(2)}) %all-to-all-start.2) | async-done | bytes 163872 | tf_op jit(solution)/shard_map/all_to_all | solution.py:23
  147.8 0.7 reshape.550
  148.5 3.4 %all-to-all-start.3 = ((bf16[8,64,128]{2,1,0:T(8,128)(2,1)}), bf16[8,64,128]{2,1,0:T(8,128)(2,1)S(1)}, u32[]{:S(2)}, u32[]{:S(2)}) async-start(bf16[8,64,128]{2,1,0:T(8,128)(2,1)} %reshape.550), calls=%async_computation.3 | async-start | bytes 262144 | tf_op jit(solution)/shard_map/all_to_all | solution.py:27
  152.1 0.6 fusion.6
  152.7 7.0 %all-to-all-done.3 = bf16[8,64,128]{2,1,0:T(8,128)(2,1)S(1)} async-done(((bf16[8,64,128]{2,1,0:T(8,128)(2,1)}), bf16[8,64,128]{2,1,0:T(8,128)(2,1)S(1)}, u32[]{:S(2)}, u32[]{:S(2)}) %all-to-all-start.3) | async-done | bytes 131104 | tf_op jit(solution)/shard_map/all_to_all | solution.py:27
  159.8 1.3 slice.234.refs_0_
  161.1 1.9 collective-permute-start.10
  163.0 4.8 %collective-permute-start.9 = (bf16[2048,256]{1,0:T(8,128)(2,1)S(1)}, bf16[2048,256]{1,0:T(8,128)(2,1)}, u32[]{:S(2)}, u32[]{:S(2)}) collective-permute-start(bf16[2048,256]{1,0:T(8,128)(2,1)S(1)} %slice.234.refs_0_), channel_id=1, source_target_pairs={{0,6},{2,0},{4,2},{6,4},{1,7},{3,1},{5,3},{7,5},{8,14},{10,8},{12,... | collective-permute-start | bytes 3145736 | tf_op jit(solution)/shard_map/ppermute | solution.py:71
  167.8 1.4 multiply_reduce_fusion
  169.1 6.3 %shard_map.154 = bf16[4,256,384]{2,1,0:T(8,128)(2,1)} custom-call(s32[3]{0:T(128)} %pad_add_fusion.spot, bf16[256,1024]{1,0:T(8,128)(2,1)} %copy-done.3, bf16[256,1024]{1,0:T(8,128)(2,1)} %get-tuple-element.20.refs_1_.refs_5_, bf16[256,1024]{1,0:T(8,128)(2,1)} %copy-done.4, bf16[256,1024]{1,0:T(8,128)(2,1)} %get-tuple-element.19.refs_3_.refs_7_, ...), custom_call_target="tpu_custom_call" | custom-call | flops 3000000000 | bytes 6291456 | tf_op jit(solution)/shard_map/pallas_call | solution.py:147
  175.4 1.1 multiply_convert_fusion.2
  176.5 2.2 collective-permute-start.4
  179.0 5.2 %collective-permute-done.10.refs_3_ = bf16[2048,256]{1,0:T(8,128)(2,1)S(1)} collective-permute-done((bf16[2048,256]{1,0:T(8,128)(2,1)S(1)}, bf16[2048,256]{1,0:T(8,128)(2,1)S(1)}, u32[]{:S(2)}, u32[]{:S(2)}) %collective-permute-start.10) | collective-permute-done | bytes 1048608 | tf_op jit(solution)/shard_map/ppermute | solution.py:71
  184.2 1.9 collective-permute-start.11
  186.1 1.1 slice.236
  187.2 4.6 %collective-permute-start.12 = (bf16[1024,256]{1,0:T(8,128)(2,1)S(1)}, bf16[1024,256]{1,0:T(8,128)(2,1)S(1)}, u32[]{:S(2)}, u32[]{:S(2)}) collective-permute-start(bf16[1024,256]{1,0:T(8,128)(2,1)S(1)} %slice.236), channel_id=1, source_target_pairs={{0,6},{2,0},{4,2},{6,4},{1,7},{3,1},{5,3},{7,5},{8,14},{10,8},{12,... | collective-permute-start | bytes 1572872 | tf_op jit(solution)/shard_map/ppermute | solution.py:71
  191.9 1.2 fusion.19
  193.0 1.1 fusion.15
  194.2 3.5 %all-to-all-start.4 = ((bf16[4,256,256]{2,1,0:T(8,128)(2,1)}), bf16[4,256,256]{2,1,0:T(8,128)(2,1)S(1)}, u32[]{:S(2)}, u32[]{:S(2)}) async-start(bf16[4,256,256]{2,1,0:T(8,128)(2,1)} %fusion.15), calls=%async_computation.4 | async-start | bytes 1048576 | tf_op jit(solution)/shard_map/all_to_all | solution.py:27
  197.9 1.1 pad_maximum_fusion.1.refs_2_
  199.0 5.6 %all-to-all-done.4.parts = bf16[4,256,256]{2,1,0:T(8,128)(2,1)S(1)} async-done(((bf16[4,256,256]{2,1,0:T(8,128)(2,1)}), bf16[4,256,256]{2,1,0:T(8,128)(2,1)S(1)}, u32[]{:S(2)}, u32[]{:S(2)}) %all-to-all-start.4) | async-done | bytes 524320 | tf_op jit(solution)/shard_map/all_to_all | solution.py:27
  204.6 0.8 copy-done.2
  205.4 4.6 %shard_map.156 = bf16[256,2048]{1,0:T(8,128)(2,1)} custom-call(s32[3]{0:T(128)} %pad_add_fusion.spot, bf16[4,256,256]{2,1,0:T(8,128)(2,1)} %copy-done.2, bf16[2048,256]{1,0:T(8,128)(2,1)} %copy-done.1, bf16[2048,256]{1,0:T(8,128)(2,1)} %collective-permute-done.9.refs_1_, bf16[2048,256]{1,0:T(8,128)(2,1)} %pad_maximum_fusion.1.refs_2_, ...), custom_call_target="tpu_custom_call" | custom-call | flops 2000000000 | bytes 6291456 | tf_op jit(solution)/shard_map/pallas_call | solution.py:147
  210.0 12.6 %all_to_all.30 = bf16[2,128,2048]{2,1,0:T(8,128)(2,1)S(1)} all-to-all(bf16[2,128,2048]{2,1,0:T(8,128)(2,1)} %bitcast.131), channel_id=1, replica_groups=mesh['z'=8,'y_hi'=4,'y_lo'=2,'fs'=4,'tp'=2] {'tp'}, dimensions={0} | all-to-all | bytes 2097152 | tf_op jit(solution)/shard_map/all_to_all | solution.py:27
  222.6 1.1 reduce_sum.52
  (137 shorter events, 6.4 us)
Async XLA Ops:
  6.5 54.1 %copy-start = (f32[3,1024]{1,0:T(4,128)S(1)}, f32[3,1024]{1,0:T(4,128)}, u32[]{:S(2)}) copy-start(f32[3,1024]{1,0:T(4,128)} %param.21) | copy-start | bytes 36868
  8.1 12.7 %copy-start.10 = (bf16[32,128]{1,0:T(8,128)(2,1)S(1)}, bf16[32,128]{1,0:T(8,128)(2,1)}, u32[]{:S(2)}) copy-start(bf16[32,128]{1,0:T(8,128)(2,1)} %param.18) | copy-start | bytes 24580
  8.1 12.7 %copy-start.11 = (bf16[32,128]{1,0:T(8,128)(2,1)S(1)}, bf16[32,128]{1,0:T(8,128)(2,1)}, u32[]{:S(2)}) copy-start(bf16[32,128]{1,0:T(8,128)(2,1)} %param.19) | copy-start | bytes 24580
  8.1 12.7 %copy-start.15 = (bf16[32,128]{1,0:T(8,128)(2,1)S(1)}, bf16[32,128]{1,0:T(8,128)(2,1)}, u32[]{:S(2)}) copy-start(bf16[32,128]{1,0:T(8,128)(2,1)} %param.24) | copy-start | bytes 24580
  8.1 12.7 %copy-start.16 = (bf16[32,128]{1,0:T(8,128)(2,1)S(1)}, bf16[32,128]{1,0:T(8,128)(2,1)}, u32[]{:S(2)}) copy-start(bf16[32,128]{1,0:T(8,128)(2,1)} %param.23) | copy-start | bytes 24580
  8.1 12.7 %copy-start.17 = (bf16[32,128]{1,0:T(8,128)(2,1)S(1)}, bf16[32,128]{1,0:T(8,128)(2,1)}, u32[]{:S(2)}) copy-start(bf16[32,128]{1,0:T(8,128)(2,1)} %param.22) | copy-start | bytes 24580
  8.1 12.7 %copy-start.12 = (bf16[32,128]{1,0:T(8,128)(2,1)S(1)}, bf16[32,128]{1,0:T(8,128)(2,1)}, u32[]{:S(2)}) copy-start(bf16[32,128]{1,0:T(8,128)(2,1)} %param.20) | copy-start | bytes 24580
  8.1 12.8 %copy-start.13 = (bf16[128,32]{0,1:T(8,128)(2,1)S(1)}, bf16[128,32]{0,1:T(8,128)(2,1)}, u32[]{:S(2)}) copy-start(bf16[128,32]{0,1:T(8,128)(2,1)} %param.30) | copy-start | bytes 24580
  8.2 12.8 %copy-start.14 = (bf16[128,32]{0,1:T(8,128)(2,1)S(1)}, bf16[128,32]{0,1:T(8,128)(2,1)}, u32[]{:S(2)}) copy-start(bf16[128,32]{0,1:T(8,128)(2,1)} %param.31) | copy-start | bytes 24580
  10.6 33.8 %copy-start.3 = (bf16[256,1024]{1,0:T(8,128)(2,1)}, bf16[256,1024]{1,0:T(8,128)(2,1)S(1)}, u32[]{:S(2)}) copy-start(bf16[256,1024]{1,0:T(8,128)(2,1)S(1)} %get-tuple-element.21.refs_0_.refs_4_) | copy-start | bytes 1572868
  10.6 22.3 %collective-permute-start = (bf16[256,1024]{1,0:T(8,128)(2,1)S(1)}, bf16[256,1024]{1,0:T(8,128)(2,1)S(1)}, u32[]{:S(2)}, u32[]{:S(2)}) collective-permute-start(bf16[256,1024]{1,0:T(8,128)(2,1)S(1)} %get-tuple-element.21.refs_0_.refs_4_), channel_id=1, source_target_pairs={{0,6},{2,0},{4,2},{6,4},{1,7},{3,1},{5,3},{7,5},{8,14},{10,8},{12,... | collective-permute-start | bytes 1572872 | tf_op jit(solution)/shard_map/ppermute | solution.py:71
  15.8 17.2 %collective-permute-start.1 = (bf16[256,1024]{1,0:T(8,128)(2,1)S(1)}, bf16[256,1024]{1,0:T(8,128)(2,1)S(1)}, u32[]{:S(2)}, u32[]{:S(2)}) collective-permute-start(bf16[256,1024]{1,0:T(8,128)(2,1)S(1)} %get-tuple-element.21.refs_0_.refs_4_), channel_id=1, source_target_pairs={{0,4},{2,6},{4,0},{6,2},{1,5},{3,7},{5,1},{7,3},{8,12},{10,14},{12... | collective-permute-start | bytes 1572872 | tf_op jit(solution)/shard_map/ppermute | solution.py:71
  18.3 26.1 %collective-permute-start.2 = (bf16[256,1024]{1,0:T(8,128)(2,1)S(1)}, bf16[256,1024]{1,0:T(8,128)(2,1)}, u32[]{:S(2)}, u32[]{:S(2)}) collective-permute-start(bf16[256,1024]{1,0:T(8,128)(2,1)S(1)} %get-tuple-element.21.refs_0_.refs_4_), channel_id=1, source_target_pairs={{0,2},{2,4},{4,6},{6,0},{1,3},{3,5},{5,7},{7,1},{8,10},{10,12},{12... | collective-permute-start | bytes 1572872 | tf_op jit(solution)/shard_map/ppermute | solution.py:71
  20.9 0.8 copy-start.9
  21.7 27.7 %all-to-all-start = ((bf16[16,32,384]{2,1,0:T(8,128)(2,1)}), bf16[16,32,384]{2,1,0:T(8,128)(2,1)S(1)}, u32[]{:S(2)}, u32[]{:S(2)}) async-start(bf16[16,32,384]{2,1,0:T(8,128)(2,1)} %broadcast_in_dim.93), calls=%async_computation | async-start | bytes 786432 | tf_op jit(solution)/shard_map/all_to_all | solution.py:23
  32.9 126.8 %all-gather.2.cloned.1.call-start = ((), (), s32[]{:S(2)}) async-start(), calls=%async_computation.6 | async-start | bytes 2662400 | tf_op jit(solution)/shard_map/all_gather | solution.py:196
  33.0 11.4 %copy-start.4 = (bf16[256,1024]{1,0:T(8,128)(2,1)}, bf16[256,1024]{1,0:T(8,128)(2,1)S(1)}, u32[]{:S(2)}) copy-start(bf16[256,1024]{1,0:T(8,128)(2,1)S(1)} %collective-permute-done.refs_2_.refs_6_) | copy-start | bytes 1572868
  33.0 11.4 %copy-start.5 = (bf16[256,1024]{1,0:T(8,128)(2,1)}, bf16[256,1024]{1,0:T(8,128)(2,1)S(1)}, u32[]{:S(2)}) copy-start(bf16[256,1024]{1,0:T(8,128)(2,1)S(1)} %collective-permute-done.1.refs_4_.refs_8_) | copy-start | bytes 1572868
  45.6 49.5 %collective-permute-start.3 = (bf16[768,1024]{1,0:T(8,128)(2,1)S(1)}, bf16[768,1024]{1,0:T(8,128)(2,1)S(1)}, u32[]{:S(2)}, u32[]{:S(2)}) collective-permute-start(bf16[768,1024]{1,0:T(8,128)(2,1)S(1)} %pad_maximum_fusion), channel_id=1, source_target_pairs={{0,1},{1,0},{2,3},{3,2},{4,5},{5,4},{6,7},{7,6},{8,9},{9,8},{10,11... | collective-permute-start | bytes 4718600 | tf_op jit(solution)/shard_map/ppermute | solution.py:31
  49.4 46.8 %copy-start.6 = (bf16[16,32,384]{2,1,0:T(8,128)(2,1)}, bf16[16,32,384]{2,1,0:T(8,128)(2,1)S(1)}, u32[]{:S(2)}) copy-start(bf16[16,32,384]{2,1,0:T(8,128)(2,1)S(1)} %all-to-all-done) | copy-start | bytes 1179652
  49.4 20.5 %collective-permute-start.6 = (bf16[512,384]{1,0:T(8,128)(2,1)S(1)}, bf16[512,384]{1,0:T(8,128)(2,1)}, u32[]{:S(2)}, u32[]{:S(2)}) collective-permute-start(bf16[512,384]{1,0:T(8,128)(2,1)S(1)} %bitcast.135), channel_id=1, source_target_pairs={{0,16},{16,32},{32,48},{48,0},{1,17},{17,33},{33,49},{49,1},{2,18}... | collective-permute-start | bytes 1179656 | tf_op jit(solution)/shard_map/ppermute | solution.py:71
  53.7 23.9 %collective-permute-start.5 = (bf16[512,384]{1,0:T(8,128)(2,1)S(1)}, bf16[512,384]{1,0:T(8,128)(2,1)}, u32[]{:S(2)}, u32[]{:S(2)}) collective-permute-start(bf16[512,384]{1,0:T(8,128)(2,1)S(1)} %bitcast.136), channel_id=1, source_target_pairs={{0,48},{16,0},{32,16},{48,32},{1,49},{17,1},{33,17},{49,33},{2,50}... | collective-permute-start | bytes 1179656 | tf_op jit(solution)/shard_map/ppermute | solution.py:71
  70.9 12.2 %collective-permute-start.7 = (bf16[256,384]{1,0:T(8,128)(2,1)S(1)}, bf16[256,384]{1,0:T(8,128)(2,1)S(1)}, u32[]{:S(2)}, u32[]{:S(2)}) collective-permute-start(bf16[256,384]{1,0:T(8,128)(2,1)S(1)} %slice.214), channel_id=1, source_target_pairs={{0,16},{16,32},{32,48},{48,0},{1,17},{17,33},{33,49},{49,1},{2,18}... | collective-permute-start | bytes 589832 | tf_op jit(solution)/shard_map/ppermute | solution.py:71
  78.5 15.7 %collective-permute-start.8 = (bf16[256,384]{1,0:T(8,128)(2,1)S(1)}, bf16[256,384]{1,0:T(8,128)(2,1)S(1)}, u32[]{:S(2)}, u32[]{:S(2)}) collective-permute-start(bf16[256,384]{1,0:T(8,128)(2,1)S(1)} %slice.215), channel_id=1, source_target_pairs={{0,48},{16,0},{32,16},{48,32},{1,49},{17,1},{33,17},{49,33},{2,50}... | collective-permute-start | bytes 589832 | tf_op jit(solution)/shard_map/ppermute | solution.py:71
  96.3 8.2 %copy-start.19 = (f32[1,256,1]{1,2,0:T(1,128)S(1)}, f32[1,256,1]{1,2,0:T(1,128)}, u32[]{:S(2)}) copy-start(f32[1,256,1]{1,2,0:T(1,128)} %get-tuple-element.22) | copy-start | bytes 3076
  96.3 8.2 %copy-start.20 = (f32[1,256,1]{1,2,0:T(1,128)S(1)}, f32[1,256,1]{1,2,0:T(1,128)}, u32[]{:S(2)}) copy-start(f32[1,256,1]{1,2,0:T(1,128)} %get-tuple-element.23) | copy-start | bytes 3076
  96.3 8.2 %copy-start.21 = (f32[1,256,1]{1,2,0:T(1,128)S(1)}, f32[1,256,1]{1,2,0:T(1,128)}, u32[]{:S(2)}) copy-start(f32[1,256,1]{1,2,0:T(1,128)} %get-tuple-element.24) | copy-start | bytes 3076
  96.3 8.2 %copy-start.22 = (f32[1,256,1]{1,2,0:T(1,128)S(1)}, f32[1,256,1]{1,2,0:T(1,128)}, u32[]{:S(2)}) copy-start(f32[1,256,1]{1,2,0:T(1,128)} %get-tuple-element.25) | copy-start | bytes 3076
  96.3 18.7 %copy-start.18 = (f32[3,128]{1,0:T(4,128)S(1)}, f32[3,128]{1,0:T(4,128)}, u32[]{:S(2)}) copy-start(f32[3,128]{1,0:T(4,128)} %constant_dynamic-slice_fusion.8) | copy-start | bytes 4612
  110.5 41.6 %copy-start.8 = (bf16[4,256,384]{2,1,0:T(8,128)(2,1)S(1)}, bf16[4,256,384]{2,1,0:T(8,128)(2,1)}, u32[]{:S(2)}) copy-start(bf16[4,256,384]{2,1,0:T(8,128)(2,1)} %get-tuple-element.12) | copy-start | bytes 2359300
  110.5 14.8 %all-to-all-start.1 = ((bf16[8,80,128]{2,1,0:T(8,128)(2,1)}), bf16[8,80,128]{2,1,0:T(8,128)(2,1)S(1)}, u32[]{:S(2)}, u32[]{:S(2)}) async-start(bf16[8,80,128]{2,1,0:T(8,128)(2,1)} %pad_maximum_fusion.3), calls=%async_computation.1 | async-start | bytes 327680 | tf_op jit(solution)/shard_map/all_to_all | solution.py:27
  127.5 19.0 %all-to-all-start.2 = ((bf16[8,80,128]{2,1,0:T(8,128)(2,1)}), bf16[8,80,128]{2,1,0:T(8,128)(2,1)S(1)}, u32[]{:S(2)}, u32[]{:S(2)}) async-start(bf16[8,80,128]{2,1,0:T(8,128)(2,1)} %broadcast_in_dim.102), calls=%async_computation.2 | async-start | bytes 327680 | tf_op jit(solution)/shard_map/all_to_all | solution.py:23
  148.5 11.2 %all-to-all-start.3 = ((bf16[8,64,128]{2,1,0:T(8,128)(2,1)}), bf16[8,64,128]{2,1,0:T(8,128)(2,1)S(1)}, u32[]{:S(2)}, u32[]{:S(2)}) async-start(bf16[8,64,128]{2,1,0:T(8,128)(2,1)} %reshape.550), calls=%async_computation.3 | async-start | bytes 262144 | tf_op jit(solution)/shard_map/all_to_all | solution.py:27
  161.0 14.4 %copy-start.1 = (bf16[2048,256]{1,0:T(8,128)(2,1)}, bf16[2048,256]{1,0:T(8,128)(2,1)S(1)}, u32[]{:S(2)}) copy-start(bf16[2048,256]{1,0:T(8,128)(2,1)S(1)} %slice.234.refs_0_) | copy-start | bytes 3145732
  161.1 23.1 %collective-permute-start.10 = (bf16[2048,256]{1,0:T(8,128)(2,1)S(1)}, bf16[2048,256]{1,0:T(8,128)(2,1)S(1)}, u32[]{:S(2)}, u32[]{:S(2)}) collective-permute-start(bf16[2048,256]{1,0:T(8,128)(2,1)S(1)} %slice.234.refs_0_), channel_id=1, source_target_pairs={{0,2},{2,4},{4,6},{6,0},{1,3},{3,5},{5,7},{7,1},{8,10},{10,12},{12... | collective-permute-start | bytes 3145736 | tf_op jit(solution)/shard_map/ppermute | solution.py:71
  163.0 23.1 %collective-permute-start.9 = (bf16[2048,256]{1,0:T(8,128)(2,1)S(1)}, bf16[2048,256]{1,0:T(8,128)(2,1)}, u32[]{:S(2)}, u32[]{:S(2)}) collective-permute-start(bf16[2048,256]{1,0:T(8,128)(2,1)S(1)} %slice.234.refs_0_), channel_id=1, source_target_pairs={{0,6},{2,0},{4,2},{6,4},{1,7},{3,1},{5,3},{7,5},{8,14},{10,8},{12,... | collective-permute-start | bytes 3145736 | tf_op jit(solution)/shard_map/ppermute | solution.py:71
  176.5 15.3 %collective-permute-start.4 = (bf16[4,2,128]{2,1,0:T(2,128)(2,1)S(1)}, bf16[4,2,128]{2,1,0:T(2,128)(2,1)S(1)}, u32[]{:S(2)}, u32[]{:S(2)}) collective-permute-start(bf16[4,2,128]{2,1,0:T(2,128)(2,1)S(1)} %slice.210), channel_id=1, source_target_pairs={{0,8},{8,16},{16,24},{24,32},{32,40},{40,48},{48,56},{56,64},{64,7... | collective-permute-start | bytes 6152 | tf_op jit(solution)/shard_map/ppermute | solution.py:36
  184.2 8.9 %copy-start.7 = (bf16[2048,256]{1,0:T(8,128)(2,1)}, bf16[2048,256]{1,0:T(8,128)(2,1)S(1)}, u32[]{:S(2)}) copy-start(bf16[2048,256]{1,0:T(8,128)(2,1)S(1)} %collective-permute-done.10.refs_3_) | copy-start | bytes 3145732
  184.2 13.5 %collective-permute-start.11 = (bf16[1024,256]{1,0:T(8,128)(2,1)S(1)}, bf16[1024,256]{1,0:T(8,128)(2,1)S(1)}, u32[]{:S(2)}, u32[]{:S(2)}) collective-permute-start(bf16[1024,256]{1,0:T(8,128)(2,1)S(1)} %slice.235), channel_id=1, source_target_pairs={{0,2},{2,4},{4,6},{6,0},{1,3},{3,5},{5,7},{7,1},{8,10},{10,12},{12... | collective-permute-start | bytes 1572872 | tf_op jit(solution)/shard_map/ppermute | solution.py:71
  187.2 10.7 %collective-permute-start.12 = (bf16[1024,256]{1,0:T(8,128)(2,1)S(1)}, bf16[1024,256]{1,0:T(8,128)(2,1)S(1)}, u32[]{:S(2)}, u32[]{:S(2)}) collective-permute-start(bf16[1024,256]{1,0:T(8,128)(2,1)S(1)} %slice.236), channel_id=1, source_target_pairs={{0,6},{2,0},{4,2},{6,4},{1,7},{3,1},{5,3},{7,5},{8,14},{10,8},{12,... | collective-permute-start | bytes 1572872 | tf_op jit(solution)/shard_map/ppermute | solution.py:71
  194.2 10.4 %all-to-all-start.4 = ((bf16[4,256,256]{2,1,0:T(8,128)(2,1)}), bf16[4,256,256]{2,1,0:T(8,128)(2,1)S(1)}, u32[]{:S(2)}, u32[]{:S(2)}) async-start(bf16[4,256,256]{2,1,0:T(8,128)(2,1)} %fusion.15), calls=%async_computation.4 | async-start | bytes 1048576 | tf_op jit(solution)/shard_map/all_to_all | solution.py:27
  204.6 0.8 copy-start.2
Sparse Core Ops, SparseCore 0:
  48.1 87.7 all-gather.1

commit v7 on v6

--- a/solution.py
+++ b/solution.py
@@ -81,7 +81,7 @@
     behind = ring(array, axis, 1)
     first = ring(behind[:cut], axis, 1)
     second = ring(ahead[cut:], axis, -1)
-    return ahead, jnp.concatenate([first, second], axis=0), behind
+    return ahead, first, second, behind
 
 
 def rolled(array, by):
@@ -90,68 +90,123 @@
     return lax.dynamic_slice_in_dim(twice, (size - by) % size, size, 0)
 
 
-def matmuls(core, pieces, weights, left, out):
+def pack_kernel(*refs):
+    parts, rest, mem = refs[:8], refs[8], refs[9]
+    wide = parts[0].shape[1]
+    for k in range(3):
+        for copy in range(mem.shape[0]):
+            mem[copy, :, k * wide : (k + 1) * wide] = parts[k][...]
+    for k in range(5):
+        rest[:, k * wide : (k + 1) * wide] = parts[3 + k][...]
+
+
+def piece(refs, k, other):
+    tokens = refs[0].shape[0]
+    if k == 0:
+        return refs[other][...]
+    if other:
+        return refs[5][(k - 1) * tokens : k * tokens, :]
+    return refs[1 + k][...]
+
+
+def matmul(core, pieces, weights, k, out):
     half = pieces[0].shape[1]
     first = pl.multiple_of(core * half, half)
     second = pl.multiple_of((1 - core) * half, half)
-    right = left + out.shape[2]
-    for k in range(4):
-        mixed = jnp.dot(
-            pieces[2 * k][...],
-            weights[pl.ds(first, half), left:right],
-            preferred_element_type=F32,
-        )
-        mixed += jnp.dot(
-            pieces[2 * k + 1][...],
-            weights[pl.ds(second, half), left:right],
-            preferred_element_type=F32,
-        )
-        out[k] = mixed.astype(BF16)
-
-
-def project_mem_kernel(spot, *refs):
-    parts, pieces, gate_rows = refs[:4], refs[4:12], refs[12]
-    out, gates, weights = refs[13:]
+    wide = out.shape[2]
+    mixed = jnp.dot(
+        piece(pieces, k, 0), weights[pl.ds(first, half), :wide], preferred_element_type=F32
+    )
+    mixed += jnp.dot(
+        piece(pieces, k, 1), weights[pl.ds(second, half), :wide], preferred_element_type=F32
+    )
+    out[k] = mixed.astype(BF16)
+
+
+def project_mem_kernel(spot, bias, *refs):
+    parts, pieces, gate_rows, decay = refs[:5], refs[5:11], refs[11], refs[12]
+    out, packed, sums_out, entry_out, weights = refs[13:]
     core = spot[0]
-    for k in range(4):
+    for k, sources in enumerate(((0, 0), (1, 1), (2, 3), (4, 4))):
         place = (spot[2] + k) % 4
         for z in range(8):
             start = pl.multiple_of((z * 4 + place) * 64, 64)
-            weights[pl.ds(start, 64), :] = parts[k][pl.ds(z * 64, 64), :]
-    matmuls(core, pieces, weights, 0, out)
+            source = parts[sources[z // 4]]
+            row = (z * 64) % source.shape[0]
+            weights[pl.ds(start, 64), :] = source[row : row + 64, :]
     dims = (((1,), (1,)), ((), ()))
+    gates = [
+        dot(gate_rows[core], piece(pieces, k, 0), dims)
+        + dot(gate_rows[1 - core], piece(pieces, k, 1), dims)
+        for k in range(4)
+    ]
+    entry = jnp.concatenate([g[0:1] for g in gates], axis=0) + bias[0]
+    forget = jnp.concatenate([g[1:2] for g in gates], axis=0) + bias[1]
+    small = jnp.exp(-jnp.abs(forget))
+    series = small * (1.0 - small * (0.5 - small * (1.0 / 3.0)))
+    softened = jnp.where(small < 1e-3, series, jnp.log(1.0 + small))
+    log_forget = jnp.minimum(forget, 0.0) - softened + decay[...]
+    tokens = entry.shape[1]
+    shape = (tokens, tokens)
+    upto = lax.broadcasted_iota(jnp.int32, shape, 0) <= lax.broadcasted_iota(jnp.int32, shape, 1)
+    sums = jnp.dot(
+        log_forget, upto.astype(F32), preferred_element_type=F32, precision=HIGHEST
+    )
+    sums_out[...] = sums
+    entry_out[...] = entry
+    total = sums[:, tokens - 1 :]
+    local_logs = total - sums + entry
+    peak = jnp.max(local_logs, axis=1, keepdims=True)
+    local_weights = jnp.exp(local_logs - peak) * HEAD_DIM ** (-0.5)
+    columns = jnp.concatenate([local_weights, local_weights], axis=0).T
     for k in range(4):
-        rows = dot(gate_rows[core], pieces[2 * k][...], dims)
-        gates[k] = rows + dot(gate_rows[1 - core], pieces[2 * k + 1][...], dims)
+        matmul(core, pieces, weights, k, out)
+        value = out[k, :, 2 * HEAD_DIM :].astype(F32)
+        weighted = (value * columns[:, k : k + 1]).astype(BF16)
+        state = dot(weighted, out[k, :, HEAD_DIM : 2 * HEAD_DIM], (((0,), (0,)), ((), ())))
+        state = state.astype(BF16)
+        for c in range(8):
+            packed[c, k * 16 : (k + 1) * 16, :] = state[c * 16 : (c + 1) * 16, :]
+    numbers = jnp.concatenate([total, peak], axis=0)
+    first = numbers.astype(BF16).astype(F32)
+    second = (numbers - first).astype(BF16).astype(F32)
+    third = numbers - first - second
+    numbers = jnp.concatenate([first, second, third, third], axis=0)
+    numbers = jnp.broadcast_to(numbers, (32, HEAD_DIM)).astype(BF16)
+    for c in range(8):
+        packed[c, 64:96, :] = numbers
 
 
 def project_conv_kernel(spot, *refs):
-    matmuls(spot[0], refs[:8], refs[8], 0, refs[9])
-
-
-def output_kernel(spot, parts, *refs):
-    weights, out = refs[:4], refs[4]
+    for k in range(4):
+        matmul(spot[0], refs[:6], refs[6], k, refs[7])
+
+
+def output_kernel(spot, parts, own, ahead, first, second, behind, out):
     dims = (((1,), (1,)), ((), ()))
-    mixed = dot(parts[spot[1]], weights[0][...], dims)
-    for k in range(1, 4):
-        mixed += dot(parts[(spot[1] + k) % 4], weights[k][...], dims)
-    out[...] = mixed.astype(BF16)
+    half = first.shape[0]
+    for side, far in enumerate((first, second)):
+        rows = slice(side * half, (side + 1) * half)
+        mixed = dot(parts[spot[1]], own[rows, :], dims)
+        mixed += dot(parts[(spot[1] + 1) % 4], ahead[rows, :], dims)
+        mixed += dot(parts[(spot[1] + 2) % 4], far[...], dims)
+        mixed += dot(parts[(spot[1] + 3) % 4], behind[rows, :], dims)
+        out[:, rows] = mixed.astype(BF16)
 
 
 def in_vmem(count):
     return [pl.BlockSpec(memory_space=pltpu.VMEM)] * count
 
 
-def call(kernel, shapes, spot, arrays, flops, scratch=()):
-    smem = [pl.BlockSpec(memory_space=pltpu.SMEM)] if spot is not None else []
+def call(kernel, shapes, scalars, arrays, flops, scratch=()):
     return pl.pallas_call(
         kernel,
         out_shape=tuple(jax.ShapeDtypeStruct(shape, dtype) for shape, dtype in shapes),
-        in_specs=smem + in_vmem(len(arrays)),
+        in_specs=[pl.BlockSpec(memory_space=pltpu.SMEM)] * len(scalars) + in_vmem(len(arrays)),
         out_specs=tuple(in_vmem(len(shapes))),
         scratch_shapes=list(scratch),
         cost_estimate=pl.CostEstimate(flops=flops, bytes_accessed=6 << 20, transcendentals=0),
-    )(*([spot] if spot is not None else []), *arrays)
+    )(*scalars, *arrays)
 
 
 def shards(
@@ -185,12 +240,16 @@
     spot = jnp.stack([core, place_x, place_y]).astype(jnp.int32)
 
     channels = w_conv_gate.shape[1]
-    w_rest = jnp.concatenate(
-        [w_conv_gate, w_conv_mult, w_conv_in, w_out_conv.T, w_out_mem.T], axis=1
-    )
-    w_mem = jnp.concatenate([w_query, w_key, w_value], axis=1)
-    w_rest, w_mem = lax.optimization_barrier((w_rest, w_mem))
-    w_mem = everyone(w_mem, ("z", "y_lo")).reshape(-1, w_mem.shape[1])
+    shard = w_query.shape
+    pairs = 2 * lax.axis_size("z")
+    w_rest, w_mem = call(
+        pack_kernel,
+        [((shard[0], 5 * shard[1]), BF16), ((pairs, shard[0], 3 * shard[1]), BF16)],
+        [],
+        [w_query, w_key, w_value, w_conv_gate, w_conv_mult, w_conv_in, w_out_conv.T, w_out_mem.T],
+        10**6,
+    )
+    w_mem = exchanged(w_mem, ("z", "y_lo")).reshape(-1, w_mem.shape[2])
     w_mem = (w_mem, *relayed(w_mem, "y_hi"))
 
     w_rest = lax.all_gather(w_rest, SP, axis=0, tiled=True)
@@ -204,9 +263,9 @@
     mine = lax.dynamic_slice_in_dim(normed, core * half, half, 1)
     pieces = [mine, lax.dynamic_slice_in_dim(normed, (1 - core) * half, half, 1)]
     others = around(mine, "fs")
-    swapped = other_core(jnp.concatenate(others, axis=0))
-    for k, piece in enumerate(others):
-        pieces += [piece, swapped[k * tokens : (k + 1) * tokens]]
+    together = jnp.concatenate(others, axis=0)
+    swapped = other_core(together)
+    pieces += [*others, swapped]
 
     gate_rows = jnp.concatenate(
         [
@@ -216,40 +275,31 @@
         axis=1,
     ).T
     gate_rows = jnp.pad(gate_rows, ((0, 14), (0, 0))).reshape(16, 2, half).transpose(1, 0, 2)
-    qkv, gates = call(
+    bias = lax.dynamic_slice_in_dim(gate_bias, head, 1, 1)[:, 0]
+    decay = lax.dynamic_slice_in_dim(decay_shift, head, 1, 2)[..., 0]
+    decay = jnp.concatenate([lax.dynamic_slice_in_dim(decay, k, 1, 0) for k in order], axis=0)
+    places = lax.axis_size(Y)
+    cut = HEAD_DIM // places
+    qkv, packed, sums, entry = call(
         project_mem_kernel,
-        [((seqs, tokens, 3 * HEAD_DIM), BF16), ((seqs, 16, tokens), F32)],
-        spot,
-        [*w_mem, *pieces, gate_rows],
+        [
+            ((seqs, tokens, 3 * HEAD_DIM), BF16),
+            ((places, seqs * cut + 32, HEAD_DIM), BF16),
+            ((seqs, tokens), F32),
+            ((seqs, tokens), F32),
+        ],
+        [spot, bias],
+        [*w_mem, *pieces, gate_rows, decay],
         10**9 * 3,
         [pltpu.VMEM((width, 3 * HEAD_DIM), BF16)],
     )
     query, key, value = (qkv[..., k * HEAD_DIM : (k + 1) * HEAD_DIM] for k in range(3))
-    bias = lax.dynamic_slice_in_dim(gate_bias, head, 1, 1)
-    decay = lax.dynamic_slice_in_dim(decay_shift, head, 1, 2)[..., 0]
-    decay = jnp.concatenate([lax.dynamic_slice_in_dim(decay, k, 1, 0) for k in order], axis=0)
-    entry = gates[:, 0] + bias[0]
-    log_forget = jax.nn.log_sigmoid(gates[:, 1] + bias[1]) + decay
-    sums = jnp.cumsum(log_forget, axis=-1)
-    total = sums[:, -1]
-    local_logs = total[:, None] - sums + entry
-    peak = jnp.max(local_logs, axis=-1)
     scale = HEAD_DIM ** (-0.5)
-    local_weights = jnp.exp(local_logs - peak[:, None]) * scale
-
-    weighted = (local_weights[..., None] * value.astype(F32)).astype(BF16)
-    state = dot(weighted, key, (((1,), (1,)), ((0,), (0,))))
-
-    places = lax.axis_size(Y)
-    cut = HEAD_DIM // places
-    slices = state.astype(BF16).reshape(seqs, places, cut, HEAD_DIM).transpose(1, 0, 2, 3)
-    slices = slices.reshape(places, seqs * cut, HEAD_DIM)
-    numbers = jnp.broadcast_to(numbers_row(total, peak), (places, 16, HEAD_DIM))
-    packed = jnp.concatenate([slices, numbers], axis=1)
+
     packed = exchanged(packed, Y)
     line = jnp.arange(places)
     after = (line[:, None] > line[None, :]).astype(F32)
-    totals, peaks = numbers_of(packed[:, seqs * cut], seqs)
+    totals, peaks = numbers_of(packed[:, seqs * cut :, 0], seqs)
     states = packed[:, : seqs * cut].reshape(places, seqs, cut * HEAD_DIM)
     earlier = jnp.arange(places + 1)[:, None] > line[None, :]
     sums_in, logs = segment_logs(totals, peaks, earlier, after)
@@ -286,7 +336,7 @@
     (conv,) = call(
         project_conv_kernel,
         [((seqs, tokens, 3 * channels), BF16)],
-        spot,
+        [spot],
         [*pieces, w_rest],
         10**9 * 3,
     )
@@ -317,9 +367,7 @@
     mem_out = (cell * gain).astype(BF16)
     both = rolled(jnp.concatenate([conv_out, mem_out], axis=-1), place_x)
     both = exchanged(both, "fs")
-    (output,) = call(
-        output_kernel, [((tokens, width), BF16)], spot, [both, *w_out], 10**9 * 2
-    )
+    (output,) = call(output_kernel, [((tokens, width), BF16)], [spot], [both, *w_out], 10**9 * 2)
 
     cores = lax.axis_size("tp")
     parts = exchanged(output.reshape(cores, tokens // cores, width), "tp")

time: 232 us -> 239 us (1.030)
  blocking collectives: 12.6 us -> 24.1 us
  waiting for transfers between devices: 65.7 us -> 75 us
  other arithmetic: 19 us -> 10 us
  Pallas kernels: 17.7 us -> 20.6 us
  local copies, waits for them, and re-layouts: 18.1 us -> 15.5 us
  matrix products: 4.66 us -> 2.09 us
    all_to_all x3, starting transfers between devices: 11.3 us -> 28.9 us  [exchanged(): return lax.all_to_all(array, axis, split_axis=0, concat_axis=0, tiled=True)]
    all_to_all x2 -> x1, starting transfers between devices: 21.8 us -> 6.5 us  [everyone(): return lax.all_to_all(copies, axis, split_axis=0, concat_axis=0, tiled=True)]
    all_to_all x1 -> x2, blocking collectives: 12.6 us -> 24.1 us  [exchanged(): return lax.all_to_all(array, axis, split_axis=0, concat_axis=0, tiled=True)]
    all_to_all x3, waiting for transfers between devices: 22.9 us -> 28 us  [exchanged(): return lax.all_to_all(array, axis, split_axis=0, concat_axis=0, tiled=True)]
    ppermute x11, starting transfers between devices: 40.8 us -> 36.5 us  [ring(): lax.ppermute(array, axis, [(i, (i + by) % peers) for i in range(peers)])]
    concatenate x5 -> x2, other arithmetic: 3.7 us -> 0.72 us  [the longest x1 0.6 us: shards(): jnp.concatenate([lax.dynamic_slice_in_dim(decay, k, 1, 0) for k in order]...]
    pallas_call x3 -> x4, Pallas kernels: 17.7 us -> 20.6 us  [call(): pl.pallas_call(kernel, out_shape=tuple((jax.ShapeDtypeStruct(shape, dtype...]
    dot_general x3 -> x2, matrix products: 3.56 us -> 0.99 us  [dot(): return lax.dot_general(a, b, dims, preferred_element_type=F32)]
  transfers between devices with their start and end apart: 19 -> 18, of which waited for: 10 -> 13; matrix products, arithmetic and copies ran while one was open for 15% -> 8% of each run, Pallas kernels for 6% -> 7%
where the time goes in v7:
time: 239 us; the launch traced here: 238 us
  starting transfers between devices  76.5 us (32%)
  waiting for transfers between devices  75 us (31%)
  blocking collectives  24.1 us (10%)
  Pallas kernels  20.6 us (9%)
  local copies, waits for them, and re-layouts  15.5 us (6%)
  between operations  14 us (6%)
  other arithmetic  10 us (4%)
    ppermute x11, waiting for transfers between devices, ring(): lax.ppermute(array, axis, [(i, (i + by) % peers) for i in range(peers)])  37.8 us
    ppermute x11, starting transfers between devices, ring(): lax.ppermute(array, axis, [(i, (i + by) % peers) for i in range(peers)])  36.5 us
    all_to_all x3, starting transfers between devices, exchanged(): return lax.all_to_all(array, axis, split_axis=0, concat_axis=0, tiled=True)  28.9 us
    all_to_all x3, waiting for transfers between devices, exchanged(): return lax.all_to_all(array, axis, split_axis=0, concat_axis=0, tiled=True)  28 us
    all_to_all x2, blocking collectives, exchanged(): return lax.all_to_all(array, axis, split_axis=0, concat_axis=0, tiled=True)  24.1 us
    pallas_call x4, Pallas kernels, call(): pl.pallas_call(kernel, out_shape=tuple((jax.ShapeDtypeStruct(shape, dtype...  20.6 us
    all_to_all x1, waiting for transfers between devices, everyone(): return lax.all_to_all(copies, axis, split_axis=0, concat_axis=0, tiled=True)  8.08 us
    all_to_all x1, starting transfers between devices, everyone(): return lax.all_to_all(copies, axis, split_axis=0, concat_axis=0, tiled=True)  6.5 us
  transfers between devices with their start and end apart: 18, of which 13 were waited for; matrix products, arithmetic and copies ran while one was open for 8% of the time, Pallas kernels for 7%

profile of v7, /device:TPU:1, one launch (start us, length us, event | category | flops | bytes accessed | tf_op | source)
XLA Modules:
  0.0 237.8 jit_solution(16426664366954717032)
XLA Ops:
  6.5 1.5 fusion.2
  8.1 1.5 fusion.4
  9.6 0.9 constant_dynamic-slice_fusion.9
  10.5 5.2 %collective-permute-start = (bf16[256,1024]{1,0:T(8,128)(2,1)S(1)}, bf16[256,1024]{1,0:T(8,128)(2,1)S(1)}, u32[]{:S(2)}, u32[]{:S(2)}) collective-permute-start(bf16[256,1024]{1,0:T(8,128)(2,1)S(1)} %get-tuple-element.20.refs_0_.refs_5_), channel_id=1, source_target_pairs={{0,6},{2,0},{4,2},{6,4},{1,7},{3,1},{5,3},{7,5},{8,14},{10,8},{12,... | collective-permute-start | bytes 1572872 | tf_op jit(solution)/shard_map/ppermute | solution.py:71
  15.7 2.4 %collective-permute-start.1 = (bf16[256,1024]{1,0:T(8,128)(2,1)S(1)}, bf16[256,1024]{1,0:T(8,128)(2,1)S(1)}, u32[]{:S(2)}, u32[]{:S(2)}) collective-permute-start(bf16[256,1024]{1,0:T(8,128)(2,1)S(1)} %get-tuple-element.20.refs_0_.refs_5_), channel_id=1, source_target_pairs={{0,4},{2,6},{4,0},{6,2},{1,5},{3,7},{5,1},{7,3},{8,12},{10,14},{12... | collective-permute-start | bytes 1572872 | tf_op jit(solution)/shard_map/ppermute | solution.py:71
  18.1 2.5 %collective-permute-start.2 = (bf16[256,1024]{1,0:T(8,128)(2,1)S(1)}, bf16[256,1024]{1,0:T(8,128)(2,1)S(1)}, u32[]{:S(2)}, u32[]{:S(2)}) collective-permute-start(bf16[256,1024]{1,0:T(8,128)(2,1)S(1)} %get-tuple-element.20.refs_0_.refs_5_), channel_id=1, source_target_pairs={{0,2},{2,4},{4,6},{6,0},{1,3},{3,5},{5,7},{7,1},{8,10},{10,12},{12... | collective-permute-start | bytes 1572872 | tf_op jit(solution)/shard_map/ppermute | solution.py:71
  20.7 7.0 %collective-permute-done.refs_2_.refs_7_ = bf16[256,1024]{1,0:T(8,128)(2,1)S(1)} collective-permute-done((bf16[256,1024]{1,0:T(8,128)(2,1)S(1)}, bf16[256,1024]{1,0:T(8,128)(2,1)S(1)}, u32[]{:S(2)}, u32[]{:S(2)}) %collective-permute-start) | collective-permute-done | bytes 524320 | tf_op jit(solution)/shard_map/ppermute | solution.py:71
  27.6 1.5 collective-permute-done.1.refs_3_.refs_8_
  29.1 15.1 %collective-permute-done.2.refs_4_.refs_9_ = bf16[256,1024]{1,0:T(8,128)(2,1)S(1)} collective-permute-done((bf16[256,1024]{1,0:T(8,128)(2,1)S(1)}, bf16[256,1024]{1,0:T(8,128)(2,1)S(1)}, u32[]{:S(2)}, u32[]{:S(2)}) %collective-permute-start.2) | collective-permute-done | bytes 524320 | tf_op jit(solution)/shard_map/ppermute | solution.py:71
  44.3 2.4 %collective-permute-start.3 = (bf16[768,1024]{1,0:T(8,128)(2,1)S(1)}, bf16[768,1024]{1,0:T(8,128)(2,1)}, u32[]{:S(2)}, u32[]{:S(2)}) collective-permute-start(bf16[768,1024]{1,0:T(8,128)(2,1)S(1)} %pad_maximum_fusion), channel_id=1, source_target_pairs={{0,1},{1,0},{2,3},{3,2},{4,5},{5,4},{6,7},{7,6},{8,9},{9,8},{10,11... | collective-permute-start | bytes 4718600 | tf_op jit(solution)/shard_map/ppermute | solution.py:31
  46.7 1.6 shard_map.154
  48.4 11.2 %all-to-all-start = ((bf16[16,32,384]{2,1,0:T(8,128)(2,1)}), bf16[16,32,384]{2,1,0:T(8,128)(2,1)S(1)}, u32[]{:S(2)}, u32[]{:S(2)}) async-start(bf16[16,32,384]{2,1,0:T(8,128)(2,1)} %get-tuple-element.12), calls=%async_computation | async-start | bytes 786432 | tf_op jit(solution)/shard_map/all_to_all | solution.py:27
  59.6 0.7 all-gather.2.cloned.1.call-update
  60.3 12.0 %all-to-all-done = bf16[16,32,384]{2,1,0:T(8,128)(2,1)S(1)} async-done(((bf16[16,32,384]{2,1,0:T(8,128)(2,1)}), bf16[16,32,384]{2,1,0:T(8,128)(2,1)S(1)}, u32[]{:S(2)}, u32[]{:S(2)}) %all-to-all-start) | async-done | bytes 393248 | tf_op jit(solution)/shard_map/all_to_all | solution.py:27
  72.3 4.2 %collective-permute-start.6 = (bf16[512,384]{1,0:T(8,128)(2,1)S(1)}, bf16[512,384]{1,0:T(8,128)(2,1)}, u32[]{:S(2)}, u32[]{:S(2)}) collective-permute-start(bf16[512,384]{1,0:T(8,128)(2,1)S(1)} %bitcast.102), channel_id=1, source_target_pairs={{0,16},{16,32},{32,48},{48,0},{1,17},{17,33},{33,49},{49,1},{2,18}... | collective-permute-start | bytes 1179656 | tf_op jit(solution)/shard_map/ppermute | solution.py:71
  76.5 3.2 %collective-permute-start.5 = (bf16[512,384]{1,0:T(8,128)(2,1)S(1)}, bf16[512,384]{1,0:T(8,128)(2,1)}, u32[]{:S(2)}, u32[]{:S(2)}) collective-permute-start(bf16[512,384]{1,0:T(8,128)(2,1)S(1)} %bitcast.103), channel_id=1, source_target_pairs={{0,48},{16,0},{32,16},{48,32},{1,49},{17,1},{33,17},{49,33},{2,50}... | collective-permute-start | bytes 1179656 | tf_op jit(solution)/shard_map/ppermute | solution.py:71
  79.7 1.4 constant_dynamic-slice_fusion.5
  81.1 0.7 maximum_bitcast_fusion
  81.9 0.6 copy.82
  82.5 1.4 fusion.61.bias
  83.9 0.8 fusion.62
  84.7 0.5 collective-permute-done.6.refs_4_
  85.2 0.9 slice.168
  86.1 3.3 %collective-permute-start.7 = (bf16[256,384]{1,0:T(8,128)(2,1)S(1)}, bf16[256,384]{1,0:T(8,128)(2,1)S(1)}, u32[]{:S(2)}, u32[]{:S(2)}) collective-permute-start(bf16[256,384]{1,0:T(8,128)(2,1)S(1)} %slice.168), channel_id=1, source_target_pairs={{0,16},{16,32},{32,48},{48,0},{1,17},{17,33},{33,49},{49,1},{2,18}... | collective-permute-start | bytes 589832 | tf_op jit(solution)/shard_map/ppermute | solution.py:71
  89.5 1.6 collective-permute-done.5.refs_1_
  91.1 0.9 slice.169
  92.0 2.4 %collective-permute-start.8 = (bf16[256,384]{1,0:T(8,128)(2,1)S(1)}, bf16[256,384]{1,0:T(8,128)(2,1)S(1)}, u32[]{:S(2)}, u32[]{:S(2)}) collective-permute-start(bf16[256,384]{1,0:T(8,128)(2,1)S(1)} %slice.169), channel_id=1, source_target_pairs={{0,48},{16,0},{32,16},{48,32},{1,49},{17,1},{33,17},{49,33},{2,50}... | collective-permute-start | bytes 589832 | tf_op jit(solution)/shard_map/ppermute | solution.py:71
  94.5 0.6 pad_add_fusion.spot
  95.1 0.6 pad_maximum_fusion.2.refs_12_
  95.7 7.1 %collective-permute-done.7.refs_2_ = bf16[256,384]{1,0:T(8,128)(2,1)S(1)} collective-permute-done((bf16[256,384]{1,0:T(8,128)(2,1)S(1)}, bf16[256,384]{1,0:T(8,128)(2,1)S(1)}, u32[]{:S(2)}, u32[]{:S(2)}) %collective-permute-start.7) | collective-permute-done | bytes 196640 | tf_op jit(solution)/shard_map/ppermute | solution.py:71
  102.8 0.4 collective-permute-done.8.refs_3_
  103.5 0.4 copy-done.12
  103.9 8.1 %shard_map.156 = (bf16[4,256,384]{2,1,0:T(8,128)(2,1)}, bf16[8,96,128]{2,1,0:T(8,128)(2,1)}, f32[4,256]{1,0:T(4,128)}, f32[4,256]{1,0:T(4,128)}) custom-call(s32[3]{0:T(128)} %pad_add_fusion.spot, f32[2]{0:T(128)} %fusion.61.bias, bf16[512,384]{1,0:T(8,128)(2,1)} %bitcast.104, bf16[512,384]{1,0:T(8,128)(2,1)} %collective-permute-done.5.refs_1_, ...), custom_call_target="tpu_custom_call" | custom-call | flops 3000000000 | bytes 6291456 | tf_op jit(solution)/shard_map/pallas_call | solution.py:202
  112.0 14.4 %all-to-all-start.1 = ((bf16[8,96,128]{2,1,0:T(8,128)(2,1)}), bf16[8,96,128]{2,1,0:T(8,128)(2,1)S(1)}, u32[]{:S(2)}, u32[]{:S(2)}) async-start(bf16[8,96,128]{2,1,0:T(8,128)(2,1)} %get-tuple-element.14), calls=%async_computation.1 | async-start | bytes 393216 | tf_op jit(solution)/shard_map/all_to_all | solution.py:27
  126.4 9.0 %all-to-all-done.1 = bf16[8,96,128]{2,1,0:T(8,128)(2,1)S(1)} async-done(((bf16[8,96,128]{2,1,0:T(8,128)(2,1)}), bf16[8,96,128]{2,1,0:T(8,128)(2,1)S(1)}, u32[]{:S(2)}, u32[]{:S(2)}) %all-to-all-start.1) | async-done | bytes 196640 | tf_op jit(solution)/shard_map/all_to_all | solution.py:27
  137.0 0.7 broadcast_in_dim.90
  137.7 6.5 %all-to-all-start.2 = ((bf16[8,80,128]{2,1,0:T(8,128)(2,1)}), bf16[8,80,128]{2,1,0:T(8,128)(2,1)S(1)}, u32[]{:S(2)}, u32[]{:S(2)}) async-start(bf16[8,80,128]{2,1,0:T(8,128)(2,1)} %broadcast_in_dim.90), calls=%async_computation.2 | async-start | bytes 327680 | tf_op jit(solution)/shard_map/all_to_all | solution.py:23
  144.3 0.8 dynamic_slice.63
  145.1 0.4 fusion.13
  145.5 8.1 %all-to-all-done.2 = bf16[8,80,128]{2,1,0:T(8,128)(2,1)S(1)} async-done(((bf16[8,80,128]{2,1,0:T(8,128)(2,1)}), bf16[8,80,128]{2,1,0:T(8,128)(2,1)S(1)}, u32[]{:S(2)}, u32[]{:S(2)}) %all-to-all-start.2) | async-done | bytes 163872 | tf_op jit(solution)/shard_map/all_to_all | solution.py:23
  154.7 0.7 reshape.238
  155.5 3.4 %all-to-all-start.3 = ((bf16[8,64,128]{2,1,0:T(8,128)(2,1)}), bf16[8,64,128]{2,1,0:T(8,128)(2,1)S(1)}, u32[]{:S(2)}, u32[]{:S(2)}) async-start(bf16[8,64,128]{2,1,0:T(8,128)(2,1)} %reshape.238), calls=%async_computation.3 | async-start | bytes 262144 | tf_op jit(solution)/shard_map/all_to_all | solution.py:27
  159.1 0.6 fusion.6
  159.7 7.0 %all-to-all-done.3 = bf16[8,64,128]{2,1,0:T(8,128)(2,1)S(1)} async-done(((bf16[8,64,128]{2,1,0:T(8,128)(2,1)}), bf16[8,64,128]{2,1,0:T(8,128)(2,1)S(1)}, u32[]{:S(2)}, u32[]{:S(2)}) %all-to-all-start.3) | async-done | bytes 131104 | tf_op jit(solution)/shard_map/all_to_all | solution.py:27
  166.7 0.4 multiply_reduce_fusion
  167.1 1.3 slice.186.own
  168.4 1.9 collective-permute-start.10
  170.4 4.8 %collective-permute-start.9 = (bf16[2048,256]{1,0:T(8,128)(2,1)S(1)}, bf16[2048,256]{1,0:T(8,128)(2,1)}, u32[]{:S(2)}, u32[]{:S(2)}) collective-permute-start(bf16[2048,256]{1,0:T(8,128)(2,1)S(1)} %slice.186.own), channel_id=1, source_target_pairs={{0,6},{2,0},{4,2},{6,4},{1,7},{3,1},{5,3},{7,5},{8,14},{10,8},{12,... | collective-permute-start | bytes 3145736 | tf_op jit(solution)/shard_map/ppermute | solution.py:71
  175.2 6.3 %shard_map.155 = bf16[4,256,384]{2,1,0:T(8,128)(2,1)} custom-call(s32[3]{0:T(128)} %pad_add_fusion.spot, bf16[256,1024]{1,0:T(8,128)(2,1)} %copy-done.2, bf16[256,1024]{1,0:T(8,128)(2,1)} %get-tuple-element.19.refs_1_.refs_6_, bf16[256,1024]{1,0:T(8,128)(2,1)} %copy-done.3, bf16[256,1024]{1,0:T(8,128)(2,1)} %copy-done.4, bf16[256,1024]{1,0:T(8,128)(2,1)} %copy-done.5, ...), custom_call_target="tpu_custom_call" | custom-call | flops 3000000000 | bytes 6291456 | tf_op jit(solution)/shard_map/pallas_call | solution.py:202
  181.4 1.1 multiply_convert_fusion.1
  182.6 2.2 collective-permute-start.4
  185.0 0.5 collective-permute-done.4
  185.6 4.6 %collective-permute-done.10.behind = bf16[2048,256]{1,0:T(8,128)(2,1)} collective-permute-done((bf16[2048,256]{1,0:T(8,128)(2,1)S(1)}, bf16[2048,256]{1,0:T(8,128)(2,1)}, u32[]{:S(2)}, u32[]{:S(2)}) %collective-permute-start.10) | collective-permute-done | bytes 1048608 | tf_op jit(solution)/shard_map/ppermute | solution.py:71
  190.2 1.1 slice.187
  191.2 1.9 collective-permute-start.11
  193.2 1.1 slice.188
  194.3 4.6 %collective-permute-start.12 = (bf16[1024,256]{1,0:T(8,128)(2,1)S(1)}, bf16[1024,256]{1,0:T(8,128)(2,1)}, u32[]{:S(2)}, u32[]{:S(2)}) collective-permute-start(bf16[1024,256]{1,0:T(8,128)(2,1)S(1)} %slice.188), channel_id=1, source_target_pairs={{0,6},{2,0},{4,2},{6,4},{1,7},{3,1},{5,3},{7,5},{8,14},{10,8},{12,... | collective-permute-start | bytes 1572872 | tf_op jit(solution)/shard_map/ppermute | solution.py:71
  198.8 1.2 fusion.19
  200.0 0.3 fusion.15
  200.4 11.5 %all_to_all.30.parts = bf16[4,256,256]{2,1,0:T(8,128)(2,1)} all-to-all(bf16[4,256,256]{2,1,0:T(8,128)(2,1)S(1)} %fusion.15), channel_id=1, replica_groups=mesh['z'=8,'y_hi'=4,'y_lo'=2,'fs'=4,'tp'=2] {'fs'}, dimensions={0} | all-to-all | bytes 1048576 | tf_op jit(solution)/shard_map/all_to_all | solution.py:27
  211.8 0.8 copy-done.10
  212.6 4.6 %shard_map.157 = bf16[256,2048]{1,0:T(8,128)(2,1)} custom-call(s32[3]{0:T(128)} %pad_add_fusion.spot, bf16[4,256,256]{2,1,0:T(8,128)(2,1)} %all_to_all.30.parts, bf16[2048,256]{1,0:T(8,128)(2,1)} %copy-done.1, bf16[2048,256]{1,0:T(8,128)(2,1)} %collective-permute-done.9.ahead, bf16[1024,256]{1,0:T(8,128)(2,1)} %copy-done.10, ...), custom_call_target="tpu_custom_call" | custom-call | flops 2000000000 | bytes 6291456 | tf_op jit(solution)/shard_map/pallas_call | solution.py:202
  217.2 12.7 %all_to_all.31 = bf16[2,128,2048]{2,1,0:T(8,128)(2,1)S(1)} all-to-all(bf16[2,128,2048]{2,1,0:T(8,128)(2,1)} %bitcast.99), channel_id=1, replica_groups=mesh['z'=8,'y_hi'=4,'y_lo'=2,'fs'=4,'tp'=2] {'tp'}, dimensions={0} | all-to-all | bytes 2097152 | tf_op jit(solution)/shard_map/all_to_all | solution.py:27
  229.9 1.1 reduce_sum.52
  (83 shorter events, 3.8 us)
Async XLA Ops:
  6.5 119.9 %copy-start = (f32[3,1024]{1,0:T(4,128)S(1)}, f32[3,1024]{1,0:T(4,128)}, u32[]{:S(2)}) copy-start(f32[3,1024]{1,0:T(4,128)} %param.21) | copy-start | bytes 36868
  10.5 70.6 %copy-start.2 = (bf16[256,1024]{1,0:T(8,128)(2,1)}, bf16[256,1024]{1,0:T(8,128)(2,1)S(1)}, u32[]{:S(2)}) copy-start(bf16[256,1024]{1,0:T(8,128)(2,1)S(1)} %get-tuple-element.20.refs_0_.refs_5_) | copy-start | bytes 1572868
  10.5 17.1 %collective-permute-start = (bf16[256,1024]{1,0:T(8,128)(2,1)S(1)}, bf16[256,1024]{1,0:T(8,128)(2,1)S(1)}, u32[]{:S(2)}, u32[]{:S(2)}) collective-permute-start(bf16[256,1024]{1,0:T(8,128)(2,1)S(1)} %get-tuple-element.20.refs_0_.refs_5_), channel_id=1, source_target_pairs={{0,6},{2,0},{4,2},{6,4},{1,7},{3,1},{5,3},{7,5},{8,14},{10,8},{12,... | collective-permute-start | bytes 1572872 | tf_op jit(solution)/shard_map/ppermute | solution.py:71
  15.7 13.4 %collective-permute-start.1 = (bf16[256,1024]{1,0:T(8,128)(2,1)S(1)}, bf16[256,1024]{1,0:T(8,128)(2,1)S(1)}, u32[]{:S(2)}, u32[]{:S(2)}) collective-permute-start(bf16[256,1024]{1,0:T(8,128)(2,1)S(1)} %get-tuple-element.20.refs_0_.refs_5_), channel_id=1, source_target_pairs={{0,4},{2,6},{4,0},{6,2},{1,5},{3,7},{5,1},{7,3},{8,12},{10,14},{12... | collective-permute-start | bytes 1572872 | tf_op jit(solution)/shard_map/ppermute | solution.py:71
  18.1 26.0 %collective-permute-start.2 = (bf16[256,1024]{1,0:T(8,128)(2,1)S(1)}, bf16[256,1024]{1,0:T(8,128)(2,1)S(1)}, u32[]{:S(2)}, u32[]{:S(2)}) collective-permute-start(bf16[256,1024]{1,0:T(8,128)(2,1)S(1)} %get-tuple-element.20.refs_0_.refs_5_), channel_id=1, source_target_pairs={{0,2},{2,4},{4,6},{6,0},{1,3},{3,5},{5,7},{7,1},{8,10},{10,12},{12... | collective-permute-start | bytes 1572872 | tf_op jit(solution)/shard_map/ppermute | solution.py:71
  27.6 53.5 %copy-start.3 = (bf16[256,1024]{1,0:T(8,128)(2,1)}, bf16[256,1024]{1,0:T(8,128)(2,1)S(1)}, u32[]{:S(2)}) copy-start(bf16[256,1024]{1,0:T(8,128)(2,1)S(1)} %collective-permute-done.refs_2_.refs_7_) | copy-start | bytes 1572868
  29.1 52.0 %copy-start.4 = (bf16[256,1024]{1,0:T(8,128)(2,1)}, bf16[256,1024]{1,0:T(8,128)(2,1)S(1)}, u32[]{:S(2)}) copy-start(bf16[256,1024]{1,0:T(8,128)(2,1)S(1)} %collective-permute-done.1.refs_3_.refs_8_) | copy-start | bytes 1572868
  44.2 2.5 %copy-start.5 = (bf16[256,1024]{1,0:T(8,128)(2,1)}, bf16[256,1024]{1,0:T(8,128)(2,1)S(1)}, u32[]{:S(2)}) copy-start(bf16[256,1024]{1,0:T(8,128)(2,1)S(1)} %collective-permute-done.2.refs_4_.refs_9_) | copy-start | bytes 1572868
  44.3 58.9 %collective-permute-start.3 = (bf16[768,1024]{1,0:T(8,128)(2,1)S(1)}, bf16[768,1024]{1,0:T(8,128)(2,1)}, u32[]{:S(2)}, u32[]{:S(2)}) collective-permute-start(bf16[768,1024]{1,0:T(8,128)(2,1)S(1)} %pad_maximum_fusion), channel_id=1, source_target_pairs={{0,1},{1,0},{2,3},{3,2},{4,5},{5,4},{6,7},{7,6},{8,9},{9,8},{10,11... | collective-permute-start | bytes 4718600 | tf_op jit(solution)/shard_map/ppermute | solution.py:31
  48.4 23.9 %all-to-all-start = ((bf16[16,32,384]{2,1,0:T(8,128)(2,1)}), bf16[16,32,384]{2,1,0:T(8,128)(2,1)S(1)}, u32[]{:S(2)}, u32[]{:S(2)}) async-start(bf16[16,32,384]{2,1,0:T(8,128)(2,1)} %get-tuple-element.12), calls=%async_computation | async-start | bytes 786432 | tf_op jit(solution)/shard_map/all_to_all | solution.py:27
  59.5 107.6 %all-gather.2.cloned.1.call-start = ((), (), s32[]{:S(2)}) async-start(), calls=%async_computation.6 | async-start | bytes 2662400 | tf_op jit(solution)/shard_map/all_gather | solution.py:255
  72.3 30.9 %copy-start.6 = (bf16[16,32,384]{2,1,0:T(8,128)(2,1)}, bf16[16,32,384]{2,1,0:T(8,128)(2,1)S(1)}, u32[]{:S(2)}) copy-start(bf16[16,32,384]{2,1,0:T(8,128)(2,1)S(1)} %all-to-all-done) | copy-start | bytes 1179652
  72.3 12.9 %collective-permute-start.6 = (bf16[512,384]{1,0:T(8,128)(2,1)S(1)}, bf16[512,384]{1,0:T(8,128)(2,1)}, u32[]{:S(2)}, u32[]{:S(2)}) collective-permute-start(bf16[512,384]{1,0:T(8,128)(2,1)S(1)} %bitcast.102), channel_id=1, source_target_pairs={{0,16},{16,32},{32,48},{48,0},{1,17},{17,33},{33,49},{49,1},{2,18}... | collective-permute-start | bytes 1179656 | tf_op jit(solution)/shard_map/ppermute | solution.py:71
  76.5 14.6 %collective-permute-start.5 = (bf16[512,384]{1,0:T(8,128)(2,1)S(1)}, bf16[512,384]{1,0:T(8,128)(2,1)}, u32[]{:S(2)}, u32[]{:S(2)}) collective-permute-start(bf16[512,384]{1,0:T(8,128)(2,1)S(1)} %bitcast.103), channel_id=1, source_target_pairs={{0,48},{16,0},{32,16},{48,32},{1,49},{17,1},{33,17},{49,33},{2,50}... | collective-permute-start | bytes 1179656 | tf_op jit(solution)/shard_map/ppermute | solution.py:71
  86.1 16.7 %collective-permute-start.7 = (bf16[256,384]{1,0:T(8,128)(2,1)S(1)}, bf16[256,384]{1,0:T(8,128)(2,1)S(1)}, u32[]{:S(2)}, u32[]{:S(2)}) collective-permute-start(bf16[256,384]{1,0:T(8,128)(2,1)S(1)} %slice.168), channel_id=1, source_target_pairs={{0,16},{16,32},{32,48},{48,0},{1,17},{17,33},{33,49},{49,1},{2,18}... | collective-permute-start | bytes 589832 | tf_op jit(solution)/shard_map/ppermute | solution.py:71
  92.0 11.2 %collective-permute-start.8 = (bf16[256,384]{1,0:T(8,128)(2,1)S(1)}, bf16[256,384]{1,0:T(8,128)(2,1)S(1)}, u32[]{:S(2)}, u32[]{:S(2)}) collective-permute-start(bf16[256,384]{1,0:T(8,128)(2,1)S(1)} %slice.169), channel_id=1, source_target_pairs={{0,48},{16,0},{32,16},{48,32},{1,49},{17,1},{33,17},{49,33},{2,50}... | collective-permute-start | bytes 589832 | tf_op jit(solution)/shard_map/ppermute | solution.py:71
  102.8 0.7 copy-start.11
  103.2 0.7 copy-start.12
  112.0 33.1 %copy-start.8 = (f32[4,256]{1,0:T(4,128)S(1)}, f32[4,256]{1,0:T(4,128)}, u32[]{:S(2)}) copy-start(f32[4,256]{1,0:T(4,128)} %get-tuple-element.13) | copy-start | bytes 12292
  112.0 33.1 %copy-start.9 = (f32[4,256]{1,0:T(4,128)S(1)}, f32[4,256]{1,0:T(4,128)}, u32[]{:S(2)}) copy-start(f32[4,256]{1,0:T(4,128)} %get-tuple-element.15) | copy-start | bytes 12292
  112.0 47.1 %copy-start.7 = (bf16[4,256,384]{2,1,0:T(8,128)(2,1)S(1)}, bf16[4,256,384]{2,1,0:T(8,128)(2,1)}, u32[]{:S(2)}) copy-start(bf16[4,256,384]{2,1,0:T(8,128)(2,1)} %get-tuple-element.16) | copy-start | bytes 2359300
  112.0 23.4 %all-to-all-start.1 = ((bf16[8,96,128]{2,1,0:T(8,128)(2,1)}), bf16[8,96,128]{2,1,0:T(8,128)(2,1)S(1)}, u32[]{:S(2)}, u32[]{:S(2)}) async-start(bf16[8,96,128]{2,1,0:T(8,128)(2,1)} %get-tuple-element.14), calls=%async_computation.1 | async-start | bytes 393216 | tf_op jit(solution)/shard_map/all_to_all | solution.py:27
  137.7 15.8 %all-to-all-start.2 = ((bf16[8,80,128]{2,1,0:T(8,128)(2,1)}), bf16[8,80,128]{2,1,0:T(8,128)(2,1)S(1)}, u32[]{:S(2)}, u32[]{:S(2)}) async-start(bf16[8,80,128]{2,1,0:T(8,128)(2,1)} %broadcast_in_dim.90), calls=%async_computation.2 | async-start | bytes 327680 | tf_op jit(solution)/shard_map/all_to_all | solution.py:23
  155.5 11.2 %all-to-all-start.3 = ((bf16[8,64,128]{2,1,0:T(8,128)(2,1)}), bf16[8,64,128]{2,1,0:T(8,128)(2,1)S(1)}, u32[]{:S(2)}, u32[]{:S(2)}) async-start(bf16[8,64,128]{2,1,0:T(8,128)(2,1)} %reshape.238), calls=%async_computation.3 | async-start | bytes 262144 | tf_op jit(solution)/shard_map/all_to_all | solution.py:27
  168.4 13.0 %copy-start.1 = (bf16[2048,256]{1,0:T(8,128)(2,1)}, bf16[2048,256]{1,0:T(8,128)(2,1)S(1)}, u32[]{:S(2)}) copy-start(bf16[2048,256]{1,0:T(8,128)(2,1)S(1)} %slice.186.own) | copy-start | bytes 3145732
  168.4 21.7 %collective-permute-start.10 = (bf16[2048,256]{1,0:T(8,128)(2,1)S(1)}, bf16[2048,256]{1,0:T(8,128)(2,1)}, u32[]{:S(2)}, u32[]{:S(2)}) collective-permute-start(bf16[2048,256]{1,0:T(8,128)(2,1)S(1)} %slice.186.own), channel_id=1, source_target_pairs={{0,2},{2,4},{4,6},{6,0},{1,3},{3,5},{5,7},{7,1},{8,10},{10,12},{12... | collective-permute-start | bytes 3145736 | tf_op jit(solution)/shard_map/ppermute | solution.py:71
  170.4 22.8 %collective-permute-start.9 = (bf16[2048,256]{1,0:T(8,128)(2,1)S(1)}, bf16[2048,256]{1,0:T(8,128)(2,1)}, u32[]{:S(2)}, u32[]{:S(2)}) collective-permute-start(bf16[2048,256]{1,0:T(8,128)(2,1)S(1)} %slice.186.own), channel_id=1, source_target_pairs={{0,6},{2,0},{4,2},{6,4},{1,7},{3,1},{5,3},{7,5},{8,14},{10,8},{12,... | collective-permute-start | bytes 3145736 | tf_op jit(solution)/shard_map/ppermute | solution.py:71
  182.6 2.9 %collective-permute-start.4 = (bf16[4,2,128]{2,1,0:T(2,128)(2,1)S(1)}, bf16[4,2,128]{2,1,0:T(2,128)(2,1)S(1)}, u32[]{:S(2)}, u32[]{:S(2)}) collective-permute-start(bf16[4,2,128]{2,1,0:T(2,128)(2,1)S(1)} %slice.164), channel_id=1, source_target_pairs={{0,8},{8,16},{16,24},{24,32},{32,40},{40,48},{48,56},{56,64},{64,7... | collective-permute-start | bytes 6152 | tf_op jit(solution)/shard_map/ppermute | solution.py:36
  191.2 20.6 %collective-permute-start.11 = (bf16[1024,256]{1,0:T(8,128)(2,1)S(1)}, bf16[1024,256]{1,0:T(8,128)(2,1)S(1)}, u32[]{:S(2)}, u32[]{:S(2)}) collective-permute-start(bf16[1024,256]{1,0:T(8,128)(2,1)S(1)} %slice.187), channel_id=1, source_target_pairs={{0,2},{2,4},{4,6},{6,0},{1,3},{3,5},{5,7},{7,1},{8,10},{10,12},{12... | collective-permute-start | bytes 1572872 | tf_op jit(solution)/shard_map/ppermute | solution.py:71
  194.3 17.6 %collective-permute-start.12 = (bf16[1024,256]{1,0:T(8,128)(2,1)S(1)}, bf16[1024,256]{1,0:T(8,128)(2,1)}, u32[]{:S(2)}, u32[]{:S(2)}) collective-permute-start(bf16[1024,256]{1,0:T(8,128)(2,1)S(1)} %slice.188), channel_id=1, source_target_pairs={{0,6},{2,0},{4,2},{6,4},{1,7},{3,1},{5,3},{7,5},{8,14},{10,8},{12,... | collective-permute-start | bytes 1572872 | tf_op jit(solution)/shard_map/ppermute | solution.py:71
  211.8 0.8 copy-start.10
Sparse Core Ops, SparseCore 0:
  63.3 87.4 all-gather.1

commit v8 on v7

--- a/solution.py
+++ b/solution.py
@@ -97,7 +97,8 @@
         for copy in range(mem.shape[0]):
             mem[copy, :, k * wide : (k + 1) * wide] = parts[k][...]
     for k in range(5):
-        rest[:, k * wide : (k + 1) * wide] = parts[3 + k][...]
+        for copy in range(rest.shape[0]):
+            rest[copy, :, k * wide : (k + 1) * wide] = parts[3 + k][...]
 
 
 def piece(refs, k, other):
@@ -241,10 +242,11 @@
 
     channels = w_conv_gate.shape[1]
     shard = w_query.shape
+    places = lax.axis_size(Y)
     pairs = 2 * lax.axis_size("z")
     w_rest, w_mem = call(
         pack_kernel,
-        [((shard[0], 5 * shard[1]), BF16), ((pairs, shard[0], 3 * shard[1]), BF16)],
+        [((places, shard[0], 5 * shard[1]), BF16), ((pairs, shard[0], 3 * shard[1]), BF16)],
         [],
         [w_query, w_key, w_value, w_conv_gate, w_conv_mult, w_conv_in, w_out_conv.T, w_out_mem.T],
         10**6,
@@ -252,7 +254,8 @@
     w_mem = exchanged(w_mem, ("z", "y_lo")).reshape(-1, w_mem.shape[2])
     w_mem = (w_mem, *relayed(w_mem, "y_hi"))
 
-    w_rest = lax.all_gather(w_rest, SP, axis=0, tiled=True)
+    w_rest = exchanged(w_rest, Y).reshape(-1, w_rest.shape[2])
+    w_rest = lax.all_gather(w_rest, "z", axis=0, tiled=True)
     w_own = w_rest[:, 3 * channels :]
     w_out = (w_own, *relayed(w_own, "fs"))
 

time: 239 us -> 252 us (1.054)
  waiting for transfers between devices: 75 us -> 95.4 us
  local copies, waits for them, and re-layouts: 15.5 us -> 12.1 us
  blocking collectives: 24.1 us -> 21.5 us
    ppermute x11, waiting for transfers between devices: 37.8 us -> 51.1 us  [ring(): lax.ppermute(array, axis, [(i, (i + by) % peers) for i in range(peers)])]
    all_gather x1, waiting for transfers between devices: 0.01 us -> 5.97 us  [shards(): w_rest = lax.all_gather(w_rest, 'z', axis=0, tiled=True)]
    all_to_all x1, starting transfers between devices: 6.5 us -> 3.38 us  [everyone(): return lax.all_to_all(copies, axis, split_axis=0, concat_axis=0, tiled=True)]
    all_to_all x2, blocking collectives: 24.1 us -> 21.5 us  [exchanged(): return lax.all_to_all(array, axis, split_axis=0, concat_axis=0, tiled=True)]
    all_to_all x3 -> x4, starting transfers between devices: 28.9 us -> 30.8 us  [exchanged(): return lax.all_to_all(array, axis, split_axis=0, concat_axis=0, tiled=True)]
    all_to_all x3 -> x4, waiting for transfers between devices: 28 us -> 28 us  [exchanged(): return lax.all_to_all(array, axis, split_axis=0, concat_axis=0, tiled=True)]
  transfers between devices with their start and end apart: 18 -> 19, of which waited for: 13 -> 13; matrix products, arithmetic and copies ran while one was open for 8% -> 6% of each run, Pallas kernels for 7% -> 6%
where the time goes in v8:
time: 252 us; the launch traced here: 251 us
  waiting for transfers between devices  95.4 us (38%)
  starting transfers between devices  75.5 us (30%)
  blocking collectives  21.5 us (9%)
  Pallas kernels  20.7 us (8%)
  between operations  14.1 us (6%)
  local copies, waits for them, and re-layouts  12.1 us (5%)
  other arithmetic  9.38 us (4%)
    ppermute x11, waiting for transfers between devices, ring(): lax.ppermute(array, axis, [(i, (i + by) % peers) for i in range(peers)])  51.1 us
    ppermute x11, starting transfers between devices, ring(): lax.ppermute(array, axis, [(i, (i + by) % peers) for i in range(peers)])  36.1 us
    all_to_all x4, starting transfers between devices, exchanged(): return lax.all_to_all(array, axis, split_axis=0, concat_axis=0, tiled=True)  30.8 us
    all_to_all x4, waiting for transfers between devices, exchanged(): return lax.all_to_all(array, axis, split_axis=0, concat_axis=0, tiled=True)  28 us
    all_to_all x2, blocking collectives, exchanged(): return lax.all_to_all(array, axis, split_axis=0, concat_axis=0, tiled=True)  21.5 us
    pallas_call x4, Pallas kernels, call(): pl.pallas_call(kernel, out_shape=tuple((jax.ShapeDtypeStruct(shape, dtype...  20.7 us
    all_to_all x1, waiting for transfers between devices, everyone(): return lax.all_to_all(copies, axis, split_axis=0, concat_axis=0, tiled=True)  9.27 us
    all_gather x1, waiting for transfers between devices, shards(): w_rest = lax.all_gather(w_rest, 'z', axis=0, tiled=True)  5.97 us
  transfers between devices with their start and end apart: 19, of which 13 were waited for; matrix products, arithmetic and copies ran while one was open for 6% of the time, Pallas kernels for 6%

profile of v8, /device:TPU:1, one launch (start us, length us, event | category | flops | bytes accessed | tf_op | source)
XLA Modules:
  0.0 250.8 jit_solution(7998202427374502810)
XLA Ops:
  6.5 1.5 fusion.2
  8.1 1.5 fusion.4
  9.6 0.9 constant_dynamic-slice_fusion.9
  10.5 5.3 %collective-permute-start = (bf16[256,1024]{1,0:T(8,128)(2,1)S(1)}, bf16[256,1024]{1,0:T(8,128)(2,1)S(1)}, u32[]{:S(2)}, u32[]{:S(2)}) collective-permute-start(bf16[256,1024]{1,0:T(8,128)(2,1)S(1)} %get-tuple-element.20.refs_0_.refs_5_), channel_id=1, source_target_pairs={{0,6},{2,0},{4,2},{6,4},{1,7},{3,1},{5,3},{7,5},{8,14},{10,8},{12,... | collective-permute-start | bytes 1572872 | tf_op jit(solution)/shard_map/ppermute | solution.py:71
  15.8 2.4 collective-permute-start.1
  18.3 2.5 %collective-permute-start.2 = (bf16[256,1024]{1,0:T(8,128)(2,1)S(1)}, bf16[256,1024]{1,0:T(8,128)(2,1)S(1)}, u32[]{:S(2)}, u32[]{:S(2)}) collective-permute-start(bf16[256,1024]{1,0:T(8,128)(2,1)S(1)} %get-tuple-element.20.refs_0_.refs_5_), channel_id=1, source_target_pairs={{0,2},{2,4},{4,6},{6,0},{1,3},{3,5},{5,7},{7,1},{8,10},{10,12},{12... | collective-permute-start | bytes 1572872 | tf_op jit(solution)/shard_map/ppermute | solution.py:71
  20.8 7.0 %collective-permute-done.refs_2_.refs_7_ = bf16[256,1024]{1,0:T(8,128)(2,1)S(1)} collective-permute-done((bf16[256,1024]{1,0:T(8,128)(2,1)S(1)}, bf16[256,1024]{1,0:T(8,128)(2,1)S(1)}, u32[]{:S(2)}, u32[]{:S(2)}) %collective-permute-start) | collective-permute-done | bytes 524320 | tf_op jit(solution)/shard_map/ppermute | solution.py:71
  27.8 1.5 collective-permute-done.1.refs_3_.refs_8_
  29.2 15.1 %collective-permute-done.2.refs_4_.refs_9_ = bf16[256,1024]{1,0:T(8,128)(2,1)S(1)} collective-permute-done((bf16[256,1024]{1,0:T(8,128)(2,1)S(1)}, bf16[256,1024]{1,0:T(8,128)(2,1)S(1)}, u32[]{:S(2)}, u32[]{:S(2)}) %collective-permute-start.2) | collective-permute-done | bytes 524320 | tf_op jit(solution)/shard_map/ppermute | solution.py:71
  44.4 2.4 collective-permute-start.3
  46.9 1.7 shard_map.154
  48.6 11.2 %all-to-all-start.1 = ((bf16[16,32,384]{2,1,0:T(8,128)(2,1)}), bf16[16,32,384]{2,1,0:T(8,128)(2,1)}, u32[]{:S(2)}, u32[]{:S(2)}) async-start(bf16[16,32,384]{2,1,0:T(8,128)(2,1)} %get-tuple-element.12), calls=%async_computation.1 | async-start | bytes 786432 | tf_op jit(solution)/shard_map/all_to_all | solution.py:27
  59.8 12.8 %all-to-all-done.1 = bf16[16,32,384]{2,1,0:T(8,128)(2,1)} async-done(((bf16[16,32,384]{2,1,0:T(8,128)(2,1)}), bf16[16,32,384]{2,1,0:T(8,128)(2,1)}, u32[]{:S(2)}, u32[]{:S(2)}) %all-to-all-start.1) | async-done | bytes 393248 | tf_op jit(solution)/shard_map/all_to_all | solution.py:27
  72.6 7.1 %all-to-all-start = ((bf16[8,32,640]{2,1,0:T(8,128)(2,1)}), bf16[8,32,640]{2,1,0:T(8,128)(2,1)S(1)}, u32[]{:S(2)}, u32[]{:S(2)}) async-start(bf16[8,32,640]{2,1,0:T(8,128)(2,1)} %get-tuple-element.11), calls=%async_computation | async-start | bytes 655360 | tf_op jit(solution)/shard_map/all_to_all | solution.py:27
  79.7 4.3 %collective-permute-start.6 = (bf16[512,384]{1,0:T(8,128)(2,1)}, bf16[512,384]{1,0:T(8,128)(2,1)S(1)}, u32[]{:S(2)}, u32[]{:S(2)}) collective-permute-start(bf16[512,384]{1,0:T(8,128)(2,1)} %bitcast.11.refs_0_), channel_id=1, source_target_pairs={{0,16},{16,32},{32,48},{48,0},{1,17},{17,33},{33,49},{49,1},{2,18}... | collective-permute-start | bytes 1179656 | tf_op jit(solution)/shard_map/ppermute | solution.py:71
  83.9 3.1 %collective-permute-start.5 = (bf16[512,384]{1,0:T(8,128)(2,1)}, bf16[512,384]{1,0:T(8,128)(2,1)S(1)}, u32[]{:S(2)}, u32[]{:S(2)}) collective-permute-start(bf16[512,384]{1,0:T(8,128)(2,1)} %bitcast.11.refs_0_), channel_id=1, source_target_pairs={{0,48},{16,0},{32,16},{48,32},{1,49},{17,1},{33,17},{49,33},{2,50}... | collective-permute-start | bytes 1179656 | tf_op jit(solution)/shard_map/ppermute | solution.py:71
  87.1 0.8 constant_dynamic-slice_fusion.5
  88.0 0.6 copy.82
  88.6 0.7 fusion.61.bias
  89.3 0.8 fusion.62
  90.1 13.2 %collective-permute-done.6.refs_4_ = bf16[512,384]{1,0:T(8,128)(2,1)S(1)} collective-permute-done((bf16[512,384]{1,0:T(8,128)(2,1)}, bf16[512,384]{1,0:T(8,128)(2,1)S(1)}, u32[]{:S(2)}, u32[]{:S(2)}) %collective-permute-start.6) | collective-permute-done | bytes 393248 | tf_op jit(solution)/shard_map/ppermute | solution.py:71
  103.4 1.9 collective-permute-start.7
  105.3 2.6 %collective-permute-done.5.refs_1_ = bf16[512,384]{1,0:T(8,128)(2,1)S(1)} collective-permute-done((bf16[512,384]{1,0:T(8,128)(2,1)}, bf16[512,384]{1,0:T(8,128)(2,1)S(1)}, u32[]{:S(2)}, u32[]{:S(2)}) %collective-permute-start.5) | collective-permute-done | bytes 393248 | tf_op jit(solution)/shard_map/ppermute | solution.py:71
  107.9 3.3 %collective-permute-start.8 = (bf16[256,384]{1,0:T(8,128)(2,1)S(1)}, bf16[256,384]{1,0:T(8,128)(2,1)S(1)}, u32[]{:S(2)}, u32[]{:S(2)}) collective-permute-start(bf16[256,384]{1,0:T(8,128)(2,1)S(1)} %slice.169), channel_id=1, source_target_pairs={{0,48},{16,0},{32,16},{48,32},{1,49},{17,1},{33,17},{49,33},{2,50}... | collective-permute-start | bytes 589832 | tf_op jit(solution)/shard_map/ppermute | solution.py:71
  111.2 0.7 pad_add_fusion.spot
  111.9 0.6 pad_maximum_fusion.2.refs_12_
  112.5 4.8 %collective-permute-done.8.refs_3_ = bf16[256,384]{1,0:T(8,128)(2,1)S(1)} collective-permute-done((bf16[256,384]{1,0:T(8,128)(2,1)S(1)}, bf16[256,384]{1,0:T(8,128)(2,1)S(1)}, u32[]{:S(2)}, u32[]{:S(2)}) %collective-permute-start.8) | collective-permute-done | bytes 196640 | tf_op jit(solution)/shard_map/ppermute | solution.py:71
  117.4 0.7 copy-done.17
  118.0 8.1 %shard_map.156 = (bf16[4,256,384]{2,1,0:T(8,128)(2,1)}, bf16[8,96,128]{2,1,0:T(8,128)(2,1)}, f32[4,256]{1,0:T(4,128)}, f32[4,256]{1,0:T(4,128)}) custom-call(s32[3]{0:T(128)} %pad_add_fusion.spot, f32[2]{0:T(128)} %fusion.61.bias, bf16[512,384]{1,0:T(8,128)(2,1)} %bitcast.11.refs_0_, bf16[512,384]{1,0:T(8,128)(2,1)} %copy-done.9, ...), custom_call_target="tpu_custom_call" | custom-call | flops 3000000000 | bytes 6291456 | tf_op jit(solution)/shard_map/pallas_call | solution.py:203
  126.2 9.2 %all-to-all-start.2 = ((bf16[8,96,128]{2,1,0:T(8,128)(2,1)}), bf16[8,96,128]{2,1,0:T(8,128)(2,1)S(1)}, u32[]{:S(2)}, u32[]{:S(2)}) async-start(bf16[8,96,128]{2,1,0:T(8,128)(2,1)} %get-tuple-element.14), calls=%async_computation.2 | async-start | bytes 393216 | tf_op jit(solution)/shard_map/all_to_all | solution.py:27
  135.5 0.6 all-gather.2.cloned.1.call-update
  136.1 8.2 %all-to-all-done.2 = bf16[8,96,128]{2,1,0:T(8,128)(2,1)S(1)} async-done(((bf16[8,96,128]{2,1,0:T(8,128)(2,1)}), bf16[8,96,128]{2,1,0:T(8,128)(2,1)S(1)}, u32[]{:S(2)}, u32[]{:S(2)}) %all-to-all-start.2) | async-done | bytes 196640 | tf_op jit(solution)/shard_map/all_to_all | solution.py:27
  145.9 0.7 broadcast_in_dim.90
  146.6 3.4 %all-to-all-start.3 = ((bf16[8,80,128]{2,1,0:T(8,128)(2,1)}), bf16[8,80,128]{2,1,0:T(8,128)(2,1)S(1)}, u32[]{:S(2)}, u32[]{:S(2)}) async-start(bf16[8,80,128]{2,1,0:T(8,128)(2,1)} %broadcast_in_dim.90), calls=%async_computation.3 | async-start | bytes 327680 | tf_op jit(solution)/shard_map/all_to_all | solution.py:23
  150.0 0.8 dynamic_slice.63
  150.8 0.4 fusion.13
  151.2 9.3 %all-to-all-done.3 = bf16[8,80,128]{2,1,0:T(8,128)(2,1)S(1)} async-done(((bf16[8,80,128]{2,1,0:T(8,128)(2,1)}), bf16[8,80,128]{2,1,0:T(8,128)(2,1)S(1)}, u32[]{:S(2)}, u32[]{:S(2)}) %all-to-all-start.3) | async-done | bytes 163872 | tf_op jit(solution)/shard_map/all_to_all | solution.py:23
  160.8 0.2 fusion.73
  161.3 0.2 fusion.1
  161.7 0.7 reshape.242
  162.4 3.4 %all-to-all-start.4 = ((bf16[8,64,128]{2,1,0:T(8,128)(2,1)}), bf16[8,64,128]{2,1,0:T(8,128)(2,1)S(1)}, u32[]{:S(2)}, u32[]{:S(2)}) async-start(bf16[8,64,128]{2,1,0:T(8,128)(2,1)} %reshape.242), calls=%async_computation.4 | async-start | bytes 262144 | tf_op jit(solution)/shard_map/all_to_all | solution.py:27
  166.1 0.6 fusion.6
  166.7 7.0 %all-to-all-done.4 = bf16[8,64,128]{2,1,0:T(8,128)(2,1)S(1)} async-done(((bf16[8,64,128]{2,1,0:T(8,128)(2,1)}), bf16[8,64,128]{2,1,0:T(8,128)(2,1)S(1)}, u32[]{:S(2)}, u32[]{:S(2)}) %all-to-all-start.4) | async-done | bytes 131104 | tf_op jit(solution)/shard_map/all_to_all | solution.py:27
  173.7 0.4 multiply_reduce_fusion
  174.1 6.0 %all-gather.2.cloned.1.call-done.refs_6_ = bf16[2048,640]{1,0:T(8,128)(2,1)} async-done(((bf16[256,640]{1,0:T(8,128)(2,1)}), bf16[2048,640]{1,0:T(8,128)(2,1)}) %all-gather.2.cloned.1.call-update) | async-done | bytes 2621456 | tf_op jit(solution)/shard_map/all_gather | solution.py:258
  180.1 1.3 slice.186.own
  181.4 2.7 %collective-permute-start.10 = (bf16[2048,256]{1,0:T(8,128)(2,1)S(1)}, bf16[2048,256]{1,0:T(8,128)(2,1)S(1)}, u32[]{:S(2)}, u32[]{:S(2)}) collective-permute-start(bf16[2048,256]{1,0:T(8,128)(2,1)S(1)} %slice.186.own), channel_id=1, source_target_pairs={{0,2},{2,4},{4,6},{6,0},{1,3},{3,5},{5,7},{7,1},{8,10},{10,12},{12... | collective-permute-start | bytes 3145736 | tf_op jit(solution)/shard_map/ppermute | solution.py:71
  184.0 4.0 %collective-permute-start.9 = (bf16[2048,256]{1,0:T(8,128)(2,1)S(1)}, bf16[2048,256]{1,0:T(8,128)(2,1)}, u32[]{:S(2)}, u32[]{:S(2)}) collective-permute-start(bf16[2048,256]{1,0:T(8,128)(2,1)S(1)} %slice.186.own), channel_id=1, source_target_pairs={{0,6},{2,0},{4,2},{6,4},{1,7},{3,1},{5,3},{7,5},{8,14},{10,8},{12,... | collective-permute-start | bytes 3145736 | tf_op jit(solution)/shard_map/ppermute | solution.py:71
  188.1 6.3 %shard_map.155 = bf16[4,256,384]{2,1,0:T(8,128)(2,1)} custom-call(s32[3]{0:T(128)} %pad_add_fusion.spot, bf16[256,1024]{1,0:T(8,128)(2,1)} %copy-done.3, bf16[256,1024]{1,0:T(8,128)(2,1)} %get-tuple-element.19.refs_1_.refs_6_, bf16[256,1024]{1,0:T(8,128)(2,1)} %copy-done.4, bf16[256,1024]{1,0:T(8,128)(2,1)} %copy-done.5, bf16[256,1024]{1,0:T(8,128)(2,1)} %copy-done.6, ...), custom_call_target="tpu_custom_call" | custom-call | flops 3000000000 | bytes 6291456 | tf_op jit(solution)/shard_map/pallas_call | solution.py:203
  194.4 1.1 multiply_convert_fusion.1
  195.5 2.8 %collective-permute-start.4 = (bf16[4,2,128]{2,1,0:T(2,128)(2,1)S(1)}, bf16[4,2,128]{2,1,0:T(2,128)(2,1)S(1)}, u32[]{:S(2)}, u32[]{:S(2)}) collective-permute-start(bf16[4,2,128]{2,1,0:T(2,128)(2,1)S(1)} %slice.164), channel_id=1, source_target_pairs={{0,8},{8,16},{16,24},{24,32},{32,40},{40,48},{48,56},{56,64},{64,7... | collective-permute-start | bytes 6152 | tf_op jit(solution)/shard_map/ppermute | solution.py:36
  198.5 0.5 collective-permute-done.4
  199.1 6.9 %collective-permute-done.10.behind = bf16[2048,256]{1,0:T(8,128)(2,1)S(1)} collective-permute-done((bf16[2048,256]{1,0:T(8,128)(2,1)S(1)}, bf16[2048,256]{1,0:T(8,128)(2,1)S(1)}, u32[]{:S(2)}, u32[]{:S(2)}) %collective-permute-start.10) | collective-permute-done | bytes 1048608 | tf_op jit(solution)/shard_map/ppermute | solution.py:71
  206.0 1.9 collective-permute-start.11
  207.9 1.1 slice.188
  209.0 4.6 %collective-permute-start.12 = (bf16[1024,256]{1,0:T(8,128)(2,1)S(1)}, bf16[1024,256]{1,0:T(8,128)(2,1)S(1)}, u32[]{:S(2)}, u32[]{:S(2)}) collective-permute-start(bf16[1024,256]{1,0:T(8,128)(2,1)S(1)} %slice.188), channel_id=1, source_target_pairs={{0,6},{2,0},{4,2},{6,4},{1,7},{3,1},{5,3},{7,5},{8,14},{10,8},{12,... | collective-permute-start | bytes 1572872 | tf_op jit(solution)/shard_map/ppermute | solution.py:71
  213.6 1.2 fusion.19
  214.7 0.3 fusion.15
  215.1 10.8 %all_to_all.35.parts = bf16[4,256,256]{2,1,0:T(8,128)(2,1)} all-to-all(bf16[4,256,256]{2,1,0:T(8,128)(2,1)S(1)} %fusion.15), channel_id=1, replica_groups=mesh['z'=8,'y_hi'=4,'y_lo'=2,'fs'=4,'tp'=2] {'fs'}, dimensions={0} | all-to-all | bytes 1048576 | tf_op jit(solution)/shard_map/all_to_all | solution.py:27
  225.9 0.8 copy-done.14
  226.7 0.8 copy-done.15
  227.5 4.6 %shard_map.157 = bf16[256,2048]{1,0:T(8,128)(2,1)} custom-call(s32[3]{0:T(128)} %pad_add_fusion.spot, bf16[4,256,256]{2,1,0:T(8,128)(2,1)} %all_to_all.35.parts, bf16[2048,256]{1,0:T(8,128)(2,1)} %copy-done.2, bf16[2048,256]{1,0:T(8,128)(2,1)} %collective-permute-done.9.ahead, bf16[1024,256]{1,0:T(8,128)(2,1)} %copy-done.14, bf16[1024,256]{1,0:T(8,128)(2,1)} %copy-done.15, ...), custom_call_target="tpu_custom_call" | custom-call | flops 2000000000 | bytes 6291456 | tf_op jit(solution)/shard_map/pallas_call | solution.py:203
  232.1 10.7 %all_to_all.36 = bf16[2,128,2048]{2,1,0:T(8,128)(2,1)S(1)} all-to-all(bf16[2,128,2048]{2,1,0:T(8,128)(2,1)} %bitcast.101), channel_id=1, replica_groups=mesh['z'=8,'y_hi'=4,'y_lo'=2,'fs'=4,'tp'=2] {'tp'}, dimensions={0} | all-to-all | bytes 2097152 | tf_op jit(solution)/shard_map/all_to_all | solution.py:27
  242.8 1.1 reduce_sum.52
  (95 shorter events, 3.2 us)
Async XLA Ops:
  6.5 128.9 %copy-start = (f32[3,1024]{1,0:T(4,128)S(1)}, f32[3,1024]{1,0:T(4,128)}, u32[]{:S(2)}) copy-start(f32[3,1024]{1,0:T(4,128)} %param.21) | copy-start | bytes 36868
  10.5 62.1 %copy-start.3 = (bf16[256,1024]{1,0:T(8,128)(2,1)}, bf16[256,1024]{1,0:T(8,128)(2,1)S(1)}, u32[]{:S(2)}) copy-start(bf16[256,1024]{1,0:T(8,128)(2,1)S(1)} %get-tuple-element.20.refs_0_.refs_5_) | copy-start | bytes 1572868
  10.5 78.1 %copy-start.13 = (f32[2,8]{1,0:T(2,128)S(1)}, f32[2,8]{1,0:T(2,128)}, u32[]{:S(2)}) copy-start(f32[2,8]{1,0:T(2,128)} %param.27) | copy-start | bytes 196
  10.5 17.3 %collective-permute-start = (bf16[256,1024]{1,0:T(8,128)(2,1)S(1)}, bf16[256,1024]{1,0:T(8,128)(2,1)S(1)}, u32[]{:S(2)}, u32[]{:S(2)}) collective-permute-start(bf16[256,1024]{1,0:T(8,128)(2,1)S(1)} %get-tuple-element.20.refs_0_.refs_5_), channel_id=1, source_target_pairs={{0,6},{2,0},{4,2},{6,4},{1,7},{3,1},{5,3},{7,5},{8,14},{10,8},{12,... | collective-permute-start | bytes 1572872 | tf_op jit(solution)/shard_map/ppermute | solution.py:71
  15.8 13.4 %collective-permute-start.1 = (bf16[256,1024]{1,0:T(8,128)(2,1)S(1)}, bf16[256,1024]{1,0:T(8,128)(2,1)S(1)}, u32[]{:S(2)}, u32[]{:S(2)}) collective-permute-start(bf16[256,1024]{1,0:T(8,128)(2,1)S(1)} %get-tuple-element.20.refs_0_.refs_5_), channel_id=1, source_target_pairs={{0,4},{2,6},{4,0},{6,2},{1,5},{3,7},{5,1},{7,3},{8,12},{10,14},{12... | collective-permute-start | bytes 1572872 | tf_op jit(solution)/shard_map/ppermute | solution.py:71
  18.3 26.0 %collective-permute-start.2 = (bf16[256,1024]{1,0:T(8,128)(2,1)S(1)}, bf16[256,1024]{1,0:T(8,128)(2,1)S(1)}, u32[]{:S(2)}, u32[]{:S(2)}) collective-permute-start(bf16[256,1024]{1,0:T(8,128)(2,1)S(1)} %get-tuple-element.20.refs_0_.refs_5_), channel_id=1, source_target_pairs={{0,2},{2,4},{4,6},{6,0},{1,3},{3,5},{5,7},{7,1},{8,10},{10,12},{12... | collective-permute-start | bytes 1572872 | tf_op jit(solution)/shard_map/ppermute | solution.py:71
  27.8 44.9 %copy-start.4 = (bf16[256,1024]{1,0:T(8,128)(2,1)}, bf16[256,1024]{1,0:T(8,128)(2,1)S(1)}, u32[]{:S(2)}) copy-start(bf16[256,1024]{1,0:T(8,128)(2,1)S(1)} %collective-permute-done.refs_2_.refs_7_) | copy-start | bytes 1572868
  29.2 43.4 %copy-start.5 = (bf16[256,1024]{1,0:T(8,128)(2,1)}, bf16[256,1024]{1,0:T(8,128)(2,1)S(1)}, u32[]{:S(2)}) copy-start(bf16[256,1024]{1,0:T(8,128)(2,1)S(1)} %collective-permute-done.1.refs_3_.refs_8_) | copy-start | bytes 1572868
  44.3 2.5 %copy-start.6 = (bf16[256,1024]{1,0:T(8,128)(2,1)}, bf16[256,1024]{1,0:T(8,128)(2,1)S(1)}, u32[]{:S(2)}) copy-start(bf16[256,1024]{1,0:T(8,128)(2,1)S(1)} %collective-permute-done.2.refs_4_.refs_9_) | copy-start | bytes 1572868
  44.4 72.9 %collective-permute-start.3 = (bf16[768,1024]{1,0:T(8,128)(2,1)S(1)}, bf16[768,1024]{1,0:T(8,128)(2,1)}, u32[]{:S(2)}, u32[]{:S(2)}) collective-permute-start(bf16[768,1024]{1,0:T(8,128)(2,1)S(1)} %pad_maximum_fusion), channel_id=1, source_target_pairs={{0,1},{1,0},{2,3},{3,2},{4,5},{5,4},{6,7},{7,6},{8,9},{9,8},{10,11... | collective-permute-start | bytes 4718600 | tf_op jit(solution)/shard_map/ppermute | solution.py:31
  48.6 24.0 %all-to-all-start.1 = ((bf16[16,32,384]{2,1,0:T(8,128)(2,1)}), bf16[16,32,384]{2,1,0:T(8,128)(2,1)}, u32[]{:S(2)}, u32[]{:S(2)}) async-start(bf16[16,32,384]{2,1,0:T(8,128)(2,1)} %get-tuple-element.12), calls=%async_computation.1 | async-start | bytes 786432 | tf_op jit(solution)/shard_map/all_to_all | solution.py:27
  72.6 53.5 %all-to-all-start = ((bf16[8,32,640]{2,1,0:T(8,128)(2,1)}), bf16[8,32,640]{2,1,0:T(8,128)(2,1)S(1)}, u32[]{:S(2)}, u32[]{:S(2)}) async-start(bf16[8,32,640]{2,1,0:T(8,128)(2,1)} %get-tuple-element.11), calls=%async_computation | async-start | bytes 655360 | tf_op jit(solution)/shard_map/all_to_all | solution.py:27
  79.7 23.6 %collective-permute-start.6 = (bf16[512,384]{1,0:T(8,128)(2,1)}, bf16[512,384]{1,0:T(8,128)(2,1)S(1)}, u32[]{:S(2)}, u32[]{:S(2)}) collective-permute-start(bf16[512,384]{1,0:T(8,128)(2,1)} %bitcast.11.refs_0_), channel_id=1, source_target_pairs={{0,16},{16,32},{32,48},{48,0},{1,17},{17,33},{33,49},{49,1},{2,18}... | collective-permute-start | bytes 1179656 | tf_op jit(solution)/shard_map/ppermute | solution.py:71
  83.9 23.9 %collective-permute-start.5 = (bf16[512,384]{1,0:T(8,128)(2,1)}, bf16[512,384]{1,0:T(8,128)(2,1)S(1)}, u32[]{:S(2)}, u32[]{:S(2)}) collective-permute-start(bf16[512,384]{1,0:T(8,128)(2,1)} %bitcast.11.refs_0_), channel_id=1, source_target_pairs={{0,48},{16,0},{32,16},{48,32},{1,49},{17,1},{33,17},{49,33},{2,50}... | collective-permute-start | bytes 1179656 | tf_op jit(solution)/shard_map/ppermute | solution.py:71
  103.3 14.0 %copy-start.8 = (bf16[512,384]{1,0:T(8,128)(2,1)}, bf16[512,384]{1,0:T(8,128)(2,1)S(1)}, u32[]{:S(2)}) copy-start(bf16[512,384]{1,0:T(8,128)(2,1)S(1)} %collective-permute-done.6.refs_4_) | copy-start | bytes 1179652
  103.4 9.1 %collective-permute-start.7 = (bf16[256,384]{1,0:T(8,128)(2,1)S(1)}, bf16[256,384]{1,0:T(8,128)(2,1)S(1)}, u32[]{:S(2)}, u32[]{:S(2)}) collective-permute-start(bf16[256,384]{1,0:T(8,128)(2,1)S(1)} %slice.168), channel_id=1, source_target_pairs={{0,16},{16,32},{32,48},{48,0},{1,17},{17,33},{33,49},{49,1},{2,18}... | collective-permute-start | bytes 589832 | tf_op jit(solution)/shard_map/ppermute | solution.py:71
  107.9 9.5 %copy-start.9 = (bf16[512,384]{1,0:T(8,128)(2,1)}, bf16[512,384]{1,0:T(8,128)(2,1)S(1)}, u32[]{:S(2)}) copy-start(bf16[512,384]{1,0:T(8,128)(2,1)S(1)} %collective-permute-done.5.refs_1_) | copy-start | bytes 1179652
  107.9 9.4 %collective-permute-start.8 = (bf16[256,384]{1,0:T(8,128)(2,1)S(1)}, bf16[256,384]{1,0:T(8,128)(2,1)S(1)}, u32[]{:S(2)}, u32[]{:S(2)}) collective-permute-start(bf16[256,384]{1,0:T(8,128)(2,1)S(1)} %slice.169), channel_id=1, source_target_pairs={{0,48},{16,0},{32,16},{48,32},{1,49},{17,1},{33,17},{49,33},{2,50}... | collective-permute-start | bytes 589832 | tf_op jit(solution)/shard_map/ppermute | solution.py:71
  112.5 4.9 %copy-start.16 = (bf16[256,384]{1,0:T(8,128)(2,1)}, bf16[256,384]{1,0:T(8,128)(2,1)S(1)}, u32[]{:S(2)}) copy-start(bf16[256,384]{1,0:T(8,128)(2,1)S(1)} %collective-permute-done.7.refs_2_) | copy-start | bytes 589828
  117.4 0.7 copy-start.17
  126.1 24.7 %copy-start.11 = (f32[4,256]{1,0:T(4,128)S(1)}, f32[4,256]{1,0:T(4,128)}, u32[]{:S(2)}) copy-start(f32[4,256]{1,0:T(4,128)} %get-tuple-element.13) | copy-start | bytes 12292
  126.1 24.7 %copy-start.12 = (f32[4,256]{1,0:T(4,128)S(1)}, f32[4,256]{1,0:T(4,128)}, u32[]{:S(2)}) copy-start(f32[4,256]{1,0:T(4,128)} %get-tuple-element.15) | copy-start | bytes 12292
  126.2 9.3 %copy-start.1 = (bf16[8,32,640]{2,1,0:T(8,128)(2,1)}, bf16[8,32,640]{2,1,0:T(8,128)(2,1)S(1)}, u32[]{:S(2)}) copy-start(bf16[8,32,640]{2,1,0:T(8,128)(2,1)S(1)} %all-to-all-done) | copy-start | bytes 983044
  126.2 18.1 %all-to-all-start.2 = ((bf16[8,96,128]{2,1,0:T(8,128)(2,1)}), bf16[8,96,128]{2,1,0:T(8,128)(2,1)S(1)}, u32[]{:S(2)}, u32[]{:S(2)}) async-start(bf16[8,96,128]{2,1,0:T(8,128)(2,1)} %get-tuple-element.14), calls=%async_computation.2 | async-start | bytes 393216 | tf_op jit(solution)/shard_map/all_to_all | solution.py:27
  135.4 30.7 %copy-start.10 = (bf16[4,256,384]{2,1,0:T(8,128)(2,1)S(1)}, bf16[4,256,384]{2,1,0:T(8,128)(2,1)}, u32[]{:S(2)}) copy-start(bf16[4,256,384]{2,1,0:T(8,128)(2,1)} %get-tuple-element.16) | copy-start | bytes 2359300
  135.4 44.7 %all-gather.2.cloned.1.call-start = ((), (), s32[]{:S(2)}) async-start(), calls=%async_computation.7 | async-start | bytes 2949120 | tf_op jit(solution)/shard_map/all_gather | solution.py:258
  146.6 13.9 %all-to-all-start.3 = ((bf16[8,80,128]{2,1,0:T(8,128)(2,1)}), bf16[8,80,128]{2,1,0:T(8,128)(2,1)S(1)}, u32[]{:S(2)}, u32[]{:S(2)}) async-start(bf16[8,80,128]{2,1,0:T(8,128)(2,1)} %broadcast_in_dim.90), calls=%async_computation.3 | async-start | bytes 327680 | tf_op jit(solution)/shard_map/all_to_all | solution.py:23
  162.4 11.2 %all-to-all-start.4 = ((bf16[8,64,128]{2,1,0:T(8,128)(2,1)}), bf16[8,64,128]{2,1,0:T(8,128)(2,1)S(1)}, u32[]{:S(2)}, u32[]{:S(2)}) async-start(bf16[8,64,128]{2,1,0:T(8,128)(2,1)} %reshape.242), calls=%async_computation.4 | async-start | bytes 262144 | tf_op jit(solution)/shard_map/all_to_all | solution.py:27
  181.4 13.0 %copy-start.2 = (bf16[2048,256]{1,0:T(8,128)(2,1)}, bf16[2048,256]{1,0:T(8,128)(2,1)S(1)}, u32[]{:S(2)}) copy-start(bf16[2048,256]{1,0:T(8,128)(2,1)S(1)} %slice.186.own) | copy-start | bytes 3145732
  181.4 24.6 %collective-permute-start.10 = (bf16[2048,256]{1,0:T(8,128)(2,1)S(1)}, bf16[2048,256]{1,0:T(8,128)(2,1)S(1)}, u32[]{:S(2)}, u32[]{:S(2)}) collective-permute-start(bf16[2048,256]{1,0:T(8,128)(2,1)S(1)} %slice.186.own), channel_id=1, source_target_pairs={{0,2},{2,4},{4,6},{6,0},{1,3},{3,5},{5,7},{7,1},{8,10},{10,12},{12... | collective-permute-start | bytes 3145736 | tf_op jit(solution)/shard_map/ppermute | solution.py:71
  184.0 23.9 %collective-permute-start.9 = (bf16[2048,256]{1,0:T(8,128)(2,1)S(1)}, bf16[2048,256]{1,0:T(8,128)(2,1)}, u32[]{:S(2)}, u32[]{:S(2)}) collective-permute-start(bf16[2048,256]{1,0:T(8,128)(2,1)S(1)} %slice.186.own), channel_id=1, source_target_pairs={{0,6},{2,0},{4,2},{6,4},{1,7},{3,1},{5,3},{7,5},{8,14},{10,8},{12,... | collective-permute-start | bytes 3145736 | tf_op jit(solution)/shard_map/ppermute | solution.py:71
  195.5 3.5 %collective-permute-start.4 = (bf16[4,2,128]{2,1,0:T(2,128)(2,1)S(1)}, bf16[4,2,128]{2,1,0:T(2,128)(2,1)S(1)}, u32[]{:S(2)}, u32[]{:S(2)}) collective-permute-start(bf16[4,2,128]{2,1,0:T(2,128)(2,1)S(1)} %slice.164), channel_id=1, source_target_pairs={{0,8},{8,16},{16,24},{24,32},{32,40},{40,48},{48,56},{56,64},{64,7... | collective-permute-start | bytes 6152 | tf_op jit(solution)/shard_map/ppermute | solution.py:36
  205.9 8.8 %copy-start.7 = (bf16[2048,256]{1,0:T(8,128)(2,1)}, bf16[2048,256]{1,0:T(8,128)(2,1)S(1)}, u32[]{:S(2)}) copy-start(bf16[2048,256]{1,0:T(8,128)(2,1)S(1)} %collective-permute-done.10.behind) | copy-start | bytes 3145732
  206.0 19.9 %collective-permute-start.11 = (bf16[1024,256]{1,0:T(8,128)(2,1)S(1)}, bf16[1024,256]{1,0:T(8,128)(2,1)S(1)}, u32[]{:S(2)}, u32[]{:S(2)}) collective-permute-start(bf16[1024,256]{1,0:T(8,128)(2,1)S(1)} %slice.187), channel_id=1, source_target_pairs={{0,2},{2,4},{4,6},{6,0},{1,3},{3,5},{5,7},{7,1},{8,10},{10,12},{12... | collective-permute-start | bytes 1572872 | tf_op jit(solution)/shard_map/ppermute | solution.py:71
  209.0 16.9 %collective-permute-start.12 = (bf16[1024,256]{1,0:T(8,128)(2,1)S(1)}, bf16[1024,256]{1,0:T(8,128)(2,1)S(1)}, u32[]{:S(2)}, u32[]{:S(2)}) collective-permute-start(bf16[1024,256]{1,0:T(8,128)(2,1)S(1)} %slice.188), channel_id=1, source_target_pairs={{0,6},{2,0},{4,2},{6,4},{1,7},{3,1},{5,3},{7,5},{8,14},{10,8},{12,... | collective-permute-start | bytes 1572872 | tf_op jit(solution)/shard_map/ppermute | solution.py:71
  225.9 0.8 copy-start.14
  226.7 0.8 copy-start.15
Sparse Core Ops, SparseCore 0:
  138.3 41.7 all-gather.1

commit v9 on v7

--- a/solution.py
+++ b/solution.py
@@ -296,6 +296,15 @@
     query, key, value = (qkv[..., k * HEAD_DIM : (k + 1) * HEAD_DIM] for k in range(3))
     scale = HEAD_DIM ** (-0.5)
 
+    spans = jnp.arange(tokens)
+    causal = spans[:, None] >= spans[None, :]
+    pair_logs = jnp.where(causal, sums[:, :, None] - sums[:, None, :] + entry[:, None, :], -jnp.inf)
+    inner_peak = jnp.max(pair_logs, axis=-1)
+    scores = scale * jnp.exp(pair_logs - inner_peak[..., None])
+    scores = scores * dot(query, key, (((2,), (2,)), ((0,), (0,))))
+    inner = dot(scores.astype(BF16), value, (((2,), (1,)), ((0,), (0,))))
+    inner = lax.optimization_barrier(inner)
+
     packed = exchanged(packed, Y)
     line = jnp.arange(places)
     after = (line[:, None] > line[None, :]).astype(F32)
@@ -350,18 +359,12 @@
     for j in range(1, taps):
         mixed = mixed + tap_rows[j] * padded[:, j : j + tokens]
     conv_out = (gate.astype(F32) * mixed).astype(BF16)
-    spans = jnp.arange(tokens)
-    causal = spans[:, None] >= spans[None, :]
-    pair_logs = jnp.where(
-        causal, sums[:, :, None] - sums[:, None, :] + entry[:, None, :], -jnp.inf
-    )
     carried_logs = sums + prior_peak
-    row_peak = jnp.maximum(carried_logs, jnp.max(pair_logs, axis=-1))
-    inner_weights = jnp.exp(pair_logs - row_peak[..., None]) * scale
+    row_peak = jnp.maximum(carried_logs, inner_peak)
+    inner_scale = jnp.exp(inner_peak - row_peak)
     carried_weights = jnp.exp(carried_logs - row_peak)
-    scores = inner_weights * dot(query, key, (((2,), (2,)), ((0,), (0,))))
     cell = carried_weights[..., None] * dot(query, prior_state, (((2,), (2,)), ((0,), (0,))))
-    cell = cell + dot(scores.astype(BF16), value, (((2,), (1,)), ((0,), (0,))))
+    cell = cell + inner_scale[..., None] * inner
     cell = cell * lax.rsqrt(jnp.mean(cell * cell, axis=-1, keepdims=True) + EPSILON)
     gain = lax.dynamic_slice_in_dim(head_gain, head * HEAD_DIM, HEAD_DIM, 0)
     mem_out = (cell * gain).astype(BF16)

time: 239 us -> 240 us (level)
  no operation moved by 1% of the time
where the time goes in v9:
time: 240 us; the launch traced here: 238 us
  starting transfers between devices  76.5 us (32%)
  waiting for transfers between devices  75 us (31%)
  blocking collectives  24.1 us (10%)
  Pallas kernels  20.6 us (9%)
  local copies, waits for them, and re-layouts  15.5 us (6%)
  between operations  14 us (6%)
  other arithmetic  10 us (4%)
    ppermute x11, waiting for transfers between devices, ring(): lax.ppermute(array, axis, [(i, (i + by) % peers) for i in range(peers)])  37.8 us
    ppermute x11, starting transfers between devices, ring(): lax.ppermute(array, axis, [(i, (i + by) % peers) for i in range(peers)])  36.5 us
    all_to_all x3, starting transfers between devices, exchanged(): return lax.all_to_all(array, axis, split_axis=0, concat_axis=0, tiled=True)  28.9 us
    all_to_all x3, waiting for transfers between devices, exchanged(): return lax.all_to_all(array, axis, split_axis=0, concat_axis=0, tiled=True)  28 us
    all_to_all x2, blocking collectives, exchanged(): return lax.all_to_all(array, axis, split_axis=0, concat_axis=0, tiled=True)  24.1 us
    pallas_call x4, Pallas kernels, call(): pl.pallas_call(kernel, out_shape=tuple((jax.ShapeDtypeStruct(shape, dtype...  20.6 us
    all_to_all x1, waiting for transfers between devices, everyone(): return lax.all_to_all(copies, axis, split_axis=0, concat_axis=0, tiled=True)  8.08 us
    all_to_all x1, starting transfers between devices, everyone(): return lax.all_to_all(copies, axis, split_axis=0, concat_axis=0, tiled=True)  6.5 us
  transfers between devices with their start and end apart: 18, of which 13 were waited for; matrix products, arithmetic and copies ran while one was open for 8% of the time, Pallas kernels for 7%

profile of v9, /device:TPU:1, one launch (start us, length us, event | category | flops | bytes accessed | tf_op | source)
XLA Modules:
  0.0 238.1 jit_solution(11224647997841792948)
XLA Ops:
  6.5 1.5 fusion.2
  8.1 1.5 fusion.4
  9.6 0.9 constant_dynamic-slice_fusion.9
  10.5 5.2 %collective-permute-start = (bf16[256,1024]{1,0:T(8,128)(2,1)S(1)}, bf16[256,1024]{1,0:T(8,128)(2,1)S(1)}, u32[]{:S(2)}, u32[]{:S(2)}) collective-permute-start(bf16[256,1024]{1,0:T(8,128)(2,1)S(1)} %get-tuple-element.20.refs_0_.refs_5_), channel_id=1, source_target_pairs={{0,6},{2,0},{4,2},{6,4},{1,7},{3,1},{5,3},{7,5},{8,14},{10,8},{12,... | collective-permute-start | bytes 1572872 | tf_op jit(solution)/shard_map/ppermute | solution.py:71
  15.7 2.4 %collective-permute-start.1 = (bf16[256,1024]{1,0:T(8,128)(2,1)S(1)}, bf16[256,1024]{1,0:T(8,128)(2,1)S(1)}, u32[]{:S(2)}, u32[]{:S(2)}) collective-permute-start(bf16[256,1024]{1,0:T(8,128)(2,1)S(1)} %get-tuple-element.20.refs_0_.refs_5_), channel_id=1, source_target_pairs={{0,4},{2,6},{4,0},{6,2},{1,5},{3,7},{5,1},{7,3},{8,12},{10,14},{12... | collective-permute-start | bytes 1572872 | tf_op jit(solution)/shard_map/ppermute | solution.py:71
  18.1 2.5 %collective-permute-start.2 = (bf16[256,1024]{1,0:T(8,128)(2,1)S(1)}, bf16[256,1024]{1,0:T(8,128)(2,1)S(1)}, u32[]{:S(2)}, u32[]{:S(2)}) collective-permute-start(bf16[256,1024]{1,0:T(8,128)(2,1)S(1)} %get-tuple-element.20.refs_0_.refs_5_), channel_id=1, source_target_pairs={{0,2},{2,4},{4,6},{6,0},{1,3},{3,5},{5,7},{7,1},{8,10},{10,12},{12... | collective-permute-start | bytes 1572872 | tf_op jit(solution)/shard_map/ppermute | solution.py:71
  20.7 7.0 %collective-permute-done.refs_2_.refs_7_ = bf16[256,1024]{1,0:T(8,128)(2,1)S(1)} collective-permute-done((bf16[256,1024]{1,0:T(8,128)(2,1)S(1)}, bf16[256,1024]{1,0:T(8,128)(2,1)S(1)}, u32[]{:S(2)}, u32[]{:S(2)}) %collective-permute-start) | collective-permute-done | bytes 524320 | tf_op jit(solution)/shard_map/ppermute | solution.py:71
  27.6 1.5 collective-permute-done.1.refs_3_.refs_8_
  29.1 15.1 %collective-permute-done.2.refs_4_.refs_9_ = bf16[256,1024]{1,0:T(8,128)(2,1)S(1)} collective-permute-done((bf16[256,1024]{1,0:T(8,128)(2,1)S(1)}, bf16[256,1024]{1,0:T(8,128)(2,1)S(1)}, u32[]{:S(2)}, u32[]{:S(2)}) %collective-permute-start.2) | collective-permute-done | bytes 524320 | tf_op jit(solution)/shard_map/ppermute | solution.py:71
  44.3 2.4 %collective-permute-start.3 = (bf16[768,1024]{1,0:T(8,128)(2,1)S(1)}, bf16[768,1024]{1,0:T(8,128)(2,1)}, u32[]{:S(2)}, u32[]{:S(2)}) collective-permute-start(bf16[768,1024]{1,0:T(8,128)(2,1)S(1)} %pad_maximum_fusion), channel_id=1, source_target_pairs={{0,1},{1,0},{2,3},{3,2},{4,5},{5,4},{6,7},{7,6},{8,9},{9,8},{10,11... | collective-permute-start | bytes 4718600 | tf_op jit(solution)/shard_map/ppermute | solution.py:31
  46.7 1.6 shard_map.154
  48.4 11.2 %all-to-all-start = ((bf16[16,32,384]{2,1,0:T(8,128)(2,1)}), bf16[16,32,384]{2,1,0:T(8,128)(2,1)S(1)}, u32[]{:S(2)}, u32[]{:S(2)}) async-start(bf16[16,32,384]{2,1,0:T(8,128)(2,1)} %get-tuple-element.12), calls=%async_computation | async-start | bytes 786432 | tf_op jit(solution)/shard_map/all_to_all | solution.py:27
  59.6 0.7 all-gather.2.cloned.1.call-update
  60.3 12.0 %all-to-all-done = bf16[16,32,384]{2,1,0:T(8,128)(2,1)S(1)} async-done(((bf16[16,32,384]{2,1,0:T(8,128)(2,1)}), bf16[16,32,384]{2,1,0:T(8,128)(2,1)S(1)}, u32[]{:S(2)}, u32[]{:S(2)}) %all-to-all-start) | async-done | bytes 393248 | tf_op jit(solution)/shard_map/all_to_all | solution.py:27
  72.3 4.2 %collective-permute-start.6 = (bf16[512,384]{1,0:T(8,128)(2,1)S(1)}, bf16[512,384]{1,0:T(8,128)(2,1)}, u32[]{:S(2)}, u32[]{:S(2)}) collective-permute-start(bf16[512,384]{1,0:T(8,128)(2,1)S(1)} %bitcast.102), channel_id=1, source_target_pairs={{0,16},{16,32},{32,48},{48,0},{1,17},{17,33},{33,49},{49,1},{2,18}... | collective-permute-start | bytes 1179656 | tf_op jit(solution)/shard_map/ppermute | solution.py:71
  76.5 3.2 %collective-permute-start.5 = (bf16[512,384]{1,0:T(8,128)(2,1)S(1)}, bf16[512,384]{1,0:T(8,128)(2,1)}, u32[]{:S(2)}, u32[]{:S(2)}) collective-permute-start(bf16[512,384]{1,0:T(8,128)(2,1)S(1)} %bitcast.103), channel_id=1, source_target_pairs={{0,48},{16,0},{32,16},{48,32},{1,49},{17,1},{33,17},{49,33},{2,50}... | collective-permute-start | bytes 1179656 | tf_op jit(solution)/shard_map/ppermute | solution.py:71
  79.7 1.4 constant_dynamic-slice_fusion.5
  81.1 0.7 maximum_bitcast_fusion
  81.9 0.6 copy.72
  82.5 1.4 fusion.63.bias
  83.9 0.8 fusion.64
  84.7 0.5 collective-permute-done.6.refs_4_
  85.2 0.9 slice.168
  86.1 3.3 %collective-permute-start.7 = (bf16[256,384]{1,0:T(8,128)(2,1)S(1)}, bf16[256,384]{1,0:T(8,128)(2,1)S(1)}, u32[]{:S(2)}, u32[]{:S(2)}) collective-permute-start(bf16[256,384]{1,0:T(8,128)(2,1)S(1)} %slice.168), channel_id=1, source_target_pairs={{0,16},{16,32},{32,48},{48,0},{1,17},{17,33},{33,49},{49,1},{2,18}... | collective-permute-start | bytes 589832 | tf_op jit(solution)/shard_map/ppermute | solution.py:71
  89.5 1.6 collective-permute-done.5.refs_1_
  91.1 0.9 slice.169
  92.0 2.4 %collective-permute-start.8 = (bf16[256,384]{1,0:T(8,128)(2,1)S(1)}, bf16[256,384]{1,0:T(8,128)(2,1)S(1)}, u32[]{:S(2)}, u32[]{:S(2)}) collective-permute-start(bf16[256,384]{1,0:T(8,128)(2,1)S(1)} %slice.169), channel_id=1, source_target_pairs={{0,48},{16,0},{32,16},{48,32},{1,49},{17,1},{33,17},{49,33},{2,50}... | collective-permute-start | bytes 589832 | tf_op jit(solution)/shard_map/ppermute | solution.py:71
  94.5 0.6 pad_add_fusion.spot
  95.1 0.6 pad_maximum_fusion.2.refs_12_
  95.7 7.1 %collective-permute-done.7.refs_2_ = bf16[256,384]{1,0:T(8,128)(2,1)S(1)} collective-permute-done((bf16[256,384]{1,0:T(8,128)(2,1)S(1)}, bf16[256,384]{1,0:T(8,128)(2,1)S(1)}, u32[]{:S(2)}, u32[]{:S(2)}) %collective-permute-start.7) | collective-permute-done | bytes 196640 | tf_op jit(solution)/shard_map/ppermute | solution.py:71
  102.8 0.4 collective-permute-done.8.refs_3_
  103.5 0.4 copy-done.12
  103.9 8.1 %shard_map.156 = (bf16[4,256,384]{2,1,0:T(8,128)(2,1)}, bf16[8,96,128]{2,1,0:T(8,128)(2,1)}, f32[4,256]{1,0:T(4,128)}, f32[4,256]{1,0:T(4,128)}) custom-call(s32[3]{0:T(128)} %pad_add_fusion.spot, f32[2]{0:T(128)} %fusion.63.bias, bf16[512,384]{1,0:T(8,128)(2,1)} %bitcast.104, bf16[512,384]{1,0:T(8,128)(2,1)} %collective-permute-done.5.refs_1_, ...), custom_call_target="tpu_custom_call" | custom-call | flops 3000000000 | bytes 6291456 | tf_op jit(solution)/shard_map/pallas_call | solution.py:202
  112.0 14.4 %all-to-all-start.1 = ((bf16[8,96,128]{2,1,0:T(8,128)(2,1)}), bf16[8,96,128]{2,1,0:T(8,128)(2,1)S(1)}, u32[]{:S(2)}, u32[]{:S(2)}) async-start(bf16[8,96,128]{2,1,0:T(8,128)(2,1)} %get-tuple-element.14), calls=%async_computation.1 | async-start | bytes 393216 | tf_op jit(solution)/shard_map/all_to_all | solution.py:27
  126.4 9.0 %all-to-all-done.1 = bf16[8,96,128]{2,1,0:T(8,128)(2,1)S(1)} async-done(((bf16[8,96,128]{2,1,0:T(8,128)(2,1)}), bf16[8,96,128]{2,1,0:T(8,128)(2,1)S(1)}, u32[]{:S(2)}, u32[]{:S(2)}) %all-to-all-start.1) | async-done | bytes 196640 | tf_op jit(solution)/shard_map/all_to_all | solution.py:27
  137.0 0.7 broadcast_in_dim.91
  137.7 6.5 %all-to-all-start.2 = ((bf16[8,80,128]{2,1,0:T(8,128)(2,1)}), bf16[8,80,128]{2,1,0:T(8,128)(2,1)S(1)}, u32[]{:S(2)}, u32[]{:S(2)}) async-start(bf16[8,80,128]{2,1,0:T(8,128)(2,1)} %broadcast_in_dim.91), calls=%async_computation.2 | async-start | bytes 327680 | tf_op jit(solution)/shard_map/all_to_all | solution.py:23
  144.3 0.8 dynamic_slice.63
  145.1 0.4 fusion.13
  145.5 8.1 %all-to-all-done.2 = bf16[8,80,128]{2,1,0:T(8,128)(2,1)S(1)} async-done(((bf16[8,80,128]{2,1,0:T(8,128)(2,1)}), bf16[8,80,128]{2,1,0:T(8,128)(2,1)S(1)}, u32[]{:S(2)}, u32[]{:S(2)}) %all-to-all-start.2) | async-done | bytes 163872 | tf_op jit(solution)/shard_map/all_to_all | solution.py:23
  154.7 0.7 reshape.239
  155.5 3.4 %all-to-all-start.3 = ((bf16[8,64,128]{2,1,0:T(8,128)(2,1)}), bf16[8,64,128]{2,1,0:T(8,128)(2,1)S(1)}, u32[]{:S(2)}, u32[]{:S(2)}) async-start(bf16[8,64,128]{2,1,0:T(8,128)(2,1)} %reshape.239), calls=%async_computation.3 | async-start | bytes 262144 | tf_op jit(solution)/shard_map/all_to_all | solution.py:27
  158.9 0.6 fusion.6
  159.7 7.0 %all-to-all-done.3 = bf16[8,64,128]{2,1,0:T(8,128)(2,1)S(1)} async-done(((bf16[8,64,128]{2,1,0:T(8,128)(2,1)}), bf16[8,64,128]{2,1,0:T(8,128)(2,1)S(1)}, u32[]{:S(2)}, u32[]{:S(2)}) %all-to-all-start.3) | async-done | bytes 131104 | tf_op jit(solution)/shard_map/all_to_all | solution.py:27
  166.7 0.7 multiply_reduce_fusion
  167.4 1.3 slice.186.own
  168.7 1.9 collective-permute-start.10
  170.7 4.8 %collective-permute-start.9 = (bf16[2048,256]{1,0:T(8,128)(2,1)S(1)}, bf16[2048,256]{1,0:T(8,128)(2,1)}, u32[]{:S(2)}, u32[]{:S(2)}) collective-permute-start(bf16[2048,256]{1,0:T(8,128)(2,1)S(1)} %slice.186.own), channel_id=1, source_target_pairs={{0,6},{2,0},{4,2},{6,4},{1,7},{3,1},{5,3},{7,5},{8,14},{10,8},{12,... | collective-permute-start | bytes 3145736 | tf_op jit(solution)/shard_map/ppermute | solution.py:71
  175.4 6.3 %shard_map.155 = bf16[4,256,384]{2,1,0:T(8,128)(2,1)} custom-call(s32[3]{0:T(128)} %pad_add_fusion.spot, bf16[256,1024]{1,0:T(8,128)(2,1)} %copy-done.2, bf16[256,1024]{1,0:T(8,128)(2,1)} %get-tuple-element.19.refs_1_.refs_6_, bf16[256,1024]{1,0:T(8,128)(2,1)} %copy-done.3, bf16[256,1024]{1,0:T(8,128)(2,1)} %copy-done.4, bf16[256,1024]{1,0:T(8,128)(2,1)} %copy-done.5, ...), custom_call_target="tpu_custom_call" | custom-call | flops 3000000000 | bytes 6291456 | tf_op jit(solution)/shard_map/pallas_call | solution.py:202
  181.7 1.1 multiply_convert_fusion.1
  182.8 2.2 collective-permute-start.4
  185.3 0.5 collective-permute-done.4
  185.8 4.6 %collective-permute-done.10.behind = bf16[2048,256]{1,0:T(8,128)(2,1)} collective-permute-done((bf16[2048,256]{1,0:T(8,128)(2,1)S(1)}, bf16[2048,256]{1,0:T(8,128)(2,1)}, u32[]{:S(2)}, u32[]{:S(2)}) %collective-permute-start.10) | collective-permute-done | bytes 1048608 | tf_op jit(solution)/shard_map/ppermute | solution.py:71
  190.4 1.1 slice.187
  191.5 1.9 collective-permute-start.11
  193.5 1.1 slice.188
  194.5 4.6 %collective-permute-start.12 = (bf16[1024,256]{1,0:T(8,128)(2,1)S(1)}, bf16[1024,256]{1,0:T(8,128)(2,1)}, u32[]{:S(2)}, u32[]{:S(2)}) collective-permute-start(bf16[1024,256]{1,0:T(8,128)(2,1)S(1)} %slice.188), channel_id=1, source_target_pairs={{0,6},{2,0},{4,2},{6,4},{1,7},{3,1},{5,3},{7,5},{8,14},{10,8},{12,... | collective-permute-start | bytes 1572872 | tf_op jit(solution)/shard_map/ppermute | solution.py:71
  199.1 1.2 fusion.19
  200.3 0.3 fusion.15
  200.6 11.5 %all_to_all.30.parts = bf16[4,256,256]{2,1,0:T(8,128)(2,1)} all-to-all(bf16[4,256,256]{2,1,0:T(8,128)(2,1)S(1)} %fusion.15), channel_id=1, replica_groups=mesh['z'=8,'y_hi'=4,'y_lo'=2,'fs'=4,'tp'=2] {'fs'}, dimensions={0} | all-to-all | bytes 1048576 | tf_op jit(solution)/shard_map/all_to_all | solution.py:27
  212.1 0.8 copy-done.10
  212.9 4.6 %shard_map.157 = bf16[256,2048]{1,0:T(8,128)(2,1)} custom-call(s32[3]{0:T(128)} %pad_add_fusion.spot, bf16[4,256,256]{2,1,0:T(8,128)(2,1)} %all_to_all.30.parts, bf16[2048,256]{1,0:T(8,128)(2,1)} %copy-done.1, bf16[2048,256]{1,0:T(8,128)(2,1)} %collective-permute-done.9.ahead, bf16[1024,256]{1,0:T(8,128)(2,1)} %copy-done.10, ...), custom_call_target="tpu_custom_call" | custom-call | flops 2000000000 | bytes 6291456 | tf_op jit(solution)/shard_map/pallas_call | solution.py:202
  217.5 12.7 %all_to_all.31 = bf16[2,128,2048]{2,1,0:T(8,128)(2,1)S(1)} all-to-all(bf16[2,128,2048]{2,1,0:T(8,128)(2,1)} %bitcast.99), channel_id=1, replica_groups=mesh['z'=8,'y_hi'=4,'y_lo'=2,'fs'=4,'tp'=2] {'tp'}, dimensions={0} | all-to-all | bytes 2097152 | tf_op jit(solution)/shard_map/all_to_all | solution.py:27
  230.2 1.1 reduce_sum.52
  (83 shorter events, 3.8 us)
Async XLA Ops:
  6.5 119.9 %copy-start = (f32[3,1024]{1,0:T(4,128)S(1)}, f32[3,1024]{1,0:T(4,128)}, u32[]{:S(2)}) copy-start(f32[3,1024]{1,0:T(4,128)} %param.21) | copy-start | bytes 36868
  10.5 70.6 %copy-start.2 = (bf16[256,1024]{1,0:T(8,128)(2,1)}, bf16[256,1024]{1,0:T(8,128)(2,1)S(1)}, u32[]{:S(2)}) copy-start(bf16[256,1024]{1,0:T(8,128)(2,1)S(1)} %get-tuple-element.20.refs_0_.refs_5_) | copy-start | bytes 1572868
  10.5 17.1 %collective-permute-start = (bf16[256,1024]{1,0:T(8,128)(2,1)S(1)}, bf16[256,1024]{1,0:T(8,128)(2,1)S(1)}, u32[]{:S(2)}, u32[]{:S(2)}) collective-permute-start(bf16[256,1024]{1,0:T(8,128)(2,1)S(1)} %get-tuple-element.20.refs_0_.refs_5_), channel_id=1, source_target_pairs={{0,6},{2,0},{4,2},{6,4},{1,7},{3,1},{5,3},{7,5},{8,14},{10,8},{12,... | collective-permute-start | bytes 1572872 | tf_op jit(solution)/shard_map/ppermute | solution.py:71
  15.7 13.4 %collective-permute-start.1 = (bf16[256,1024]{1,0:T(8,128)(2,1)S(1)}, bf16[256,1024]{1,0:T(8,128)(2,1)S(1)}, u32[]{:S(2)}, u32[]{:S(2)}) collective-permute-start(bf16[256,1024]{1,0:T(8,128)(2,1)S(1)} %get-tuple-element.20.refs_0_.refs_5_), channel_id=1, source_target_pairs={{0,4},{2,6},{4,0},{6,2},{1,5},{3,7},{5,1},{7,3},{8,12},{10,14},{12... | collective-permute-start | bytes 1572872 | tf_op jit(solution)/shard_map/ppermute | solution.py:71
  18.1 26.0 %collective-permute-start.2 = (bf16[256,1024]{1,0:T(8,128)(2,1)S(1)}, bf16[256,1024]{1,0:T(8,128)(2,1)S(1)}, u32[]{:S(2)}, u32[]{:S(2)}) collective-permute-start(bf16[256,1024]{1,0:T(8,128)(2,1)S(1)} %get-tuple-element.20.refs_0_.refs_5_), channel_id=1, source_target_pairs={{0,2},{2,4},{4,6},{6,0},{1,3},{3,5},{5,7},{7,1},{8,10},{10,12},{12... | collective-permute-start | bytes 1572872 | tf_op jit(solution)/shard_map/ppermute | solution.py:71
  27.6 53.5 %copy-start.3 = (bf16[256,1024]{1,0:T(8,128)(2,1)}, bf16[256,1024]{1,0:T(8,128)(2,1)S(1)}, u32[]{:S(2)}) copy-start(bf16[256,1024]{1,0:T(8,128)(2,1)S(1)} %collective-permute-done.refs_2_.refs_7_) | copy-start | bytes 1572868
  29.1 52.0 %copy-start.4 = (bf16[256,1024]{1,0:T(8,128)(2,1)}, bf16[256,1024]{1,0:T(8,128)(2,1)S(1)}, u32[]{:S(2)}) copy-start(bf16[256,1024]{1,0:T(8,128)(2,1)S(1)} %collective-permute-done.1.refs_3_.refs_8_) | copy-start | bytes 1572868
  44.2 2.5 %copy-start.5 = (bf16[256,1024]{1,0:T(8,128)(2,1)}, bf16[256,1024]{1,0:T(8,128)(2,1)S(1)}, u32[]{:S(2)}) copy-start(bf16[256,1024]{1,0:T(8,128)(2,1)S(1)} %collective-permute-done.2.refs_4_.refs_9_) | copy-start | bytes 1572868
  44.3 58.9 %collective-permute-start.3 = (bf16[768,1024]{1,0:T(8,128)(2,1)S(1)}, bf16[768,1024]{1,0:T(8,128)(2,1)}, u32[]{:S(2)}, u32[]{:S(2)}) collective-permute-start(bf16[768,1024]{1,0:T(8,128)(2,1)S(1)} %pad_maximum_fusion), channel_id=1, source_target_pairs={{0,1},{1,0},{2,3},{3,2},{4,5},{5,4},{6,7},{7,6},{8,9},{9,8},{10,11... | collective-permute-start | bytes 4718600 | tf_op jit(solution)/shard_map/ppermute | solution.py:31
  48.4 23.9 %all-to-all-start = ((bf16[16,32,384]{2,1,0:T(8,128)(2,1)}), bf16[16,32,384]{2,1,0:T(8,128)(2,1)S(1)}, u32[]{:S(2)}, u32[]{:S(2)}) async-start(bf16[16,32,384]{2,1,0:T(8,128)(2,1)} %get-tuple-element.12), calls=%async_computation | async-start | bytes 786432 | tf_op jit(solution)/shard_map/all_to_all | solution.py:27
  59.5 107.9 %all-gather.2.cloned.1.call-start = ((), (), s32[]{:S(2)}) async-start(), calls=%async_computation.6 | async-start | bytes 2662400 | tf_op jit(solution)/shard_map/all_gather | solution.py:255
  72.3 30.9 %copy-start.6 = (bf16[16,32,384]{2,1,0:T(8,128)(2,1)}, bf16[16,32,384]{2,1,0:T(8,128)(2,1)S(1)}, u32[]{:S(2)}) copy-start(bf16[16,32,384]{2,1,0:T(8,128)(2,1)S(1)} %all-to-all-done) | copy-start | bytes 1179652
  72.3 12.9 %collective-permute-start.6 = (bf16[512,384]{1,0:T(8,128)(2,1)S(1)}, bf16[512,384]{1,0:T(8,128)(2,1)}, u32[]{:S(2)}, u32[]{:S(2)}) collective-permute-start(bf16[512,384]{1,0:T(8,128)(2,1)S(1)} %bitcast.102), channel_id=1, source_target_pairs={{0,16},{16,32},{32,48},{48,0},{1,17},{17,33},{33,49},{49,1},{2,18}... | collective-permute-start | bytes 1179656 | tf_op jit(solution)/shard_map/ppermute | solution.py:71
  76.5 14.6 %collective-permute-start.5 = (bf16[512,384]{1,0:T(8,128)(2,1)S(1)}, bf16[512,384]{1,0:T(8,128)(2,1)}, u32[]{:S(2)}, u32[]{:S(2)}) collective-permute-start(bf16[512,384]{1,0:T(8,128)(2,1)S(1)} %bitcast.103), channel_id=1, source_target_pairs={{0,48},{16,0},{32,16},{48,32},{1,49},{17,1},{33,17},{49,33},{2,50}... | collective-permute-start | bytes 1179656 | tf_op jit(solution)/shard_map/ppermute | solution.py:71
  86.1 16.7 %collective-permute-start.7 = (bf16[256,384]{1,0:T(8,128)(2,1)S(1)}, bf16[256,384]{1,0:T(8,128)(2,1)S(1)}, u32[]{:S(2)}, u32[]{:S(2)}) collective-permute-start(bf16[256,384]{1,0:T(8,128)(2,1)S(1)} %slice.168), channel_id=1, source_target_pairs={{0,16},{16,32},{32,48},{48,0},{1,17},{17,33},{33,49},{49,1},{2,18}... | collective-permute-start | bytes 589832 | tf_op jit(solution)/shard_map/ppermute | solution.py:71
  92.0 11.2 %collective-permute-start.8 = (bf16[256,384]{1,0:T(8,128)(2,1)S(1)}, bf16[256,384]{1,0:T(8,128)(2,1)S(1)}, u32[]{:S(2)}, u32[]{:S(2)}) collective-permute-start(bf16[256,384]{1,0:T(8,128)(2,1)S(1)} %slice.169), channel_id=1, source_target_pairs={{0,48},{16,0},{32,16},{48,32},{1,49},{17,1},{33,17},{49,33},{2,50}... | collective-permute-start | bytes 589832 | tf_op jit(solution)/shard_map/ppermute | solution.py:71
  102.8 0.7 copy-start.11
  103.2 0.7 copy-start.12
  112.0 33.1 %copy-start.8 = (f32[4,256]{1,0:T(4,128)S(1)}, f32[4,256]{1,0:T(4,128)}, u32[]{:S(2)}) copy-start(f32[4,256]{1,0:T(4,128)} %get-tuple-element.13) | copy-start | bytes 12292
  112.0 33.1 %copy-start.9 = (f32[4,256]{1,0:T(4,128)S(1)}, f32[4,256]{1,0:T(4,128)}, u32[]{:S(2)}) copy-start(f32[4,256]{1,0:T(4,128)} %get-tuple-element.15) | copy-start | bytes 12292
  112.0 46.9 %copy-start.7 = (bf16[4,256,384]{2,1,0:T(8,128)(2,1)S(1)}, bf16[4,256,384]{2,1,0:T(8,128)(2,1)}, u32[]{:S(2)}) copy-start(bf16[4,256,384]{2,1,0:T(8,128)(2,1)} %get-tuple-element.16) | copy-start | bytes 2359300
  112.0 23.4 %all-to-all-start.1 = ((bf16[8,96,128]{2,1,0:T(8,128)(2,1)}), bf16[8,96,128]{2,1,0:T(8,128)(2,1)S(1)}, u32[]{:S(2)}, u32[]{:S(2)}) async-start(bf16[8,96,128]{2,1,0:T(8,128)(2,1)} %get-tuple-element.14), calls=%async_computation.1 | async-start | bytes 393216 | tf_op jit(solution)/shard_map/all_to_all | solution.py:27
  137.7 15.8 %all-to-all-start.2 = ((bf16[8,80,128]{2,1,0:T(8,128)(2,1)}), bf16[8,80,128]{2,1,0:T(8,128)(2,1)S(1)}, u32[]{:S(2)}, u32[]{:S(2)}) async-start(bf16[8,80,128]{2,1,0:T(8,128)(2,1)} %broadcast_in_dim.91), calls=%async_computation.2 | async-start | bytes 327680 | tf_op jit(solution)/shard_map/all_to_all | solution.py:23
  155.5 11.2 %all-to-all-start.3 = ((bf16[8,64,128]{2,1,0:T(8,128)(2,1)}), bf16[8,64,128]{2,1,0:T(8,128)(2,1)S(1)}, u32[]{:S(2)}, u32[]{:S(2)}) async-start(bf16[8,64,128]{2,1,0:T(8,128)(2,1)} %reshape.239), calls=%async_computation.3 | async-start | bytes 262144 | tf_op jit(solution)/shard_map/all_to_all | solution.py:27
  168.7 13.0 %copy-start.1 = (bf16[2048,256]{1,0:T(8,128)(2,1)}, bf16[2048,256]{1,0:T(8,128)(2,1)S(1)}, u32[]{:S(2)}) copy-start(bf16[2048,256]{1,0:T(8,128)(2,1)S(1)} %slice.186.own) | copy-start | bytes 3145732
  168.7 21.7 %collective-permute-start.10 = (bf16[2048,256]{1,0:T(8,128)(2,1)S(1)}, bf16[2048,256]{1,0:T(8,128)(2,1)}, u32[]{:S(2)}, u32[]{:S(2)}) collective-permute-start(bf16[2048,256]{1,0:T(8,128)(2,1)S(1)} %slice.186.own), channel_id=1, source_target_pairs={{0,2},{2,4},{4,6},{6,0},{1,3},{3,5},{5,7},{7,1},{8,10},{10,12},{12... | collective-permute-start | bytes 3145736 | tf_op jit(solution)/shard_map/ppermute | solution.py:71
  170.7 22.8 %collective-permute-start.9 = (bf16[2048,256]{1,0:T(8,128)(2,1)S(1)}, bf16[2048,256]{1,0:T(8,128)(2,1)}, u32[]{:S(2)}, u32[]{:S(2)}) collective-permute-start(bf16[2048,256]{1,0:T(8,128)(2,1)S(1)} %slice.186.own), channel_id=1, source_target_pairs={{0,6},{2,0},{4,2},{6,4},{1,7},{3,1},{5,3},{7,5},{8,14},{10,8},{12,... | collective-permute-start | bytes 3145736 | tf_op jit(solution)/shard_map/ppermute | solution.py:71
  182.8 2.9 %collective-permute-start.4 = (bf16[4,2,128]{2,1,0:T(2,128)(2,1)S(1)}, bf16[4,2,128]{2,1,0:T(2,128)(2,1)S(1)}, u32[]{:S(2)}, u32[]{:S(2)}) collective-permute-start(bf16[4,2,128]{2,1,0:T(2,128)(2,1)S(1)} %slice.164), channel_id=1, source_target_pairs={{0,8},{8,16},{16,24},{24,32},{32,40},{40,48},{48,56},{56,64},{64,7... | collective-permute-start | bytes 6152 | tf_op jit(solution)/shard_map/ppermute | solution.py:36
  191.5 20.6 %collective-permute-start.11 = (bf16[1024,256]{1,0:T(8,128)(2,1)S(1)}, bf16[1024,256]{1,0:T(8,128)(2,1)S(1)}, u32[]{:S(2)}, u32[]{:S(2)}) collective-permute-start(bf16[1024,256]{1,0:T(8,128)(2,1)S(1)} %slice.187), channel_id=1, source_target_pairs={{0,2},{2,4},{4,6},{6,0},{1,3},{3,5},{5,7},{7,1},{8,10},{10,12},{12... | collective-permute-start | bytes 1572872 | tf_op jit(solution)/shard_map/ppermute | solution.py:71
  194.5 17.6 %collective-permute-start.12 = (bf16[1024,256]{1,0:T(8,128)(2,1)S(1)}, bf16[1024,256]{1,0:T(8,128)(2,1)}, u32[]{:S(2)}, u32[]{:S(2)}) collective-permute-start(bf16[1024,256]{1,0:T(8,128)(2,1)S(1)} %slice.188), channel_id=1, source_target_pairs={{0,6},{2,0},{4,2},{6,4},{1,7},{3,1},{5,3},{7,5},{8,14},{10,8},{12,... | collective-permute-start | bytes 1572872 | tf_op jit(solution)/shard_map/ppermute | solution.py:71
  212.1 0.8 copy-start.10
Sparse Core Ops, SparseCore 0:
  63.3 87.4 all-gather.1
